TPU v7x, 32 devices: a whole 2x2x4 slice. The times are simulated.
32 devices in a mesh: sp: 4 (over y, x), tp: 8 (over z, core).
Axes of the slice: x: 2, y: 2, z: 4, core: 2. Of those that a mesh axis runs over, the one named last changes fastest.
Arguments:
- tokens: bfloat16 [1536, 2048], P('sp', 'tp'), may hold values from -110 to 110
- documents: int32 [1536], P('sp'), may hold values from 0 to 1, never falling along the last dimension, each value on 1 to 1152 neighbouring positions
- pre_gain: float32 [3, 2048], replicated, may hold values from 0.1 to 1.9
- query_weight: bfloat16 [3, 2048, 2048], P(None, 'tp'), may hold values from -0.125 to 0.125
- key_weight: bfloat16 [3, 2048, 2048], P(None, 'tp'), may hold values from -0.125 to 0.125
- value_weight: bfloat16 [3, 2048, 2048], P(None, 'tp'), may hold values from -0.125 to 0.125
- gate_weight: bfloat16 [3, 2048, 2048], P(None, 'tp'), may hold values from -0.125 to 0.125
- out_weight: bfloat16 [3, 2048, 2048], P(None, 'tp'), may hold values from -0.70710678 to 0.70710678
- position_bias: float32 [3, 32, 257], P(None, 'tp'), may hold values from -4 to 302
- post_gain: float32 [3, 2048], replicated, may hold values from 0.1 to 1.9
Outputs:
- updated: bfloat16 [1536, 2048], P('sp', 'tp')
Inputs may be any that keep to these rules, and one draw needn't show every extreme that they name: `documents`: document numbers never fall, every number from 0 to 1 is used, each document holds at most 1152 positions.
All inputs are finite; a program needn't handle non-finite values.
Results may differ from a plain program's by a relative error of at most 0.015.
Values may be sent and summed in bfloat16 or wider, within the bound.
No kernel may reach another device: no remote copies, remote signals or barrier semaphores. Data moves between devices by JAX's collectives and lax.ppermute only.
A program may use at most 64 MiB of HBM per device.

v0:
```python
import jax
import jax.numpy as jnp
from jax import lax
from jax.sharding import PartitionSpec as P

D = 2048
HD = 64
BLOCK = 64
PAST_BLOCKS = 4
LAYERS = 3
PAST = 256
CLIP = 128


norm_eps = 1e-06
inner_dims = (((1,), (1,)), ((), ()))


def from_behind(block, axis, distance):
    devices = range(lax.axis_size(axis))
    route = [(i - distance, i) for i in devices if i - distance in devices]
    return lax.ppermute(block, axis, route)


def band_allowed():
    row_block = (jnp.arange(2 * BLOCK) // BLOCK)[:, None]
    col_block = (jnp.arange(PAST + 2 * BLOCK) // BLOCK)[None, :]
    return (col_block >= row_block) & (col_block <= row_block + PAST_BLOCKS)


def bias_blocks(bias_table):
    group_rows = 2 * BLOCK
    window_cols = PAST + 2 * BLOCK
    skew_len = group_rows + window_cols - 1
    distance = jnp.clip(PAST + group_rows - 1 - jnp.arange(skew_len), -CLIP, CLIP) + CLIP
    picked = jnp.sum(
        jnp.where(
            distance[None, :, None] == jnp.arange(2 * CLIP + 1)[None, None, :],
            bias_table[:, None, :],
            0.0,
        ),
        axis=2,
    )
    tiled = jnp.tile(picked, (1, group_rows))
    skewed = tiled[:, group_rows - 1 : group_rows - 1 + group_rows * (skew_len - 1)]
    return skewed.reshape(-1, group_rows, skew_len - 1)[:, :, :window_cols]


def attend(query_rows, key_ext, value_ext, query_docs, doc_ext, bias_band, first_group, last_group):
    group_rows = 2 * BLOCK
    groups = last_group - first_group
    head_count = bias_band.shape[0]
    steps = PAST // group_rows + 1
    key_blocks = key_ext.reshape(-1, group_rows, head_count, HD)
    value_blocks = value_ext.reshape(-1, group_rows, head_count, HD)
    doc_blocks = doc_ext.reshape(-1, group_rows)
    key_win = jnp.concatenate(
        [key_blocks[first_group + offset : last_group + offset] for offset in range(steps)], axis=1
    )
    value_win = jnp.concatenate(
        [value_blocks[first_group + offset : last_group + offset] for offset in range(steps)],
        axis=1,
    )
    doc_win = jnp.concatenate(
        [doc_blocks[first_group + offset : last_group + offset] for offset in range(steps)], axis=1
    )
    query_groups = query_rows.reshape(groups, group_rows, head_count, HD)
    query_tags = query_docs.reshape(groups, group_rows)
    scores = jnp.einsum(
        "gqhd,gkhd->ghqk", query_groups, key_win, preferred_element_type=jnp.float32
    )
    scores = scores * HD ** (-0.5) + bias_band[None]
    allowed = band_allowed()[None, None] & (
        query_tags[:, None, :, None] == doc_win[:, None, None, :]
    )
    scores = jnp.where(allowed, scores, -1e30)
    row_max = jnp.max(scores, axis=3, keepdims=True)
    lifted = jnp.exp(scores - row_max)
    weights_bf = (lifted / jnp.sum(lifted, axis=3, keepdims=True)).astype(jnp.bfloat16)
    attended = jnp.einsum(
        "ghqk,gkhd->gqhd", weights_bf, value_win, preferred_element_type=jnp.float32
    )
    return attended.reshape(groups * group_rows, head_count * HD)


def fetch_fringe(key_rows, value_rows, doc_tags):
    tail_start = key_rows.shape[0] - PAST
    tail = jnp.stack([key_rows[tail_start:], value_rows[tail_start:]])
    fringe, fringe_docs = from_behind((tail, doc_tags[tail_start:]), "sp", 1)
    return (
        jnp.concatenate([fringe[0], key_rows]),
        jnp.concatenate([fringe[1], value_rows]),
        jnp.concatenate([fringe_docs, doc_tags]),
    )


def finish_columns(resid_cols, branch, gain_cols):
    branch_wide = branch.astype(jnp.float32)
    total_sq = lax.psum(jnp.sum(branch_wide * branch_wide, axis=1), "tp")
    inv_out = lax.rsqrt(total_sq / D + norm_eps)[:, None]
    return (resid_cols.astype(jnp.float32) + branch_wide * inv_out * gain_cols).astype(jnp.bfloat16)


def local(
    tokens,
    documents,
    pre_gain,
    query_weight,
    key_weight,
    value_weight,
    gate_weight,
    out_weight,
    position_bias,
    post_gain,
):
    tok_rows = tokens.shape[0]
    own_cols = tokens.shape[1]
    col_start = lax.axis_index("tp") * own_cols
    group_rows = 2 * BLOCK
    groups = tok_rows // group_rows
    doc_tags = documents + 1
    residual = lax.all_gather(tokens, "tp", axis=1, tiled=True)
    for layer_index in range(LAYERS):
        weights = (
            query_weight[layer_index],
            key_weight[layer_index],
            value_weight[layer_index],
            gate_weight[layer_index],
        )
        gain_row = pre_gain[layer_index]
        resid_wide = residual.astype(jnp.float32)
        inv_in = lax.rsqrt(jnp.mean(resid_wide * resid_wide, axis=1, keepdims=True) + norm_eps)
        normed = (resid_wide * gain_row).astype(jnp.bfloat16)
        queries, key_rows, value_rows, gate_rows = [
            (
                inv_in
                * lax.dot_general(normed, weight, inner_dims, preferred_element_type=jnp.float32)
            ).astype(jnp.bfloat16)
            for weight in weights
        ]
        bias_band = bias_blocks(position_bias[layer_index])
        key_ext, value_ext, doc_ext = fetch_fringe(key_rows, value_rows, doc_tags)
        attended = attend(queries, key_ext, value_ext, doc_tags, doc_ext, bias_band, 0, groups)
        mixed_rows = (attended * jax.nn.silu(gate_rows.astype(jnp.float32))).astype(jnp.bfloat16)
        out_local = out_weight[layer_index]
        branch = lax.dot_general(
            lax.all_gather(mixed_rows, "tp", axis=1, tiled=True),
            out_local,
            inner_dims,
            preferred_element_type=jnp.float32,
        ).astype(jnp.bfloat16)
        gain_out = post_gain[layer_index]
        if layer_index + 1 < LAYERS:
            whole_branch = lax.all_gather(branch, "tp", axis=1, tiled=True).astype(jnp.float32)
            inv_out = lax.rsqrt(
                jnp.mean(whole_branch * whole_branch, axis=1, keepdims=True) + norm_eps
            )
            residual = (residual.astype(jnp.float32) + whole_branch * inv_out * gain_out).astype(
                jnp.bfloat16
            )
        else:
            residual = finish_columns(
                lax.dynamic_slice_in_dim(residual, col_start, own_cols, 1),
                branch,
                lax.dynamic_slice_in_dim(gain_out, col_start, own_cols),
            )
    return residual


def solution(mesh):
    placed = (
        P("sp", "tp"),
        P("sp"),
        P(),
        P(None, "tp", None),
        P(None, "tp", None),
        P(None, "tp", None),
        P(None, "tp", None),
        P(None, "tp", None),
        P(None, "tp", None),
        P(),
    )
    return jax.shard_map(
        local, mesh=mesh, in_specs=placed, out_specs=P("sp", "tp"), check_vma=False
    )
```

profile of v0, /device:TPU:0, one launch (start us, length us, event | category | flops | bytes accessed | tf_op | source)
XLA Modules:
  0.0 291.9 jit_solution(16148980980989822733)
XLA Ops:
  8.0 4.9 %collective-permute-start.1 = (s32[256]{0:T(256)S(1)}, s32[256]{0:T(256)S(1)}, u32[]{:S(2)}, u32[]{:S(2)}) collective-permute-start(s32[256]{0:T(256)S(1)} %slice.276), channel_id=1, source_target_pairs={{0,8},{8,16},{16,24},{1,9},{9,17},{17,25},{2,10},{10,18},{18,26},{... | collective-permute-start | bytes 3080 | tf_op jit(solution)/shard_map/ppermute | solution.py:22
  14.2 2.1 select_reduce_fusion.2
  16.2 1.5 fusion.203
  18.0 1.2 tile.13
  19.8 1.1 reshape.269
  21.0 1.0 compare_and_fusion
  22.0 16.9 %all-gather.7.cloned.1.call-done = bf16[384,2048]{1,0:T(8,128)(2,1)} async-done(((bf16[384,256]{1,0:T(8,128)(2,1)}), bf16[384,2048]{1,0:T(8,128)(2,1)}) %all-gather.7.cloned.1.call-update) | async-done | bytes 1572880 | tf_op jit(solution)/shard_map/all_gather | solution.py:122
  38.9 1.8 fusion.9
  40.7 2.4 fusion.31
  43.4 1.8 fusion.32
  45.5 2.4 collective-permute-start
  47.9 0.9 copy.97
  48.8 1.8 fusion.33
  50.6 1.0 reshape.280
  51.6 0.9 copy.90
  52.5 1.3 collective-permute-done
  54.1 0.9 copy.95
  55.2 0.9 copy.96
  57.0 4.2 %fusion.204 = (f32[3,4,128]{2,1,0:T(4,128)}, f32[3,4,128,384]{3,2,1,0:T(8,128)}) fusion(f32[4,128,384]{2,1,0:T(8,128)S(1)} %slice-done, pred[3,128,384]{2,1,0:T(8,128)(4,1)} %compare_and_fusion, bf16[3,128,4,64]{1,3,2,0:T(8,128)(2,1)} %copy.97, bf16[3,128,4,64]{1,3,2,0:T(8,128)(2,1)} %copy.96, bf16[3,128,4,64]{1,3,2,0:T(8,128)(2,1)S(1)} %copy-done.11, ...), kind=kOutput, calls=%fused_computation.247 | convolution fusion | flops 80216448 | bytes 4085760 | tf_op jit(solution)/shard_map/sub | solution.py:78
  61.3 2.4 convolution_bitcast_fusion.2
  64.5 2.5 multiply_convert_fusion.2
  67.3 27.5 %all-gather.9.cloned.1.call-done = bf16[384,2048]{1,0:T(8,128)(2,1)} async-done(((bf16[384,256]{1,0:T(8,128)(2,1)}), bf16[384,2048]{1,0:T(8,128)(2,1)}) %all-gather.9.cloned.1.call-update) | async-done | bytes 1572880 | tf_op jit(solution)/shard_map/all_gather | solution.py:147
  94.8 3.0 %convolution_convert_fusion.2 = bf16[384,256]{1,0:T(8,128)(2,1)} fusion(bf16[384,2048]{1,0:T(8,128)(2,1)} %all-gather.9.cloned.1.call-done, bf16[3,256,2048]{2,1,0:T(8,128)(2,1)} %param.17), kind=kOutput, calls=%fused_computation.72 | convolution fusion | flops 402751488 | bytes 2818048 | tf_op jit(solution)/shard_map/dot_general | solution.py:146
  98.0 2.2 tile.30
  100.2 1.8 slice.360
  102.0 2.1 reshape.272
  104.7 19.1 %all-gather.11.cloned.1.call-done = bf16[384,2048]{1,0:T(8,128)(2,1)} async-done(((bf16[384,256]{1,0:T(8,128)(2,1)}), bf16[384,2048]{1,0:T(8,128)(2,1)}) %all-gather.11.cloned.1.call-update) | async-done | bytes 1572880 | tf_op jit(solution)/shard_map/all_gather | solution.py:154
  123.8 1.9 fusion.3
  125.8 0.9 fusion.12
  126.7 1.8 fusion.37
  128.6 1.8 fusion.36
  130.9 2.5 collective-permute-start.2
  133.5 1.8 fusion.38
  135.3 1.0 reshape.288
  136.3 0.9 copy.114
  137.2 0.9 copy.107
  138.0 1.3 collective-permute-done.2
  140.7 0.9 copy.106
  142.3 0.9 copy.113
  143.2 4.3 %fusion.209 = (f32[3,4,128]{2,1,0:T(4,128)}, f32[3,4,128,384]{3,2,1,0:T(8,128)}) fusion(f32[4,128,384]{2,1,0:T(8,128)S(1)} %slice-done.1, pred[3,128,384]{2,1,0:T(8,128)(4,1)} %compare_and_fusion, bf16[3,128,4,64]{1,3,2,0:T(8,128)(2,1)} %copy.114, bf16[3,128,4,64]{1,3,2,0:T(8,128)(2,1)} %copy.113, bf16[3,128,4,64]{1,3,2,0:T(8,128)(2,1)S(1)} %copy.112, ...), kind=kOutput, calls=%fused_computation.248 | convolution fusion | flops 80216448 | bytes 4085760 | tf_op jit(solution)/shard_map/sub | solution.py:78
  147.5 2.4 convolution_bitcast_fusion.1
  150.6 2.5 multiply_convert_fusion.1
  153.5 27.5 %all-gather.13.cloned.1.call-done = bf16[384,2048]{1,0:T(8,128)(2,1)} async-done(((bf16[384,256]{1,0:T(8,128)(2,1)}), bf16[384,2048]{1,0:T(8,128)(2,1)}) %all-gather.13.cloned.1.call-update) | async-done | bytes 1572880 | tf_op jit(solution)/shard_map/all_gather | solution.py:147
  180.9 3.0 %convolution_convert_fusion.1 = bf16[384,256]{1,0:T(8,128)(2,1)} fusion(bf16[384,2048]{1,0:T(8,128)(2,1)} %all-gather.13.cloned.1.call-done, bf16[3,256,2048]{2,1,0:T(8,128)(2,1)} %param.17), kind=kOutput, calls=%fused_computation.71 | convolution fusion | flops 402751488 | bytes 2818048 | tf_op jit(solution)/shard_map/dot_general | solution.py:146
  184.1 2.2 tile.32
  186.3 1.8 slice.370
  188.2 2.1 reshape.275
  190.3 19.7 %all-gather.15.cloned.1.call-done = bf16[384,2048]{1,0:T(8,128)(2,1)} async-done(((bf16[384,256]{1,0:T(8,128)(2,1)}), bf16[384,2048]{1,0:T(8,128)(2,1)}) %all-gather.15.cloned.1.call-update) | async-done | bytes 1572880 | tf_op jit(solution)/shard_map/all_gather | solution.py:154
  210.0 1.9 fusion.5
  211.9 0.9 fusion.7
  212.9 1.8 fusion.42
  214.7 1.8 fusion.41
  217.1 2.8 collective-permute-start.3
  219.9 2.5 fusion.43
  222.4 1.9 reshape.296
  224.3 0.9 copy.131
  225.2 0.9 copy.124
  229.0 0.9 copy.130
  229.9 4.3 %fusion.214 = (f32[3,4,128]{2,1,0:T(4,128)}, f32[3,4,128,384]{3,2,1,0:T(8,128)}) fusion(f32[4,128,384]{2,1,0:T(8,128)S(1)} %slice-done.2, pred[3,128,384]{2,1,0:T(8,128)(4,1)} %compare_and_fusion, bf16[3,128,4,64]{1,3,2,0:T(8,128)(2,1)} %copy.131, bf16[3,128,4,64]{1,3,2,0:T(8,128)(2,1)} %copy.130, bf16[3,128,4,64]{1,3,2,0:T(8,128)(2,1)S(1)} %copy.129, ...), kind=kOutput, calls=%fused_computation.249 | convolution fusion | flops 80216448 | bytes 4085760 | tf_op jit(solution)/shard_map/sub | solution.py:78
  234.1 2.4 convolution_bitcast_fusion
  237.3 2.5 multiply_convert_fusion
  240.6 26.5 %all-gather.17.cloned.1.call-done = bf16[384,2048]{1,0:T(8,128)(2,1)} async-done(((bf16[384,256]{1,0:T(8,128)(2,1)}), bf16[384,2048]{1,0:T(8,128)(2,1)}) %all-gather.17.cloned.1.call-update) | async-done | bytes 1572880 | tf_op jit(solution)/shard_map/all_gather | solution.py:147
  267.1 2.4 multiply_reduce_fusion
  269.5 14.7 %psum.7 = f32[384]{0:T(512)S(1)} all-reduce(f32[384]{0:T(512)S(1)} %get-tuple-element.49), channel_id=1, replica_groups=mesh['sp'=4,'tp'=8] {'tp'}, use_global_device_ids=true, to_apply=%region_15.16 | all-reduce | flops 384 | bytes 3072 | tf_op jit(solution)/shard_map/psum | solution.py:99
  (139 shorter events, 16.6 us)
Async XLA Ops:
  6.5 32.4 %all-gather.7.cloned.1.call-start = ((), (), s32[]{:S(2)}) async-start(), calls=%async_computation | async-start | bytes 1769472 | tf_op jit(solution)/shard_map/all_gather | solution.py:122
  7.3 87.5 %all-gather.9.cloned.1.call-start = ((), (), s32[]{:S(2)}) async-start(), calls=%async_computation.1 | async-start | bytes 1769472 | tf_op jit(solution)/shard_map/all_gather | solution.py:147
  8.0 13.0 %collective-permute-start.1 = (s32[256]{0:T(256)S(1)}, s32[256]{0:T(256)S(1)}, u32[]{:S(2)}, u32[]{:S(2)}) collective-permute-start(s32[256]{0:T(256)S(1)} %slice.276), channel_id=1, source_target_pairs={{0,8},{8,16},{16,24},{1,9},{9,17},{17,25},{2,10},{10,18},{18,26},{... | collective-permute-start | bytes 3080 | tf_op jit(solution)/shard_map/ppermute | solution.py:22
  17.7 31.1 %copy-start.16 = (f32[1,2048]{1,0:T(1,128)}, f32[1,2048]{1,0:T(1,128)S(1)}, u32[]{:S(2)}) copy-start(f32[1,2048]{1,0:T(1,128)S(1)} %get-tuple-element.34) | copy-start | bytes 24580
  21.0 19.8 %copy-start.3 = (f32[4,128,510]{2,1,0:T(8,128)}, f32[4,128,510]{2,1,0:T(8,128)S(1)}, u32[]{:S(2)}) copy-start(f32[4,128,510]{2,1,0:T(8,128)S(1)} %reshape.269) | copy-start | bytes 3133444
  40.7 8.1 %copy-start.18 = (f32[384]{0:T(512)}, f32[384]{0:T(512)S(1)}, u32[]{:S(2)}) copy-start(f32[384]{0:T(512)S(1)} %add_rsqrt_fusion.5) | copy-start | bytes 4612
  40.7 2.7 copy-start
  45.5 8.3 %collective-permute-start = (bf16[2,256,256]{2,1,0:T(8,128)(2,1)S(1)}, bf16[2,256,256]{2,1,0:T(8,128)(2,1)S(1)}, u32[]{:S(2)}, u32[]{:S(2)}) collective-permute-start(bf16[2,256,256]{2,1,0:T(8,128)(2,1)S(1)} %pad_maximum_fusion), channel_id=1, source_target_pairs={{0,8},{8,16},{16,24},{1,9},{9,17},{17,25},{2,10},{10,18},{18,26},{... | collective-permute-start | bytes 786440 | tf_op jit(solution)/shard_map/ppermute | solution.py:22
  54.1 2.9 slice-start
  56.1 0.9 copy-start.11
  57.0 4.2 %copy-start.5 = (bf16[3,128,4,64]{1,3,2,0:T(8,128)(2,1)S(1)}, bf16[3,128,4,64]{1,3,2,0:T(8,128)(2,1)}, u32[]{:S(2)}) copy-start(bf16[3,128,4,64]{1,3,2,0:T(8,128)(2,1)} %copy.90) | copy-start | bytes 589828
  63.7 0.8 copy-start.17
  63.7 0.8 copy-start.19
  67.0 56.8 %all-gather.11.cloned.1.call-start = ((), (), s32[]{:S(2)}) async-start(), calls=%async_computation.2 | async-start | bytes 1769472 | tf_op jit(solution)/shard_map/all_gather | solution.py:154
  97.8 83.2 %all-gather.13.cloned.1.call-start = ((), (), s32[]{:S(2)}) async-start(), calls=%async_computation.3 | async-start | bytes 1769472 | tf_op jit(solution)/shard_map/all_gather | solution.py:147
  100.2 3.9 %copy-start.12 = (f32[3,2048]{1,0:T(4,128)S(1)}, f32[3,2048]{1,0:T(4,128)}, u32[]{:S(2)}) copy-start(f32[3,2048]{1,0:T(4,128)} %param.19) | copy-start | bytes 73732
  123.8 1.9 copy-start.1
  125.8 1.0 copy-start.14
  126.7 6.8 %copy-start.20 = (f32[384]{0:T(512)}, f32[384]{0:T(512)S(1)}, u32[]{:S(2)}) copy-start(f32[384]{0:T(512)S(1)} %add_rsqrt_fusion.3) | copy-start | bytes 4612
  130.9 8.5 %collective-permute-start.2 = (bf16[2,256,256]{2,1,0:T(8,128)(2,1)S(1)}, bf16[2,256,256]{2,1,0:T(8,128)(2,1)S(1)}, u32[]{:S(2)}, u32[]{:S(2)}) collective-permute-start(bf16[2,256,256]{2,1,0:T(8,128)(2,1)S(1)} %pad_maximum_fusion.1), channel_id=1, source_target_pairs={{0,8},{8,16},{16,24},{1,9},{9,17},{17,25},{2,10},{10,18},{18,26},{... | collective-permute-start | bytes 786440 | tf_op jit(solution)/shard_map/ppermute | solution.py:22
  139.7 3.5 %slice-start.1 = ((f32[4,128,510]{2,1,0:T(8,128)}), f32[4,128,384]{2,1,0:T(8,128)S(1)}, s32[]{:S(2)}) async-start(f32[4,128,510]{2,1,0:T(8,128)} %reshape.272), calls=%async_computation.7 | async-start | bytes 1572864 | tf_op jit(solution)/shard_map/slice | solution.py:46
  143.2 4.3 %copy-start.6 = (bf16[3,128,4,64]{1,3,2,0:T(8,128)(2,1)S(1)}, bf16[3,128,4,64]{1,3,2,0:T(8,128)(2,1)}, u32[]{:S(2)}) copy-start(bf16[3,128,4,64]{1,3,2,0:T(8,128)(2,1)} %copy.107) | copy-start | bytes 589828
  143.2 4.3 %copy-start.8 = (bf16[3,128,4,64]{1,3,2,0:T(8,128)(2,1)S(1)}, bf16[3,128,4,64]{1,3,2,0:T(8,128)(2,1)}, u32[]{:S(2)}) copy-start(bf16[3,128,4,64]{1,3,2,0:T(8,128)(2,1)} %copy.105) | copy-start | bytes 589828
  143.2 4.3 %copy-start.10 = (bf16[3,128,4,64]{1,3,2,0:T(8,128)(2,1)S(1)}, bf16[3,128,4,64]{1,3,2,0:T(8,128)(2,1)}, u32[]{:S(2)}) copy-start(bf16[3,128,4,64]{1,3,2,0:T(8,128)(2,1)} %copy.106) | copy-start | bytes 589828
  147.4 3.2 %copy-start.15 = (f32[1,2048]{1,0:T(1,128)S(1)}, f32[1,2048]{1,0:T(1,128)}, u32[]{:S(2)}) copy-start(f32[1,2048]{1,0:T(1,128)} %get-tuple-element.35) | copy-start | bytes 24580
  147.4 3.2 %copy-start.21 = (f32[384]{0:T(512)S(1)}, f32[384]{0:T(512)}, u32[]{:S(2)}) copy-start(f32[384]{0:T(512)} %copy-done.20) | copy-start | bytes 4612
  153.2 56.8 %all-gather.15.cloned.1.call-start = ((), (), s32[]{:S(2)}) async-start(), calls=%async_computation.4 | async-start | bytes 1769472 | tf_op jit(solution)/shard_map/all_gather | solution.py:154
  184.0 83.1 %all-gather.17.cloned.1.call-start = ((), (), s32[]{:S(2)}) async-start(), calls=%async_computation.5 | async-start | bytes 1769472 | tf_op jit(solution)/shard_map/all_gather | solution.py:147
  210.0 1.9 copy-start.2
  211.9 0.9 copy-start.13
  217.1 9.0 %collective-permute-start.3 = (bf16[2,256,256]{2,1,0:T(8,128)(2,1)S(1)}, bf16[2,256,256]{2,1,0:T(8,128)(2,1)S(1)}, u32[]{:S(2)}, u32[]{:S(2)}) collective-permute-start(bf16[2,256,256]{2,1,0:T(8,128)(2,1)S(1)} %pad_maximum_fusion.2), channel_id=1, source_target_pairs={{0,8},{8,16},{16,24},{1,9},{9,17},{17,25},{2,10},{10,18},{18,26},{... | collective-permute-start | bytes 786440 | tf_op jit(solution)/shard_map/ppermute | solution.py:22
  226.3 3.5 %slice-start.2 = ((f32[4,128,510]{2,1,0:T(8,128)}), f32[4,128,384]{2,1,0:T(8,128)S(1)}, s32[]{:S(2)}) async-start(f32[4,128,510]{2,1,0:T(8,128)} %reshape.275), calls=%async_computation.8 | async-start | bytes 1572864 | tf_op jit(solution)/shard_map/slice | solution.py:46
  229.8 4.3 %copy-start.4 = (bf16[3,128,4,64]{1,3,2,0:T(8,128)(2,1)S(1)}, bf16[3,128,4,64]{1,3,2,0:T(8,128)(2,1)}, u32[]{:S(2)}) copy-start(bf16[3,128,4,64]{1,3,2,0:T(8,128)(2,1)} %copy.124) | copy-start | bytes 589828
  229.9 4.3 %copy-start.7 = (bf16[3,128,4,64]{1,3,2,0:T(8,128)(2,1)S(1)}, bf16[3,128,4,64]{1,3,2,0:T(8,128)(2,1)}, u32[]{:S(2)}) copy-start(bf16[3,128,4,64]{1,3,2,0:T(8,128)(2,1)} %copy.122) | copy-start | bytes 589828
  229.9 4.3 %copy-start.9 = (bf16[3,128,4,64]{1,3,2,0:T(8,128)(2,1)S(1)}, bf16[3,128,4,64]{1,3,2,0:T(8,128)(2,1)}, u32[]{:S(2)}) copy-start(bf16[3,128,4,64]{1,3,2,0:T(8,128)(2,1)} %copy.123) | copy-start | bytes 589828
Sparse Core Ops, SparseCore 0:
  8.9 29.9 all-gather.6
  67.2 27.5 all-gather.8
  97.9 25.8 all-gather.10
  153.3 27.5 all-gather.12
  184.1 25.8 all-gather.14
  240.0 27.0 all-gather.16
where the time goes:
time: 293 us; the launch traced here: 292 us
  waiting for transfers between devices  141 us (48%)
  matrix products  53.6 us (18%)
  local copies, waits for them, and re-layouts  42.8 us (15%)
  blocking collectives  14.7 us (5%)
  between operations  14.2 us (5%)
  starting transfers between devices  13.2 us (5%)
  other arithmetic  12.5 us (4%)
    all_gather x3, waiting for transfers between devices, local(): lax.all_gather(mixed_rows, 'tp', axis=1, tiled=True)  81.5 us
    all_gather x2, waiting for transfers between devices, local(): lax.all_gather(branch, 'tp', axis=1, tiled=True).astype(jnp.float32)  38.8 us
    dot_general x12, matrix products, local(): lax.dot_general(normed, weight, inner_dims, preferred_element_type=jnp.fl...  25.4 us
    all_gather x1, waiting for transfers between devices, local(): residual = lax.all_gather(tokens, 'tp', axis=1, tiled=True)  16.9 us
    psum x1, blocking collectives, finish_columns(): total_sq = lax.psum(jnp.sum(branch_wide * branch_wide, axis=1), 'tp')  14.7 us
    sub x3, matrix products, attend(): lifted = jnp.exp(scores - row_max)  12.7 us
    ppermute x4, starting transfers between devices, from_behind(): return lax.ppermute(block, axis, route)  12.6 us
    slice x18, local copies, waits for them, and re-layouts, attend(): key_blocks[first_group + offset:last_group + offset]  8.39 us
  transfers between devices with their start and end apart: 10, of which 8 were waited for; matrix products, arithmetic and copies ran while one was open for 13% of the time, Pallas kernels for 0%

commit v1 on v0

v1 whole, which is shorter than its diff:
```python
import functools

import jax
import jax.numpy as jnp
from jax import lax
from jax.experimental import pallas as pl
from jax.experimental.pallas import tpu as pltpu
from jax.sharding import PartitionSpec as P

D = 2048
HD = 64
BLOCK = 64
PAST_BLOCKS = 4
LAYERS = 3
PAST = 256
CLIP = 128
GROUP = 2 * BLOCK
WINDOW = PAST + GROUP
SKEW = 512
CORES = 2
FAR = -1e30

norm_eps = 1e-06
rows_by_rows = (((1,), (1,)), ((), ()))
vmem = pl.BlockSpec(memory_space=pltpu.VMEM)
smem = pl.BlockSpec(memory_space=pltpu.SMEM)
anywhere = pl.BlockSpec(memory_space=pl.ANY)
params = pltpu.CompilerParams(vmem_limit_bytes=40 * 1024 * 1024)


def bias_base(position_bias):
    layers, heads, _ = position_bias.shape
    far = position_bias[:, :, 2 * CLIP :]
    ahead = PAST - CLIP + 1
    near = position_bias[:, :, 2 * CLIP - 1 : 0 : -1]
    rest = SKEW - ahead - near.shape[2]
    return jnp.concatenate(
        [
            jnp.broadcast_to(far, (layers, heads, ahead)),
            near,
            jnp.broadcast_to(far, (layers, heads, rest)),
        ],
        axis=2,
    )


def setup_body(base_ref, row_docs_ref, col_docs_ref, band_ref, mask_ref):
    layers, heads, _ = base_ref.shape
    row_block = lax.broadcasted_iota(jnp.int32, (GROUP, WINDOW), 0) // BLOCK
    col_block = lax.broadcasted_iota(jnp.int32, (GROUP, WINDOW), 1) // BLOCK
    allowed = (col_block >= row_block) & (col_block <= row_block + PAST_BLOCKS)
    for layer in range(layers):
        for head in range(heads):
            row = base_ref[layer, head : head + 1, :]
            skewed = pltpu.roll(
                jnp.broadcast_to(row, (GROUP, SKEW)), 0, 1, stride=1, stride_axis=0
            )
            band_ref[layer, head] = jnp.where(allowed, skewed[:, :WINDOW], FAR)
    for group in range(mask_ref.shape[0]):
        start = group * GROUP
        own = col_docs_ref[start : start + GROUP, :]
        seen = row_docs_ref[:, start : start + WINDOW]
        mask_ref[group] = jnp.where(own == seen, 0.0, FAR)


def setup(base, row_docs, col_docs):
    layers, heads, _ = base.shape
    groups = col_docs.shape[0] // GROUP
    return pl.pallas_call(
        setup_body,
        out_shape=(
            jax.ShapeDtypeStruct((layers, heads, GROUP, WINDOW), jnp.float32),
            jax.ShapeDtypeStruct((groups, GROUP, WINDOW), jnp.float32),
        ),
        in_specs=[vmem, vmem, vmem],
        out_specs=(vmem, vmem),
        compiler_params=params,
        name="setup",
    )(base, row_docs, col_docs)


def block_columns(core, blocks):
    if len(blocks) == 1:
        return [(blocks[0], 0, 0)]
    width = blocks[0].shape[2]
    return [
        (ref, z, pl.multiple_of((CORES * z + (core if side == 0 else 1 - core)) * width, 128))
        for side, ref in enumerate(blocks)
        for z in range(ref.shape[0])
    ]


def proj_body(layer, first, count, *refs):
    core_ref = refs[0]
    blocks = refs[1 : 1 + count]
    rest = list(refs[1 + count :])
    if not first:
        resid_ref, post_ref = rest[:2]
        rest = rest[2:]
    pre_ref = rest[0]
    weights = rest[1:5]
    if first:
        resid_out, q_ref, kv_ref, tail_ref, gate_ref = rest[5:10]
    else:
        resid_out, q_ref, kv_ref, tail_ref, gate_ref = rest[5:10]
    weight_buf, normed_ref, inv_ref, sems = rest[10:]
    copies = [
        pltpu.make_async_copy(weight.at[layer], weight_buf.at[at], sems.at[at])
        for at, weight in enumerate(weights)
    ]
    for copy in copies:
        copy.start()
    rows = normed_ref.shape[0]
    step = BLOCK
    placed = block_columns(core_ref[0], blocks)
    width = blocks[0].shape[2]

    def lane_sum(square):
        total = square[:, :128]
        for at in range(128, square.shape[1], 128):
            total = total + square[:, at : at + 128]
        return total

    def one(index, carry):
        at = pl.ds(pl.multiple_of(index * step, step), step)
        if not first:
            total = jnp.zeros((step, 128), jnp.float32)
            for ref, z, _ in placed:
                part = ref[z, at, :].astype(jnp.float32)
                total = total + lane_sum(part * part)
            inv_out = lax.rsqrt(jnp.sum(total, axis=1, keepdims=True) / D + norm_eps)
        total = jnp.zeros((step, 128), jnp.float32)
        for ref, z, col in placed:
            cols = pl.ds(col, width)
            if first:
                new = ref[z, at, :]
            else:
                part = ref[z, at, :].astype(jnp.float32)
                old = resid_ref[at, cols].astype(jnp.float32)
                new = (old + part * inv_out * post_ref[:, cols]).astype(jnp.bfloat16)
            resid_out[at, cols] = new
            wide = new.astype(jnp.float32)
            total = total + lane_sum(wide * wide)
            normed_ref[at, cols] = (wide * pre_ref[:, cols]).astype(jnp.bfloat16)
        inv_in = lax.rsqrt(jnp.sum(total, axis=1, keepdims=True) / D + norm_eps)
        inv_ref[at, :] = jnp.broadcast_to(inv_in, (step, 128))
        return carry

    lax.fori_loop(0, rows // step, one, 0)
    own = q_ref.shape[1]
    tail_start = rows - PAST
    inv = inv_ref[:, :1]
    for at, copy in enumerate(copies):
        copy.wait()
        product = lax.dot_general(
            normed_ref[...], weight_buf[at], rows_by_rows, preferred_element_type=jnp.float32
        )
        product = (product * inv).astype(jnp.bfloat16)
        if at < 2:
            kv_ref[:, at * own : (at + 1) * own] = product
            tail_ref[:, at * own : (at + 1) * own] = product[tail_start:]
        elif at == 2:
            q_ref[...] = product * jnp.bfloat16(HD ** (-0.5))
        else:
            gate_ref[...] = product


def project(layer, core, blocks, resid, post, pre, weights):
    first = resid is None
    rows = blocks[0].shape[1]
    own = weights[0].shape[1]
    bf = jnp.bfloat16
    operands = [core, *blocks] + ([] if first else [resid, post]) + [pre, *weights]
    specs = [smem] + [vmem] * len(blocks) + ([] if first else [vmem, vmem]) + [vmem]
    specs = specs + [anywhere] * 4
    return pl.pallas_call(
        functools.partial(proj_body, layer, first, len(blocks)),
        out_shape=(
            jax.ShapeDtypeStruct((rows, D), bf),
            jax.ShapeDtypeStruct((rows, own), bf),
            jax.ShapeDtypeStruct((rows, 2 * own), bf),
            jax.ShapeDtypeStruct((PAST, 2 * own), bf),
            jax.ShapeDtypeStruct((rows, own), bf),
        ),
        in_specs=specs,
        out_specs=(vmem,) * 5,
        scratch_shapes=[
            pltpu.VMEM((4, own, D), bf),
            pltpu.VMEM((rows, D), bf),
            pltpu.VMEM((rows, 128), jnp.float32),
            pltpu.SemaphoreType.DMA((4,)),
        ],
        compiler_params=params,
        name="project",
    )(*operands)


def attend_body(q_ref, kv_ref, halo_ref, gate_ref, band_ref, mask_ref, mixed_ref, ext_ref):
    rows, own = q_ref.shape
    span = min(own, 128)
    ext_ref[:PAST, :] = halo_ref[...]
    ext_ref[PAST:, :] = kv_ref[...]
    lane = lax.broadcasted_iota(jnp.int32, (GROUP, span), 1) // HD
    for group in range(rows // GROUP):
        at = slice(group * GROUP, (group + 1) * GROUP)
        seen = slice(group * GROUP, group * GROUP + WINDOW)
        mask = mask_ref[group]
        for start in range(0, own, span):
            cols = slice(start, start + span)
            query = q_ref[at, cols]
            keys = ext_ref[seen, cols]
            values = ext_ref[seen, own + start : own + start + span]
            result = None
            for sub in range(span // HD):
                picked = jnp.where(lane == sub, query, jnp.zeros_like(query))
                scores = lax.dot_general(
                    picked, keys, rows_by_rows, preferred_element_type=jnp.float32
                )
                scores = scores + band_ref[0, start // HD + sub] + mask
                lifted = jnp.exp(scores - jnp.max(scores, axis=1, keepdims=True))
                total = jnp.sum(lifted, axis=1, keepdims=True)
                part = jnp.dot(
                    lifted.astype(jnp.bfloat16), values, preferred_element_type=jnp.float32
                )
                part = part / total
                result = part if result is None else jnp.where(lane == sub, part, result)
            gate = gate_ref[at, cols].astype(jnp.float32)
            mixed_ref[at, cols] = (result * (gate / (1.0 + jnp.exp(-gate)))).astype(jnp.bfloat16)


def attend(layer, q, kv, halo, gate, band, mask):
    rows, own = q.shape
    whole = lambda a: pl.BlockSpec(a.shape, lambda i: (0,) * a.ndim)
    picked = pl.BlockSpec((1,) + band.shape[1:], lambda i: (layer, 0, 0, 0))
    return pl.pallas_call(
        attend_body,
        grid=(1,),
        out_shape=jax.ShapeDtypeStruct((rows, own), jnp.bfloat16),
        in_specs=[whole(q), whole(kv), whole(halo), whole(gate), picked, whole(mask)],
        out_specs=whole(q),
        scratch_shapes=[pltpu.VMEM((PAST + rows, 2 * own), jnp.bfloat16)],
        compiler_params=params,
        name="attend",
    )(q, kv, halo, gate, band, mask)


def out_body(layer, count, last, *refs):
    core_ref = refs[0]
    blocks = refs[1 : 1 + count]
    weight_ref, branch_ref = refs[1 + count : 3 + count]
    rest = refs[3 + count :]
    if last:
        square_ref, rest = rest[0], rest[1:]
    weight_buf, mixed_ref, sem = rest
    copy = pltpu.make_async_copy(weight_ref.at[layer], weight_buf, sem)
    copy.start()
    width = blocks[0].shape[2]
    for ref, z, col in block_columns(core_ref[0], blocks):
        mixed_ref[:, pl.ds(col, width)] = ref[z]
    copy.wait()
    branch = lax.dot_general(
        mixed_ref[...], weight_buf[...], rows_by_rows, preferred_element_type=jnp.float32
    ).astype(jnp.bfloat16)
    branch_ref[...] = branch
    if last:
        wide = branch.astype(jnp.float32)
        total = jnp.sum(wide * wide, axis=1, keepdims=True)
        square_ref[...] = jnp.transpose(jnp.broadcast_to(total, (total.shape[0], 128)))[:8]


def out_project(layer, core, blocks, weight, last):
    rows = blocks[0].shape[1]
    own = weight.shape[1]
    shapes = [jax.ShapeDtypeStruct((rows, own), jnp.bfloat16)]
    if last:
        shapes.append(jax.ShapeDtypeStruct((8, rows), jnp.float32))
    return pl.pallas_call(
        functools.partial(out_body, layer, len(blocks), last),
        out_shape=tuple(shapes),
        in_specs=[smem] + [vmem] * len(blocks) + [anywhere],
        out_specs=(vmem,) * len(shapes),
        scratch_shapes=[
            pltpu.VMEM((own, D), jnp.bfloat16),
            pltpu.VMEM((rows, D), jnp.bfloat16),
            pltpu.SemaphoreType.DMA,
        ],
        compiler_params=params,
        name="out_project",
    )(core, *blocks, weight)


def finish_body(resid_ref, branch_ref, gain_ref, *refs):
    out_ref = refs[-1]
    total = refs[0][...]
    for ref in refs[1:-1]:
        total = total + ref[...]
    rows = out_ref.shape[0]
    column = jnp.transpose(jnp.broadcast_to(total[:1], (128, rows)))[:, :1]
    inv_out = lax.rsqrt(column / D + norm_eps)
    old = resid_ref[...].astype(jnp.float32)
    branch = branch_ref[...].astype(jnp.float32)
    out_ref[...] = (old + branch * inv_out * gain_ref[...]).astype(jnp.bfloat16)


def finish(resid_cols, branch, gain_cols, totals):
    return pl.pallas_call(
        finish_body,
        out_shape=jax.ShapeDtypeStruct(branch.shape, jnp.bfloat16),
        in_specs=[vmem] * (3 + len(totals)),
        out_specs=vmem,
        compiler_params=params,
        name="finish",
    )(resid_cols, branch, gain_cols, *totals)


def partner(x):
    size = lax.axis_size("tp")
    return lax.ppermute(x, "tp", [(i, i ^ 1) for i in range(size)])


def gather(x):
    size = lax.axis_size("tp")
    if x.shape[1] % 128 or size % CORES:
        return (lax.all_gather(x, "tp", axis=1, tiled=True)[None],)
    lines = [list(range(core, size, CORES)) for core in range(CORES)]
    own = lax.all_gather(x, "tp", axis=0, axis_index_groups=lines)
    return own, partner(own)


def total_over_features(square):
    size = lax.axis_size("tp")
    if size % CORES or size > 8:
        return (lax.psum(square, "tp"),)
    both = square + partner(square)
    return (both,) + tuple(
        lax.ppermute(both, "tp", [(i, (i + hop) % size) for i in range(size)])
        for hop in range(CORES, size, CORES)
    )


def from_behind(block):
    size = lax.axis_size("sp")
    return lax.ppermute(block, "sp", [(i, (i + 1) % size) for i in range(size)])


def local(
    tokens,
    documents,
    pre_gain,
    query_weight,
    key_weight,
    value_weight,
    gate_weight,
    out_weight,
    position_bias,
    post_gain,
):
    rows, own = tokens.shape
    tp_at = lax.axis_index("tp")
    core = jnp.reshape(tp_at % CORES, (1,)).astype(jnp.int32)
    doc_tags = documents + 1
    behind = from_behind(doc_tags[rows - PAST :])
    behind = jnp.where(lax.axis_index("sp") == 0, 0, behind)
    row_docs = jnp.concatenate([behind, doc_tags])[None, :]
    col_docs = doc_tags[:, None]
    blocks = gather(tokens)
    band, mask = setup(bias_base(position_bias), row_docs, col_docs)
    residual = None
    for layer in range(LAYERS):
        residual, q, kv, tail, gate = project(
            layer,
            core,
            blocks,
            residual,
            post_gain[layer - 1 : layer] if layer else None,
            pre_gain[layer : layer + 1],
            (key_weight, value_weight, query_weight, gate_weight),
        )
        halo = from_behind(tail)
        mixed = attend(layer, q, kv, halo, gate, band, mask)
        last = layer + 1 == LAYERS
        result = out_project(layer, core, gather(mixed), out_weight, last)
        if not last:
            blocks = gather(result[0])
    branch, square = result
    start = tp_at * own
    return finish(
        lax.dynamic_slice_in_dim(residual, start, own, 1),
        branch,
        lax.dynamic_slice_in_dim(post_gain[LAYERS - 1 :], start, own, 1),
        total_over_features(square),
    )


def solution(mesh):
    placed = (
        P("sp", "tp"),
        P("sp"),
        P(),
        P(None, "tp", None),
        P(None, "tp", None),
        P(None, "tp", None),
        P(None, "tp", None),
        P(None, "tp", None),
        P(None, "tp", None),
        P(),
    )
    return jax.shard_map(
        local, mesh=mesh, in_specs=placed, out_specs=P("sp", "tp"), check_vma=False
    )
```

time: 293 us -> 206 us (0.70)
  waiting for transfers between devices: 141 us -> 41.5 us
  blocking collectives: 14.7 us -> 112 us
  matrix products: 53.6 us -> 0 us
  Pallas kernels: 0 us -> 33.5 us
  local copies, waits for them, and re-layouts: 42.8 us -> 11.1 us
  between operations: 14.2 us -> 0.23 us
  other arithmetic: 12.5 us -> 0.78 us
  starting transfers between devices: 13.2 us -> 6.78 us
    all_gather x6 -> x0, waiting for transfers between devices: 137 us -> none  [the longest x3 81.5 us: local(): lax.all_gather(mixed_rows, 'tp', axis=1, tiled=True)]
    all_gather x0 -> x6, blocking collectives: none -> 112 us  [gather(): own = lax.all_gather(x, 'tp', axis=0, axis_index_groups=lines)]
    dot_general x18 -> x0, matrix products: 40.9 us -> none  [the longest x12 25.4 us: local(): lax.dot_general(normed, weight, inner_dims, preferred_element_type=jnp.fl...]
    ppermute x4 -> x14, waiting for transfers between devices: 2.7 us -> 41.5 us  [the longest x4 24.8 us: from_behind(): return lax.ppermute(block, 'sp', [(i, (i + 1) % size) for i in range(size)])]
    pallas_call x0 -> x11, Pallas kernels: none -> 33.5 us  [the longest x3 17.7 us: project(): pl.pallas_call(functools.partial(proj_body, layer, first, len(blocks)), o...]
    slice x49 -> x5, local copies, waits for them, and re-layouts: 23.2 us -> 2.51 us  [the longest x1 0.9 us: local(): pre_gain[layer:layer + 1]]
    psum x1 -> x0, blocking collectives: 14.7 us -> none  [finish_columns(): total_sq = lax.psum(jnp.sum(branch_wide * branch_wide, axis=1), 'tp')]
    sub x3 -> x0, matrix products: 12.7 us -> none  [attend(): lifted = jnp.exp(scores - row_max)]
  transfers between devices with their start and end apart: 10 -> 14, of which waited for: 8 -> 11; matrix products, arithmetic and copies ran while one was open for 13% -> 2% of each run, Pallas kernels for 0% -> 3%
where the time goes in v1:
time: 206 us
  blocking collectives  112 us (54%)
  waiting for transfers between devices  41.5 us (20%)
  Pallas kernels  33.5 us (16%)
  local copies, waits for them, and re-layouts  11.1 us (5%)
  starting transfers between devices  6.78 us (3%)
    all_gather x6, blocking collectives, gather(): own = lax.all_gather(x, 'tp', axis=0, axis_index_groups=lines)  112 us
    ppermute x4, waiting for transfers between devices, from_behind(): return lax.ppermute(block, 'sp', [(i, (i + 1) % size) for i in range(size)])  24.8 us
    pallas_call x3, Pallas kernels, project(): pl.pallas_call(functools.partial(proj_body, layer, first, len(blocks)), o...  17.7 us
    ppermute x7, waiting for transfers between devices, partner(): return lax.ppermute(x, 'tp', [(i, i ^ 1) for i in range(size)])  12.8 us
    pallas_call x3, Pallas kernels, attend(): pl.pallas_call(attend_body, grid=(1,), out_shape=jax.ShapeDtypeStruct((ro...  9.82 us
    unnamed x22, local copies, waits for them, and re-layouts  7.36 us
    pallas_call x3, Pallas kernels, out_project(): pl.pallas_call(functools.partial(out_body, layer, len(blocks), last), out...  4.19 us
  transfers between devices with their start and end apart: 14, of which 11 were waited for; matrix products, arithmetic and copies ran while one was open for 2% of the time, Pallas kernels for 3%

profile of v1, /device:TPU:0, one launch (start us, length us, event | category | flops | bytes accessed | tf_op | source)
XLA Modules:
  0.0 205.9 jit_solution(13748770055443151748)
XLA Ops:
  0.0 21.5 %all-gather = bf16[1536,256]{1,0:T(8,128)(2,1)S(1)} all-gather(bf16[384,256]{1,0:T(8,128)(2,1)} %param.10), channel_id=2, replica_groups={{0,2,4,6},{1,3,5,7},{8,10,12,14},{9,11,13,15},{16,18,20,22},{17,19,21,2..., dimensions={0}, use_global_device_ids=true | all-gather | bytes 983040 | tf_op jit(solution)/shard_map/all_gather | solution.py:326
  21.5 0.0 collective-permute-start
  21.5 0.7 broadcast_add_fusion
  22.2 1.5 collective-permute-start.2
  23.7 0.8 slice.29
  24.5 0.2 reverse
  24.7 0.1 slice.37
  24.7 0.8 slice_reduce_fusion
  25.5 0.1 broadcast_in_dim.24
  25.6 0.1 broadcast_in_dim.23
  25.7 0.1 pad_maximum_fusion.base_ref
  25.8 0.9 fusion.1
  26.7 0.1 broadcast_in_dim.28.col_docs_ref
  26.8 0.0 collective-permute-done.refs_2_
  26.8 0.0 copy-start.1
  26.8 1.9 copy-done.1
  28.7 1.9 copy-done.3
  30.6 1.9 copy-done.5
  32.5 5.4 %project.3 = (bf16[384,2048]{1,0:T(8,128)(2,1)S(1)}, bf16[384,256]{1,0:T(8,128)(2,1)S(1)}, bf16[384,512]{1,0:T(8,128)(2,1)S(1)}, bf16[256,512]{1,0:T(8,128)(2,1)S(1)}, bf16[384,256]{1,0:T(8,128)(2,1)S(1)}) custom-call(s32[1]{0:T(128)} %bitcast.refs_0_, bf16[4,384,256]{2,1,0:T(8,128)(2,1)S(1)} %bitcast.17, ...), custom_call_target="tpu_custom_call" | custom-call | tf_op jit(solution)/shard_map/project/pallas_call | solution.py:176
  37.8 0.0 copy-start
  37.9 1.5 collective-permute-start.1
  39.4 0.0 collective-permute-done.2
  39.4 0.9 setup.1
  40.4 6.9 %collective-permute-done.1.halo_ref = bf16[256,512]{1,0:T(8,128)(2,1)S(1)} collective-permute-done((bf16[256,512]{1,0:T(8,128)(2,1)S(1)}, bf16[256,512]{1,0:T(8,128)(2,1)S(1)}, u32[]{:S(2)}, u32[]{:S(2)}) %collective-permute-start.1) | collective-permute-done | bytes 262176 | tf_op jit(solution)/shard_map/ppermute | solution.py:343
  47.2 3.3 %attend.3 = bf16[384,256]{1,0:T(8,128)(2,1)S(1)} custom-call(bf16[384,256]{1,0:T(8,128)(2,1)S(1)} %get-tuple-element.24.q_ref, bf16[384,512]{1,0:T(8,128)(2,1)S(1)} %get-tuple-element.25.kv_ref, bf16[256,512]{1,0:T(8,128)(2,1)S(1)} %collective-permute-done.1.halo_ref, bf16[384,256]{1,0:T(8,128)(2,1)S(1)} %get-tuple-element.27.gate_ref, ...), custom_call_target="tpu_custom_call" | custom-call | tf_op jit(solution)/shard_map/attend/pallas_call | solution.py:235
  50.5 0.0 copy-start.4
  50.5 18.1 %all-gather.1 = bf16[1536,256]{1,0:T(8,128)(2,1)S(1)} all-gather(bf16[384,256]{1,0:T(8,128)(2,1)S(1)} %attend.3), channel_id=3, replica_groups={{0,2,4,6},{1,3,5,7},{8,10,12,14},{9,11,13,15},{16,18,20,22},{17,19,21,2..., dimensions={0}, use_global_device_ids=true | all-gather | bytes 983040 | tf_op jit(solution)/shard_map/all_gather | solution.py:326
  68.7 0.0 collective-permute-start.3
  68.7 2.3 %collective-permute-done.3.refs_2_ = bf16[4,384,256]{2,1,0:T(8,128)(2,1)S(1)} collective-permute-done((bf16[4,384,256]{2,1,0:T(8,128)(2,1)S(1)}, bf16[4,384,256]{2,1,0:T(8,128)(2,1)S(1)}, u32[]{:S(2)}, u32[]{:S(2)}) %collective-permute-start.3) | collective-permute-done | bytes 786464 | tf_op jit(solution)/shard_map/ppermute | solution.py:318
  71.0 0.9 out_project.3
  71.9 18.0 %all-gather.2 = bf16[1536,256]{1,0:T(8,128)(2,1)S(1)} all-gather(bf16[384,256]{1,0:T(8,128)(2,1)S(1)} %out_project.3), channel_id=4, replica_groups={{0,2,4,6},{1,3,5,7},{8,10,12,14},{9,11,13,15},{16,18,20,22},{17,19,21,2..., dimensions={0}, use_global_device_ids=true | all-gather | bytes 983040 | tf_op jit(solution)/shard_map/all_gather | solution.py:326
  89.9 0.0 collective-permute-start.4
  89.9 2.3 %collective-permute-done.4.refs_2_ = bf16[4,384,256]{2,1,0:T(8,128)(2,1)S(1)} collective-permute-done((bf16[4,384,256]{2,1,0:T(8,128)(2,1)S(1)}, bf16[4,384,256]{2,1,0:T(8,128)(2,1)S(1)}, u32[]{:S(2)}, u32[]{:S(2)}) %collective-permute-start.4) | collective-permute-done | bytes 786464 | tf_op jit(solution)/shard_map/ppermute | solution.py:318
  92.1 0.0 copy-done.4
  92.2 1.4 copy-done.7
  93.6 6.2 %project.4 = (bf16[384,2048]{1,0:T(8,128)(2,1)S(1)}, bf16[384,256]{1,0:T(8,128)(2,1)S(1)}, bf16[384,512]{1,0:T(8,128)(2,1)S(1)}, bf16[256,512]{1,0:T(8,128)(2,1)S(1)}, bf16[384,256]{1,0:T(8,128)(2,1)S(1)}) custom-call(s32[1]{0:T(128)} %bitcast.refs_0_, bf16[4,384,256]{2,1,0:T(8,128)(2,1)S(1)} %bitcast.9, ...), custom_call_target="tpu_custom_call" | custom-call | tf_op jit(solution)/shard_map/project/pallas_call | solution.py:176
  99.7 0.6 collective-permute-start.5
  100.4 8.7 %collective-permute-done.5.halo_ref = bf16[256,512]{1,0:T(8,128)(2,1)S(1)} collective-permute-done((bf16[256,512]{1,0:T(8,128)(2,1)S(1)}, bf16[256,512]{1,0:T(8,128)(2,1)S(1)}, u32[]{:S(2)}, u32[]{:S(2)}) %collective-permute-start.5) | collective-permute-done | bytes 262176 | tf_op jit(solution)/shard_map/ppermute | solution.py:343
  109.0 3.3 %attend.4 = bf16[384,256]{1,0:T(8,128)(2,1)S(1)} custom-call(bf16[384,256]{1,0:T(8,128)(2,1)S(1)} %get-tuple-element.31.q_ref, bf16[384,512]{1,0:T(8,128)(2,1)S(1)} %get-tuple-element.32.kv_ref, bf16[256,512]{1,0:T(8,128)(2,1)S(1)} %collective-permute-done.5.halo_ref, bf16[384,256]{1,0:T(8,128)(2,1)S(1)} %get-tuple-element.34.gate_ref, ...), custom_call_target="tpu_custom_call" | custom-call | tf_op jit(solution)/shard_map/attend/pallas_call | solution.py:235
  112.3 17.9 %all-gather.3 = bf16[1536,256]{1,0:T(8,128)(2,1)S(1)} all-gather(bf16[384,256]{1,0:T(8,128)(2,1)S(1)} %attend.4), channel_id=5, replica_groups={{0,2,4,6},{1,3,5,7},{8,10,12,14},{9,11,13,15},{16,18,20,22},{17,19,21,2..., dimensions={0}, use_global_device_ids=true | all-gather | bytes 983040 | tf_op jit(solution)/shard_map/all_gather | solution.py:326
  130.2 0.0 collective-permute-start.6
  130.2 2.3 %collective-permute-done.6.refs_2_ = bf16[4,384,256]{2,1,0:T(8,128)(2,1)S(1)} collective-permute-done((bf16[4,384,256]{2,1,0:T(8,128)(2,1)S(1)}, bf16[4,384,256]{2,1,0:T(8,128)(2,1)S(1)}, u32[]{:S(2)}, u32[]{:S(2)}) %collective-permute-start.6) | collective-permute-done | bytes 786464 | tf_op jit(solution)/shard_map/ppermute | solution.py:318
  132.5 0.9 out_project.4
  133.4 18.2 %all-gather.4 = bf16[1536,256]{1,0:T(8,128)(2,1)S(1)} all-gather(bf16[384,256]{1,0:T(8,128)(2,1)S(1)} %out_project.4), channel_id=6, replica_groups={{0,2,4,6},{1,3,5,7},{8,10,12,14},{9,11,13,15},{16,18,20,22},{17,19,21,2..., dimensions={0}, use_global_device_ids=true | all-gather | bytes 983040 | tf_op jit(solution)/shard_map/all_gather | solution.py:326
  151.7 0.0 collective-permute-start.7
  151.7 2.3 %collective-permute-done.7.refs_2_ = bf16[4,384,256]{2,1,0:T(8,128)(2,1)S(1)} collective-permute-done((bf16[4,384,256]{2,1,0:T(8,128)(2,1)S(1)}, bf16[4,384,256]{2,1,0:T(8,128)(2,1)S(1)}, u32[]{:S(2)}, u32[]{:S(2)}) %collective-permute-start.7) | collective-permute-done | bytes 786464 | tf_op jit(solution)/shard_map/ppermute | solution.py:318
  153.9 6.2 %project.5 = (bf16[384,2048]{1,0:T(8,128)(2,1)S(1)}, bf16[384,256]{1,0:T(8,128)(2,1)S(1)}, bf16[384,512]{1,0:T(8,128)(2,1)S(1)}, bf16[256,512]{1,0:T(8,128)(2,1)S(1)}, bf16[384,256]{1,0:T(8,128)(2,1)S(1)}) custom-call(s32[1]{0:T(128)} %bitcast.refs_0_, bf16[4,384,256]{2,1,0:T(8,128)(2,1)S(1)} %bitcast.11, ...), custom_call_target="tpu_custom_call" | custom-call | tf_op jit(solution)/shard_map/project/pallas_call | solution.py:176
  160.1 0.1 collective-permute-start.8
  160.2 9.2 %collective-permute-done.8.halo_ref = bf16[256,512]{1,0:T(8,128)(2,1)S(1)} collective-permute-done((bf16[256,512]{1,0:T(8,128)(2,1)S(1)}, bf16[256,512]{1,0:T(8,128)(2,1)S(1)}, u32[]{:S(2)}, u32[]{:S(2)}) %collective-permute-start.8) | collective-permute-done | bytes 262176 | tf_op jit(solution)/shard_map/ppermute | solution.py:343
  169.4 3.3 %attend.5 = bf16[384,256]{1,0:T(8,128)(2,1)S(1)} custom-call(bf16[384,256]{1,0:T(8,128)(2,1)S(1)} %get-tuple-element.37.q_ref, bf16[384,512]{1,0:T(8,128)(2,1)S(1)} %get-tuple-element.38.kv_ref, bf16[256,512]{1,0:T(8,128)(2,1)S(1)} %collective-permute-done.8.halo_ref, bf16[384,256]{1,0:T(8,128)(2,1)S(1)} %get-tuple-element.40.gate_ref, ...), custom_call_target="tpu_custom_call" | custom-call | tf_op jit(solution)/shard_map/attend/pallas_call | solution.py:235
  172.7 18.2 %all-gather.5 = bf16[1536,256]{1,0:T(8,128)(2,1)} all-gather(bf16[384,256]{1,0:T(8,128)(2,1)S(1)} %attend.5), channel_id=7, replica_groups={{0,2,4,6},{1,3,5,7},{8,10,12,14},{9,11,13,15},{16,18,20,22},{17,19,21,2..., dimensions={0}, use_global_device_ids=true | all-gather | bytes 983040 | tf_op jit(solution)/shard_map/all_gather | solution.py:326
  190.9 0.0 collective-permute-start.9
  190.9 2.6 %collective-permute-done.9.refs_2_ = bf16[4,384,256]{2,1,0:T(8,128)(2,1)} collective-permute-done((bf16[4,384,256]{2,1,0:T(8,128)(2,1)}, bf16[4,384,256]{2,1,0:T(8,128)(2,1)}, u32[]{:S(2)}, u32[]{:S(2)}) %collective-permute-start.9) | collective-permute-done | bytes 786464 | tf_op jit(solution)/shard_map/ppermute | solution.py:318
  193.5 2.4 %out_project.5 = (bf16[384,256]{1,0:T(8,128)(2,1)S(1)}, f32[8,384]{1,0:T(8,128)S(1)}) custom-call(s32[1]{0:T(128)} %bitcast.refs_0_, bf16[4,384,256]{2,1,0:T(8,128)(2,1)} %bitcast.6.refs_1_, bf16[4,384,256]{2,1,0:T(8,128)(2,1)} %collective-permute-done.9.refs_2_, bf16[3,256,2048]{2,1,0:T(8,128)(2,1)S(1)} %copy-done), custom_call_target="tpu_custom_call" | custom-call | tf_op jit(solution)/shard_map/out_project/pallas_call | solution.py:277
  195.9 0.2 collective-permute-start.10
  196.1 1.0 collective-permute-done.10
  197.2 2.3 %collective-permute-start.13 = (f32[8,384]{1,0:T(8,128)S(1)}, f32[8,384]{1,0:T(8,128)S(1)}, u32[]{:S(2)}, u32[]{:S(2)}) collective-permute-start(f32[8,384]{1,0:T(8,128)S(1)} %add.21.refs_0_), channel_id=1, source_target_pairs={{0,6},{1,7},{2,0},{3,1},{4,2},{5,3},{6,4},{7,5},{8,14},{9,15},{10,... | collective-permute-start | bytes 36872 | tf_op jit(solution)/shard_map/ppermute | solution.py:336
  199.5 0.0 collective-permute-start.12
  199.5 0.6 collective-permute-start.11
  200.0 0.9 constant_dynamic-slice_fusion.1.resid_ref
  201.0 0.0 collective-permute-done.13.refs_3_
  201.0 3.0 %collective-permute-done.12.refs_2_ = f32[8,384]{1,0:T(8,128)S(1)} collective-permute-done((f32[8,384]{1,0:T(8,128)S(1)}, f32[8,384]{1,0:T(8,128)S(1)}, u32[]{:S(2)}, u32[]{:S(2)}) %collective-permute-start.12) | collective-permute-done | bytes 12320 | tf_op jit(solution)/shard_map/ppermute | solution.py:336
  204.0 0.9 collective-permute-done.11.refs_1_
  205.0 0.9 finish.1
  (19 shorter events, 0.1 us)
Async XLA Ops:
  21.5 5.3 %collective-permute-start = (bf16[4,384,256]{2,1,0:T(8,128)(2,1)S(1)}, bf16[4,384,256]{2,1,0:T(8,128)(2,1)S(1)}, u32[]{:S(2)}, u32[]{:S(2)}) collective-permute-start(bf16[4,384,256]{2,1,0:T(8,128)(2,1)S(1)} %bitcast.16), channel_id=1, source_target_pairs={{0,1},{1,0},{2,3},{3,2},{4,5},{5,4},{6,7},{7,6},{8,9},{9,8},{10,11... | collective-permute-start | bytes 2359304 | tf_op jit(solution)/shard_map/ppermute | solution.py:318
  22.2 17.2 %collective-permute-start.2 = (s32[256]{0:T(256)S(1)}, s32[256]{0:T(256)S(1)}, u32[]{:S(2)}, u32[]{:S(2)}) collective-permute-start(s32[256]{0:T(256)S(1)} %slice.30), channel_id=1, source_target_pairs={{0,8},{8,16},{16,24},{24,0},{1,9},{9,17},{17,25},{25,1},{2,10},{10... | collective-permute-start | bytes 3080 | tf_op jit(solution)/shard_map/ppermute | solution.py:343
  26.8 1.9 copy-start.1
  28.7 1.9 copy-start.3
  30.6 1.9 copy-start.5
  37.8 12.7 %copy-start.6 = (bf16[384,2048]{1,0:T(8,128)(2,1)}, bf16[384,2048]{1,0:T(8,128)(2,1)S(1)}, u32[]{:S(2)}) copy-start(bf16[384,2048]{1,0:T(8,128)(2,1)S(1)} %get-tuple-element.30.refs_3_) | copy-start | bytes 4718596
  37.8 33.1 %copy-start = (bf16[3,256,2048]{2,1,0:T(8,128)(2,1)S(1)}, bf16[3,256,2048]{2,1,0:T(8,128)(2,1)}, u32[]{:S(2)}) copy-start(bf16[3,256,2048]{2,1,0:T(8,128)(2,1)} %refs_3_.5) | copy-start | bytes 9437188
  37.9 9.4 %collective-permute-start.1 = (bf16[256,512]{1,0:T(8,128)(2,1)S(1)}, bf16[256,512]{1,0:T(8,128)(2,1)S(1)}, u32[]{:S(2)}, u32[]{:S(2)}) collective-permute-start(bf16[256,512]{1,0:T(8,128)(2,1)S(1)} %get-tuple-element.26), channel_id=1, source_target_pairs={{0,8},{8,16},{16,24},{24,0},{1,9},{9,17},{17,25},{25,1},{2,10},{10... | collective-permute-start | bytes 786440 | tf_op jit(solution)/shard_map/ppermute | solution.py:343
  50.5 41.6 %copy-start.4 = (bf16[3,256,2048]{2,1,0:T(8,128)(2,1)S(1)}, bf16[3,256,2048]{2,1,0:T(8,128)(2,1)}, u32[]{:S(2)}) copy-start(bf16[3,256,2048]{2,1,0:T(8,128)(2,1)} %refs_7_.5) | copy-start | bytes 9437188
  68.7 21.2 %copy-start.9 = (f32[3,2048]{1,0:T(4,128)S(1)}, f32[3,2048]{1,0:T(4,128)}, u32[]{:S(2)}) copy-start(f32[3,2048]{1,0:T(4,128)} %param.19) | copy-start | bytes 73732
  68.7 23.5 %copy-start.2 = (bf16[3,256,2048]{2,1,0:T(8,128)(2,1)S(1)}, bf16[3,256,2048]{2,1,0:T(8,128)(2,1)}, u32[]{:S(2)}) copy-start(bf16[3,256,2048]{2,1,0:T(8,128)(2,1)} %refs_6_.5) | copy-start | bytes 9437188
  68.7 2.3 %collective-permute-start.3 = (bf16[4,384,256]{2,1,0:T(8,128)(2,1)S(1)}, bf16[4,384,256]{2,1,0:T(8,128)(2,1)S(1)}, u32[]{:S(2)}, u32[]{:S(2)}) collective-permute-start(bf16[4,384,256]{2,1,0:T(8,128)(2,1)S(1)} %bitcast.12), channel_id=1, source_target_pairs={{0,1},{1,0},{2,3},{3,2},{4,5},{5,4},{6,7},{7,6},{8,9},{9,8},{10,11... | collective-permute-start | bytes 2359304 | tf_op jit(solution)/shard_map/ppermute | solution.py:318
  89.9 2.3 %collective-permute-start.4 = (bf16[4,384,256]{2,1,0:T(8,128)(2,1)S(1)}, bf16[4,384,256]{2,1,0:T(8,128)(2,1)S(1)}, u32[]{:S(2)}, u32[]{:S(2)}) collective-permute-start(bf16[4,384,256]{2,1,0:T(8,128)(2,1)S(1)} %bitcast.8), channel_id=1, source_target_pairs={{0,1},{1,0},{2,3},{3,2},{4,5},{5,4},{6,7},{7,6},{8,9},{9,8},{10,11... | collective-permute-start | bytes 2359304 | tf_op jit(solution)/shard_map/ppermute | solution.py:318
  92.2 1.4 copy-start.7
  99.7 9.3 %collective-permute-start.5 = (bf16[256,512]{1,0:T(8,128)(2,1)S(1)}, bf16[256,512]{1,0:T(8,128)(2,1)S(1)}, u32[]{:S(2)}, u32[]{:S(2)}) collective-permute-start(bf16[256,512]{1,0:T(8,128)(2,1)S(1)} %get-tuple-element.33), channel_id=1, source_target_pairs={{0,8},{8,16},{16,24},{24,0},{1,9},{9,17},{17,25},{25,1},{2,10},{10... | collective-permute-start | bytes 786440 | tf_op jit(solution)/shard_map/ppermute | solution.py:343
  130.2 2.3 %collective-permute-start.6 = (bf16[4,384,256]{2,1,0:T(8,128)(2,1)S(1)}, bf16[4,384,256]{2,1,0:T(8,128)(2,1)S(1)}, u32[]{:S(2)}, u32[]{:S(2)}) collective-permute-start(bf16[4,384,256]{2,1,0:T(8,128)(2,1)S(1)} %bitcast.14), channel_id=1, source_target_pairs={{0,1},{1,0},{2,3},{3,2},{4,5},{5,4},{6,7},{7,6},{8,9},{9,8},{10,11... | collective-permute-start | bytes 2359304 | tf_op jit(solution)/shard_map/ppermute | solution.py:318
  151.7 2.3 %collective-permute-start.7 = (bf16[4,384,256]{2,1,0:T(8,128)(2,1)S(1)}, bf16[4,384,256]{2,1,0:T(8,128)(2,1)S(1)}, u32[]{:S(2)}, u32[]{:S(2)}) collective-permute-start(bf16[4,384,256]{2,1,0:T(8,128)(2,1)S(1)} %bitcast.10), channel_id=1, source_target_pairs={{0,1},{1,0},{2,3},{3,2},{4,5},{5,4},{6,7},{7,6},{8,9},{9,8},{10,11... | collective-permute-start | bytes 2359304 | tf_op jit(solution)/shard_map/ppermute | solution.py:318
  160.1 30.8 %copy-start.8 = (bf16[384,2048]{1,0:T(8,128)(2,1)}, bf16[384,2048]{1,0:T(8,128)(2,1)S(1)}, u32[]{:S(2)}) copy-start(bf16[384,2048]{1,0:T(8,128)(2,1)S(1)} %get-tuple-element.36) | copy-start | bytes 4718596
  160.1 9.3 %collective-permute-start.8 = (bf16[256,512]{1,0:T(8,128)(2,1)S(1)}, bf16[256,512]{1,0:T(8,128)(2,1)S(1)}, u32[]{:S(2)}, u32[]{:S(2)}) collective-permute-start(bf16[256,512]{1,0:T(8,128)(2,1)S(1)} %get-tuple-element.39), channel_id=1, source_target_pairs={{0,8},{8,16},{16,24},{24,0},{1,9},{9,17},{17,25},{25,1},{2,10},{10... | collective-permute-start | bytes 786440 | tf_op jit(solution)/shard_map/ppermute | solution.py:343
  190.9 2.6 %collective-permute-start.9 = (bf16[4,384,256]{2,1,0:T(8,128)(2,1)}, bf16[4,384,256]{2,1,0:T(8,128)(2,1)}, u32[]{:S(2)}, u32[]{:S(2)}) collective-permute-start(bf16[4,384,256]{2,1,0:T(8,128)(2,1)} %bitcast.6.refs_1_), channel_id=1, source_target_pairs={{0,1},{1,0},{2,3},{3,2},{4,5},{5,4},{6,7},{7,6},{8,9},{9,8},{10,11... | collective-permute-start | bytes 2359304 | tf_op jit(solution)/shard_map/ppermute | solution.py:318
  195.9 1.2 collective-permute-start.10
  197.2 3.8 %collective-permute-start.13 = (f32[8,384]{1,0:T(8,128)S(1)}, f32[8,384]{1,0:T(8,128)S(1)}, u32[]{:S(2)}, u32[]{:S(2)}) collective-permute-start(f32[8,384]{1,0:T(8,128)S(1)} %add.21.refs_0_), channel_id=1, source_target_pairs={{0,6},{1,7},{2,0},{3,1},{4,2},{5,3},{6,4},{7,5},{8,14},{9,15},{10,... | collective-permute-start | bytes 36872 | tf_op jit(solution)/shard_map/ppermute | solution.py:336
  199.5 4.6 %collective-permute-start.12 = (f32[8,384]{1,0:T(8,128)S(1)}, f32[8,384]{1,0:T(8,128)S(1)}, u32[]{:S(2)}, u32[]{:S(2)}) collective-permute-start(f32[8,384]{1,0:T(8,128)S(1)} %add.21.refs_0_), channel_id=1, source_target_pairs={{0,4},{1,5},{2,6},{3,7},{4,0},{5,1},{6,2},{7,3},{8,12},{9,13},{10,... | collective-permute-start | bytes 36872 | tf_op jit(solution)/shard_map/ppermute | solution.py:336
  199.5 5.5 %collective-permute-start.11 = (f32[8,384]{1,0:T(8,128)S(1)}, f32[8,384]{1,0:T(8,128)S(1)}, u32[]{:S(2)}, u32[]{:S(2)}) collective-permute-start(f32[8,384]{1,0:T(8,128)S(1)} %add.21.refs_0_), channel_id=1, source_target_pairs={{0,2},{1,3},{2,4},{3,5},{4,6},{5,7},{6,0},{7,1},{8,10},{9,11},{10,... | collective-permute-start | bytes 36872 | tf_op jit(solution)/shard_map/ppermute | solution.py:336

commit v2 on v1

v2 whole, which is shorter than its diff:
```python
import functools

import jax
import jax.numpy as jnp
from jax import lax
from jax.experimental import pallas as pl
from jax.experimental.pallas import tpu as pltpu
from jax.sharding import PartitionSpec as P

D = 2048
HD = 64
BLOCK = 64
PAST_BLOCKS = 4
LAYERS = 3
PAST = 256
CLIP = 128
GROUP = 2 * BLOCK
WINDOW = PAST + GROUP
SKEW = 512
CORES = 2
FAR = -1e30

norm_eps = 1e-06
rows_by_rows = (((1,), (1,)), ((), ()))
vmem = pl.BlockSpec(memory_space=pltpu.VMEM)
smem = pl.BlockSpec(memory_space=pltpu.SMEM)
hbm = pl.BlockSpec(memory_space=pltpu.HBM)
params = pltpu.CompilerParams(vmem_limit_bytes=40 * 1024 * 1024)


def turn(vector, axis):
    size = GROUP
    diagonal = lax.broadcasted_iota(jnp.int32, (size, size), 0) == lax.broadcasted_iota(
        jnp.int32, (size, size), 1
    )
    spread = jnp.where(diagonal, jnp.broadcast_to(vector, (size, size)), jnp.zeros_like(vector))
    return jnp.sum(spread, axis=axis, keepdims=True)


def setup_body(sp_ref, bias_ref, docs_ref, behind_ref, band_ref, mask_ref):
    layers, heads, entries = bias_ref.shape
    row_block = lax.broadcasted_iota(jnp.int32, (GROUP, WINDOW), 0) // BLOCK
    col_block = lax.broadcasted_iota(jnp.int32, (GROUP, WINDOW), 1) // BLOCK
    allowed = (col_block >= row_block) & (col_block <= row_block + PAST_BLOCKS)
    shift = lax.broadcasted_iota(jnp.int32, (entries, SKEW), 1)
    entry = jnp.where(shift < WINDOW, jnp.minimum(PAST - shift, CLIP) + CLIP, 2 * CLIP)
    pick = (lax.broadcasted_iota(jnp.int32, (entries, SKEW), 0) == entry).astype(jnp.float32)
    for layer in range(layers):
        base = lax.dot_general(
            bias_ref[layer],
            pick,
            (((1,), (0,)), ((), ())),
            precision=lax.Precision.HIGHEST,
            preferred_element_type=jnp.float32,
        )
        for head in range(heads):
            row = jnp.broadcast_to(base[head : head + 1, :], (GROUP, SKEW))
            skewed = pltpu.roll(row, 0, 1, stride=1, stride_axis=0)
            band_ref[layer, head] = jnp.where(allowed, skewed[:, :WINDOW], FAR)
    behind = jnp.where(sp_ref[0] == 0, -1, behind_ref[...])
    docs = docs_ref[...]
    seen = jnp.concatenate([behind, docs], axis=1)
    for group in range(mask_ref.shape[0]):
        start = group * GROUP
        own = turn(docs[:, start : start + GROUP], 1)
        mask_ref[group] = jnp.where(own == seen[:, start : start + WINDOW], 0.0, FAR)


def setup(sp_at, position_bias, docs, behind):
    layers, heads, _ = position_bias.shape
    groups = docs.shape[1] // GROUP
    return pl.pallas_call(
        setup_body,
        out_shape=(
            jax.ShapeDtypeStruct((layers, heads, GROUP, WINDOW), jnp.float32),
            jax.ShapeDtypeStruct((groups, GROUP, WINDOW), jnp.float32),
        ),
        in_specs=[smem, vmem, vmem, vmem],
        out_specs=(vmem, vmem),
        compiler_params=params,
        name="setup",
    )(sp_at, position_bias, docs, behind)


def block_columns(core, blocks):
    if len(blocks) == 1:
        return [(blocks[0], 0, 0)]
    width = blocks[0].shape[2]
    return [
        (ref, z, pl.multiple_of((CORES * z + (core if side == 0 else 1 - core)) * width, 128))
        for side, ref in enumerate(blocks)
        for z in range(ref.shape[0])
    ]


def lane_sum(square):
    total = square[:, :128]
    for at in range(128, square.shape[1], 128):
        total = total + square[:, at : at + 128]
    return total


def update_rows(core, blocks, offset, resid_ref, post_ref, pre_ref, resid_out, normed_ref, inv_ref):
    step = BLOCK
    placed = block_columns(core, blocks)
    width = blocks[0].shape[2]

    def one(index, carry):
        at = pl.ds(pl.multiple_of(index * step, step), step)
        source = pl.ds(pl.multiple_of(offset + index * step, step), step)
        if resid_ref is not None:
            total = jnp.zeros((step, 128), jnp.float32)
            for ref, z, _ in placed:
                part = ref[z, source, :].astype(jnp.float32)
                total = total + lane_sum(part * part)
            inv_out = lax.rsqrt(jnp.sum(total, axis=1, keepdims=True) / D + norm_eps)
        total = jnp.zeros((step, 128), jnp.float32)
        for ref, z, col in placed:
            cols = pl.ds(col, width)
            if resid_ref is None:
                new = ref[z, source, :]
            else:
                part = ref[z, source, :].astype(jnp.float32)
                old = resid_ref[at, cols].astype(jnp.float32)
                new = (old + part * inv_out * post_ref[:, cols]).astype(jnp.bfloat16)
            resid_out[at, cols] = new
            wide = new.astype(jnp.float32)
            total = total + lane_sum(wide * wide)
            normed_ref[at, cols] = (wide * pre_ref[:, cols]).astype(jnp.bfloat16)
        inv_in = lax.rsqrt(jnp.sum(total, axis=1, keepdims=True) / D + norm_eps)
        inv_ref[at, :] = jnp.broadcast_to(inv_in, (step, 128))
        return carry

    lax.fori_loop(0, resid_out.shape[0] // step, one, 0)


def scaled_product(normed_ref, inv_ref, weight):
    product = lax.dot_general(
        normed_ref[...], weight, rows_by_rows, preferred_element_type=jnp.float32
    )
    return (product * inv_ref[:, :1]).astype(jnp.bfloat16)


def fetch(layer, weights, weight_buf, sems):
    copies = [
        pltpu.make_async_copy(weight.at[layer], weight_buf.at[at], sems.at[at])
        for at, weight in enumerate(weights)
    ]
    for copy in copies:
        copy.start()
    return copies


def tail_body(layer, first, count, offset, *refs):
    core_ref, refs = refs[0], refs[1:]
    blocks, refs = refs[:count], refs[count:]
    resid_ref = post_ref = None
    if not first:
        (resid_ref, post_ref), refs = refs[:2], refs[2:]
    pre_ref, weights = refs[0], refs[1:3]
    resid_out, normed_ref, inv_ref, tail_ref, weight_buf, sems = refs[3:]
    copies = fetch(layer, weights, weight_buf, sems)
    update_rows(
        core_ref[0], blocks, offset, resid_ref, post_ref, pre_ref, resid_out, normed_ref, inv_ref
    )
    own = weight_buf.shape[1]
    for at, copy in enumerate(copies):
        copy.wait()
        tail_ref[:, at * own : (at + 1) * own] = scaled_product(
            normed_ref, inv_ref, weight_buf[at]
        )


def project_tail(layer, core, blocks, resid, post, pre, weights):
    first = resid is None
    rows = blocks[0].shape[1]
    own = weights[0].shape[1]
    bf = jnp.bfloat16
    operands = [core, *blocks] + ([] if first else [resid, post]) + [pre, *weights]
    specs = [smem] + [vmem] * (len(operands) - 3) + [hbm] * 2
    return pl.pallas_call(
        functools.partial(tail_body, layer, first, len(blocks), rows - PAST),
        out_shape=(
            jax.ShapeDtypeStruct((PAST, D), bf),
            jax.ShapeDtypeStruct((PAST, D), bf),
            jax.ShapeDtypeStruct((PAST, 128), jnp.float32),
            jax.ShapeDtypeStruct((PAST, 2 * own), bf),
        ),
        in_specs=specs,
        out_specs=(vmem,) * 4,
        scratch_shapes=[pltpu.VMEM((2, own, D), bf), pltpu.SemaphoreType.DMA((2,))],
        compiler_params=params,
        name="project_tail",
    )(*operands)


def attend_group(query, gate, ext_ref, seen, band_ref, mask, own):
    span = min(own, 128)
    lane = lax.broadcasted_iota(jnp.int32, (GROUP, span), 1) // HD
    results = []
    for start in range(0, own, span):
        cols = slice(start, start + span)
        keys = ext_ref[seen, cols]
        values = ext_ref[seen, own + start : own + start + span]
        result = None
        for sub in range(span // HD):
            picked = jnp.where(lane == sub, query[:, cols], jnp.zeros((), query.dtype))
            scores = lax.dot_general(
                picked, keys, rows_by_rows, preferred_element_type=jnp.float32
            )
            scores = scores + band_ref[0, start // HD + sub] + mask
            lifted = jnp.exp(scores - jnp.max(scores, axis=1, keepdims=True))
            total = jnp.sum(lifted, axis=1, keepdims=True)
            part = jnp.dot(lifted.astype(jnp.bfloat16), values, preferred_element_type=jnp.float32)
            part = part / total
            result = part if result is None else jnp.where(lane == sub, part, result)
        wide = gate[:, cols].astype(jnp.float32)
        results.append((result * (wide / (1.0 + jnp.exp(-wide)))).astype(jnp.bfloat16))
    return results


def store_group(mixed_ref, at, results):
    start = 0
    for result in results:
        mixed_ref[at, start : start + result.shape[1]] = result
        start = start + result.shape[1]


def local_body(layer, first, count, *refs):
    core_ref, refs = refs[0], refs[1:]
    blocks, refs = refs[:count], refs[count:]
    resid_ref = post_ref = None
    if not first:
        (resid_ref, post_ref), refs = refs[:2], refs[2:]
    pre_ref, tail_normed_ref, tail_inv_ref, tail_ref, band_ref, mask_ref = refs[:6]
    weights = refs[6:10]
    resid_out, head_ref, query_out, gate_out, mixed_ref = refs[10:15]
    weight_buf, sems, normed_ref, inv_ref, ext_ref = refs[15:]
    copies = fetch(layer, weights, weight_buf, sems)
    head_rows = resid_out.shape[0]
    update_rows(
        core_ref[0], blocks, 0, resid_ref, post_ref, pre_ref, resid_out, normed_ref, inv_ref
    )
    own = weight_buf.shape[1]
    rest = query_out.shape[0]
    cut = rest - head_rows
    pieces = []
    for at, copy in enumerate(copies):
        copy.wait()
        head = scaled_product(normed_ref, inv_ref, weight_buf[at])
        if at < 2:
            head_ref[:, at * own : (at + 1) * own] = head
            continue
        tail = scaled_product(tail_normed_ref, tail_inv_ref, weight_buf[at])
        if at == 2:
            head = head * jnp.bfloat16(HD ** (-0.5))
            tail = tail * jnp.bfloat16(HD ** (-0.5))
        target = query_out if at == 2 else gate_out
        target[:head_rows] = head
        target[head_rows:] = tail[:cut]
        pieces.append(tail[cut:])
    ext_ref[:head_rows] = head_ref[...]
    ext_ref[head_rows:] = tail_ref[...]
    groups = mask_ref.shape[0]
    for index, group in enumerate(range(rest // GROUP, groups)):
        at = slice(index * GROUP, (index + 1) * GROUP)
        seen = slice(group * GROUP - PAST, group * GROUP - PAST + WINDOW)
        store_group(
            mixed_ref,
            at,
            attend_group(
                pieces[0][at], pieces[1][at], ext_ref, seen, band_ref, mask_ref[group], own
            ),
        )


def layer_of(band, layer):
    return pl.BlockSpec((1,) + band.shape[1:], lambda i: (layer, 0, 0, 0))


def whole_of(shape):
    return pl.BlockSpec(shape, lambda i: (0,) * len(shape))


def project_local(layer, core, blocks, resid, post, pre, tail_parts, band, mask, weights):
    first = resid is None
    rows = blocks[0].shape[1]
    own = weights[0].shape[1]
    head_rows = rows - PAST
    bf = jnp.bfloat16
    moved = [*blocks] + ([] if first else [resid, post]) + [pre, *tail_parts]
    operands = [core, *moved, band, mask, *weights]
    specs = [smem] + [whole_of(a.shape) for a in moved] + [layer_of(band, layer)]
    specs = specs + [whole_of(mask.shape)] + [hbm] * 4
    shapes = [
        ((head_rows, D), bf),
        ((head_rows, 2 * own), bf),
        ((PAST, own), bf),
        ((PAST, own), bf),
        ((rows - PAST, own), bf),
    ]
    return pl.pallas_call(
        functools.partial(local_body, layer, first, len(blocks)),
        grid=(1,),
        out_shape=tuple(jax.ShapeDtypeStruct(shape, kind) for shape, kind in shapes),
        in_specs=specs,
        out_specs=tuple(whole_of(shape) for shape, _ in shapes),
        scratch_shapes=[
            pltpu.VMEM((4, own, D), bf),
            pltpu.SemaphoreType.DMA((4,)),
            pltpu.VMEM((head_rows, D), bf),
            pltpu.VMEM((head_rows, 128), jnp.float32),
            pltpu.VMEM((rows, 2 * own), bf),
        ],
        compiler_params=params,
        name="project_local",
    )(*operands)


def attend_body(
    query_ref, gate_ref, head_ref, tail_ref, halo_ref, local_ref, band_ref, mask_ref, mixed_ref, ext_ref
):
    head_rows, own = head_ref.shape[0], query_ref.shape[1]
    rest = query_ref.shape[0]
    ext_ref[:PAST] = halo_ref[...]
    ext_ref[PAST : PAST + head_rows] = head_ref[...]
    ext_ref[PAST + head_rows :] = tail_ref[...]
    mixed_ref[rest:] = local_ref[...]
    for group in range(rest // GROUP):
        at = slice(group * GROUP, (group + 1) * GROUP)
        seen = slice(group * GROUP, group * GROUP + WINDOW)
        store_group(
            mixed_ref,
            at,
            attend_group(
                query_ref[at], gate_ref[at], ext_ref, seen, band_ref, mask_ref[group], own
            ),
        )


def attend(layer, query, gate, head, tail, halo, local_mixed, band, mask):
    own = query.shape[1]
    rows = head.shape[0] + tail.shape[0]
    moved = [query, gate, head, tail, halo, local_mixed]
    return pl.pallas_call(
        attend_body,
        grid=(1,),
        out_shape=jax.ShapeDtypeStruct((rows, own), jnp.bfloat16),
        in_specs=[whole_of(a.shape) for a in moved]
        + [layer_of(band, layer), whole_of(mask.shape)],
        out_specs=whole_of((rows, own)),
        scratch_shapes=[pltpu.VMEM((PAST + rows, 2 * own), jnp.bfloat16)],
        compiler_params=params,
        name="attend",
    )(*moved, band, mask)


def out_body(layer, count, last, *refs):
    core_ref = refs[0]
    blocks = refs[1 : 1 + count]
    weight_ref, branch_ref = refs[1 + count : 3 + count]
    rest = refs[3 + count :]
    if last:
        square_ref, rest = rest[0], rest[1:]
    weight_buf, mixed_ref, sem = rest
    copy = pltpu.make_async_copy(weight_ref.at[layer], weight_buf, sem)
    copy.start()
    width = blocks[0].shape[2]
    for ref, z, col in block_columns(core_ref[0], blocks):
        mixed_ref[:, pl.ds(col, width)] = ref[z]
    copy.wait()
    branch = lax.dot_general(
        mixed_ref[...], weight_buf[...], rows_by_rows, preferred_element_type=jnp.float32
    ).astype(jnp.bfloat16)
    branch_ref[...] = branch
    if last:
        wide = branch.astype(jnp.float32)
        total = jnp.sum(wide * wide, axis=1, keepdims=True)
        for start in range(0, total.shape[0], GROUP):
            square_ref[:, start : start + GROUP] = turn(total[start : start + GROUP], 0)


def out_project(layer, core, blocks, weight, last):
    rows = blocks[0].shape[1]
    own = weight.shape[1]
    shapes = [jax.ShapeDtypeStruct((rows, own), jnp.bfloat16)]
    if last:
        shapes.append(jax.ShapeDtypeStruct((1, rows), jnp.float32))
    return pl.pallas_call(
        functools.partial(out_body, layer, len(blocks), last),
        out_shape=tuple(shapes),
        in_specs=[smem] + [vmem] * len(blocks) + [hbm],
        out_specs=(vmem,) * len(shapes),
        scratch_shapes=[
            pltpu.VMEM((own, D), jnp.bfloat16),
            pltpu.VMEM((rows, D), jnp.bfloat16),
            pltpu.SemaphoreType.DMA,
        ],
        compiler_params=params,
        name="out_project",
    )(core, *blocks, weight)


def finish_body(resid_ref, branch_ref, gain_ref, *refs):
    out_ref = refs[-1]
    total = refs[0][...]
    for ref in refs[1:-1]:
        total = total + ref[...]
    for start in range(0, out_ref.shape[0], GROUP):
        at = slice(start, start + GROUP)
        inv_out = lax.rsqrt(turn(total[:, at], 1) / D + norm_eps)
        old = resid_ref[at].astype(jnp.float32)
        branch = branch_ref[at].astype(jnp.float32)
        out_ref[at] = (old + branch * inv_out * gain_ref[...]).astype(jnp.bfloat16)


def finish(resid_cols, branch, gain_cols, totals):
    return pl.pallas_call(
        finish_body,
        out_shape=jax.ShapeDtypeStruct(branch.shape, jnp.bfloat16),
        in_specs=[vmem] * (3 + len(totals)),
        out_specs=vmem,
        compiler_params=params,
        name="finish",
    )(resid_cols, branch, gain_cols, *totals)


def partner(x):
    size = lax.axis_size("tp")
    return lax.ppermute(x, "tp", [(i, i ^ 1) for i in range(size)])


def gather(x):
    size = lax.axis_size("tp")
    if x.shape[1] % 128 or size % CORES:
        return (lax.all_gather(x, "tp", axis=1, tiled=True)[None],)
    lines = [list(range(core, size, CORES)) for core in range(CORES)]
    own = lax.all_gather(x, "tp", axis=0, axis_index_groups=lines)
    return own, partner(own)


def total_over_features(square):
    size = lax.axis_size("tp")
    if size % CORES or size > 8:
        return (lax.psum(square, "tp"),)
    both = square + partner(square)
    return (both,) + tuple(
        lax.ppermute(both, "tp", [(i, (i + hop) % size) for i in range(size)])
        for hop in range(CORES, size, CORES)
    )


def from_behind(block):
    size = lax.axis_size("sp")
    return lax.ppermute(block, "sp", [(i, (i + 1) % size) for i in range(size)])


def local(
    tokens,
    documents,
    pre_gain,
    query_weight,
    key_weight,
    value_weight,
    gate_weight,
    out_weight,
    position_bias,
    post_gain,
):
    rows, own = tokens.shape
    tp_at = lax.axis_index("tp")
    core = jnp.reshape(tp_at % CORES, (1,)).astype(jnp.int32)
    sp_at = jnp.reshape(lax.axis_index("sp"), (1,)).astype(jnp.int32)
    docs = documents[None, :]
    behind = from_behind(docs[:, rows - PAST :])
    blocks = gather(tokens)
    band, mask = setup(sp_at, position_bias, docs, behind)
    tail_resid = head_resid = None
    for layer in range(LAYERS):
        post = post_gain[layer - 1 : layer] if layer else None
        pre = pre_gain[layer : layer + 1]
        tail_resid, normed, inv, tail = project_tail(
            layer, core, blocks, tail_resid, post, pre, (key_weight, value_weight)
        )
        halo = from_behind(tail)
        head_resid, head, query, gate, local_mixed = project_local(
            layer,
            core,
            blocks,
            head_resid,
            post,
            pre,
            (normed, inv, tail),
            band,
            mask,
            (key_weight, value_weight, query_weight, gate_weight),
        )
        mixed = attend(layer, query, gate, head, tail, halo, local_mixed, band, mask)
        last = layer + 1 == LAYERS
        result = out_project(layer, core, gather(mixed), out_weight, last)
        if not last:
            blocks = gather(result[0])
    branch, square = result
    start = tp_at * own
    resid_cols = jnp.concatenate(
        [lax.dynamic_slice_in_dim(part, start, own, 1) for part in (head_resid, tail_resid)]
    )
    return finish(
        resid_cols,
        branch,
        lax.dynamic_slice_in_dim(post_gain[LAYERS - 1 :], start, own, 1),
        total_over_features(square),
    )


def solution(mesh):
    placed = (
        P("sp", "tp"),
        P("sp"),
        P(),
        P(None, "tp", None),
        P(None, "tp", None),
        P(None, "tp", None),
        P(None, "tp", None),
        P(None, "tp", None),
        P(None, "tp", None),
        P(),
    )
    return jax.shard_map(
        local, mesh=mesh, in_specs=placed, out_specs=P("sp", "tp"), check_vma=False
    )
```

time: 206 us -> 208 us (level)
  waiting for transfers between devices: 41.5 us -> 29.5 us
  local copies, waits for them, and re-layouts: 11.1 us -> 21 us
  Pallas kernels: 33.5 us -> 37.3 us
    ppermute x4, waiting for transfers between devices: 24.8 us -> 13.8 us  [from_behind(): return lax.ppermute(block, 'sp', [(i, (i + 1) % size) for i in range(size)])]
    unnamed x22 -> x52, local copies, waits for them, and re-layouts: 7.36 us -> 17.2 us
    pallas_call x3 -> x6, Pallas kernels: 17.7 us -> 22.5 us  [the longest x3 14.3 us: project_local(): pl.pallas_call(functools.partial(local_body, layer, first, len(blocks)),...]
  transfers between devices with their start and end apart: 14 -> 14, of which waited for: 11 -> 12; matrix products, arithmetic and copies ran while one was open for 2% -> 2% of each run, Pallas kernels for 3% -> 8%
where the time goes in v2:
time: 208 us; the launch traced here: 207 us
  blocking collectives  112 us (54%)
  Pallas kernels  37.3 us (18%)
  waiting for transfers between devices  29.5 us (14%)
  local copies, waits for them, and re-layouts  21 us (10%)
  starting transfers between devices  7.01 us (3%)
    all_gather x6, blocking collectives, gather(): own = lax.all_gather(x, 'tp', axis=0, axis_index_groups=lines)  112 us
    unnamed x52, local copies, waits for them, and re-layouts  17.2 us
    pallas_call x3, Pallas kernels, project_local(): pl.pallas_call(functools.partial(local_body, layer, first, len(blocks)),...  14.3 us
    ppermute x4, waiting for transfers between devices, from_behind(): return lax.ppermute(block, 'sp', [(i, (i + 1) % size) for i in range(size)])  13.8 us
    ppermute x7, waiting for transfers between devices, partner(): return lax.ppermute(x, 'tp', [(i, i ^ 1) for i in range(size)])  11 us
    pallas_call x3, Pallas kernels, project_tail(): pl.pallas_call(functools.partial(tail_body, layer, first, len(blocks), ro...  8.26 us
    pallas_call x3, Pallas kernels, attend(): pl.pallas_call(attend_body, grid=(1,), out_shape=jax.ShapeDtypeStruct((ro...  7.79 us
    ppermute x3, waiting for transfers between devices, total_over_features(): lax.ppermute(both, 'tp', [(i, (i + hop) % size) for i in range(size)])  4.76 us
  transfers between devices with their start and end apart: 14, of which 12 were waited for; matrix products, arithmetic and copies ran while one was open for 2% of the time, Pallas kernels for 8%

profile of v2, /device:TPU:0, one launch (start us, length us, event | category | flops | bytes accessed | tf_op | source)
XLA Modules:
  0.0 206.9 jit_solution(13827148491064348694)
XLA Ops:
  0.0 21.5 %all-gather = bf16[1536,256]{1,0:T(8,128)(2,1)S(1)} all-gather(bf16[384,256]{1,0:T(8,128)(2,1)} %param.10), channel_id=2, replica_groups={{0,2,4,6},{1,3,5,7},{8,10,12,14},{9,11,13,15},{16,18,20,22},{17,19,21,2..., dimensions={0}, use_global_device_ids=true | all-gather | bytes 983040 | tf_op jit(solution)/shard_map/all_gather | solution.py:438
  21.5 0.0 collective-permute-start
  21.5 0.9 copy-done.8
  22.4 1.5 fusion.1
  23.9 0.9 copy-done.11
  24.8 1.9 copy-done
  26.7 1.9 copy-done.2
  28.6 1.1 copy-done.9
  29.7 1.1 copy-done.12
  30.8 2.4 %project_tail.3 = (bf16[256,2048]{1,0:T(8,128)(2,1)S(1)}, bf16[256,2048]{1,0:T(8,128)(2,1)S(1)}, f32[256,128]{1,0:T(8,128)S(1)}, bf16[256,512]{1,0:T(8,128)(2,1)S(1)}) custom-call(s32[1]{0:T(128)} %bitcast.refs_0_, bf16[4,384,256]{2,1,0:T(8,128)(2,1)S(1)} %bitcast.9, bf16[4,384,256]{2,1,0:T(8,128)(2,1)S(1)} %copy-done.12, ...), custom_call_target="tpu_custom_call" | custom-call | tf_op jit(solution)/shard_map/project_tail/pallas_call | solution.py:181
  33.2 1.0 copy-done.14
  34.2 1.0 copy-done.16
  35.2 1.5 collective-permute-start.2
  36.7 0.5 slice.28
  37.2 0.6 copy-done.21
  37.8 1.5 collective-permute-start.1
  39.3 5.7 %collective-permute-done.1.behind_ref = s32[1,256]{1,0:T(1,128)} collective-permute-done((s32[1,256]{1,0:T(1,128)}, s32[1,256]{1,0:T(1,128)}, u32[]{:S(2)}, u32[]{:S(2)}) %collective-permute-start.1) | collective-permute-done | bytes 1056 | tf_op jit(solution)/shard_map/ppermute | solution.py:455
  45.0 0.7 copy-done.19
  45.7 0.7 copy-done.22
  46.4 2.0 setup.1
  48.4 0.0 copy-start.3
  48.4 1.9 copy-done.3
  50.3 1.1 copy-done.10
  51.4 1.1 copy-done.13
  52.6 1.2 copy-done.17
  53.8 4.6 %project_local.3 = (bf16[128,2048]{1,0:T(8,128)(2,1)S(1)}, bf16[128,512]{1,0:T(8,128)(2,1)S(1)}, bf16[256,256]{1,0:T(8,128)(2,1)S(1)}, bf16[256,256]{1,0:T(8,128)(2,1)S(1)}, bf16[128,256]{1,0:T(8,128)(2,1)S(1)}) custom-call(s32[1]{0:T(128)} %bitcast.refs_0_, bf16[4,384,256]{2,1,0:T(8,128)(2,1)S(1)} %bitcast.10, bf16[4,384,256]{2,1,0:T(8,128)(2,1)S(1)} %copy-done.13, ...), custom_call_target="tpu_custom_call" | custom-call | tf_op jit(solution)/shard_map/project_local/pallas_call | solution.py:302
  58.4 0.0 copy-start.5
  58.4 3.3 %attend.3 = bf16[384,256]{1,0:T(8,128)(2,1)S(1)} custom-call(bf16[256,256]{1,0:T(8,128)(2,1)S(1)} %get-tuple-element.41.query_ref, bf16[256,256]{1,0:T(8,128)(2,1)S(1)} %get-tuple-element.42.gate_ref, bf16[128,512]{1,0:T(8,128)(2,1)S(1)} %get-tuple-element.43.head_ref, bf16[256,512]{1,0:T(8,128)(2,1)S(1)} %get-tuple-element.38.refs_6_.tail_ref, ...), custom_call_target="tpu_custom_call" | custom-call | tf_op jit(solution)/shard_map/attend/pallas_call | solution.py:345
  61.7 17.9 %all-gather.1 = bf16[1536,256]{1,0:T(8,128)(2,1)S(1)} all-gather(bf16[384,256]{1,0:T(8,128)(2,1)S(1)} %attend.3), channel_id=3, replica_groups={{0,2,4,6},{1,3,5,7},{8,10,12,14},{9,11,13,15},{16,18,20,22},{17,19,21,2..., dimensions={0}, use_global_device_ids=true | all-gather | bytes 983040 | tf_op jit(solution)/shard_map/all_gather | solution.py:438
  79.7 0.1 collective-permute-start.3
  79.7 2.3 %collective-permute-done.3.refs_2_ = bf16[4,384,256]{2,1,0:T(8,128)(2,1)S(1)} collective-permute-done((bf16[4,384,256]{2,1,0:T(8,128)(2,1)S(1)}, bf16[4,384,256]{2,1,0:T(8,128)(2,1)S(1)}, u32[]{:S(2)}, u32[]{:S(2)}) %collective-permute-start.3) | collective-permute-done | bytes 786464 | tf_op jit(solution)/shard_map/ppermute | solution.py:430
  82.0 0.9 out_project.3
  82.9 18.2 %all-gather.2 = bf16[1536,256]{1,0:T(8,128)(2,1)S(1)} all-gather(bf16[384,256]{1,0:T(8,128)(2,1)S(1)} %out_project.3), channel_id=4, replica_groups={{0,2,4,6},{1,3,5,7},{8,10,12,14},{9,11,13,15},{16,18,20,22},{17,19,21,2..., dimensions={0}, use_global_device_ids=true | all-gather | bytes 983040 | tf_op jit(solution)/shard_map/all_gather | solution.py:438
  101.1 2.3 %collective-permute-done.4.refs_2_ = bf16[4,384,256]{2,1,0:T(8,128)(2,1)S(1)} collective-permute-done((bf16[4,384,256]{2,1,0:T(8,128)(2,1)S(1)}, bf16[4,384,256]{2,1,0:T(8,128)(2,1)S(1)}, u32[]{:S(2)}, u32[]{:S(2)}) %collective-permute-start.4) | collective-permute-done | bytes 786464 | tf_op jit(solution)/shard_map/ppermute | solution.py:430
  103.4 2.9 %project_tail.4 = (bf16[256,2048]{1,0:T(8,128)(2,1)S(1)}, bf16[256,2048]{1,0:T(8,128)(2,1)S(1)}, f32[256,128]{1,0:T(8,128)S(1)}, bf16[256,512]{1,0:T(8,128)(2,1)S(1)}) custom-call(s32[1]{0:T(128)} %bitcast.refs_0_, bf16[4,384,256]{2,1,0:T(8,128)(2,1)S(1)} %bitcast.12, bf16[4,384,256]{2,1,0:T(8,128)(2,1)S(1)} %collective-permute-done.4.refs_2_, ...), custom_call_target="tpu_custom_call" | custom-call | tf_op jit(solution)/shard_map/project_tail/pallas_call | solution.py:181
  106.3 0.8 collective-permute-start.5
  107.2 4.8 %project_local.4 = (bf16[128,2048]{1,0:T(8,128)(2,1)S(1)}, bf16[128,512]{1,0:T(8,128)(2,1)S(1)}, bf16[256,256]{1,0:T(8,128)(2,1)S(1)}, bf16[256,256]{1,0:T(8,128)(2,1)S(1)}, bf16[128,256]{1,0:T(8,128)(2,1)S(1)}) custom-call(s32[1]{0:T(128)} %bitcast.refs_0_, bf16[4,384,256]{2,1,0:T(8,128)(2,1)S(1)} %bitcast.13, ...), custom_call_target="tpu_custom_call" | custom-call | tf_op jit(solution)/shard_map/project_local/pallas_call | solution.py:302
  112.0 0.0 copy-start.6
  112.0 3.8 %collective-permute-done.5.halo_ref = bf16[256,512]{1,0:T(8,128)(2,1)S(1)} collective-permute-done((bf16[256,512]{1,0:T(8,128)(2,1)S(1)}, bf16[256,512]{1,0:T(8,128)(2,1)S(1)}, u32[]{:S(2)}, u32[]{:S(2)}) %collective-permute-start.5) | collective-permute-done | bytes 262176 | tf_op jit(solution)/shard_map/ppermute | solution.py:455
  115.8 2.2 %attend.4 = bf16[384,256]{1,0:T(8,128)(2,1)S(1)} custom-call(bf16[256,256]{1,0:T(8,128)(2,1)S(1)} %get-tuple-element.50.query_ref, bf16[256,256]{1,0:T(8,128)(2,1)S(1)} %get-tuple-element.51.gate_ref, bf16[128,512]{1,0:T(8,128)(2,1)S(1)} %get-tuple-element.52.head_ref, bf16[256,512]{1,0:T(8,128)(2,1)S(1)} %get-tuple-element.49.refs_8_.tail_ref, ...), custom_call_target="tpu_custom_call" | custom-call | tf_op jit(solution)/shard_map/attend/pallas_call | solution.py:345
  118.1 17.9 %all-gather.3 = bf16[1536,256]{1,0:T(8,128)(2,1)S(1)} all-gather(bf16[384,256]{1,0:T(8,128)(2,1)S(1)} %attend.4), channel_id=5, replica_groups={{0,2,4,6},{1,3,5,7},{8,10,12,14},{9,11,13,15},{16,18,20,22},{17,19,21,2..., dimensions={0}, use_global_device_ids=true | all-gather | bytes 983040 | tf_op jit(solution)/shard_map/all_gather | solution.py:438
  136.0 2.3 %collective-permute-done.6.refs_2_ = bf16[4,384,256]{2,1,0:T(8,128)(2,1)S(1)} collective-permute-done((bf16[4,384,256]{2,1,0:T(8,128)(2,1)S(1)}, bf16[4,384,256]{2,1,0:T(8,128)(2,1)S(1)}, u32[]{:S(2)}, u32[]{:S(2)}) %collective-permute-start.6) | collective-permute-done | bytes 786464 | tf_op jit(solution)/shard_map/ppermute | solution.py:430
  138.2 0.9 out_project.4
  139.2 18.0 %all-gather.4 = bf16[1536,256]{1,0:T(8,128)(2,1)S(1)} all-gather(bf16[384,256]{1,0:T(8,128)(2,1)S(1)} %out_project.4), channel_id=6, replica_groups={{0,2,4,6},{1,3,5,7},{8,10,12,14},{9,11,13,15},{16,18,20,22},{17,19,21,2..., dimensions={0}, use_global_device_ids=true | all-gather | bytes 983040 | tf_op jit(solution)/shard_map/all_gather | solution.py:438
  157.2 2.3 %collective-permute-done.7.refs_2_ = bf16[4,384,256]{2,1,0:T(8,128)(2,1)S(1)} collective-permute-done((bf16[4,384,256]{2,1,0:T(8,128)(2,1)S(1)}, bf16[4,384,256]{2,1,0:T(8,128)(2,1)S(1)}, u32[]{:S(2)}, u32[]{:S(2)}) %collective-permute-start.7) | collective-permute-done | bytes 786464 | tf_op jit(solution)/shard_map/ppermute | solution.py:430
  159.5 2.9 %project_tail.5 = (bf16[256,2048]{1,0:T(8,128)(2,1)S(1)}, bf16[256,2048]{1,0:T(8,128)(2,1)S(1)}, f32[256,128]{1,0:T(8,128)S(1)}, bf16[256,512]{1,0:T(8,128)(2,1)S(1)}) custom-call(s32[1]{0:T(128)} %bitcast.refs_0_, bf16[4,384,256]{2,1,0:T(8,128)(2,1)S(1)} %bitcast.15, bf16[4,384,256]{2,1,0:T(8,128)(2,1)S(1)} %collective-permute-done.7.refs_2_, ...), custom_call_target="tpu_custom_call" | custom-call | tf_op jit(solution)/shard_map/project_tail/pallas_call | solution.py:181
  162.4 0.1 collective-permute-start.8
  162.5 4.9 %project_local.5 = (bf16[128,2048]{1,0:T(8,128)(2,1)S(1)}, bf16[128,512]{1,0:T(8,128)(2,1)S(1)}, bf16[256,256]{1,0:T(8,128)(2,1)S(1)}, bf16[256,256]{1,0:T(8,128)(2,1)S(1)}, bf16[128,256]{1,0:T(8,128)(2,1)S(1)}) custom-call(s32[1]{0:T(128)} %bitcast.refs_0_, bf16[4,384,256]{2,1,0:T(8,128)(2,1)S(1)} %bitcast.16, ...), custom_call_target="tpu_custom_call" | custom-call | tf_op jit(solution)/shard_map/project_local/pallas_call | solution.py:302
  167.4 0.0 copy-start.7
  167.4 4.3 %collective-permute-done.8.halo_ref = bf16[256,512]{1,0:T(8,128)(2,1)S(1)} collective-permute-done((bf16[256,512]{1,0:T(8,128)(2,1)S(1)}, bf16[256,512]{1,0:T(8,128)(2,1)S(1)}, u32[]{:S(2)}, u32[]{:S(2)}) %collective-permute-start.8) | collective-permute-done | bytes 262176 | tf_op jit(solution)/shard_map/ppermute | solution.py:455
  171.7 2.2 %attend.5 = bf16[384,256]{1,0:T(8,128)(2,1)S(1)} custom-call(bf16[256,256]{1,0:T(8,128)(2,1)S(1)} %get-tuple-element.61.query_ref, bf16[256,256]{1,0:T(8,128)(2,1)S(1)} %get-tuple-element.62.gate_ref, bf16[128,512]{1,0:T(8,128)(2,1)S(1)} %get-tuple-element.63.head_ref, bf16[256,512]{1,0:T(8,128)(2,1)S(1)} %get-tuple-element.58.refs_8_.tail_ref, ...), custom_call_target="tpu_custom_call" | custom-call | tf_op jit(solution)/shard_map/attend/pallas_call | solution.py:345
  174.0 18.2 %all-gather.5 = bf16[1536,256]{1,0:T(8,128)(2,1)} all-gather(bf16[384,256]{1,0:T(8,128)(2,1)S(1)} %attend.5), channel_id=7, replica_groups={{0,2,4,6},{1,3,5,7},{8,10,12,14},{9,11,13,15},{16,18,20,22},{17,19,21,2..., dimensions={0}, use_global_device_ids=true | all-gather | bytes 983040 | tf_op jit(solution)/shard_map/all_gather | solution.py:438
  192.2 0.9 constant_dynamic-slice_fusion.1
  193.1 1.7 collective-permute-done.9.refs_2_
  194.8 2.4 %out_project.5 = (bf16[384,256]{1,0:T(8,128)(2,1)S(1)}, f32[1,384]{1,0:T(1,128)S(1)}) custom-call(s32[1]{0:T(128)} %bitcast.refs_0_, bf16[4,384,256]{2,1,0:T(8,128)(2,1)} %bitcast.7.refs_1_, bf16[4,384,256]{2,1,0:T(8,128)(2,1)} %collective-permute-done.9.refs_2_, bf16[3,256,2048]{2,1,0:T(8,128)(2,1)S(1)} %copy-done.7), custom_call_target="tpu_custom_call" | custom-call | tf_op jit(solution)/shard_map/out_project/pallas_call | solution.py:389
  197.2 0.2 collective-permute-start.10
  197.4 0.8 constant_dynamic-slice_fusion.2
  198.2 0.2 collective-permute-done.10
  198.4 2.3 %collective-permute-start.13 = (f32[1,384]{1,0:T(1,128)S(1)}, f32[1,384]{1,0:T(1,128)S(1)}, u32[]{:S(2)}, u32[]{:S(2)}) collective-permute-start(f32[1,384]{1,0:T(1,128)S(1)} %add.14.refs_0_), channel_id=1, source_target_pairs={{0,6},{1,7},{2,0},{3,1},{4,2},{5,3},{6,4},{7,5},{8,14},{9,15},{10,... | collective-permute-start | bytes 4616 | tf_op jit(solution)/shard_map/ppermute | solution.py:448
  200.7 0.6 collective-permute-start.11
  201.3 0.7 collective-permute-done.13.refs_3_
  202.0 3.2 %collective-permute-done.12.refs_2_ = f32[1,384]{1,0:T(1,128)S(1)} collective-permute-done((f32[1,384]{1,0:T(1,128)S(1)}, f32[1,384]{1,0:T(1,128)S(1)}, u32[]{:S(2)}, u32[]{:S(2)}) %collective-permute-start.12) | collective-permute-done | bytes 1568 | tf_op jit(solution)/shard_map/ppermute | solution.py:448
  205.1 0.9 collective-permute-done.11.refs_1_
  206.0 0.9 finish.1
  (45 shorter events, 0.1 us)
Async XLA Ops:
  21.5 2.4 %collective-permute-start = (bf16[4,384,256]{2,1,0:T(8,128)(2,1)S(1)}, bf16[4,384,256]{2,1,0:T(8,128)(2,1)S(1)}, u32[]{:S(2)}, u32[]{:S(2)}) collective-permute-start(bf16[4,384,256]{2,1,0:T(8,128)(2,1)S(1)} %bitcast.8), channel_id=1, source_target_pairs={{0,1},{1,0},{2,3},{3,2},{4,5},{5,4},{6,7},{7,6},{8,9},{9,8},{10,11... | collective-permute-start | bytes 2359304 | tf_op jit(solution)/shard_map/ppermute | solution.py:430
  21.5 0.9 copy-start.8
  23.9 0.9 copy-start.11
  24.8 1.9 copy-start
  26.7 1.9 copy-start.2
  28.6 1.1 copy-start.9
  29.7 1.1 copy-start.12
  30.8 5.9 %copy-start.25 = (s32[384]{0:T(512)S(1)}, s32[384]{0:T(512)}, u32[]{:S(2)}) copy-start(s32[384]{0:T(512)} %param.11) | copy-start | bytes 4612
  30.8 17.6 %copy-start.1 = (bf16[3,256,2048]{2,1,0:T(8,128)(2,1)S(1)}, bf16[3,256,2048]{2,1,0:T(8,128)(2,1)}, u32[]{:S(2)}) copy-start(bf16[3,256,2048]{2,1,0:T(8,128)(2,1)} %refs_11_.5) | copy-start | bytes 9437188
  33.2 1.0 copy-start.14
  34.2 1.0 copy-start.16
  35.2 23.2 %collective-permute-start.2 = (bf16[256,512]{1,0:T(8,128)(2,1)S(1)}, bf16[256,512]{1,0:T(8,128)(2,1)}, u32[]{:S(2)}, u32[]{:S(2)}) collective-permute-start(bf16[256,512]{1,0:T(8,128)(2,1)S(1)} %get-tuple-element.38.refs_6_.tail_ref), channel_id=1, source_target_pairs={{0,8},{8,16},{16,24},{24,0},{1,9},{9,17},{17,25},{25,1},{2,10},{10... | collective-permute-start | bytes 786440 | tf_op jit(solution)/shard_map/ppermute | solution.py:455
  37.2 0.6 copy-start.21
  37.8 7.2 %collective-permute-start.1 = (s32[1,256]{1,0:T(1,128)}, s32[1,256]{1,0:T(1,128)}, u32[]{:S(2)}, u32[]{:S(2)}) collective-permute-start(s32[1,256]{1,0:T(1,128)} %slice.28), channel_id=1, source_target_pairs={{0,8},{8,16},{16,24},{24,0},{1,9},{9,17},{17,25},{25,1},{2,10},{10... | collective-permute-start | bytes 3080 | tf_op jit(solution)/shard_map/ppermute | solution.py:455
  45.0 0.7 copy-start.19
  45.7 0.7 copy-start.22
  48.4 1.9 copy-start.3
  50.3 1.1 copy-start.10
  51.4 1.1 copy-start.13
  52.6 1.2 copy-start.17
  58.4 23.6 %copy-start.5 = (bf16[3,256,2048]{2,1,0:T(8,128)(2,1)S(1)}, bf16[3,256,2048]{2,1,0:T(8,128)(2,1)}, u32[]{:S(2)}) copy-start(bf16[3,256,2048]{2,1,0:T(8,128)(2,1)} %refs_3_.5) | copy-start | bytes 9437188
  79.6 21.5 %copy-start.24 = (f32[3,2048]{1,0:T(4,128)S(1)}, f32[3,2048]{1,0:T(4,128)}, u32[]{:S(2)}) copy-start(f32[3,2048]{1,0:T(4,128)} %param.19) | copy-start | bytes 73732
  79.6 23.7 %copy-start.4 = (bf16[3,256,2048]{2,1,0:T(8,128)(2,1)S(1)}, bf16[3,256,2048]{2,1,0:T(8,128)(2,1)}, u32[]{:S(2)}) copy-start(bf16[3,256,2048]{2,1,0:T(8,128)(2,1)} %refs_12_.5) | copy-start | bytes 9437188
  79.7 23.7 %copy-start.15 = (bf16[256,2048]{1,0:T(8,128)(2,1)S(1)}, bf16[256,2048]{1,0:T(8,128)(2,1)}, u32[]{:S(2)}) copy-start(bf16[256,2048]{1,0:T(8,128)(2,1)} %copy-done.14) | copy-start | bytes 3145732
  79.7 23.7 %copy-start.18 = (f32[1,2048]{1,0:T(1,128)S(1)}, f32[1,2048]{1,0:T(1,128)}, u32[]{:S(2)}) copy-start(f32[1,2048]{1,0:T(1,128)} %get-tuple-element.72.refs_5_) | copy-start | bytes 24580
  79.7 2.4 %collective-permute-start.3 = (bf16[4,384,256]{2,1,0:T(8,128)(2,1)S(1)}, bf16[4,384,256]{2,1,0:T(8,128)(2,1)S(1)}, u32[]{:S(2)}, u32[]{:S(2)}) collective-permute-start(bf16[4,384,256]{2,1,0:T(8,128)(2,1)S(1)} %bitcast.17), channel_id=1, source_target_pairs={{0,1},{1,0},{2,3},{3,2},{4,5},{5,4},{6,7},{7,6},{8,9},{9,8},{10,11... | collective-permute-start | bytes 2359304 | tf_op jit(solution)/shard_map/ppermute | solution.py:430
  101.1 2.3 %collective-permute-start.4 = (bf16[4,384,256]{2,1,0:T(8,128)(2,1)S(1)}, bf16[4,384,256]{2,1,0:T(8,128)(2,1)S(1)}, u32[]{:S(2)}, u32[]{:S(2)}) collective-permute-start(bf16[4,384,256]{2,1,0:T(8,128)(2,1)S(1)} %bitcast.11), channel_id=1, source_target_pairs={{0,1},{1,0},{2,3},{3,2},{4,5},{5,4},{6,7},{7,6},{8,9},{9,8},{10,11... | collective-permute-start | bytes 2359304 | tf_op jit(solution)/shard_map/ppermute | solution.py:430
  106.3 9.5 %collective-permute-start.5 = (bf16[256,512]{1,0:T(8,128)(2,1)S(1)}, bf16[256,512]{1,0:T(8,128)(2,1)S(1)}, u32[]{:S(2)}, u32[]{:S(2)}) collective-permute-start(bf16[256,512]{1,0:T(8,128)(2,1)S(1)} %get-tuple-element.49.refs_8_.tail_ref), channel_id=1, source_target_pairs={{0,8},{8,16},{16,24},{24,0},{1,9},{9,17},{17,25},{25,1},{2,10},{10... | collective-permute-start | bytes 786440 | tf_op jit(solution)/shard_map/ppermute | solution.py:455
  112.0 26.2 %copy-start.6 = (bf16[3,256,2048]{2,1,0:T(8,128)(2,1)S(1)}, bf16[3,256,2048]{2,1,0:T(8,128)(2,1)}, u32[]{:S(2)}) copy-start(bf16[3,256,2048]{2,1,0:T(8,128)(2,1)} %refs_3_.5) | copy-start | bytes 9437188
  136.0 2.3 %collective-permute-start.6 = (bf16[4,384,256]{2,1,0:T(8,128)(2,1)S(1)}, bf16[4,384,256]{2,1,0:T(8,128)(2,1)S(1)}, u32[]{:S(2)}, u32[]{:S(2)}) collective-permute-start(bf16[4,384,256]{2,1,0:T(8,128)(2,1)S(1)} %bitcast.19), channel_id=1, source_target_pairs={{0,1},{1,0},{2,3},{3,2},{4,5},{5,4},{6,7},{7,6},{8,9},{9,8},{10,11... | collective-permute-start | bytes 2359304 | tf_op jit(solution)/shard_map/ppermute | solution.py:430
  157.2 2.3 %collective-permute-start.7 = (bf16[4,384,256]{2,1,0:T(8,128)(2,1)S(1)}, bf16[4,384,256]{2,1,0:T(8,128)(2,1)S(1)}, u32[]{:S(2)}, u32[]{:S(2)}) collective-permute-start(bf16[4,384,256]{2,1,0:T(8,128)(2,1)S(1)} %bitcast.14), channel_id=1, source_target_pairs={{0,1},{1,0},{2,3},{3,2},{4,5},{5,4},{6,7},{7,6},{8,9},{9,8},{10,11... | collective-permute-start | bytes 2359304 | tf_op jit(solution)/shard_map/ppermute | solution.py:430
  162.4 5.0 %copy-start.20 = (bf16[256,2048]{1,0:T(8,128)(2,1)}, bf16[256,2048]{1,0:T(8,128)(2,1)S(1)}, u32[]{:S(2)}) copy-start(bf16[256,2048]{1,0:T(8,128)(2,1)S(1)} %get-tuple-element.60) | copy-start | bytes 3145732
  162.4 9.3 %collective-permute-start.8 = (bf16[256,512]{1,0:T(8,128)(2,1)S(1)}, bf16[256,512]{1,0:T(8,128)(2,1)S(1)}, u32[]{:S(2)}, u32[]{:S(2)}) collective-permute-start(bf16[256,512]{1,0:T(8,128)(2,1)S(1)} %get-tuple-element.58.refs_8_.tail_ref), channel_id=1, source_target_pairs={{0,8},{8,16},{16,24},{24,0},{1,9},{9,17},{17,25},{25,1},{2,10},{10... | collective-permute-start | bytes 786440 | tf_op jit(solution)/shard_map/ppermute | solution.py:455
  167.4 24.8 %copy-start.23 = (bf16[128,2048]{1,0:T(8,128)(2,1)}, bf16[128,2048]{1,0:T(8,128)(2,1)S(1)}, u32[]{:S(2)}) copy-start(bf16[128,2048]{1,0:T(8,128)(2,1)S(1)} %get-tuple-element.59) | copy-start | bytes 1572868
  167.4 27.4 %copy-start.7 = (bf16[3,256,2048]{2,1,0:T(8,128)(2,1)S(1)}, bf16[3,256,2048]{2,1,0:T(8,128)(2,1)}, u32[]{:S(2)}) copy-start(bf16[3,256,2048]{2,1,0:T(8,128)(2,1)} %refs_3_.5) | copy-start | bytes 9437188
  192.2 2.6 %collective-permute-start.9 = (bf16[4,384,256]{2,1,0:T(8,128)(2,1)}, bf16[4,384,256]{2,1,0:T(8,128)(2,1)}, u32[]{:S(2)}, u32[]{:S(2)}) collective-permute-start(bf16[4,384,256]{2,1,0:T(8,128)(2,1)} %bitcast.7.refs_1_), channel_id=1, source_target_pairs={{0,1},{1,0},{2,3},{3,2},{4,5},{5,4},{6,7},{7,6},{8,9},{9,8},{10,11... | collective-permute-start | bytes 2359304 | tf_op jit(solution)/shard_map/ppermute | solution.py:430
  197.2 1.2 collective-permute-start.10
  198.4 3.6 %collective-permute-start.13 = (f32[1,384]{1,0:T(1,128)S(1)}, f32[1,384]{1,0:T(1,128)S(1)}, u32[]{:S(2)}, u32[]{:S(2)}) collective-permute-start(f32[1,384]{1,0:T(1,128)S(1)} %add.14.refs_0_), channel_id=1, source_target_pairs={{0,6},{1,7},{2,0},{3,1},{4,2},{5,3},{6,4},{7,5},{8,14},{9,15},{10,... | collective-permute-start | bytes 4616 | tf_op jit(solution)/shard_map/ppermute | solution.py:448
  200.7 4.5 %collective-permute-start.12 = (f32[1,384]{1,0:T(1,128)S(1)}, f32[1,384]{1,0:T(1,128)S(1)}, u32[]{:S(2)}, u32[]{:S(2)}) collective-permute-start(f32[1,384]{1,0:T(1,128)S(1)} %add.14.refs_0_), channel_id=1, source_target_pairs={{0,4},{1,5},{2,6},{3,7},{4,0},{5,1},{6,2},{7,3},{8,12},{9,13},{10,... | collective-permute-start | bytes 4616 | tf_op jit(solution)/shard_map/ppermute | solution.py:448
  200.7 5.4 %collective-permute-start.11 = (f32[1,384]{1,0:T(1,128)S(1)}, f32[1,384]{1,0:T(1,128)S(1)}, u32[]{:S(2)}, u32[]{:S(2)}) collective-permute-start(f32[1,384]{1,0:T(1,128)S(1)} %add.14.refs_0_), channel_id=1, source_target_pairs={{0,2},{1,3},{2,4},{3,5},{4,6},{5,7},{6,0},{7,1},{8,10},{9,11},{10,... | collective-permute-start | bytes 4616 | tf_op jit(solution)/shard_map/ppermute | solution.py:448

commit v3 on v2

--- a/solution.py
+++ b/solution.py
@@ -23,9 +23,8 @@
 norm_eps = 1e-06
 rows_by_rows = (((1,), (1,)), ((), ()))
 vmem = pl.BlockSpec(memory_space=pltpu.VMEM)
-smem = pl.BlockSpec(memory_space=pltpu.SMEM)
 hbm = pl.BlockSpec(memory_space=pltpu.HBM)
-params = pltpu.CompilerParams(vmem_limit_bytes=40 * 1024 * 1024)
+params = pltpu.CompilerParams(vmem_limit_bytes=16 * 1024 * 1024)
 
 
 def turn(vector, axis):
@@ -37,7 +36,8 @@
     return jnp.sum(spread, axis=axis, keepdims=True)
 
 
-def setup_body(sp_ref, bias_ref, docs_ref, behind_ref, band_ref, mask_ref):
+def setup_body(bias_ref, docs_ref, *outs):
+    bands, mask_ref = outs[:-1], outs[-1]
     layers, heads, entries = bias_ref.shape
     row_block = lax.broadcasted_iota(jnp.int32, (GROUP, WINDOW), 0) // BLOCK
     col_block = lax.broadcasted_iota(jnp.int32, (GROUP, WINDOW), 1) // BLOCK
@@ -56,35 +56,37 @@
         for head in range(heads):
             row = jnp.broadcast_to(base[head : head + 1, :], (GROUP, SKEW))
             skewed = pltpu.roll(row, 0, 1, stride=1, stride_axis=0)
-            band_ref[layer, head] = jnp.where(allowed, skewed[:, :WINDOW], FAR)
-    behind = jnp.where(sp_ref[0] == 0, -1, behind_ref[...])
+            bands[layer][head] = jnp.where(allowed, skewed[:, :WINDOW], FAR)
     docs = docs_ref[...]
-    seen = jnp.concatenate([behind, docs], axis=1)
-    for group in range(mask_ref.shape[0]):
-        start = group * GROUP
-        own = turn(docs[:, start : start + GROUP], 1)
-        mask_ref[group] = jnp.where(own == seen[:, start : start + WINDOW], 0.0, FAR)
-
-
-def setup(sp_at, position_bias, docs, behind):
+    for index in range(mask_ref.shape[0]):
+        start = PAST + index * GROUP
+        mask_ref[index] = doc_mask(docs[:, start : start + GROUP], docs[:, start - PAST : start + GROUP])
+
+
+def doc_mask(own, seen):
+    return jnp.where(turn(own, 1) == seen, 0.0, FAR)
+
+
+def setup(position_bias, docs):
     layers, heads, _ = position_bias.shape
-    groups = docs.shape[1] // GROUP
+    groups = (docs.shape[1] - PAST) // GROUP
     return pl.pallas_call(
         setup_body,
         out_shape=(
-            jax.ShapeDtypeStruct((layers, heads, GROUP, WINDOW), jnp.float32),
+            *[jax.ShapeDtypeStruct((heads, GROUP, WINDOW), jnp.float32) for _ in range(layers)],
             jax.ShapeDtypeStruct((groups, GROUP, WINDOW), jnp.float32),
         ),
-        in_specs=[smem, vmem, vmem, vmem],
-        out_specs=(vmem, vmem),
+        in_specs=[vmem, vmem],
+        out_specs=(vmem,) * (layers + 1),
         compiler_params=params,
         name="setup",
-    )(sp_at, position_bias, docs, behind)
-
-
-def block_columns(core, blocks):
+    )(position_bias, docs)
+
+
+def block_columns(blocks):
     if len(blocks) == 1:
         return [(blocks[0], 0, 0)]
+    core = lax.rem(lax.axis_index("tp"), CORES)
     width = blocks[0].shape[2]
     return [
         (ref, z, pl.multiple_of((CORES * z + (core if side == 0 else 1 - core)) * width, 128))
@@ -100,9 +102,9 @@
     return total
 
 
-def update_rows(core, blocks, offset, resid_ref, post_ref, pre_ref, resid_out, normed_ref, inv_ref):
+def update_rows(layer, blocks, offset, resid_ref, post_ref, pre_ref, resid_out, normed_ref, inv_ref):
     step = BLOCK
-    placed = block_columns(core, blocks)
+    placed = block_columns(blocks)
     width = blocks[0].shape[2]
 
     def one(index, carry):
@@ -122,11 +124,11 @@
             else:
                 part = ref[z, source, :].astype(jnp.float32)
                 old = resid_ref[at, cols].astype(jnp.float32)
-                new = (old + part * inv_out * post_ref[:, cols]).astype(jnp.bfloat16)
+                new = (old + part * inv_out * post_ref[layer - 1 : layer, cols]).astype(jnp.bfloat16)
             resid_out[at, cols] = new
             wide = new.astype(jnp.float32)
             total = total + lane_sum(wide * wide)
-            normed_ref[at, cols] = (wide * pre_ref[:, cols]).astype(jnp.bfloat16)
+            normed_ref[at, cols] = (wide * pre_ref[layer : layer + 1, cols]).astype(jnp.bfloat16)
         inv_in = lax.rsqrt(jnp.sum(total, axis=1, keepdims=True) / D + norm_eps)
         inv_ref[at, :] = jnp.broadcast_to(inv_in, (step, 128))
         return carry
@@ -152,7 +154,6 @@
 
 
 def tail_body(layer, first, count, offset, *refs):
-    core_ref, refs = refs[0], refs[1:]
     blocks, refs = refs[:count], refs[count:]
     resid_ref = post_ref = None
     if not first:
@@ -161,7 +162,7 @@
     resid_out, normed_ref, inv_ref, tail_ref, weight_buf, sems = refs[3:]
     copies = fetch(layer, weights, weight_buf, sems)
     update_rows(
-        core_ref[0], blocks, offset, resid_ref, post_ref, pre_ref, resid_out, normed_ref, inv_ref
+        layer, blocks, offset, resid_ref, post_ref, pre_ref, resid_out, normed_ref, inv_ref
     )
     own = weight_buf.shape[1]
     for at, copy in enumerate(copies):
@@ -171,13 +172,13 @@
         )
 
 
-def project_tail(layer, core, blocks, resid, post, pre, weights):
+def project_tail(layer, blocks, resid, post, pre, weights):
     first = resid is None
     rows = blocks[0].shape[1]
     own = weights[0].shape[1]
     bf = jnp.bfloat16
-    operands = [core, *blocks] + ([] if first else [resid, post]) + [pre, *weights]
-    specs = [smem] + [vmem] * (len(operands) - 3) + [hbm] * 2
+    operands = [*blocks] + ([] if first else [resid, post]) + [pre, *weights]
+    specs = [vmem] * (len(operands) - 2) + [hbm] * 2
     return pl.pallas_call(
         functools.partial(tail_body, layer, first, len(blocks), rows - PAST),
         out_shape=(
@@ -208,7 +209,7 @@
             scores = lax.dot_general(
                 picked, keys, rows_by_rows, preferred_element_type=jnp.float32
             )
-            scores = scores + band_ref[0, start // HD + sub] + mask
+            scores = scores + band_ref[start // HD + sub] + mask
             lifted = jnp.exp(scores - jnp.max(scores, axis=1, keepdims=True))
             total = jnp.sum(lifted, axis=1, keepdims=True)
             part = jnp.dot(lifted.astype(jnp.bfloat16), values, preferred_element_type=jnp.float32)
@@ -227,7 +228,6 @@
 
 
 def local_body(layer, first, count, *refs):
-    core_ref, refs = refs[0], refs[1:]
     blocks, refs = refs[:count], refs[count:]
     resid_ref = post_ref = None
     if not first:
@@ -239,7 +239,7 @@
     copies = fetch(layer, weights, weight_buf, sems)
     head_rows = resid_out.shape[0]
     update_rows(
-        core_ref[0], blocks, 0, resid_ref, post_ref, pre_ref, resid_out, normed_ref, inv_ref
+        layer, blocks, 0, resid_ref, post_ref, pre_ref, resid_out, normed_ref, inv_ref
     )
     own = weight_buf.shape[1]
     rest = query_out.shape[0]
@@ -261,37 +261,27 @@
         pieces.append(tail[cut:])
     ext_ref[:head_rows] = head_ref[...]
     ext_ref[head_rows:] = tail_ref[...]
-    groups = mask_ref.shape[0]
-    for index, group in enumerate(range(rest // GROUP, groups)):
+    for index in range(mask_ref.shape[0]):
         at = slice(index * GROUP, (index + 1) * GROUP)
-        seen = slice(group * GROUP - PAST, group * GROUP - PAST + WINDOW)
+        seen = slice(index * GROUP, index * GROUP + WINDOW)
         store_group(
             mixed_ref,
             at,
             attend_group(
-                pieces[0][at], pieces[1][at], ext_ref, seen, band_ref, mask_ref[group], own
+                pieces[0][at], pieces[1][at], ext_ref, seen, band_ref, mask_ref[index], own
             ),
         )
 
 
-def layer_of(band, layer):
-    return pl.BlockSpec((1,) + band.shape[1:], lambda i: (layer, 0, 0, 0))
-
-
-def whole_of(shape):
-    return pl.BlockSpec(shape, lambda i: (0,) * len(shape))
-
-
-def project_local(layer, core, blocks, resid, post, pre, tail_parts, band, mask, weights):
+def project_local(layer, blocks, resid, post, pre, tail_parts, band, mask, weights):
     first = resid is None
     rows = blocks[0].shape[1]
     own = weights[0].shape[1]
     head_rows = rows - PAST
     bf = jnp.bfloat16
     moved = [*blocks] + ([] if first else [resid, post]) + [pre, *tail_parts]
-    operands = [core, *moved, band, mask, *weights]
-    specs = [smem] + [whole_of(a.shape) for a in moved] + [layer_of(band, layer)]
-    specs = specs + [whole_of(mask.shape)] + [hbm] * 4
+    operands = [*moved, band, mask, *weights]
+    specs = [vmem] * (len(moved) + 2) + [hbm] * 4
     shapes = [
         ((head_rows, D), bf),
         ((head_rows, 2 * own), bf),
@@ -301,10 +291,9 @@
     ]
     return pl.pallas_call(
         functools.partial(local_body, layer, first, len(blocks)),
-        grid=(1,),
         out_shape=tuple(jax.ShapeDtypeStruct(shape, kind) for shape, kind in shapes),
         in_specs=specs,
-        out_specs=tuple(whole_of(shape) for shape, _ in shapes),
+        out_specs=(vmem,) * len(shapes),
         scratch_shapes=[
             pltpu.VMEM((4, own, D), bf),
             pltpu.SemaphoreType.DMA((4,)),
@@ -318,7 +307,17 @@
 
 
 def attend_body(
-    query_ref, gate_ref, head_ref, tail_ref, halo_ref, local_ref, band_ref, mask_ref, mixed_ref, ext_ref
+    query_ref,
+    gate_ref,
+    head_ref,
+    tail_ref,
+    halo_ref,
+    local_ref,
+    band_ref,
+    docs_ref,
+    behind_ref,
+    mixed_ref,
+    ext_ref,
 ):
     head_rows, own = head_ref.shape[0], query_ref.shape[1]
     rest = query_ref.shape[0]
@@ -326,47 +325,46 @@
     ext_ref[PAST : PAST + head_rows] = head_ref[...]
     ext_ref[PAST + head_rows :] = tail_ref[...]
     mixed_ref[rest:] = local_ref[...]
+    docs = docs_ref[...]
+    behind = jnp.where(lax.axis_index("sp") == 0, -1, behind_ref[...])
+    docs_seen = jnp.concatenate([behind, docs], axis=1)
     for group in range(rest // GROUP):
         at = slice(group * GROUP, (group + 1) * GROUP)
         seen = slice(group * GROUP, group * GROUP + WINDOW)
+        mask = doc_mask(docs[:, at], docs_seen[:, seen])
         store_group(
             mixed_ref,
             at,
-            attend_group(
-                query_ref[at], gate_ref[at], ext_ref, seen, band_ref, mask_ref[group], own
-            ),
-        )
-
-
-def attend(layer, query, gate, head, tail, halo, local_mixed, band, mask):
+            attend_group(query_ref[at], gate_ref[at], ext_ref, seen, band_ref, mask, own),
+        )
+
+
+def attend(layer, query, gate, head, tail, halo, local_mixed, band, docs, behind):
     own = query.shape[1]
     rows = head.shape[0] + tail.shape[0]
-    moved = [query, gate, head, tail, halo, local_mixed]
+    operands = (query, gate, head, tail, halo, local_mixed, band, docs, behind)
     return pl.pallas_call(
         attend_body,
-        grid=(1,),
         out_shape=jax.ShapeDtypeStruct((rows, own), jnp.bfloat16),
-        in_specs=[whole_of(a.shape) for a in moved]
-        + [layer_of(band, layer), whole_of(mask.shape)],
-        out_specs=whole_of((rows, own)),
+        in_specs=[vmem] * len(operands),
+        out_specs=vmem,
         scratch_shapes=[pltpu.VMEM((PAST + rows, 2 * own), jnp.bfloat16)],
         compiler_params=params,
         name="attend",
-    )(*moved, band, mask)
+    )(*operands)
 
 
 def out_body(layer, count, last, *refs):
-    core_ref = refs[0]
-    blocks = refs[1 : 1 + count]
-    weight_ref, branch_ref = refs[1 + count : 3 + count]
-    rest = refs[3 + count :]
+    blocks = refs[:count]
+    weight_ref, branch_ref = refs[count : 2 + count]
+    rest = refs[2 + count :]
     if last:
         square_ref, rest = rest[0], rest[1:]
     weight_buf, mixed_ref, sem = rest
     copy = pltpu.make_async_copy(weight_ref.at[layer], weight_buf, sem)
     copy.start()
     width = blocks[0].shape[2]
-    for ref, z, col in block_columns(core_ref[0], blocks):
+    for ref, z, col in block_columns(blocks):
         mixed_ref[:, pl.ds(col, width)] = ref[z]
     copy.wait()
     branch = lax.dot_general(
@@ -374,13 +372,13 @@
     ).astype(jnp.bfloat16)
     branch_ref[...] = branch
     if last:
-        wide = branch.astype(jnp.float32)
-        total = jnp.sum(wide * wide, axis=1, keepdims=True)
-        for start in range(0, total.shape[0], GROUP):
-            square_ref[:, start : start + GROUP] = turn(total[start : start + GROUP], 0)
-
-
-def out_project(layer, core, blocks, weight, last):
+        for start in range(0, branch.shape[0], GROUP):
+            at = slice(start, start + GROUP)
+            wide = branch_ref[at].astype(jnp.float32)
+            square_ref[:, at] = turn(jnp.sum(wide * wide, axis=1, keepdims=True), 0)
+
+
+def out_project(layer, blocks, weight, last):
     rows = blocks[0].shape[1]
     own = weight.shape[1]
     shapes = [jax.ShapeDtypeStruct((rows, own), jnp.bfloat16)]
@@ -389,7 +387,7 @@
     return pl.pallas_call(
         functools.partial(out_body, layer, len(blocks), last),
         out_shape=tuple(shapes),
-        in_specs=[smem] + [vmem] * len(blocks) + [hbm],
+        in_specs=[vmem] * len(blocks) + [hbm],
         out_specs=(vmem,) * len(shapes),
         scratch_shapes=[
             pltpu.VMEM((own, D), jnp.bfloat16),
@@ -398,31 +396,47 @@
         ],
         compiler_params=params,
         name="out_project",
-    )(core, *blocks, weight)
-
-
-def finish_body(resid_ref, branch_ref, gain_ref, *refs):
+    )(*blocks, weight)
+
+
+def finish_body(head_ref, tail_ref, branch_ref, gain_ref, *refs):
     out_ref = refs[-1]
     total = refs[0][...]
     for ref in refs[1:-1]:
         total = total + ref[...]
+    own = out_ref.shape[1]
+    cols = slice(None)
+    if head_ref.shape[1] != own:
+        cols = pl.ds(pl.multiple_of(lax.axis_index("tp") * own, 128), own)
+    gain = gain_ref[gain_ref.shape[0] - 1 :, cols]
+    head_rows = head_ref.shape[0]
     for start in range(0, out_ref.shape[0], GROUP):
         at = slice(start, start + GROUP)
         inv_out = lax.rsqrt(turn(total[:, at], 1) / D + norm_eps)
-        old = resid_ref[at].astype(jnp.float32)
+        if start < head_rows:
+            old = head_ref[at, cols]
+        else:
+            old = tail_ref[start - head_rows : start - head_rows + GROUP, cols]
         branch = branch_ref[at].astype(jnp.float32)
-        out_ref[at] = (old + branch * inv_out * gain_ref[...]).astype(jnp.bfloat16)
-
-
-def finish(resid_cols, branch, gain_cols, totals):
+        out_ref[at] = (old.astype(jnp.float32) + branch * inv_out * gain).astype(jnp.bfloat16)
+
+
+def finish(head, tail, branch, gain, totals):
+    own = branch.shape[1]
+    if own % 128:
+        start = lax.axis_index("tp") * own
+        head, tail, gain = [
+            lax.dynamic_slice_in_dim(part, start, own, 1) for part in (head, tail, gain)
+        ]
+    operands = (head, tail, branch, gain, *totals)
     return pl.pallas_call(
         finish_body,
         out_shape=jax.ShapeDtypeStruct(branch.shape, jnp.bfloat16),
-        in_specs=[vmem] * (3 + len(totals)),
+        in_specs=[vmem] * len(operands),
         out_specs=vmem,
         compiler_params=params,
         name="finish",
-    )(resid_cols, branch, gain_cols, *totals)
+    )(*operands)
 
 
 def partner(x):
@@ -467,50 +481,39 @@
     position_bias,
     post_gain,
 ):
-    rows, own = tokens.shape
-    tp_at = lax.axis_index("tp")
-    core = jnp.reshape(tp_at % CORES, (1,)).astype(jnp.int32)
-    sp_at = jnp.reshape(lax.axis_index("sp"), (1,)).astype(jnp.int32)
+    rows = tokens.shape[0]
     docs = documents[None, :]
-    behind = from_behind(docs[:, rows - PAST :])
+    *bands, mask = setup(position_bias, docs)
     blocks = gather(tokens)
-    band, mask = setup(sp_at, position_bias, docs, behind)
-    tail_resid = head_resid = None
+    tail_resid = head_resid = behind = None
     for layer in range(LAYERS):
-        post = post_gain[layer - 1 : layer] if layer else None
-        pre = pre_gain[layer : layer + 1]
         tail_resid, normed, inv, tail = project_tail(
-            layer, core, blocks, tail_resid, post, pre, (key_weight, value_weight)
-        )
+            layer, blocks, tail_resid, post_gain, pre_gain, (key_weight, value_weight)
+        )
+        if behind is None:
+            tail, docs_tail = lax.optimization_barrier((tail, docs[:, rows - PAST :]))
+            behind = from_behind(docs_tail)
         halo = from_behind(tail)
         head_resid, head, query, gate, local_mixed = project_local(
             layer,
-            core,
             blocks,
             head_resid,
-            post,
-            pre,
+            post_gain,
+            pre_gain,
             (normed, inv, tail),
-            band,
+            bands[layer],
             mask,
             (key_weight, value_weight, query_weight, gate_weight),
         )
-        mixed = attend(layer, query, gate, head, tail, halo, local_mixed, band, mask)
+        mixed = attend(
+            layer, query, gate, head, tail, halo, local_mixed, bands[layer], docs, behind
+        )
         last = layer + 1 == LAYERS
-        result = out_project(layer, core, gather(mixed), out_weight, last)
+        result = out_project(layer, gather(mixed), out_weight, last)
         if not last:
             blocks = gather(result[0])
     branch, square = result
-    start = tp_at * own
-    resid_cols = jnp.concatenate(
-        [lax.dynamic_slice_in_dim(part, start, own, 1) for part in (head_resid, tail_resid)]
-    )
-    return finish(
-        resid_cols,
-        branch,
-        lax.dynamic_slice_in_dim(post_gain[LAYERS - 1 :], start, own, 1),
-        total_over_features(square),
-    )
+    return finish(head_resid, tail_resid, branch, post_gain, total_over_features(square))
 
 
 def solution(mesh):

time: 208 us -> 186 us (0.89)
  local copies, waits for them, and re-layouts: 21 us -> 7.14 us
  waiting for transfers between devices: 29.5 us -> 22.5 us
  Pallas kernels: 37.3 us -> 34.6 us
  starting transfers between devices: 7.01 us -> 9.49 us
    unnamed x52 -> x24, local copies, waits for them, and re-layouts: 17.2 us -> 6.45 us
    ppermute x4, waiting for transfers between devices: 13.8 us -> 6.36 us  [from_behind(): return lax.ppermute(block, 'sp', [(i, (i + 1) % size) for i in range(size)])]
    ppermute x7, waiting for transfers between devices: 11 us -> 14 us  [partner(): return lax.ppermute(x, 'tp', [(i, i ^ 1) for i in range(size)])]
    ppermute x3, waiting for transfers between devices: 4.76 us -> 2.12 us  [total_over_features(): lax.ppermute(both, 'tp', [(i, (i + hop) % size) for i in range(size)])]
  transfers between devices with their start and end apart: 14 -> 14, of which waited for: 12 -> 11; matrix products, arithmetic and copies ran while one was open for 2% -> 0% of each run, Pallas kernels for 8% -> 9%
where the time goes in v3:
time: 186 us; the launch traced here: 185 us
  blocking collectives  111 us (60%)
  Pallas kernels  34.6 us (19%)
  waiting for transfers between devices  22.5 us (12%)
  starting transfers between devices  9.49 us (5%)
  local copies, waits for them, and re-layouts  7.14 us (4%)
    all_gather x6, blocking collectives, gather(): own = lax.all_gather(x, 'tp', axis=0, axis_index_groups=lines)  111 us
    pallas_call x3, Pallas kernels, project_local(): pl.pallas_call(functools.partial(local_body, layer, first, len(blocks)),...  14.7 us
    ppermute x7, waiting for transfers between devices, partner(): return lax.ppermute(x, 'tp', [(i, i ^ 1) for i in range(size)])  14 us
    pallas_call x3, Pallas kernels, project_tail(): pl.pallas_call(functools.partial(tail_body, layer, first, len(blocks), ro...  8.27 us
    pallas_call x3, Pallas kernels, attend(): pl.pallas_call(attend_body, out_shape=jax.ShapeDtypeStruct((rows, own), j...  6.7 us
    unnamed x24, local copies, waits for them, and re-layouts  6.45 us
    ppermute x4, waiting for transfers between devices, from_behind(): return lax.ppermute(block, 'sp', [(i, (i + 1) % size) for i in range(size)])  6.36 us
    ppermute x4, starting transfers between devices, from_behind(): return lax.ppermute(block, 'sp', [(i, (i + 1) % size) for i in range(size)])  5.45 us
  transfers between devices with their start and end apart: 14, of which 11 were waited for; matrix products, arithmetic and copies ran while one was open for 0% of the time, Pallas kernels for 9%

profile of v3, /device:TPU:0, one launch (start us, length us, event | category | flops | bytes accessed | tf_op | source)
XLA Modules:
  0.0 185.4 jit_solution(10074279120556084586)
XLA Ops:
  0.0 21.5 %all-gather = bf16[1536,256]{1,0:T(8,128)(2,1)S(1)} all-gather(bf16[384,256]{1,0:T(8,128)(2,1)} %param.10), channel_id=2, replica_groups={{0,2,4,6},{1,3,5,7},{8,10,12,14},{9,11,13,15},{16,18,20,22},{17,19,21,2..., dimensions={0}, use_global_device_ids=true | all-gather | bytes 983040 | tf_op jit(solution)/shard_map/all_gather | solution.py:452
  21.5 0.0 collective-permute-start
  21.5 0.7 broadcast_in_dim.3.docs_ref
  22.2 1.6 collective-permute-done.refs_1_
  23.8 0.0 copy-start
  23.8 1.9 %copy-done = bf16[3,256,2048]{2,1,0:T(8,128)(2,1)S(1)} copy-done((bf16[3,256,2048]{2,1,0:T(8,128)(2,1)S(1)}, bf16[3,256,2048]{2,1,0:T(8,128)(2,1)}, u32[]{:S(2)}) %copy-start) | copy-done | bytes 3145752
  25.7 0.0 copy-start.2
  25.7 1.9 %copy-done.2 = bf16[3,256,2048]{2,1,0:T(8,128)(2,1)S(1)} copy-done((bf16[3,256,2048]{2,1,0:T(8,128)(2,1)S(1)}, bf16[3,256,2048]{2,1,0:T(8,128)(2,1)}, u32[]{:S(2)}) %copy-start.2) | copy-done | bytes 3145752
  27.6 0.8 copy-done.8
  28.3 2.4 %project_tail.3 = (bf16[256,2048]{1,0:T(8,128)(2,1)S(1)}, bf16[256,2048]{1,0:T(8,128)(2,1)S(1)}, f32[256,128]{1,0:T(8,128)S(1)}, bf16[256,512]{1,0:T(8,128)(2,1)S(1)}) custom-call(bf16[4,384,256]{2,1,0:T(8,128)(2,1)S(1)} %bitcast.13, bf16[4,384,256]{2,1,0:T(8,128)(2,1)S(1)} %collective-permute-done.refs_1_, f32[3,2048]{1,0:T(4,128)S(1)} %copy-done.8, ...), custom_call_target="tpu_custom_call" | custom-call | tf_op jit(solution)/shard_map/project_tail/pallas_call | solution.py:182
  30.7 1.5 collective-permute-start.1
  32.3 1.5 collective-permute-start.2
  33.8 0.0 copy-done.11
  33.8 1.3 setup.1
  35.1 0.0 copy-done.1
  35.1 0.0 copy-done.5
  35.1 0.0 copy-done.9
  35.1 0.0 copy-start.6
  35.1 1.9 %copy-done.6 = bf16[3,256,2048]{2,1,0:T(8,128)(2,1)S(1)} copy-done((bf16[3,256,2048]{2,1,0:T(8,128)(2,1)S(1)}, bf16[3,256,2048]{2,1,0:T(8,128)(2,1)}, u32[]{:S(2)}) %copy-start.6) | copy-done | bytes 3145752
  37.0 4.7 %project_local.3 = (bf16[128,2048]{1,0:T(8,128)(2,1)S(1)}, bf16[128,512]{1,0:T(8,128)(2,1)S(1)}, bf16[256,256]{1,0:T(8,128)(2,1)S(1)}, bf16[256,256]{1,0:T(8,128)(2,1)S(1)}, bf16[128,256]{1,0:T(8,128)(2,1)S(1)}) custom-call(bf16[4,384,256]{2,1,0:T(8,128)(2,1)S(1)} %bitcast.14, bf16[4,384,256]{2,1,0:T(8,128)(2,1)S(1)} %collective-permute-done.refs_1_, ...), custom_call_target="tpu_custom_call" | custom-call | tf_op jit(solution)/shard_map/project_local/pallas_call | solution.py:292
  41.7 0.0 collective-permute-done.2.behind_ref
  41.7 0.0 collective-permute-done.1.halo_ref
  41.7 2.2 %attend.3 = bf16[384,256]{1,0:T(8,128)(2,1)S(1)} custom-call(bf16[256,256]{1,0:T(8,128)(2,1)S(1)} %get-tuple-element.46.query_ref, bf16[256,256]{1,0:T(8,128)(2,1)S(1)} %get-tuple-element.47.gate_ref, bf16[128,512]{1,0:T(8,128)(2,1)S(1)} %get-tuple-element.48.head_ref, bf16[256,512]{1,0:T(8,128)(2,1)S(1)} %get-tuple-element.43.refs_5_.tail_ref, ...), custom_call_target="tpu_custom_call" | custom-call | tf_op jit(solution)/shard_map/attend/pallas_call | solution.py:346
  44.0 17.9 %all-gather.1 = bf16[1536,256]{1,0:T(8,128)(2,1)S(1)} all-gather(bf16[384,256]{1,0:T(8,128)(2,1)S(1)} %attend.3), channel_id=3, replica_groups={{0,2,4,6},{1,3,5,7},{8,10,12,14},{9,11,13,15},{16,18,20,22},{17,19,21,2..., dimensions={0}, use_global_device_ids=true | all-gather | bytes 983040 | tf_op jit(solution)/shard_map/all_gather | solution.py:452
  61.9 0.0 collective-permute-start.3
  61.9 2.3 %collective-permute-done.3.refs_1_ = bf16[4,384,256]{2,1,0:T(8,128)(2,1)S(1)} collective-permute-done((bf16[4,384,256]{2,1,0:T(8,128)(2,1)S(1)}, bf16[4,384,256]{2,1,0:T(8,128)(2,1)S(1)}, u32[]{:S(2)}, u32[]{:S(2)}) %collective-permute-start.3) | collective-permute-done | bytes 786464 | tf_op jit(solution)/shard_map/ppermute | solution.py:444
  64.2 0.0 copy-done.4
  64.2 0.9 out_project.3
  65.1 18.2 %all-gather.2 = bf16[1536,256]{1,0:T(8,128)(2,1)S(1)} all-gather(bf16[384,256]{1,0:T(8,128)(2,1)S(1)} %out_project.3), channel_id=4, replica_groups={{0,2,4,6},{1,3,5,7},{8,10,12,14},{9,11,13,15},{16,18,20,22},{17,19,21,2..., dimensions={0}, use_global_device_ids=true | all-gather | bytes 983040 | tf_op jit(solution)/shard_map/all_gather | solution.py:452
  83.3 0.0 collective-permute-start.4
  83.3 2.3 %collective-permute-done.4.refs_1_ = bf16[4,384,256]{2,1,0:T(8,128)(2,1)S(1)} collective-permute-done((bf16[4,384,256]{2,1,0:T(8,128)(2,1)S(1)}, bf16[4,384,256]{2,1,0:T(8,128)(2,1)S(1)}, u32[]{:S(2)}, u32[]{:S(2)}) %collective-permute-start.4) | collective-permute-done | bytes 786464 | tf_op jit(solution)/shard_map/ppermute | solution.py:444
  85.5 0.0 copy-done.3
  85.5 0.0 copy-done.10
  85.6 3.0 %project_tail.4 = (bf16[256,2048]{1,0:T(8,128)(2,1)S(1)}, bf16[256,2048]{1,0:T(8,128)(2,1)S(1)}, f32[256,128]{1,0:T(8,128)S(1)}, bf16[256,512]{1,0:T(8,128)(2,1)S(1)}) custom-call(bf16[4,384,256]{2,1,0:T(8,128)(2,1)S(1)} %bitcast.10, bf16[4,384,256]{2,1,0:T(8,128)(2,1)S(1)} %collective-permute-done.4.refs_1_, ...), custom_call_target="tpu_custom_call" | custom-call | tf_op jit(solution)/shard_map/project_tail/pallas_call | solution.py:182
  88.5 1.7 collective-permute-start.5
  90.2 0.0 copy-done.7
  90.3 5.0 %project_local.4 = (bf16[128,2048]{1,0:T(8,128)(2,1)S(1)}, bf16[128,512]{1,0:T(8,128)(2,1)S(1)}, bf16[256,256]{1,0:T(8,128)(2,1)S(1)}, bf16[256,256]{1,0:T(8,128)(2,1)S(1)}, bf16[128,256]{1,0:T(8,128)(2,1)S(1)}) custom-call(bf16[4,384,256]{2,1,0:T(8,128)(2,1)S(1)} %bitcast.11, bf16[4,384,256]{2,1,0:T(8,128)(2,1)S(1)} %collective-permute-done.4.refs_1_, ...), custom_call_target="tpu_custom_call" | custom-call | tf_op jit(solution)/shard_map/project_local/pallas_call | solution.py:292
  95.3 2.7 %collective-permute-done.5.halo_ref = bf16[256,512]{1,0:T(8,128)(2,1)S(1)} collective-permute-done((bf16[256,512]{1,0:T(8,128)(2,1)S(1)}, bf16[256,512]{1,0:T(8,128)(2,1)S(1)}, u32[]{:S(2)}, u32[]{:S(2)}) %collective-permute-start.5) | collective-permute-done | bytes 262176 | tf_op jit(solution)/shard_map/ppermute | solution.py:469
  98.0 2.2 %attend.4 = bf16[384,256]{1,0:T(8,128)(2,1)S(1)} custom-call(bf16[256,256]{1,0:T(8,128)(2,1)S(1)} %get-tuple-element.57.query_ref, bf16[256,256]{1,0:T(8,128)(2,1)S(1)} %get-tuple-element.58.gate_ref, bf16[128,512]{1,0:T(8,128)(2,1)S(1)} %get-tuple-element.59.head_ref, bf16[256,512]{1,0:T(8,128)(2,1)S(1)} %get-tuple-element.55.refs_7_.tail_ref, ...), custom_call_target="tpu_custom_call" | custom-call | tf_op jit(solution)/shard_map/attend/pallas_call | solution.py:346
  100.2 17.9 %all-gather.3 = bf16[1536,256]{1,0:T(8,128)(2,1)S(1)} all-gather(bf16[384,256]{1,0:T(8,128)(2,1)S(1)} %attend.4), channel_id=5, replica_groups={{0,2,4,6},{1,3,5,7},{8,10,12,14},{9,11,13,15},{16,18,20,22},{17,19,21,2..., dimensions={0}, use_global_device_ids=true | all-gather | bytes 983040 | tf_op jit(solution)/shard_map/all_gather | solution.py:452
  118.1 0.0 collective-permute-start.6
  118.1 2.3 %collective-permute-done.6.refs_1_ = bf16[4,384,256]{2,1,0:T(8,128)(2,1)S(1)} collective-permute-done((bf16[4,384,256]{2,1,0:T(8,128)(2,1)S(1)}, bf16[4,384,256]{2,1,0:T(8,128)(2,1)S(1)}, u32[]{:S(2)}, u32[]{:S(2)}) %collective-permute-start.6) | collective-permute-done | bytes 786464 | tf_op jit(solution)/shard_map/ppermute | solution.py:444
  120.4 0.9 out_project.4
  121.3 18.0 %all-gather.4 = bf16[1536,256]{1,0:T(8,128)(2,1)S(1)} all-gather(bf16[384,256]{1,0:T(8,128)(2,1)S(1)} %out_project.4), channel_id=6, replica_groups={{0,2,4,6},{1,3,5,7},{8,10,12,14},{9,11,13,15},{16,18,20,22},{17,19,21,2..., dimensions={0}, use_global_device_ids=true | all-gather | bytes 983040 | tf_op jit(solution)/shard_map/all_gather | solution.py:452
  139.4 0.0 collective-permute-start.7
  139.4 2.3 %collective-permute-done.7.refs_1_ = bf16[4,384,256]{2,1,0:T(8,128)(2,1)S(1)} collective-permute-done((bf16[4,384,256]{2,1,0:T(8,128)(2,1)S(1)}, bf16[4,384,256]{2,1,0:T(8,128)(2,1)S(1)}, u32[]{:S(2)}, u32[]{:S(2)}) %collective-permute-start.7) | collective-permute-done | bytes 786464 | tf_op jit(solution)/shard_map/ppermute | solution.py:444
  141.6 2.9 %project_tail.5 = (bf16[256,2048]{1,0:T(8,128)(2,1)S(1)}, bf16[256,2048]{1,0:T(8,128)(2,1)S(1)}, f32[256,128]{1,0:T(8,128)S(1)}, bf16[256,512]{1,0:T(8,128)(2,1)S(1)}) custom-call(bf16[4,384,256]{2,1,0:T(8,128)(2,1)S(1)} %bitcast.7, bf16[4,384,256]{2,1,0:T(8,128)(2,1)S(1)} %collective-permute-done.7.refs_1_, ...), custom_call_target="tpu_custom_call" | custom-call | tf_op jit(solution)/shard_map/project_tail/pallas_call | solution.py:182
  144.6 0.7 collective-permute-start.8
  145.3 5.0 %project_local.5 = (bf16[128,2048]{1,0:T(8,128)(2,1)S(1)}, bf16[128,512]{1,0:T(8,128)(2,1)S(1)}, bf16[256,256]{1,0:T(8,128)(2,1)S(1)}, bf16[256,256]{1,0:T(8,128)(2,1)S(1)}, bf16[128,256]{1,0:T(8,128)(2,1)S(1)}) custom-call(bf16[4,384,256]{2,1,0:T(8,128)(2,1)S(1)} %bitcast.8, bf16[4,384,256]{2,1,0:T(8,128)(2,1)S(1)} %collective-permute-done.7.refs_1_, ...), custom_call_target="tpu_custom_call" | custom-call | tf_op jit(solution)/shard_map/project_local/pallas_call | solution.py:292
  150.3 3.6 %collective-permute-done.8.halo_ref = bf16[256,512]{1,0:T(8,128)(2,1)S(1)} collective-permute-done((bf16[256,512]{1,0:T(8,128)(2,1)S(1)}, bf16[256,512]{1,0:T(8,128)(2,1)S(1)}, u32[]{:S(2)}, u32[]{:S(2)}) %collective-permute-start.8) | collective-permute-done | bytes 262176 | tf_op jit(solution)/shard_map/ppermute | solution.py:469
  153.9 2.2 %attend.5 = bf16[384,256]{1,0:T(8,128)(2,1)S(1)} custom-call(bf16[256,256]{1,0:T(8,128)(2,1)S(1)} %get-tuple-element.69.query_ref, bf16[256,256]{1,0:T(8,128)(2,1)S(1)} %get-tuple-element.70.gate_ref, bf16[128,512]{1,0:T(8,128)(2,1)S(1)} %get-tuple-element.71.head_ref, bf16[256,512]{1,0:T(8,128)(2,1)S(1)} %get-tuple-element.65.refs_7_.tail_ref, ...), custom_call_target="tpu_custom_call" | custom-call | tf_op jit(solution)/shard_map/attend/pallas_call | solution.py:346
  156.1 17.9 %all-gather.5 = bf16[1536,256]{1,0:T(8,128)(2,1)S(1)} all-gather(bf16[384,256]{1,0:T(8,128)(2,1)S(1)} %attend.5), channel_id=7, replica_groups={{0,2,4,6},{1,3,5,7},{8,10,12,14},{9,11,13,15},{16,18,20,22},{17,19,21,2..., dimensions={0}, use_global_device_ids=true | all-gather | bytes 983040 | tf_op jit(solution)/shard_map/all_gather | solution.py:452
  174.1 0.0 collective-permute-start.9
  174.1 2.3 %collective-permute-done.9.refs_1_ = bf16[4,384,256]{2,1,0:T(8,128)(2,1)S(1)} collective-permute-done((bf16[4,384,256]{2,1,0:T(8,128)(2,1)S(1)}, bf16[4,384,256]{2,1,0:T(8,128)(2,1)S(1)}, u32[]{:S(2)}, u32[]{:S(2)}) %collective-permute-start.9) | collective-permute-done | bytes 786464 | tf_op jit(solution)/shard_map/ppermute | solution.py:444
  176.3 1.0 out_project.5
  177.3 0.2 collective-permute-start.10
  177.5 1.0 collective-permute-done.10
  178.6 0.0 collective-permute-start.11
  178.6 2.4 %collective-permute-start.12 = (f32[1,384]{1,0:T(1,128)S(1)}, f32[1,384]{1,0:T(1,128)S(1)}, u32[]{:S(2)}, u32[]{:S(2)}) collective-permute-start(f32[1,384]{1,0:T(1,128)S(1)} %add.3.refs_0_), channel_id=1, source_target_pairs={{0,4},{1,5},{2,6},{3,7},{4,0},{5,1},{6,2},{7,3},{8,12},{9,13},{10,... | collective-permute-start | bytes 4616 | tf_op jit(solution)/shard_map/ppermute | solution.py:462
  180.9 1.5 collective-permute-start.13
  182.4 1.6 collective-permute-done.11.refs_1_
  184.0 0.0 collective-permute-done.12.refs_2_
  184.0 0.6 collective-permute-done.13.refs_3_
  184.5 0.9 finish.1
  (11 shorter events, 0.0 us)
Async XLA Ops:
  21.5 2.3 %collective-permute-start = (bf16[4,384,256]{2,1,0:T(8,128)(2,1)S(1)}, bf16[4,384,256]{2,1,0:T(8,128)(2,1)S(1)}, u32[]{:S(2)}, u32[]{:S(2)}) collective-permute-start(bf16[4,384,256]{2,1,0:T(8,128)(2,1)S(1)} %bitcast.12), channel_id=1, source_target_pairs={{0,1},{1,0},{2,3},{3,2},{4,5},{5,4},{6,7},{7,6},{8,9},{9,8},{10,11... | collective-permute-start | bytes 2359304 | tf_op jit(solution)/shard_map/ppermute | solution.py:444
  23.8 1.9 %copy-start = (bf16[3,256,2048]{2,1,0:T(8,128)(2,1)S(1)}, bf16[3,256,2048]{2,1,0:T(8,128)(2,1)}, u32[]{:S(2)}) copy-start(bf16[3,256,2048]{2,1,0:T(8,128)(2,1)} %refs_10_.5) | copy-start | bytes 9437188
  25.7 1.9 %copy-start.2 = (bf16[3,256,2048]{2,1,0:T(8,128)(2,1)S(1)}, bf16[3,256,2048]{2,1,0:T(8,128)(2,1)}, u32[]{:S(2)}) copy-start(bf16[3,256,2048]{2,1,0:T(8,128)(2,1)} %refs_11_.5) | copy-start | bytes 9437188
  27.6 0.8 copy-start.8
  28.3 5.4 %copy-start.11 = (f32[3,4,257]{2,1,0:T(4,128)S(1)}, f32[3,4,257]{2,1,0:T(4,128)}, u32[]{:S(2)}) copy-start(f32[3,4,257]{2,1,0:T(4,128)} %bias_ref.1) | copy-start | bytes 37012
  28.3 6.7 %copy-start.1 = (bf16[3,256,2048]{2,1,0:T(8,128)(2,1)S(1)}, bf16[3,256,2048]{2,1,0:T(8,128)(2,1)}, u32[]{:S(2)}) copy-start(bf16[3,256,2048]{2,1,0:T(8,128)(2,1)} %refs_10_.5) | copy-start | bytes 9437188
  28.3 6.7 %copy-start.5 = (bf16[3,256,2048]{2,1,0:T(8,128)(2,1)S(1)}, bf16[3,256,2048]{2,1,0:T(8,128)(2,1)}, u32[]{:S(2)}) copy-start(bf16[3,256,2048]{2,1,0:T(8,128)(2,1)} %refs_12_.3) | copy-start | bytes 9437188
  28.3 6.8 %copy-start.9 = (f32[3,2048]{1,0:T(4,128)S(1)}, f32[3,2048]{1,0:T(4,128)}, u32[]{:S(2)}) copy-start(f32[3,2048]{1,0:T(4,128)} %refs_4_.9) | copy-start | bytes 73732
  30.7 11.0 %collective-permute-start.1 = (bf16[256,512]{1,0:T(8,128)(2,1)S(1)}, bf16[256,512]{1,0:T(8,128)(2,1)S(1)}, u32[]{:S(2)}, u32[]{:S(2)}) collective-permute-start(bf16[256,512]{1,0:T(8,128)(2,1)S(1)} %get-tuple-element.43.refs_5_.tail_ref), channel_id=1, source_target_pairs={{0,8},{8,16},{16,24},{24,0},{1,9},{9,17},{17,25},{25,1},{2,10},{10... | collective-permute-start | bytes 786440 | tf_op jit(solution)/shard_map/ppermute | solution.py:469
  32.3 9.4 %collective-permute-start.2 = (s32[1,256]{1,0:T(1,128)S(1)}, s32[1,256]{1,0:T(1,128)S(1)}, u32[]{:S(2)}, u32[]{:S(2)}) collective-permute-start(s32[1,256]{1,0:T(1,128)S(1)} %slice.4), channel_id=1, source_target_pairs={{0,8},{8,16},{16,24},{24,0},{1,9},{9,17},{17,25},{25,1},{2,10},{10... | collective-permute-start | bytes 3080 | tf_op jit(solution)/shard_map/ppermute | solution.py:469
  35.1 1.9 %copy-start.6 = (bf16[3,256,2048]{2,1,0:T(8,128)(2,1)S(1)}, bf16[3,256,2048]{2,1,0:T(8,128)(2,1)}, u32[]{:S(2)}) copy-start(bf16[3,256,2048]{2,1,0:T(8,128)(2,1)} %refs_13_.3) | copy-start | bytes 9437188
  37.0 27.2 %copy-start.4 = (bf16[3,256,2048]{2,1,0:T(8,128)(2,1)S(1)}, bf16[3,256,2048]{2,1,0:T(8,128)(2,1)}, u32[]{:S(2)}) copy-start(bf16[3,256,2048]{2,1,0:T(8,128)(2,1)} %refs_2_.9) | copy-start | bytes 9437188
  61.9 23.7 %copy-start.3 = (bf16[3,256,2048]{2,1,0:T(8,128)(2,1)S(1)}, bf16[3,256,2048]{2,1,0:T(8,128)(2,1)}, u32[]{:S(2)}) copy-start(bf16[3,256,2048]{2,1,0:T(8,128)(2,1)} %refs_11_.5) | copy-start | bytes 9437188
  61.9 23.7 %copy-start.10 = (f32[3,2048]{1,0:T(4,128)S(1)}, f32[3,2048]{1,0:T(4,128)}, u32[]{:S(2)}) copy-start(f32[3,2048]{1,0:T(4,128)} %gain_ref.1) | copy-start | bytes 73732
  61.9 2.3 %collective-permute-start.3 = (bf16[4,384,256]{2,1,0:T(8,128)(2,1)S(1)}, bf16[4,384,256]{2,1,0:T(8,128)(2,1)S(1)}, u32[]{:S(2)}, u32[]{:S(2)}) collective-permute-start(bf16[4,384,256]{2,1,0:T(8,128)(2,1)S(1)} %bitcast.17), channel_id=1, source_target_pairs={{0,1},{1,0},{2,3},{3,2},{4,5},{5,4},{6,7},{7,6},{8,9},{9,8},{10,11... | collective-permute-start | bytes 2359304 | tf_op jit(solution)/shard_map/ppermute | solution.py:444
  83.3 2.3 %collective-permute-start.4 = (bf16[4,384,256]{2,1,0:T(8,128)(2,1)S(1)}, bf16[4,384,256]{2,1,0:T(8,128)(2,1)S(1)}, u32[]{:S(2)}, u32[]{:S(2)}) collective-permute-start(bf16[4,384,256]{2,1,0:T(8,128)(2,1)S(1)} %bitcast.9), channel_id=1, source_target_pairs={{0,1},{1,0},{2,3},{3,2},{4,5},{5,4},{6,7},{7,6},{8,9},{9,8},{10,11... | collective-permute-start | bytes 2359304 | tf_op jit(solution)/shard_map/ppermute | solution.py:444
  85.5 4.7 %copy-start.7 = (bf16[3,256,2048]{2,1,0:T(8,128)(2,1)S(1)}, bf16[3,256,2048]{2,1,0:T(8,128)(2,1)}, u32[]{:S(2)}) copy-start(bf16[3,256,2048]{2,1,0:T(8,128)(2,1)} %refs_13_.3) | copy-start | bytes 9437188
  88.5 9.5 %collective-permute-start.5 = (bf16[256,512]{1,0:T(8,128)(2,1)S(1)}, bf16[256,512]{1,0:T(8,128)(2,1)S(1)}, u32[]{:S(2)}, u32[]{:S(2)}) collective-permute-start(bf16[256,512]{1,0:T(8,128)(2,1)S(1)} %get-tuple-element.55.refs_7_.tail_ref), channel_id=1, source_target_pairs={{0,8},{8,16},{16,24},{24,0},{1,9},{9,17},{17,25},{25,1},{2,10},{10... | collective-permute-start | bytes 786440 | tf_op jit(solution)/shard_map/ppermute | solution.py:469
  118.1 2.3 %collective-permute-start.6 = (bf16[4,384,256]{2,1,0:T(8,128)(2,1)S(1)}, bf16[4,384,256]{2,1,0:T(8,128)(2,1)S(1)}, u32[]{:S(2)}, u32[]{:S(2)}) collective-permute-start(bf16[4,384,256]{2,1,0:T(8,128)(2,1)S(1)} %bitcast.19), channel_id=1, source_target_pairs={{0,1},{1,0},{2,3},{3,2},{4,5},{5,4},{6,7},{7,6},{8,9},{9,8},{10,11... | collective-permute-start | bytes 2359304 | tf_op jit(solution)/shard_map/ppermute | solution.py:444
  139.4 2.3 %collective-permute-start.7 = (bf16[4,384,256]{2,1,0:T(8,128)(2,1)S(1)}, bf16[4,384,256]{2,1,0:T(8,128)(2,1)S(1)}, u32[]{:S(2)}, u32[]{:S(2)}) collective-permute-start(bf16[4,384,256]{2,1,0:T(8,128)(2,1)S(1)} %bitcast.6), channel_id=1, source_target_pairs={{0,1},{1,0},{2,3},{3,2},{4,5},{5,4},{6,7},{7,6},{8,9},{9,8},{10,11... | collective-permute-start | bytes 2359304 | tf_op jit(solution)/shard_map/ppermute | solution.py:444
  144.6 9.3 %collective-permute-start.8 = (bf16[256,512]{1,0:T(8,128)(2,1)S(1)}, bf16[256,512]{1,0:T(8,128)(2,1)S(1)}, u32[]{:S(2)}, u32[]{:S(2)}) collective-permute-start(bf16[256,512]{1,0:T(8,128)(2,1)S(1)} %get-tuple-element.65.refs_7_.tail_ref), channel_id=1, source_target_pairs={{0,8},{8,16},{16,24},{24,0},{1,9},{9,17},{17,25},{25,1},{2,10},{10... | collective-permute-start | bytes 786440 | tf_op jit(solution)/shard_map/ppermute | solution.py:469
  174.1 2.3 %collective-permute-start.9 = (bf16[4,384,256]{2,1,0:T(8,128)(2,1)S(1)}, bf16[4,384,256]{2,1,0:T(8,128)(2,1)S(1)}, u32[]{:S(2)}, u32[]{:S(2)}) collective-permute-start(bf16[4,384,256]{2,1,0:T(8,128)(2,1)S(1)} %bitcast.15), channel_id=1, source_target_pairs={{0,1},{1,0},{2,3},{3,2},{4,5},{5,4},{6,7},{7,6},{8,9},{9,8},{10,11... | collective-permute-start | bytes 2359304 | tf_op jit(solution)/shard_map/ppermute | solution.py:444
  177.3 1.2 collective-permute-start.10
  178.6 5.4 %collective-permute-start.11 = (f32[1,384]{1,0:T(1,128)S(1)}, f32[1,384]{1,0:T(1,128)S(1)}, u32[]{:S(2)}, u32[]{:S(2)}) collective-permute-start(f32[1,384]{1,0:T(1,128)S(1)} %add.3.refs_0_), channel_id=1, source_target_pairs={{0,2},{1,3},{2,4},{3,5},{4,6},{5,7},{6,0},{7,1},{8,10},{9,11},{10,... | collective-permute-start | bytes 4616 | tf_op jit(solution)/shard_map/ppermute | solution.py:462
  178.6 5.4 %collective-permute-start.12 = (f32[1,384]{1,0:T(1,128)S(1)}, f32[1,384]{1,0:T(1,128)S(1)}, u32[]{:S(2)}, u32[]{:S(2)}) collective-permute-start(f32[1,384]{1,0:T(1,128)S(1)} %add.3.refs_0_), channel_id=1, source_target_pairs={{0,4},{1,5},{2,6},{3,7},{4,0},{5,1},{6,2},{7,3},{8,12},{9,13},{10,... | collective-permute-start | bytes 4616 | tf_op jit(solution)/shard_map/ppermute | solution.py:462
  180.9 3.6 %collective-permute-start.13 = (f32[1,384]{1,0:T(1,128)S(1)}, f32[1,384]{1,0:T(1,128)S(1)}, u32[]{:S(2)}, u32[]{:S(2)}) collective-permute-start(f32[1,384]{1,0:T(1,128)S(1)} %add.3.refs_0_), channel_id=1, source_target_pairs={{0,6},{1,7},{2,0},{3,1},{4,2},{5,3},{6,4},{7,5},{8,14},{9,15},{10,... | collective-permute-start | bytes 4616 | tf_op jit(solution)/shard_map/ppermute | solution.py:462

commit v4 on v3

v4 whole, which is shorter than its diff:
```python
import functools

import jax
import jax.numpy as jnp
from jax import lax
from jax.experimental import pallas as pl
from jax.experimental.pallas import tpu as pltpu
from jax.sharding import PartitionSpec as P

D = 2048
HD = 64
BLOCK = 64
PAST_BLOCKS = 4
LAYERS = 3
PAST = 256
CLIP = 128
GROUP = 2 * BLOCK
WINDOW = PAST + GROUP
SKEW = 512
CORES = 2
DOC_ROWS = 16
FAR = -1e30

norm_eps = 1e-06
rows_by_rows = (((1,), (1,)), ((), ()))
vmem = pl.BlockSpec(memory_space=pltpu.VMEM)
hbm = pl.BlockSpec(memory_space=pltpu.HBM)
params = pltpu.CompilerParams(vmem_limit_bytes=16 * 1024 * 1024)


def turn(vector, axis):
    size = GROUP
    diagonal = lax.broadcasted_iota(jnp.int32, (size, size), 0) == lax.broadcasted_iota(
        jnp.int32, (size, size), 1
    )
    spread = jnp.where(diagonal, jnp.broadcast_to(vector, (size, size)), jnp.zeros_like(vector))
    return jnp.sum(spread, axis=axis, keepdims=True)


def setup_body(bias_hbm, docs_ref, *refs):
    sources, refs = refs[:6], refs[6:]
    stage_ref, pre_ref, post_ref, docs_out, mask_ref, *bands = refs[:-2]
    bias_ref, sems = refs[-2:]
    bias_copy = pltpu.make_async_copy(bias_hbm, bias_ref, sems.at[6])
    bias_copy.start()
    targets = [stage_ref.at[at] for at in range(4)] + [pre_ref, post_ref]
    copies = [
        pltpu.make_async_copy(source.at[0] if at < 4 else source, target, sems.at[at])
        for at, (source, target) in enumerate(zip(sources, targets))
    ]
    for copy in copies:
        copy.start()
    docs = docs_ref[...].reshape(1, docs_ref.shape[0])
    docs_out[...] = docs
    for index in range(mask_ref.shape[0]):
        start = PAST + index * GROUP
        mask_ref[index] = doc_mask(
            docs[:, start : start + GROUP], docs[:, start - PAST : start + GROUP]
        )
    layers, heads, entries = bias_ref.shape
    row_block = lax.broadcasted_iota(jnp.int32, (GROUP, WINDOW), 0) // BLOCK
    col_block = lax.broadcasted_iota(jnp.int32, (GROUP, WINDOW), 1) // BLOCK
    allowed = (col_block >= row_block) & (col_block <= row_block + PAST_BLOCKS)
    shift = lax.broadcasted_iota(jnp.int32, (entries, SKEW), 1)
    entry = jnp.where(shift < WINDOW, jnp.minimum(PAST - shift, CLIP) + CLIP, 2 * CLIP)
    pick = (lax.broadcasted_iota(jnp.int32, (entries, SKEW), 0) == entry).astype(jnp.float32)
    bias_copy.wait()
    for layer in range(layers):
        base = lax.dot_general(
            bias_ref[layer],
            pick,
            (((1,), (0,)), ((), ())),
            precision=lax.Precision.HIGHEST,
            preferred_element_type=jnp.float32,
        )
        for head in range(heads):
            row = jnp.broadcast_to(base[head : head + 1, :], (GROUP, SKEW))
            skewed = pltpu.roll(row, 0, 1, stride=1, stride_axis=0)
            bands[layer][head] = jnp.where(allowed, skewed[:, :WINDOW], FAR)
    for copy in copies:
        copy.wait()


def doc_mask(own, seen):
    return jnp.where(turn(own, 1) == seen, 0.0, FAR)


def setup(position_bias, docs, weights, pre_gain, post_gain):
    layers, heads, _ = position_bias.shape
    rows = docs.shape[0]
    groups = (rows - PAST) // GROUP
    own = weights[0].shape[1]
    shapes = [
        jax.ShapeDtypeStruct((4, own, D), jnp.bfloat16),
        jax.ShapeDtypeStruct(pre_gain.shape, jnp.float32),
        jax.ShapeDtypeStruct(post_gain.shape, jnp.float32),
        jax.ShapeDtypeStruct((1, rows), jnp.int32),
        jax.ShapeDtypeStruct((groups, GROUP, WINDOW), jnp.float32),
        *[jax.ShapeDtypeStruct((heads, GROUP, WINDOW), jnp.float32) for _ in range(layers)],
    ]
    far = [
        pltpu.with_memory_space_constraint(a, pltpu.HBM)
        for a in (position_bias, *weights, pre_gain, post_gain)
    ]
    return pl.pallas_call(
        setup_body,
        out_shape=tuple(shapes),
        in_specs=[hbm, vmem] + [hbm] * 6,
        out_specs=(vmem,) * len(shapes),
        scratch_shapes=[
            pltpu.VMEM(position_bias.shape, jnp.float32),
            pltpu.SemaphoreType.DMA((7,)),
        ],
        compiler_params=params,
        name="setup",
    )(far[0], docs, *far[1:])


def ring_order(count):
    return [0, *range(1, count, 2), *reversed(range(2, count, 2))]


def block_columns(blocks):
    if len(blocks) == 1:
        return [(blocks[0], 0, 0)]
    core = lax.rem(lax.axis_index("tp"), CORES)
    width = blocks[0].shape[2]
    return [
        (ref, slot, pl.multiple_of((CORES * z + (core if side == 0 else 1 - core)) * width, 128))
        for side, ref in enumerate(blocks)
        for slot, z in enumerate(ring_order(ref.shape[0]))
    ]


def lane_sum(square):
    total = square[:, :128]
    for at in range(128, square.shape[1], 128):
        total = total + square[:, at : at + 128]
    return total


def update_rows(layer, blocks, offset, resid_ref, post_ref, pre_ref, resid_out, normed_ref, inv_ref):
    step = BLOCK
    placed = block_columns(blocks)
    width = blocks[0].shape[2]

    def one(index, carry):
        at = pl.ds(pl.multiple_of(index * step, step), step)
        source = pl.ds(pl.multiple_of(offset + index * step, step), step)
        if resid_ref is not None:
            total = jnp.zeros((step, 128), jnp.float32)
            for ref, z, _ in placed:
                part = ref[z, source, :].astype(jnp.float32)
                total = total + lane_sum(part * part)
            inv_out = lax.rsqrt(jnp.sum(total, axis=1, keepdims=True) / D + norm_eps)
        total = jnp.zeros((step, 128), jnp.float32)
        for ref, z, col in placed:
            cols = pl.ds(col, width)
            if resid_ref is None:
                new = ref[z, source, :]
            else:
                part = ref[z, source, :].astype(jnp.float32)
                old = resid_ref[at, cols].astype(jnp.float32)
                new = (old + part * inv_out * post_ref[layer - 1 : layer, cols]).astype(jnp.bfloat16)
            resid_out[at, cols] = new
            wide = new.astype(jnp.float32)
            total = total + lane_sum(wide * wide)
            normed_ref[at, cols] = (wide * pre_ref[layer : layer + 1, cols]).astype(jnp.bfloat16)
        inv_in = lax.rsqrt(jnp.sum(total, axis=1, keepdims=True) / D + norm_eps)
        inv_ref[at, :] = jnp.broadcast_to(inv_in, (step, 128))
        return carry

    lax.fori_loop(0, resid_out.shape[0] // step, one, 0)


def scaled_product(normed_ref, inv_ref, weight):
    product = lax.dot_general(
        normed_ref[...], weight, rows_by_rows, preferred_element_type=jnp.float32
    )
    return (product * inv_ref[:, :1]).astype(jnp.bfloat16)


def weight_of(layer, weights, at):
    return weights[0][at] if layer == 0 else weights[at][layer]


def piece_body(layer, count, offset, *refs):
    blocks, refs = refs[:count], refs[count:]
    resid_ref = post_ref = docs_ref = None
    if layer:
        (resid_ref, post_ref), refs = refs[:2], refs[2:]
    else:
        docs_ref, refs = refs[0], refs[1:]
    pre_ref, weights = refs[0], refs[1:-4]
    resid_out, normed_ref, inv_ref, kv_ref = refs[-4:]
    update_rows(
        layer, blocks, offset, resid_ref, post_ref, pre_ref, resid_out, normed_ref, inv_ref
    )
    own = kv_ref.shape[1] // 2
    for at in range(2):
        kv_ref[:GROUP, at * own : (at + 1) * own] = scaled_product(
            normed_ref, inv_ref, weight_of(layer, weights, at)
        )
    if layer == 0:
        docs = docs_ref[:, offset : offset + GROUP].astype(jnp.float32)
        kv_ref[GROUP:, :GROUP] = jnp.broadcast_to(docs, (DOC_ROWS, GROUP)).astype(jnp.bfloat16)


def project_piece(layer, blocks, offset, resid, docs, post, pre, weights):
    own = weights[0].shape[1]
    bf = jnp.bfloat16
    extra = [resid, post] if layer else [docs]
    operands = [*blocks, *extra, pre, *weights]
    kv_rows = GROUP if layer else GROUP + DOC_ROWS
    return pl.pallas_call(
        functools.partial(piece_body, layer, len(blocks), offset),
        out_shape=(
            jax.ShapeDtypeStruct((GROUP, D), bf),
            jax.ShapeDtypeStruct((GROUP, D), bf),
            jax.ShapeDtypeStruct((GROUP, 128), jnp.float32),
            jax.ShapeDtypeStruct((kv_rows, 2 * own), bf),
        ),
        in_specs=[vmem] * len(operands),
        out_specs=(vmem,) * 4,
        compiler_params=params,
        name="project_piece",
    )(*operands)


def attend_group(query, gate, ext_ref, seen, band_ref, mask, own):
    span = min(own, 128)
    lane = lax.broadcasted_iota(jnp.int32, (GROUP, span), 1) // HD
    results = []
    for start in range(0, own, span):
        cols = slice(start, start + span)
        keys = ext_ref[seen, cols]
        values = ext_ref[seen, own + start : own + start + span]
        result = None
        for sub in range(span // HD):
            picked = jnp.where(lane == sub, query[:, cols], jnp.zeros((), query.dtype))
            scores = lax.dot_general(
                picked, keys, rows_by_rows, preferred_element_type=jnp.float32
            )
            scores = scores + band_ref[start // HD + sub] + mask
            lifted = jnp.exp(scores - jnp.max(scores, axis=1, keepdims=True))
            total = jnp.sum(lifted, axis=1, keepdims=True)
            part = jnp.dot(lifted.astype(jnp.bfloat16), values, preferred_element_type=jnp.float32)
            part = part / total
            result = part if result is None else jnp.where(lane == sub, part, result)
        wide = gate[:, cols].astype(jnp.float32)
        results.append((result * (wide / (1.0 + jnp.exp(-wide)))).astype(jnp.bfloat16))
    return results


def store_group(mixed_ref, at, results):
    start = 0
    for result in results:
        mixed_ref[at, start : start + result.shape[1]] = result
        start = start + result.shape[1]


def local_body(layer, count, *refs):
    blocks, refs = refs[:count], refs[count:]
    resid_ref = post_ref = None
    if layer:
        (resid_ref, post_ref), refs = refs[:2], refs[2:]
    pieces = PAST // GROUP
    pre_ref, refs = refs[0], refs[1:]
    piece_normed, piece_inv, piece_kv = [refs[at * pieces : (at + 1) * pieces] for at in range(3)]
    refs = refs[3 * pieces :]
    band_ref, mask_ref, weights = refs[0], refs[1], refs[2:-8]
    resid_out, head_ref, query_out, gate_out, mixed_ref = refs[-8:-3]
    normed_ref, inv_ref, ext_ref = refs[-3:]
    head_rows = resid_out.shape[0]
    head_at = pl.ds(0, head_rows)
    for index in range(pieces):
        at = pl.ds(head_rows + index * GROUP, GROUP)
        normed_ref[at] = piece_normed[index][...]
        inv_ref[at] = piece_inv[index][...]
        ext_ref[at] = piece_kv[index][:GROUP]
    update_rows(
        layer,
        blocks,
        0,
        resid_ref,
        post_ref,
        pre_ref,
        resid_out,
        normed_ref.at[head_at],
        inv_ref.at[head_at],
    )
    rest, own = query_out.shape
    local = []
    for at in range(4):
        weight = weight_of(layer, weights, at)
        if at < 2:
            head = scaled_product(normed_ref.at[head_at], inv_ref.at[head_at], weight)
            head_ref[:, at * own : (at + 1) * own] = head
            continue
        product = scaled_product(normed_ref, inv_ref, weight)
        if at == 2:
            product = product * jnp.bfloat16(HD ** (-0.5))
        target = query_out if at == 2 else gate_out
        target[...] = product[:rest]
        local.append(product[rest:])
    ext_ref[head_at] = head_ref[...]
    for index in range(mask_ref.shape[0]):
        at = slice(index * GROUP, (index + 1) * GROUP)
        seen = slice(index * GROUP, index * GROUP + WINDOW)
        results = attend_group(
            local[0][at], local[1][at], ext_ref, seen, band_ref, mask_ref[index], own
        )
        store_group(mixed_ref, at, results)


def project_local(layer, blocks, resid, post, pre, pieces, band, mask, weights):
    rows = blocks[0].shape[1]
    own = weights[0].shape[1]
    head_rows = rows - PAST
    bf = jnp.bfloat16
    moved = [*blocks] + ([resid, post] if layer else []) + [pre, *pieces, band, mask]
    shapes = [
        (head_rows, D),
        (head_rows, 2 * own),
        (PAST, own),
        (PAST, own),
        (rows - PAST, own),
    ]
    return pl.pallas_call(
        functools.partial(local_body, layer, len(blocks)),
        out_shape=tuple(jax.ShapeDtypeStruct(shape, bf) for shape in shapes),
        in_specs=[vmem] * (len(moved) + len(weights)),
        out_specs=(vmem,) * len(shapes),
        scratch_shapes=[
            pltpu.VMEM((rows, D), bf),
            pltpu.VMEM((rows, 128), jnp.float32),
            pltpu.VMEM((rows, 2 * own), bf),
        ],
        compiler_params=params,
        name="project_local",
    )(*moved, *weights)


def attend_body(layer, *refs):
    pieces = PAST // GROUP
    piece_refs, halo_refs, refs = refs[:pieces], refs[pieces : 2 * pieces], refs[2 * pieces :]
    query_ref, gate_ref, head_ref, local_ref, band_ref, docs_ref = refs[:6]
    if layer:
        behind_ref, mixed_ref, ext_ref = refs[6:]
    else:
        mixed_ref, behind_ref, ext_ref = refs[6:]
        first = lax.axis_index("sp") == 0
        for index in range(pieces):
            told = halo_refs[index][GROUP : GROUP + DOC_ROWS, :GROUP].astype(jnp.float32)[:1]
            behind_ref[:, index * GROUP : (index + 1) * GROUP] = jnp.where(
                first, -1, told.astype(jnp.int32)
            )
    head_rows, own = head_ref.shape[0], query_ref.shape[1]
    rest = query_ref.shape[0]
    for index in range(pieces):
        ext_ref[index * GROUP : (index + 1) * GROUP] = halo_refs[index][:GROUP]
        start = PAST + head_rows + index * GROUP
        ext_ref[start : start + GROUP] = piece_refs[index][:GROUP]
    ext_ref[PAST : PAST + head_rows] = head_ref[...]
    mixed_ref[rest:] = local_ref[...]
    docs = docs_ref[...]
    docs_seen = jnp.concatenate([behind_ref[...], docs], axis=1)
    for group in range(rest // GROUP):
        at = slice(group * GROUP, (group + 1) * GROUP)
        seen = slice(group * GROUP, group * GROUP + WINDOW)
        mask = doc_mask(docs[:, at], docs_seen[:, seen])
        store_group(
            mixed_ref,
            at,
            attend_group(query_ref[at], gate_ref[at], ext_ref, seen, band_ref, mask, own),
        )


def attend(layer, pieces, halos, query, gate, head, local_mixed, band, docs, behind):
    own = query.shape[1]
    rows = head.shape[0] + PAST
    operands = [*pieces, *halos, query, gate, head, local_mixed, band, docs]
    shapes = [jax.ShapeDtypeStruct((rows, own), jnp.bfloat16)]
    if layer:
        operands.append(behind)
    else:
        shapes.append(jax.ShapeDtypeStruct((1, PAST), jnp.int32))
    return pl.pallas_call(
        functools.partial(attend_body, layer),
        out_shape=tuple(shapes),
        in_specs=[vmem] * len(operands),
        out_specs=(vmem,) * len(shapes),
        scratch_shapes=[pltpu.VMEM((PAST + rows, 2 * own), jnp.bfloat16)],
        compiler_params=params,
        name="attend",
    )(*operands)


def out_body(layer, count, last, *refs):
    blocks = refs[:count]
    weight_ref, branch_ref = refs[count : 2 + count]
    rest = refs[2 + count :]
    if last:
        square_ref, rest = rest[0], rest[1:]
    width = blocks[0].shape[2]
    mixed_ref = rest[0]
    for ref, z, col in block_columns(blocks):
        mixed_ref[:, pl.ds(col, width)] = ref[z]
    branch = lax.dot_general(
        mixed_ref[...], weight_ref[layer], rows_by_rows, preferred_element_type=jnp.float32
    ).astype(jnp.bfloat16)
    branch_ref[...] = branch
    if last:
        for start in range(0, branch.shape[0], GROUP):
            at = slice(start, start + GROUP)
            wide = branch_ref[at].astype(jnp.float32)
            square_ref[:, at] = turn(jnp.sum(wide * wide, axis=1, keepdims=True), 0)


def out_project(layer, blocks, weight, last):
    rows = blocks[0].shape[1]
    own = weight.shape[1]
    shapes = [jax.ShapeDtypeStruct((rows, own), jnp.bfloat16)]
    if last:
        shapes.append(jax.ShapeDtypeStruct((1, rows), jnp.float32))
    return pl.pallas_call(
        functools.partial(out_body, layer, len(blocks), last),
        out_shape=tuple(shapes),
        in_specs=[vmem] * (len(blocks) + 1),
        out_specs=(vmem,) * len(shapes),
        scratch_shapes=[pltpu.VMEM((rows, D), jnp.bfloat16)],
        compiler_params=params,
        name="out_project",
    )(*blocks, weight)


def finish_body(count, *refs):
    resid_refs, (branch_ref, gain_ref), refs = refs[:count], refs[count : count + 2], refs[count + 2 :]
    out_ref = refs[-1]
    total = refs[0][...]
    for ref in refs[1:-1]:
        total = total + ref[...]
    own = out_ref.shape[1]
    cols = slice(None)
    if gain_ref.shape[1] != own:
        cols = pl.ds(pl.multiple_of(lax.axis_index("tp") * own, 128), own)
    gain = gain_ref[gain_ref.shape[0] - 1 :, cols]
    start = 0
    for ref in resid_refs:
        for base in range(0, ref.shape[0], GROUP):
            at = slice(start, start + GROUP)
            inv_out = lax.rsqrt(turn(total[:, at], 1) / D + norm_eps)
            old = ref[base : base + GROUP, cols].astype(jnp.float32)
            branch = branch_ref[at].astype(jnp.float32)
            out_ref[at] = (old + branch * inv_out * gain).astype(jnp.bfloat16)
            start = start + GROUP


def finish(resids, branch, gain, totals):
    own = branch.shape[1]
    if own % 128:
        start = lax.axis_index("tp") * own
        *resids, gain = [
            lax.dynamic_slice_in_dim(part, start, own, 1) for part in (*resids, gain)
        ]
    operands = (*resids, branch, gain, *totals)
    return pl.pallas_call(
        functools.partial(finish_body, len(resids)),
        out_shape=jax.ShapeDtypeStruct(branch.shape, jnp.bfloat16),
        in_specs=[vmem] * len(operands),
        out_specs=vmem,
        compiler_params=params,
        name="finish",
    )(*operands)


def partner(x):
    size = lax.axis_size("tp")
    return lax.ppermute(x, "tp", [(i, i ^ 1) for i in range(size)])


def gather(x):
    size = lax.axis_size("tp")
    if x.shape[1] % 128 or size % CORES:
        return lax.all_gather(x, "tp", axis=1, tiled=True)[None]
    order = ring_order(size // CORES)
    lines = [[CORES * z + core for z in order] for core in range(CORES)]
    return lax.all_gather(x, "tp", axis=0, axis_index_groups=lines)


def swapped(own):
    return (own, partner(own)) if own.shape[2] < D else (own,)


def total_over_features(square):
    size = lax.axis_size("tp")
    if size % CORES or size > 8:
        return (lax.psum(square, "tp"),)
    both = square + partner(square)
    return (both,) + tuple(
        lax.ppermute(both, "tp", [(i, (i + hop) % size) for i in range(size)])
        for hop in range(CORES, size, CORES)
    )


def from_behind(block):
    size = lax.axis_size("sp")
    return lax.ppermute(block, "sp", [(i, (i + 1) % size) for i in range(size)])


def local(
    tokens,
    documents,
    pre_gain,
    query_weight,
    key_weight,
    value_weight,
    gate_weight,
    out_weight,
    position_bias,
    post_gain,
):
    rows = tokens.shape[0]
    starts = range(rows - PAST, rows, GROUP)
    weights = (key_weight, value_weight, query_weight, gate_weight)
    gathered, documents = lax.optimization_barrier((gather(tokens), documents))
    blocks = swapped(gathered)
    stage, pre, post, docs, mask, *bands = setup(
        position_bias, documents, weights, pre_gain, post_gain
    )
    resids = [None] * len(starts)
    head_resid = behind = None
    for layer in range(LAYERS):
        used = weights if layer else (stage,)
        made = [None] * len(starts)
        halos = [None] * len(starts)
        for index in reversed(range(len(starts))):
            made[index] = project_piece(
                layer,
                blocks,
                starts[index],
                resids[index],
                docs,
                post,
                pre,
                used[:2],
            )
            halos[index] = from_behind(made[index][3])
        resids, normed, inv, pieces = [list(part) for part in zip(*made)]
        head_resid, head, query, gate, local_mixed = project_local(
            layer,
            blocks,
            head_resid,
            post,
            pre,
            (*normed, *inv, *pieces),
            bands[layer],
            mask,
            used,
        )
        mixed, *told = attend(
            layer, pieces, halos, query, gate, head, local_mixed, bands[layer], docs, behind
        )
        behind = told[0] if told else behind
        last = layer + 1 == LAYERS
        result = out_project(layer, swapped(gather(mixed)), out_weight, last)
        if not last:
            blocks = swapped(gather(result[0]))
    branch, square = result
    return finish((head_resid, *resids), branch, post, total_over_features(square))


def solution(mesh):
    placed = (
        P("sp", "tp"),
        P("sp"),
        P(),
        P(None, "tp", None),
        P(None, "tp", None),
        P(None, "tp", None),
        P(None, "tp", None),
        P(None, "tp", None),
        P(None, "tp", None),
        P(),
    )
    return jax.shard_map(
        local, mesh=mesh, in_specs=placed, out_specs=P("sp", "tp"), check_vma=False
    )
```

time: 186 us -> 170 us (0.914)
  local copies, waits for them, and re-layouts: 7.14 us -> 0.7 us
  blocking collectives: 111 us -> 105 us
  starting transfers between devices: 9.49 us -> 14.3 us
  Pallas kernels: 34.6 us -> 30.8 us
  waiting for transfers between devices: 22.5 us -> 18.7 us
    all_gather x6, blocking collectives: 111 us -> 105 us  [gather(): return lax.all_gather(x, 'tp', axis=0, axis_index_groups=lines)]
    unnamed x24 -> x12, local copies, waits for them, and re-layouts: 6.45 us -> 0.7 us
    ppermute x4 -> x6, starting transfers between devices: 5.45 us -> 9.44 us  [from_behind(): return lax.ppermute(block, 'sp', [(i, (i + 1) % size) for i in range(size)])]
    pallas_call x11 -> x14, Pallas kernels: 31.8 us -> 28.6 us  [the longest x3 10.4 us: project_local(): pl.pallas_call(functools.partial(local_body, layer, len(blocks)), out_sha...]
    ppermute x4 -> x6, waiting for transfers between devices: 6.36 us -> 4.88 us  [from_behind(): return lax.ppermute(block, 'sp', [(i, (i + 1) % size) for i in range(size)])]
  transfers between devices with their start and end apart: 14 -> 16, of which waited for: 11 -> 13; matrix products, arithmetic and copies ran while one was open for 0% -> 0% of each run, Pallas kernels for 9% -> 10%
where the time goes in v4:
time: 170 us
  blocking collectives  105 us (62%)
  Pallas kernels  30.8 us (18%)
  waiting for transfers between devices  18.7 us (11%)
  starting transfers between devices  14.3 us (8%)
    all_gather x6, blocking collectives, gather(): return lax.all_gather(x, 'tp', axis=0, axis_index_groups=lines)  105 us
    ppermute x7, waiting for transfers between devices, partner(): return lax.ppermute(x, 'tp', [(i, i ^ 1) for i in range(size)])  12.4 us
    pallas_call x3, Pallas kernels, project_local(): pl.pallas_call(functools.partial(local_body, layer, len(blocks)), out_sha...  10.4 us
    ppermute x6, starting transfers between devices, from_behind(): return lax.ppermute(block, 'sp', [(i, (i + 1) % size) for i in range(size)])  9.44 us
    pallas_call x6, Pallas kernels, project_piece(): pl.pallas_call(functools.partial(piece_body, layer, len(blocks), offset),...  8.3 us
    pallas_call x3, Pallas kernels, attend(): pl.pallas_call(functools.partial(attend_body, layer), out_shape=tuple(sha...  6.71 us
    ppermute x6, waiting for transfers between devices, from_behind(): return lax.ppermute(block, 'sp', [(i, (i + 1) % size) for i in range(size)])  4.88 us
    ppermute x3, starting transfers between devices, total_over_features(): lax.ppermute(both, 'tp', [(i, (i + hop) % size) for i in range(size)])  4.67 us
  transfers between devices with their start and end apart: 16, of which 13 were waited for; matrix products, arithmetic and copies ran while one was open for 0% of the time, Pallas kernels for 10%

profile of v4, /device:TPU:0, one launch (start us, length us, event | category | flops | bytes accessed | tf_op | source)
XLA Modules:
  0.0 169.8 jit_solution(5277009213414413643)
XLA Ops:
  0.0 19.6 %all-gather = bf16[1536,256]{1,0:T(8,128)(2,1)S(1)} all-gather(bf16[384,256]{1,0:T(8,128)(2,1)} %param.10), channel_id=2, replica_groups={{0,2,6,4},{1,3,7,5},{8,10,14,12},{9,11,15,13},{16,18,22,20},{17,19,23,2..., dimensions={0}, use_global_device_ids=true | all-gather | bytes 983040 | tf_op jit(solution)/shard_map/all_gather | solution.py:488
  19.6 0.0 collective-permute-start
  19.6 0.0 copy-start.5
  19.6 0.7 copy-done.5
  20.3 2.3 %setup.1 = (bf16[4,256,2048]{2,1,0:T(8,128)(2,1)S(1)}, f32[3,2048]{1,0:T(4,128)S(1)}, f32[3,2048]{1,0:T(4,128)S(1)}, s32[1,384]{1,0:T(1,128)S(1)}, f32[1,128,384...) custom-call(f32[3,4,257]{2,1,0:T(4,128)} %bias_hbm.1, ...), custom_call_target="tpu_custom_call" | custom-call | tf_op jit(solution)/shard_map/setup/pallas_call | solution.py:105
  22.5 0.0 collective-permute-done.refs_1_
  22.6 1.2 project_piece.7
  23.8 1.5 collective-permute-start.2
  25.3 1.2 project_piece.6
  26.5 1.5 collective-permute-start.1
  28.0 0.0 copy-start.4
  28.0 3.3 %project_local.3 = (bf16[128,2048]{1,0:T(8,128)(2,1)S(1)}, bf16[128,512]{1,0:T(8,128)(2,1)S(1)}, bf16[256,256]{1,0:T(8,128)(2,1)S(1)}, bf16[256,256]{1,0:T(8,128)(2,1)S(1)}, bf16[128,256]{1,0:T(8,128)(2,1)S(1)}) custom-call(bf16[4,384,256]{2,1,0:T(8,128)(2,1)S(1)} %bitcast.17, bf16[4,384,256]{2,1,0:T(8,128)(2,1)S(1)} %collective-permute-done.refs_1_, ...), custom_call_target="tpu_custom_call" | custom-call | tf_op jit(solution)/shard_map/project_local/pallas_call | solution.py:329
  31.3 0.1 collective-permute-done.2.refs_3_
  31.4 2.7 %collective-permute-done.1.refs_2_ = bf16[144,512]{1,0:T(8,128)(2,1)S(1)} collective-permute-done((bf16[144,512]{1,0:T(8,128)(2,1)S(1)}, bf16[144,512]{1,0:T(8,128)(2,1)S(1)}, u32[]{:S(2)}, u32[]{:S(2)}) %collective-permute-start.1) | collective-permute-done | bytes 147488 | tf_op jit(solution)/shard_map/ppermute | solution.py:508
  34.1 2.2 %attend.3 = (bf16[384,256]{1,0:T(8,128)(2,1)S(1)}, s32[1,256]{1,0:T(1,128)S(1)}) custom-call(bf16[144,512]{1,0:T(8,128)(2,1)S(1)} %get-tuple-element.63.refs_7_.refs_0_, bf16[144,512]{1,0:T(8,128)(2,1)S(1)} %get-tuple-element.64.refs_8_.refs_1_, bf16[144,512]{1,0:T(8,128)(2,1)S(1)} %collective-permute-done.1.refs_2_, ...), custom_call_target="tpu_custom_call" | custom-call | tf_op jit(solution)/shard_map/attend/pallas_call | solution.py:388
  36.4 0.0 copy-start.1
  36.4 18.0 %all-gather.1 = bf16[1536,256]{1,0:T(8,128)(2,1)S(1)} all-gather(bf16[384,256]{1,0:T(8,128)(2,1)S(1)} %get-tuple-element.75), channel_id=3, replica_groups={{0,2,6,4},{1,3,7,5},{8,10,14,12},{9,11,15,13},{16,18,22,20},{17,19,23,2..., dimensions={0}, use_global_device_ids=true | all-gather | bytes 983040 | tf_op jit(solution)/shard_map/all_gather | solution.py:488
  54.4 0.0 collective-permute-start.3
  54.4 2.3 %collective-permute-done.3.refs_1_ = bf16[4,384,256]{2,1,0:T(8,128)(2,1)S(1)} collective-permute-done((bf16[4,384,256]{2,1,0:T(8,128)(2,1)S(1)}, bf16[4,384,256]{2,1,0:T(8,128)(2,1)S(1)}, u32[]{:S(2)}, u32[]{:S(2)}) %collective-permute-start.3) | collective-permute-done | bytes 786464 | tf_op jit(solution)/shard_map/ppermute | solution.py:479
  56.7 0.0 copy-done.4
  56.7 0.7 out_project.3
  57.4 16.9 %all-gather.2 = bf16[1536,256]{1,0:T(8,128)(2,1)S(1)} all-gather(bf16[384,256]{1,0:T(8,128)(2,1)S(1)} %out_project.3), channel_id=4, replica_groups={{0,2,6,4},{1,3,7,5},{8,10,14,12},{9,11,15,13},{16,18,22,20},{17,19,23,2..., dimensions={0}, use_global_device_ids=true | all-gather | bytes 983040 | tf_op jit(solution)/shard_map/all_gather | solution.py:488
  74.4 0.0 collective-permute-start.4
  74.4 2.3 %collective-permute-done.4.refs_1_ = bf16[4,384,256]{2,1,0:T(8,128)(2,1)S(1)} collective-permute-done((bf16[4,384,256]{2,1,0:T(8,128)(2,1)S(1)}, bf16[4,384,256]{2,1,0:T(8,128)(2,1)S(1)}, u32[]{:S(2)}, u32[]{:S(2)}) %collective-permute-start.4) | collective-permute-done | bytes 786464 | tf_op jit(solution)/shard_map/ppermute | solution.py:479
  76.7 0.0 copy-done.1
  76.7 0.0 copy-done
  76.7 1.5 project_piece.9
  78.2 0.3 collective-permute-start.6
  78.5 1.5 project_piece.8
  80.0 2.9 %collective-permute-start.5 = (bf16[128,512]{1,0:T(8,128)(2,1)S(1)}, bf16[128,512]{1,0:T(8,128)(2,1)S(1)}, u32[]{:S(2)}, u32[]{:S(2)}) collective-permute-start(bf16[128,512]{1,0:T(8,128)(2,1)S(1)} %get-tuple-element.78.refs_9_.refs_0_), channel_id=1, source_target_pairs={{0,8},{8,16},{16,24},{24,0},{1,9},{9,17},{17,25},{25,1},{2,10},{10... | collective-permute-start | bytes 393224 | tf_op jit(solution)/shard_map/ppermute | solution.py:508
  82.9 0.0 copy-done.2
  82.9 0.0 copy-done.3
  82.9 3.6 %project_local.4 = (bf16[128,2048]{1,0:T(8,128)(2,1)S(1)}, bf16[128,512]{1,0:T(8,128)(2,1)S(1)}, bf16[256,256]{1,0:T(8,128)(2,1)S(1)}, bf16[256,256]{1,0:T(8,128)(2,1)S(1)}, bf16[128,256]{1,0:T(8,128)(2,1)S(1)}) custom-call(bf16[4,384,256]{2,1,0:T(8,128)(2,1)S(1)} %bitcast.13, bf16[4,384,256]{2,1,0:T(8,128)(2,1)S(1)} %collective-permute-done.4.refs_1_, ...), custom_call_target="tpu_custom_call" | custom-call | tf_op jit(solution)/shard_map/project_local/pallas_call | solution.py:329
  86.5 0.0 collective-permute-done.6.refs_3_
  86.5 1.0 collective-permute-done.5.refs_2_
  87.5 2.2 %attend.4 = bf16[384,256]{1,0:T(8,128)(2,1)S(1)} custom-call(bf16[128,512]{1,0:T(8,128)(2,1)S(1)} %get-tuple-element.78.refs_9_.refs_0_, bf16[128,512]{1,0:T(8,128)(2,1)S(1)} %get-tuple-element.80.refs_10_.refs_1_, bf16[128,512]{1,0:T(8,128)(2,1)S(1)} %collective-permute-done.5.refs_2_, bf16[128,512]{1,0:T(8,128)(2,1)S(1)} %collective-permute-done.6.refs_3_, ...), custom_call_target="tpu_custom_call" | custom-call | tf_op jit(solution)/shard_map/attend/pallas_call | solution.py:388
  89.7 16.9 %all-gather.3 = bf16[1536,256]{1,0:T(8,128)(2,1)S(1)} all-gather(bf16[384,256]{1,0:T(8,128)(2,1)S(1)} %attend.4), channel_id=5, replica_groups={{0,2,6,4},{1,3,7,5},{8,10,14,12},{9,11,15,13},{16,18,22,20},{17,19,23,2..., dimensions={0}, use_global_device_ids=true | all-gather | bytes 983040 | tf_op jit(solution)/shard_map/all_gather | solution.py:488
  106.6 0.0 collective-permute-start.7
  106.6 2.3 %collective-permute-done.7.refs_1_ = bf16[4,384,256]{2,1,0:T(8,128)(2,1)S(1)} collective-permute-done((bf16[4,384,256]{2,1,0:T(8,128)(2,1)S(1)}, bf16[4,384,256]{2,1,0:T(8,128)(2,1)S(1)}, u32[]{:S(2)}, u32[]{:S(2)}) %collective-permute-start.7) | collective-permute-done | bytes 786464 | tf_op jit(solution)/shard_map/ppermute | solution.py:479
  108.9 0.7 out_project.4
  109.6 17.1 %all-gather.4 = bf16[1536,256]{1,0:T(8,128)(2,1)S(1)} all-gather(bf16[384,256]{1,0:T(8,128)(2,1)S(1)} %out_project.4), channel_id=6, replica_groups={{0,2,6,4},{1,3,7,5},{8,10,14,12},{9,11,15,13},{16,18,22,20},{17,19,23,2..., dimensions={0}, use_global_device_ids=true | all-gather | bytes 983040 | tf_op jit(solution)/shard_map/all_gather | solution.py:488
  126.7 0.0 collective-permute-start.8
  126.7 2.3 %collective-permute-done.8.refs_1_ = bf16[4,384,256]{2,1,0:T(8,128)(2,1)S(1)} collective-permute-done((bf16[4,384,256]{2,1,0:T(8,128)(2,1)S(1)}, bf16[4,384,256]{2,1,0:T(8,128)(2,1)S(1)}, u32[]{:S(2)}, u32[]{:S(2)}) %collective-permute-start.8) | collective-permute-done | bytes 786464 | tf_op jit(solution)/shard_map/ppermute | solution.py:479
  129.0 1.5 project_piece.11
  130.5 0.7 collective-permute-start.10
  131.2 1.5 project_piece.10
  132.7 2.4 %collective-permute-start.9 = (bf16[128,512]{1,0:T(8,128)(2,1)S(1)}, bf16[128,512]{1,0:T(8,128)(2,1)S(1)}, u32[]{:S(2)}, u32[]{:S(2)}) collective-permute-start(bf16[128,512]{1,0:T(8,128)(2,1)S(1)} %get-tuple-element.99.refs_9_.refs_0_), channel_id=1, source_target_pairs={{0,8},{8,16},{16,24},{24,0},{1,9},{9,17},{17,25},{25,1},{2,10},{10... | collective-permute-start | bytes 393224 | tf_op jit(solution)/shard_map/ppermute | solution.py:508
  135.1 3.6 %project_local.5 = (bf16[128,2048]{1,0:T(8,128)(2,1)S(1)}, bf16[128,512]{1,0:T(8,128)(2,1)S(1)}, bf16[256,256]{1,0:T(8,128)(2,1)S(1)}, bf16[256,256]{1,0:T(8,128)(2,1)S(1)}, bf16[128,256]{1,0:T(8,128)(2,1)S(1)}) custom-call(bf16[4,384,256]{2,1,0:T(8,128)(2,1)S(1)} %bitcast.9, bf16[4,384,256]{2,1,0:T(8,128)(2,1)S(1)} %collective-permute-done.8.refs_1_, ...), custom_call_target="tpu_custom_call" | custom-call | tf_op jit(solution)/shard_map/project_local/pallas_call | solution.py:329
  138.7 0.0 collective-permute-done.10.refs_3_
  138.7 1.1 collective-permute-done.9.refs_2_
  139.8 2.2 %attend.5 = bf16[384,256]{1,0:T(8,128)(2,1)S(1)} custom-call(bf16[128,512]{1,0:T(8,128)(2,1)S(1)} %get-tuple-element.99.refs_9_.refs_0_, bf16[128,512]{1,0:T(8,128)(2,1)S(1)} %get-tuple-element.100.refs_10_.refs_1_, bf16[128,512]{1,0:T(8,128)(2,1)S(1)} %collective-permute-done.9.refs_2_, bf16[128,512]{1,0:T(8,128)(2,1)S(1)} %collective-permute-done.10.refs_3_, ...), custom_call_target="tpu_custom_call" | custom-call | tf_op jit(solution)/shard_map/attend/pallas_call | solution.py:388
  142.0 16.6 %all-gather.5 = bf16[1536,256]{1,0:T(8,128)(2,1)S(1)} all-gather(bf16[384,256]{1,0:T(8,128)(2,1)S(1)} %attend.5), channel_id=7, replica_groups={{0,2,6,4},{1,3,7,5},{8,10,14,12},{9,11,15,13},{16,18,22,20},{17,19,23,2..., dimensions={0}, use_global_device_ids=true | all-gather | bytes 983040 | tf_op jit(solution)/shard_map/all_gather | solution.py:488
  158.6 0.0 collective-permute-start.11
  158.6 2.3 %collective-permute-done.11.refs_1_ = bf16[4,384,256]{2,1,0:T(8,128)(2,1)S(1)} collective-permute-done((bf16[4,384,256]{2,1,0:T(8,128)(2,1)S(1)}, bf16[4,384,256]{2,1,0:T(8,128)(2,1)S(1)}, u32[]{:S(2)}, u32[]{:S(2)}) %collective-permute-start.11) | collective-permute-done | bytes 786464 | tf_op jit(solution)/shard_map/ppermute | solution.py:479
  160.9 0.8 out_project.5
  161.7 0.2 collective-permute-start.12
  161.9 1.0 collective-permute-done.12
  162.9 1.2 collective-permute-start.13
  164.1 1.3 collective-permute-start.14
  165.4 2.3 %collective-permute-start.15 = (f32[1,384]{1,0:T(1,128)S(1)}, f32[1,384]{1,0:T(1,128)S(1)}, u32[]{:S(2)}, u32[]{:S(2)}) collective-permute-start(f32[1,384]{1,0:T(1,128)S(1)} %add.3.refs_5_), channel_id=1, source_target_pairs={{0,6},{1,7},{2,0},{3,1},{4,2},{5,3},{6,4},{7,5},{8,14},{9,15},{10,... | collective-permute-start | bytes 4616 | tf_op jit(solution)/shard_map/ppermute | solution.py:501
  167.6 0.7 collective-permute-done.13.refs_6_
  168.3 0.3 collective-permute-done.14.refs_7_
  168.6 0.4 collective-permute-done.15.refs_8_
  168.9 0.9 finish.1
  (4 shorter events, 0.0 us)
Async XLA Ops:
  19.6 3.0 %collective-permute-start = (bf16[4,384,256]{2,1,0:T(8,128)(2,1)S(1)}, bf16[4,384,256]{2,1,0:T(8,128)(2,1)S(1)}, u32[]{:S(2)}, u32[]{:S(2)}) collective-permute-start(bf16[4,384,256]{2,1,0:T(8,128)(2,1)S(1)} %bitcast.14), channel_id=1, source_target_pairs={{0,1},{1,0},{2,3},{3,2},{4,5},{5,4},{6,7},{7,6},{8,9},{9,8},{10,11... | collective-permute-start | bytes 2359304 | tf_op jit(solution)/shard_map/ppermute | solution.py:479
  19.6 0.7 copy-start.5
  23.8 7.7 %collective-permute-start.2 = (bf16[144,512]{1,0:T(8,128)(2,1)S(1)}, bf16[144,512]{1,0:T(8,128)(2,1)S(1)}, u32[]{:S(2)}, u32[]{:S(2)}) collective-permute-start(bf16[144,512]{1,0:T(8,128)(2,1)S(1)} %get-tuple-element.64.refs_8_.refs_1_), channel_id=1, source_target_pairs={{0,8},{8,16},{16,24},{24,0},{1,9},{9,17},{17,25},{25,1},{2,10},{10... | collective-permute-start | bytes 442376 | tf_op jit(solution)/shard_map/ppermute | solution.py:508
  26.5 7.6 %collective-permute-start.1 = (bf16[144,512]{1,0:T(8,128)(2,1)S(1)}, bf16[144,512]{1,0:T(8,128)(2,1)S(1)}, u32[]{:S(2)}, u32[]{:S(2)}) collective-permute-start(bf16[144,512]{1,0:T(8,128)(2,1)S(1)} %get-tuple-element.63.refs_7_.refs_0_), channel_id=1, source_target_pairs={{0,8},{8,16},{16,24},{24,0},{1,9},{9,17},{17,25},{25,1},{2,10},{10... | collective-permute-start | bytes 442376 | tf_op jit(solution)/shard_map/ppermute | solution.py:508
  28.0 28.7 %copy-start.4 = (bf16[3,256,2048]{2,1,0:T(8,128)(2,1)S(1)}, bf16[3,256,2048]{2,1,0:T(8,128)(2,1)}, u32[]{:S(2)}) copy-start(bf16[3,256,2048]{2,1,0:T(8,128)(2,1)} %refs_2_.7) | copy-start | bytes 9437188
  36.4 40.3 %copy-start.1 = (bf16[3,256,2048]{2,1,0:T(8,128)(2,1)S(1)}, bf16[3,256,2048]{2,1,0:T(8,128)(2,1)}, u32[]{:S(2)}) copy-start(bf16[3,256,2048]{2,1,0:T(8,128)(2,1)} %refs_14_.3) | copy-start | bytes 9437188
  54.4 22.2 %copy-start = (bf16[3,256,2048]{2,1,0:T(8,128)(2,1)S(1)}, bf16[3,256,2048]{2,1,0:T(8,128)(2,1)}, u32[]{:S(2)}) copy-start(bf16[3,256,2048]{2,1,0:T(8,128)(2,1)} %refs_13_.3) | copy-start | bytes 9437188
  54.4 2.3 %collective-permute-start.3 = (bf16[4,384,256]{2,1,0:T(8,128)(2,1)S(1)}, bf16[4,384,256]{2,1,0:T(8,128)(2,1)S(1)}, u32[]{:S(2)}, u32[]{:S(2)}) collective-permute-start(bf16[4,384,256]{2,1,0:T(8,128)(2,1)S(1)} %bitcast.20), channel_id=1, source_target_pairs={{0,1},{1,0},{2,3},{3,2},{4,5},{5,4},{6,7},{7,6},{8,9},{9,8},{10,11... | collective-permute-start | bytes 2359304 | tf_op jit(solution)/shard_map/ppermute | solution.py:479
  74.4 2.3 %collective-permute-start.4 = (bf16[4,384,256]{2,1,0:T(8,128)(2,1)S(1)}, bf16[4,384,256]{2,1,0:T(8,128)(2,1)S(1)}, u32[]{:S(2)}, u32[]{:S(2)}) collective-permute-start(bf16[4,384,256]{2,1,0:T(8,128)(2,1)S(1)} %bitcast.10), channel_id=1, source_target_pairs={{0,1},{1,0},{2,3},{3,2},{4,5},{5,4},{6,7},{7,6},{8,9},{9,8},{10,11... | collective-permute-start | bytes 2359304 | tf_op jit(solution)/shard_map/ppermute | solution.py:479
  78.2 8.3 %collective-permute-start.6 = (bf16[128,512]{1,0:T(8,128)(2,1)S(1)}, bf16[128,512]{1,0:T(8,128)(2,1)S(1)}, u32[]{:S(2)}, u32[]{:S(2)}) collective-permute-start(bf16[128,512]{1,0:T(8,128)(2,1)S(1)} %get-tuple-element.80.refs_10_.refs_1_), channel_id=1, source_target_pairs={{0,8},{8,16},{16,24},{24,0},{1,9},{9,17},{17,25},{25,1},{2,10},{10... | collective-permute-start | bytes 393224 | tf_op jit(solution)/shard_map/ppermute | solution.py:508
  78.5 4.4 %copy-start.2 = (bf16[3,256,2048]{2,1,0:T(8,128)(2,1)S(1)}, bf16[3,256,2048]{2,1,0:T(8,128)(2,1)}, u32[]{:S(2)}) copy-start(bf16[3,256,2048]{2,1,0:T(8,128)(2,1)} %refs_15_.3) | copy-start | bytes 9437188
  78.5 4.4 %copy-start.3 = (bf16[3,256,2048]{2,1,0:T(8,128)(2,1)S(1)}, bf16[3,256,2048]{2,1,0:T(8,128)(2,1)}, u32[]{:S(2)}) copy-start(bf16[3,256,2048]{2,1,0:T(8,128)(2,1)} %refs_16_.3) | copy-start | bytes 9437188
  80.0 7.5 %collective-permute-start.5 = (bf16[128,512]{1,0:T(8,128)(2,1)S(1)}, bf16[128,512]{1,0:T(8,128)(2,1)S(1)}, u32[]{:S(2)}, u32[]{:S(2)}) collective-permute-start(bf16[128,512]{1,0:T(8,128)(2,1)S(1)} %get-tuple-element.78.refs_9_.refs_0_), channel_id=1, source_target_pairs={{0,8},{8,16},{16,24},{24,0},{1,9},{9,17},{17,25},{25,1},{2,10},{10... | collective-permute-start | bytes 393224 | tf_op jit(solution)/shard_map/ppermute | solution.py:508
  106.6 2.3 %collective-permute-start.7 = (bf16[4,384,256]{2,1,0:T(8,128)(2,1)S(1)}, bf16[4,384,256]{2,1,0:T(8,128)(2,1)S(1)}, u32[]{:S(2)}, u32[]{:S(2)}) collective-permute-start(bf16[4,384,256]{2,1,0:T(8,128)(2,1)S(1)} %bitcast.22), channel_id=1, source_target_pairs={{0,1},{1,0},{2,3},{3,2},{4,5},{5,4},{6,7},{7,6},{8,9},{9,8},{10,11... | collective-permute-start | bytes 2359304 | tf_op jit(solution)/shard_map/ppermute | solution.py:479
  126.7 2.3 %collective-permute-start.8 = (bf16[4,384,256]{2,1,0:T(8,128)(2,1)S(1)}, bf16[4,384,256]{2,1,0:T(8,128)(2,1)S(1)}, u32[]{:S(2)}, u32[]{:S(2)}) collective-permute-start(bf16[4,384,256]{2,1,0:T(8,128)(2,1)S(1)} %bitcast.6), channel_id=1, source_target_pairs={{0,1},{1,0},{2,3},{3,2},{4,5},{5,4},{6,7},{7,6},{8,9},{9,8},{10,11... | collective-permute-start | bytes 2359304 | tf_op jit(solution)/shard_map/ppermute | solution.py:479
  130.5 8.2 %collective-permute-start.10 = (bf16[128,512]{1,0:T(8,128)(2,1)S(1)}, bf16[128,512]{1,0:T(8,128)(2,1)S(1)}, u32[]{:S(2)}, u32[]{:S(2)}) collective-permute-start(bf16[128,512]{1,0:T(8,128)(2,1)S(1)} %get-tuple-element.100.refs_10_.refs_1_), channel_id=1, source_target_pairs={{0,8},{8,16},{16,24},{24,0},{1,9},{9,17},{17,25},{25,1},{2,10},{10... | collective-permute-start | bytes 393224 | tf_op jit(solution)/shard_map/ppermute | solution.py:508
  132.7 7.1 %collective-permute-start.9 = (bf16[128,512]{1,0:T(8,128)(2,1)S(1)}, bf16[128,512]{1,0:T(8,128)(2,1)S(1)}, u32[]{:S(2)}, u32[]{:S(2)}) collective-permute-start(bf16[128,512]{1,0:T(8,128)(2,1)S(1)} %get-tuple-element.99.refs_9_.refs_0_), channel_id=1, source_target_pairs={{0,8},{8,16},{16,24},{24,0},{1,9},{9,17},{17,25},{25,1},{2,10},{10... | collective-permute-start | bytes 393224 | tf_op jit(solution)/shard_map/ppermute | solution.py:508
  158.6 2.3 %collective-permute-start.11 = (bf16[4,384,256]{2,1,0:T(8,128)(2,1)S(1)}, bf16[4,384,256]{2,1,0:T(8,128)(2,1)S(1)}, u32[]{:S(2)}, u32[]{:S(2)}) collective-permute-start(bf16[4,384,256]{2,1,0:T(8,128)(2,1)S(1)} %bitcast.18), channel_id=1, source_target_pairs={{0,1},{1,0},{2,3},{3,2},{4,5},{5,4},{6,7},{7,6},{8,9},{9,8},{10,11... | collective-permute-start | bytes 2359304 | tf_op jit(solution)/shard_map/ppermute | solution.py:479
  161.7 1.2 collective-permute-start.12
  162.9 5.4 %collective-permute-start.13 = (f32[1,384]{1,0:T(1,128)S(1)}, f32[1,384]{1,0:T(1,128)S(1)}, u32[]{:S(2)}, u32[]{:S(2)}) collective-permute-start(f32[1,384]{1,0:T(1,128)S(1)} %add.3.refs_5_), channel_id=1, source_target_pairs={{0,2},{1,3},{2,4},{3,5},{4,6},{5,7},{6,0},{7,1},{8,10},{9,11},{10,... | collective-permute-start | bytes 4616 | tf_op jit(solution)/shard_map/ppermute | solution.py:501
  164.1 4.5 %collective-permute-start.14 = (f32[1,384]{1,0:T(1,128)S(1)}, f32[1,384]{1,0:T(1,128)S(1)}, u32[]{:S(2)}, u32[]{:S(2)}) collective-permute-start(f32[1,384]{1,0:T(1,128)S(1)} %add.3.refs_5_), channel_id=1, source_target_pairs={{0,4},{1,5},{2,6},{3,7},{4,0},{5,1},{6,2},{7,3},{8,12},{9,13},{10,... | collective-permute-start | bytes 4616 | tf_op jit(solution)/shard_map/ppermute | solution.py:501
  165.4 3.6 %collective-permute-start.15 = (f32[1,384]{1,0:T(1,128)S(1)}, f32[1,384]{1,0:T(1,128)S(1)}, u32[]{:S(2)}, u32[]{:S(2)}) collective-permute-start(f32[1,384]{1,0:T(1,128)S(1)} %add.3.refs_5_), channel_id=1, source_target_pairs={{0,6},{1,7},{2,0},{3,1},{4,2},{5,3},{6,4},{7,5},{8,14},{9,15},{10,... | collective-permute-start | bytes 4616 | tf_op jit(solution)/shard_map/ppermute | solution.py:501

commit v5 on v4

v5 whole, which is shorter than its diff:
```python
import functools

import jax
import jax.numpy as jnp
from jax import lax
from jax.experimental import pallas as pl
from jax.experimental.pallas import tpu as pltpu
from jax.sharding import PartitionSpec as P

D = 2048
HD = 64
BLOCK = 64
PAST_BLOCKS = 4
LAYERS = 3
PAST = 256
CLIP = 128
GROUP = 2 * BLOCK
WINDOW = PAST + GROUP
SKEW = 512
CORES = 2
DOC_ROWS = 16
HALF = GROUP // CORES
FAR = -1e30

norm_eps = 1e-06
rows_by_rows = (((1,), (1,)), ((), ()))
vmem = pl.BlockSpec(memory_space=pltpu.VMEM)
hbm = pl.BlockSpec(memory_space=pltpu.HBM)
params = pltpu.CompilerParams(vmem_limit_bytes=16 * 1024 * 1024)


def turn(vector, axis):
    size = max(vector.shape)
    diagonal = lax.broadcasted_iota(jnp.int32, (size, size), 0) == lax.broadcasted_iota(
        jnp.int32, (size, size), 1
    )
    spread = jnp.where(diagonal, jnp.broadcast_to(vector, (size, size)), jnp.zeros_like(vector))
    return jnp.sum(spread, axis=axis, keepdims=True)


def setup_body(bias_hbm, docs_hbm, *refs):
    sources, refs = refs[:6], refs[6:]
    stage_ref, pre_ref, post_ref, docs_out, mask_ref, *bands = refs[:-3]
    bias_ref, docs_ref, sems = refs[-3:]
    bias_copy = pltpu.make_async_copy(bias_hbm, bias_ref, sems.at[6])
    bias_copy.start()
    docs_copy = pltpu.make_async_copy(docs_hbm, docs_ref, sems.at[7])
    docs_copy.start()
    targets = [stage_ref.at[at] for at in range(4)] + [pre_ref, post_ref]
    copies = [
        pltpu.make_async_copy(source.at[0] if at < 4 else source, target, sems.at[at])
        for at, (source, target) in enumerate(zip(sources, targets))
    ]
    for copy in copies:
        copy.start()
    docs_copy.wait()
    docs = docs_ref[...].reshape(1, docs_ref.shape[0])
    docs_out[...] = docs
    for index in range(mask_ref.shape[0]):
        start = PAST + index * GROUP
        mask_ref[index] = doc_mask(
            docs[:, start : start + GROUP], docs[:, start - PAST : start + GROUP]
        )
    layers, heads, entries = bias_ref.shape
    row_block = lax.broadcasted_iota(jnp.int32, (GROUP, WINDOW), 0) // BLOCK
    col_block = lax.broadcasted_iota(jnp.int32, (GROUP, WINDOW), 1) // BLOCK
    allowed = (col_block >= row_block) & (col_block <= row_block + PAST_BLOCKS)
    shift = lax.broadcasted_iota(jnp.int32, (entries, SKEW), 1)
    entry = jnp.where(shift < WINDOW, jnp.minimum(PAST - shift, CLIP) + CLIP, 2 * CLIP)
    pick = (lax.broadcasted_iota(jnp.int32, (entries, SKEW), 0) == entry).astype(jnp.float32)
    bias_copy.wait()
    for layer in range(layers):
        base = lax.dot_general(
            bias_ref[layer],
            pick,
            (((1,), (0,)), ((), ())),
            precision=lax.Precision.HIGHEST,
            preferred_element_type=jnp.float32,
        )
        for head in range(heads):
            row = jnp.broadcast_to(base[head : head + 1, :], (GROUP, SKEW))
            skewed = pltpu.roll(row, 0, 1, stride=1, stride_axis=0)
            bands[layer][head] = jnp.where(allowed, skewed[:, :WINDOW], FAR)
    for copy in copies:
        copy.wait()


def doc_mask(own, seen):
    return jnp.where(turn(own, 1) == seen, 0.0, FAR)


def setup(position_bias, docs, weights, pre_gain, post_gain):
    layers, heads, _ = position_bias.shape
    rows = docs.shape[0]
    groups = (rows - PAST) // GROUP
    own = weights[0].shape[1]
    shapes = [
        jax.ShapeDtypeStruct((4, own, D), jnp.bfloat16),
        jax.ShapeDtypeStruct(pre_gain.shape, jnp.float32),
        jax.ShapeDtypeStruct(post_gain.shape, jnp.float32),
        jax.ShapeDtypeStruct((1, rows), jnp.int32),
        jax.ShapeDtypeStruct((groups, GROUP, WINDOW), jnp.float32),
        *[jax.ShapeDtypeStruct((heads, GROUP, WINDOW), jnp.float32) for _ in range(layers)],
    ]
    far = [
        pltpu.with_memory_space_constraint(a, pltpu.HBM)
        for a in (position_bias, docs, *weights, pre_gain, post_gain)
    ]
    return pl.pallas_call(
        setup_body,
        out_shape=tuple(shapes),
        in_specs=[hbm] * 8,
        out_specs=(vmem,) * len(shapes),
        scratch_shapes=[
            pltpu.VMEM(position_bias.shape, jnp.float32),
            pltpu.VMEM(docs.shape, jnp.int32),
            pltpu.SemaphoreType.DMA((8,)),
        ],
        compiler_params=params,
        name="setup",
    )(*far)


def ring_order(count):
    return [0, *range(1, count, 2), *reversed(range(2, count, 2))]


def block_columns(blocks):
    if len(blocks) == 1:
        return [(blocks[0], 0, 0)]
    core = lax.rem(lax.axis_index("tp"), CORES)
    width = blocks[0].shape[2]
    return [
        (ref, slot, pl.multiple_of((CORES * z + (core if side == 0 else 1 - core)) * width, 128))
        for side, ref in enumerate(blocks)
        for slot, z in enumerate(ring_order(ref.shape[0]))
    ]


def lane_sum(square):
    total = square[:, :128]
    for at in range(128, square.shape[1], 128):
        total = total + square[:, at : at + 128]
    return total


def core_at():
    return lax.rem(lax.axis_index("tp"), CORES)


def half_rows(mine):
    at = core_at() if mine else 1 - core_at()
    return pl.ds(pl.multiple_of(at * HALF, HALF), HALF)


def update_half(layer, placed, source, resid_ref, post_ref, pre_ref, resid_out, normed_out):
    if layer:
        total = jnp.zeros((HALF, 128), jnp.float32)
        for ref, slot, _ in placed:
            part = ref[slot, source, :].astype(jnp.float32)
            total = total + lane_sum(part * part)
        inv_out = lax.rsqrt(jnp.sum(total, axis=1, keepdims=True) / D + norm_eps)
    total = jnp.zeros((HALF, 128), jnp.float32)
    for ref, slot, col in placed:
        cols = pl.ds(col, ref.shape[2])
        new = ref[slot, source, :]
        if layer:
            part = new.astype(jnp.float32)
            old = resid_ref[:, cols].astype(jnp.float32)
            new = (old + part * inv_out * post_ref[layer - 1 : layer, cols]).astype(jnp.bfloat16)
        resid_out[:, cols] = new
        wide = new.astype(jnp.float32)
        total = total + lane_sum(wide * wide)
    inv_in = lax.rsqrt(jnp.sum(total, axis=1, keepdims=True) / D + norm_eps)
    for ref, _, col in placed:
        cols = pl.ds(col, ref.shape[2])
        wide = resid_out[:, cols].astype(jnp.float32)
        normed_out[:, cols] = (wide * inv_in * pre_ref[layer : layer + 1, cols]).astype(jnp.bfloat16)


def norm_group(blocks, offset, pre_ref, resid_half, rows_ref, normed_ref):
    placed = block_columns(blocks)
    for half in range(CORES):
        at = pl.ds(half * HALF, HALF)
        update_half(
            0,
            placed,
            pl.ds(offset + half * HALF, HALF),
            None,
            None,
            pre_ref,
            rows_ref.at[at],
            normed_ref.at[at],
        )
    resid_half[...] = rows_ref[half_rows(True), :]


def chip_columns(ref):
    width = ref.shape[2]
    return [(ref, slot, z * width) for slot, z in enumerate(ring_order(ref.shape[0]))]


def update_body(layer, groups, blocks_ref, post_ref, pre_ref, *refs):
    count = len(groups)
    olds, news, normed = [refs[at * count : (at + 1) * count] for at in range(3)]
    placed = chip_columns(blocks_ref)
    for index, group in enumerate(groups):
        update_half(
            layer,
            placed,
            pl.ds(group * HALF, HALF),
            olds[index],
            post_ref,
            pre_ref,
            news[index],
            normed[index],
        )


def update(layer, groups, blocks, post, pre, olds):
    shape = jax.ShapeDtypeStruct((HALF, D), jnp.bfloat16)
    operands = (blocks, post, pre, *olds)
    made = pl.pallas_call(
        functools.partial(update_body, layer, groups),
        out_shape=(shape,) * (2 * len(groups)),
        in_specs=[vmem] * len(operands),
        out_specs=(vmem,) * (2 * len(groups)),
        compiler_params=params,
        name="update",
    )(*operands)
    return made[: len(groups)], made[len(groups) :]


def product(rows_ref, weight):
    return lax.dot_general(
        rows_ref[...], weight, rows_by_rows, preferred_element_type=jnp.float32
    ).astype(jnp.bfloat16)


def weight_of(layer, weights, at):
    return weights[0][at] if layer == 0 else weights[at][layer]


def first_piece_body(offset, count, *refs):
    blocks, (docs_ref, pre_ref, weights_ref) = refs[:count], refs[count : count + 3]
    resid_half, normed_ref, kv_ref, rows_ref = refs[count + 3 :]
    norm_group(blocks, offset, pre_ref, resid_half, rows_ref, normed_ref)
    own = kv_ref.shape[1] // 2
    for at in range(2):
        kv_ref[:GROUP, at * own : (at + 1) * own] = product(normed_ref, weights_ref[at])
    docs = docs_ref[:, offset : offset + GROUP].astype(jnp.float32)
    kv_ref[GROUP:, :GROUP] = jnp.broadcast_to(docs, (DOC_ROWS, GROUP)).astype(jnp.bfloat16)


def first_piece(blocks, offset, docs, pre, stage):
    own = stage.shape[1]
    bf = jnp.bfloat16
    operands = (*blocks, docs, pre, stage)
    return pl.pallas_call(
        functools.partial(first_piece_body, offset, len(blocks)),
        out_shape=(
            jax.ShapeDtypeStruct((HALF, D), bf),
            jax.ShapeDtypeStruct((GROUP, D), bf),
            jax.ShapeDtypeStruct((GROUP + DOC_ROWS, 2 * own), bf),
        ),
        in_specs=[vmem] * len(operands),
        out_specs=(vmem,) * 3,
        scratch_shapes=[pltpu.VMEM((GROUP, D), bf)],
        compiler_params=params,
        name="first_piece",
    )(*operands)


def piece_body(layer, mine_ref, other_ref, key_ref, value_ref, kv_ref, rows_ref):
    rows_ref[half_rows(True), :] = mine_ref[...]
    rows_ref[half_rows(False), :] = other_ref[...]
    own = kv_ref.shape[1] // 2
    kv_ref[:, :own] = product(rows_ref, key_ref[layer])
    kv_ref[:, own:] = product(rows_ref, value_ref[layer])


def project_piece(layer, mine, other, key_weight, value_weight):
    own = key_weight.shape[1]
    return pl.pallas_call(
        functools.partial(piece_body, layer),
        out_shape=jax.ShapeDtypeStruct((GROUP, 2 * own), jnp.bfloat16),
        in_specs=[vmem] * 4,
        out_specs=vmem,
        scratch_shapes=[pltpu.VMEM((GROUP, D), jnp.bfloat16)],
        compiler_params=params,
        name="project_piece",
    )(mine, other, key_weight, value_weight)


def attend_group(query, gate, ext_ref, seen, band_ref, mask, own):
    span = min(own, 128)
    lane = lax.broadcasted_iota(jnp.int32, (GROUP, span), 1) // HD
    results = []
    for start in range(0, own, span):
        cols = slice(start, start + span)
        keys = ext_ref[seen, cols]
        values = ext_ref[seen, own + start : own + start + span]
        result = None
        for sub in range(span // HD):
            picked = jnp.where(lane == sub, query[:, cols], jnp.zeros((), query.dtype))
            scores = lax.dot_general(
                picked, keys, rows_by_rows, preferred_element_type=jnp.float32
            )
            scores = scores + band_ref[start // HD + sub] + mask
            lifted = jnp.exp(scores - jnp.max(scores, axis=1, keepdims=True))
            total = jnp.sum(lifted, axis=1, keepdims=True)
            part = jnp.dot(lifted.astype(jnp.bfloat16), values, preferred_element_type=jnp.float32)
            part = part / total
            result = part if result is None else jnp.where(lane == sub, part, result)
        wide = gate[:, cols].astype(jnp.float32)
        results.append((result * (wide / (1.0 + jnp.exp(-wide)))).astype(jnp.bfloat16))
    return results


def store_group(mixed_ref, at, results):
    start = 0
    for result in results:
        mixed_ref[at, start : start + result.shape[1]] = result
        start = start + result.shape[1]


def local_body(layer, count, *refs):
    pieces = PAST // GROUP
    if layer == 0:
        blocks, pre_ref, refs = refs[:count], refs[count], refs[count + 1 :]
        piece_normed, refs = refs[:pieces], refs[pieces:]
    else:
        mine, other, refs = refs[:count], refs[count : 2 * count], refs[2 * count :]
    piece_kv, refs = refs[:pieces], refs[pieces:]
    band_ref, mask_ref, refs = refs[0], refs[1], refs[2:]
    if layer == 0:
        weights, refs = refs[:1], refs[1:]
        resid_half, refs = refs[0], refs[1:]
    else:
        weights, refs = refs[:4], refs[4:]
    head_ref, query_out, gate_out, mixed_ref, normed_ref, ext_ref = refs[:6]
    head_rows = head_ref.shape[0]
    head_at = pl.ds(0, head_rows)
    for index in range(pieces):
        at = pl.ds(head_rows + index * GROUP, GROUP)
        ext_ref[at] = piece_kv[index][:GROUP]
        if layer == 0:
            normed_ref[at] = piece_normed[index][...]
    if layer == 0:
        norm_group(blocks, 0, pre_ref, resid_half, refs[6], normed_ref.at[head_at])
    else:
        for group in range(count):
            rows_ref = normed_ref.at[pl.ds(group * GROUP, GROUP)]
            rows_ref[half_rows(True), :] = mine[group][...]
            rows_ref[half_rows(False), :] = other[group][...]
    rest, own = query_out.shape
    local = []
    for at in range(4):
        weight = weight_of(layer, weights, at)
        if at < 2:
            head_ref[:, at * own : (at + 1) * own] = product(normed_ref.at[head_at], weight)
            continue
        result = product(normed_ref, weight)
        if at == 2:
            result = result * jnp.bfloat16(HD ** (-0.5))
        target = query_out if at == 2 else gate_out
        target[...] = result[:rest]
        local.append(result[rest:])
    ext_ref[head_at] = head_ref[...]
    for index in range(mask_ref.shape[0]):
        at = slice(index * GROUP, (index + 1) * GROUP)
        seen = slice(index * GROUP, index * GROUP + WINDOW)
        results = attend_group(
            local[0][at], local[1][at], ext_ref, seen, band_ref, mask_ref[index], own
        )
        store_group(mixed_ref, at, results)


def project_local(layer, rows, sources, pieces, band, mask, weights):
    own = weights[0].shape[1]
    head_rows = rows - PAST
    bf = jnp.bfloat16
    operands = [*sources, *pieces, band, mask, *weights]
    count = len(sources) // 2 if layer else len(sources) - 1 - len(pieces)
    shapes = [] if layer else [(HALF, D)]
    shapes = shapes + [
        (head_rows, 2 * own),
        (PAST, own),
        (PAST, own),
        (rows - PAST, own),
    ]
    scratch = [pltpu.VMEM((rows, D), bf), pltpu.VMEM((rows, 2 * own), bf)]
    if layer == 0:
        scratch.append(pltpu.VMEM((head_rows, D), bf))
    return pl.pallas_call(
        functools.partial(local_body, layer, count),
        out_shape=tuple(jax.ShapeDtypeStruct(shape, bf) for shape in shapes),
        in_specs=[vmem] * len(operands),
        out_specs=(vmem,) * len(shapes),
        scratch_shapes=scratch,
        compiler_params=params,
        name="project_local",
    )(*operands)


def attend_body(layer, group, done, *refs):
    halo_count = PAST // GROUP - group
    chunks, refs = refs[: WINDOW // GROUP], refs[WINDOW // GROUP :]
    query_ref, gate_ref, band_ref, docs_ref, refs = *refs[:4], refs[4:]
    known = halo_count if layer else halo_count - 1
    told_refs, refs = refs[:known], refs[known:]
    done_refs, refs = refs[:done], refs[done:]
    keep_ref = give_ref = None
    if group == 0:
        (keep_ref, give_ref), refs = refs[:2], refs[2:]
    else:
        mixed_ref, refs = refs[0], refs[1:]
    told = [ref[...] for ref in told_refs]
    if layer == 0:
        arrived = chunks[0][GROUP : GROUP + DOC_ROWS, :GROUP].astype(jnp.float32)[:1]
        arrived = jnp.where(lax.axis_index("sp") == 0, -1, arrived.astype(jnp.int32))
        refs[0][...] = arrived
        told = [arrived, *told]
        refs = refs[1:]
    ext_ref = refs[0]
    if group == 0:
        mixed_ref = refs[1]
    for index, chunk in enumerate(chunks):
        ext_ref[index * GROUP : (index + 1) * GROUP] = chunk[:GROUP]
    at = slice(group * GROUP, (group + 1) * GROUP)
    docs = docs_ref[...]
    mask = doc_mask(docs[:, at], jnp.concatenate([*told, docs[:, : at.stop]], axis=1))
    own = query_ref.shape[1]
    results = attend_group(
        query_ref[at], gate_ref[at], ext_ref, slice(None), band_ref, mask, own
    )
    store_group(mixed_ref, slice(None), results)
    if group == 0:
        for index, ref in enumerate((mixed_ref, *done_refs)):
            at = slice(index * HALF, (index + 1) * HALF)
            keep_ref[at] = ref[half_rows(True), :]
            give_ref[at] = ref[half_rows(False), :]


def attend(layer, group, chunks, query, gate, band, docs, told, done):
    own = query.shape[1]
    bf = jnp.bfloat16
    operands = (*chunks, query, gate, band, docs, *told, *done)
    shapes = [jax.ShapeDtypeStruct((GROUP, own), bf)]
    scratch = [pltpu.VMEM((WINDOW, 2 * own), bf)]
    if group == 0:
        shapes = [jax.ShapeDtypeStruct(((1 + len(done)) * HALF, own), bf)] * CORES
        scratch.append(pltpu.VMEM((GROUP, own), bf))
    if layer == 0:
        shapes.append(jax.ShapeDtypeStruct((1, GROUP), jnp.int32))
    return pl.pallas_call(
        functools.partial(attend_body, layer, group, len(done)),
        out_shape=tuple(shapes),
        in_specs=[vmem] * len(operands),
        out_specs=(vmem,) * len(shapes),
        scratch_shapes=scratch,
        compiler_params=params,
        name="attend",
    )(*operands)


def by_core(action):
    for core in range(CORES):
        pl.when(core_at() == core)(functools.partial(action, core))


def join_body(keep_ref, got_ref, out_ref):
    own = keep_ref.shape[1]

    def place(core):
        out_ref[:, core * own : (core + 1) * own] = keep_ref[...]
        out_ref[:, (1 - core) * own : (2 - core) * own] = got_ref[...]

    by_core(place)


def join(keep, got):
    rows, own = keep.shape
    return pl.pallas_call(
        join_body,
        out_shape=jax.ShapeDtypeStruct((rows, CORES * own), keep.dtype),
        in_specs=[vmem] * 2,
        out_specs=vmem,
        compiler_params=params,
        name="join",
    )(keep, got)


def out_body(layer, last, blocks_ref, mine_ref, other_ref, branch_ref, *rest):
    mixed_ref = rest[-1]
    width = blocks_ref.shape[2]
    own = width // CORES
    for ref, slot, col in chip_columns(blocks_ref):
        mixed_ref[:, col : col + width] = ref[slot]
    mine = product(mixed_ref, mine_ref[layer])
    other = product(mixed_ref, other_ref[layer])

    def place(core):
        branch_ref[:, core * own : (core + 1) * own] = mine
        branch_ref[:, (1 - core) * own : (2 - core) * own] = other

    by_core(place)
    if last:
        square_ref = rest[0]
        wide = mine.astype(jnp.float32)
        total = jnp.sum(wide * wide, axis=1, keepdims=True)
        wide = other.astype(jnp.float32)
        total = total + jnp.sum(wide * wide, axis=1, keepdims=True)
        for start in range(0, total.shape[0], HALF):
            at = slice(start, start + HALF)
            square_ref[:, at] = turn(total[at], 0)


def out_project(layer, blocks, mine, other, last):
    rows, width = blocks.shape[1:]
    shapes = [jax.ShapeDtypeStruct((rows, width), jnp.bfloat16)]
    if last:
        shapes.append(jax.ShapeDtypeStruct((1, rows), jnp.float32))
    return pl.pallas_call(
        functools.partial(out_body, layer, last),
        out_shape=tuple(shapes),
        in_specs=[vmem] * 3,
        out_specs=(vmem,) * len(shapes),
        scratch_shapes=[pltpu.VMEM((rows, D), jnp.bfloat16)],
        compiler_params=params,
        name="out_project",
    )(blocks, mine, other)


def finish_body(groups, *refs):
    resid_refs, (branch_ref, gain_ref), refs = refs[:groups], refs[groups : groups + 2], refs[groups + 2 :]
    keep_ref, give_ref = refs[-2:]
    total = refs[0][...]
    for ref in refs[1:-2]:
        total = total + ref[...]
    width = branch_ref.shape[1]
    own = width // CORES
    chip = lax.div(lax.axis_index("tp"), CORES)
    cols = pl.ds(pl.multiple_of(chip * width, 128), width)
    gain = gain_ref[gain_ref.shape[0] - 1 :, cols]
    for group, ref in enumerate(resid_refs):
        at = slice(group * HALF, (group + 1) * HALF)
        inv_out = lax.rsqrt(turn(total[:, at], 1) / D + norm_eps)
        old = ref[:, cols].astype(jnp.float32)
        branch = branch_ref[at].astype(jnp.float32)
        new = (old + branch * inv_out * gain).astype(jnp.bfloat16)

        def place(core):
            keep_ref[at] = new[:, core * own : (core + 1) * own]
            give_ref[at] = new[:, (1 - core) * own : (2 - core) * own]

        by_core(place)


def finish(resids, branch, gain, totals):
    rows, width = branch.shape
    operands = (*resids, branch, gain, *totals)
    return pl.pallas_call(
        functools.partial(finish_body, len(resids)),
        out_shape=(jax.ShapeDtypeStruct((rows, width // CORES), jnp.bfloat16),) * 2,
        in_specs=[vmem] * len(operands),
        out_specs=(vmem,) * 2,
        compiler_params=params,
        name="finish",
    )(*operands)


def merge_body(keep_ref, got_ref, out_ref):
    for group in range(out_ref.shape[0] // GROUP):
        at = slice(group * HALF, (group + 1) * HALF)
        rows_ref = out_ref.at[pl.ds(group * GROUP, GROUP)]
        rows_ref[half_rows(True), :] = keep_ref[at]
        rows_ref[half_rows(False), :] = got_ref[at]


def merge(keep, got):
    rows, own = keep.shape
    return pl.pallas_call(
        merge_body,
        out_shape=jax.ShapeDtypeStruct((CORES * rows, own), keep.dtype),
        in_specs=[vmem] * 2,
        out_specs=vmem,
        compiler_params=params,
        name="merge",
    )(keep, got)


def partner(x):
    size = lax.axis_size("tp")
    return lax.ppermute(x, "tp", [(i, i ^ 1) for i in range(size)])


def gather_chips(x):
    order = ring_order(lax.axis_size("tp") // CORES)
    lines = [[CORES * z + core for z in order] for core in range(CORES)]
    return lax.all_gather(x, "tp", axis=0, axis_index_groups=lines)


def gather_tokens(x):
    if x.shape[1] % 128:
        return lax.all_gather(x, "tp", axis=1, tiled=True)[None]
    return gather_chips(x)


def swapped(own):
    return (own, partner(own)) if own.shape[2] < D else (own,)


def total_over_chips(square):
    size = lax.axis_size("tp")
    if size > 8:
        lines = [list(range(core, size, CORES)) for core in range(CORES)]
        return (lax.psum(square, "tp", axis_index_groups=lines),)
    return (square,) + tuple(
        lax.ppermute(square, "tp", [(i, (i + hop) % size) for i in range(size)])
        for hop in range(CORES, size, CORES)
    )


def from_behind(block):
    size = lax.axis_size("sp")
    return lax.ppermute(block, "sp", [(i, (i + 1) % size) for i in range(size)])


def local(
    tokens,
    documents,
    pre_gain,
    query_weight,
    key_weight,
    value_weight,
    gate_weight,
    out_weight,
    position_bias,
    post_gain,
):
    rows = tokens.shape[0]
    groups = rows // GROUP
    first = (rows - PAST) // GROUP
    weights = (key_weight, value_weight, query_weight, gate_weight)
    other_out = partner(out_weight)
    gathered, documents = lax.optimization_barrier((gather_tokens(tokens), documents))
    blocks = swapped(gathered)
    stage, pre, post, docs, mask, *bands = setup(
        position_bias, documents, weights, pre_gain, post_gain
    )
    halves, normed, other, pieces, halos = [[None] * groups for _ in range(5)]
    behind = [None] * (PAST // GROUP)
    for layer in range(LAYERS):
        if layer:
            late = tuple(range(groups - 1))
            for batch in ((groups - 1,), late[::-1]):
                made = update(layer, batch, blocks, post, pre, [halves[at] for at in batch])
                for at, half, row in zip(batch, *made):
                    halves[at], normed[at], other[at] = half, row, partner(row)
        for group in reversed(range(first, groups)):
            if layer:
                pieces[group] = project_piece(layer, normed[group], other[group], *weights[:2])
            else:
                halves[group], normed[group], pieces[group] = first_piece(
                    blocks, group * GROUP, docs, pre, stage
                )
            halos[group] = from_behind(pieces[group])
        sources = (*normed, *other) if layer else (*blocks, pre, *normed[first:])
        *half, head, query, gate, local_mixed = project_local(
            layer, rows, sources, pieces[first:], bands[layer], mask, weights if layer else (stage,)
        )
        if half:
            halves[0] = half[0]
        done = [local_mixed]
        known = [*halos[first:], head, *pieces[first:]]
        for group in reversed(range(PAST // GROUP)):
            chunks = known[group : group + WINDOW // GROUP]
            told = behind[group if layer else group + 1 :]
            made = attend(
                layer, group, chunks, query, gate, bands[layer], docs, told, done if group == 0 else []
            )
            if layer == 0:
                *made, behind[group] = made
            if group:
                done = [made[0], *done]
        keep, give = made
        last = layer + 1 == LAYERS
        mixed = gather_chips(join(keep, partner(give)))
        result = out_project(layer, mixed, out_weight, other_out, last)
        if not last:
            blocks = gather_chips(result[0])
    branch, square = result
    keep, give = finish(halves, branch, post, total_over_chips(square))
    return merge(keep, partner(give))


def solution(mesh):
    placed = (
        P("sp", "tp"),
        P("sp"),
        P(),
        P(None, "tp", None),
        P(None, "tp", None),
        P(None, "tp", None),
        P(None, "tp", None),
        P(None, "tp", None),
        P(None, "tp", None),
        P(),
    )
    return jax.shard_map(
        local, mesh=mesh, in_specs=placed, out_specs=P("sp", "tp"), check_vma=False
    )
```

time: 170 us -> 162 us (0.953)
  waiting for transfers between devices: 18.7 us -> 12.2 us
    ppermute x7 -> x12, waiting for transfers between devices: 12.4 us -> 5.93 us  [partner(): return lax.ppermute(x, 'tp', [(i, i ^ 1) for i in range(size)])]
    ppermute x7 -> x12, starting transfers between devices: 0.22 us -> 2.19 us  [partner(): return lax.ppermute(x, 'tp', [(i, i ^ 1) for i in range(size)])]
    pallas_call x17 -> x28, Pallas kernels: 30.8 us -> 29.2 us  [the longest x3 8.72 us: project_local(): pl.pallas_call(functools.partial(local_body, layer, count), out_shape=tup...]
  transfers between devices with their start and end apart: 16 -> 21, of which waited for: 13 -> 14; matrix products, arithmetic and copies ran while one was open for 0% -> 0% of each run, Pallas kernels for 10% -> 14%
where the time goes in v5:
time: 162 us
  blocking collectives  104 us (64%)
  Pallas kernels  29.2 us (18%)
  starting transfers between devices  15.7 us (10%)
  waiting for transfers between devices  12.2 us (8%)
    all_gather x6, blocking collectives, gather_chips(): return lax.all_gather(x, 'tp', axis=0, axis_index_groups=lines)  104 us
    ppermute x6, starting transfers between devices, from_behind(): return lax.ppermute(block, 'sp', [(i, (i + 1) % size) for i in range(size)])  9.39 us
    pallas_call x3, Pallas kernels, project_local(): pl.pallas_call(functools.partial(local_body, layer, count), out_shape=tup...  8.72 us
    pallas_call x6, Pallas kernels, attend(): pl.pallas_call(functools.partial(attend_body, layer, group, len(done)), o...  7.18 us
    ppermute x12, waiting for transfers between devices, partner(): return lax.ppermute(x, 'tp', [(i, i ^ 1) for i in range(size)])  5.93 us
    ppermute x6, waiting for transfers between devices, from_behind(): return lax.ppermute(block, 'sp', [(i, (i + 1) % size) for i in range(size)])  4.49 us
    ppermute x3, starting transfers between devices, total_over_chips(): lax.ppermute(square, 'tp', [(i, (i + hop) % size) for i in range(size)])  4.15 us
    pallas_call x4, Pallas kernels, project_piece(): pl.pallas_call(functools.partial(piece_body, layer), out_shape=jax.ShapeD...  3.35 us
  transfers between devices with their start and end apart: 21, of which 14 were waited for; matrix products, arithmetic and copies ran while one was open for 0% of the time, Pallas kernels for 14%

profile of v5, /device:TPU:0, one launch (start us, length us, event | category | flops | bytes accessed | tf_op | source)
XLA Modules:
  0.0 162.0 jit_solution(9981107648392870648)
XLA Ops:
  0.0 0.5 collective-permute-start.4
  0.5 19.7 %all-gather = bf16[1536,256]{1,0:T(8,128)(2,1)S(1)} all-gather(bf16[384,256]{1,0:T(8,128)(2,1)} %param.10), channel_id=2, replica_groups={{0,2,6,4},{1,3,7,5},{8,10,14,12},{9,11,15,13},{16,18,22,20},{17,19,23,2..., dimensions={0}, use_global_device_ids=true | all-gather | bytes 983040 | tf_op jit(solution)/shard_map/all_gather | solution.py:601
  20.2 2.3 %setup.1 = (bf16[4,256,2048]{2,1,0:T(8,128)(2,1)S(1)}, f32[3,2048]{1,0:T(4,128)S(1)}, f32[3,2048]{1,0:T(4,128)S(1)}, s32[1,384]{1,0:T(1,128)S(1)}, f32[1,128,384...) custom-call(f32[3,4,257]{2,1,0:T(4,128)} %bias_hbm.1, ...), custom_call_target="tpu_custom_call" | custom-call | tf_op jit(solution)/shard_map/setup/pallas_call | solution.py:109
  22.5 1.0 first_piece.3
  23.5 1.5 collective-permute-start.2
  25.1 1.0 first_piece.2
  26.1 1.5 collective-permute-start.1
  27.7 3.0 %project_local.3 = (bf16[64,2048]{1,0:T(8,128)(2,1)S(1)}, bf16[128,512]{1,0:T(8,128)(2,1)S(1)}, bf16[256,256]{1,0:T(8,128)(2,1)S(1)}, bf16[256,256]{1,0:T(8,128)(2,1)S(1)}, bf16[128,256]{1,0:T(8,128)(2,1)S(1)}) custom-call(bf16[4,384,256]{2,1,0:T(8,128)(2,1)S(1)} %bitcast.9, bf16[4,384,256]{2,1,0:T(8,128)(2,1)S(1)} %collective-permute-done.refs_1_, ...), custom_call_target="tpu_custom_call" | custom-call | tf_op jit(solution)/shard_map/project_local/pallas_call | solution.py:395
  30.7 0.5 collective-permute-done.2.refs_0_.refs_1_
  31.2 1.2 attend.6
  32.4 1.5 collective-permute-done.1.refs_0_
  33.9 1.2 attend.7
  35.1 0.1 collective-permute-start.3
  35.2 1.3 collective-permute-done.3.got_ref
  36.5 17.3 %all-gather.1 = bf16[768,512]{1,0:T(8,128)(2,1)S(1)} all-gather(bf16[192,512]{1,0:T(8,128)(2,1)S(1)} %join.3), channel_id=3, replica_groups={{0,2,6,4},{1,3,7,5},{8,10,14,12},{9,11,15,13},{16,18,22,20},{17,19,23,2..., dimensions={0}, use_global_device_ids=true | all-gather | bytes 983040 | tf_op jit(solution)/shard_map/all_gather | solution.py:601
  53.9 0.9 out_project.3
  54.7 17.1 %all-gather.2 = bf16[768,512]{1,0:T(8,128)(2,1)S(1)} all-gather(bf16[192,512]{1,0:T(8,128)(2,1)S(1)} %out_project.3), channel_id=4, replica_groups={{0,2,6,4},{1,3,7,5},{8,10,14,12},{9,11,15,13},{16,18,22,20},{17,19,23,2..., dimensions={0}, use_global_device_ids=true | all-gather | bytes 983040 | tf_op jit(solution)/shard_map/all_gather | solution.py:601
  71.8 0.4 update.5
  72.2 0.1 collective-permute-start.7
  72.3 0.5 update.4
  72.8 0.6 collective-permute-start.5
  73.3 0.1 collective-permute-start.9
  73.4 0.4 collective-permute-done.7.other_ref.refs_5_
  73.8 0.8 project_piece.5.refs_7_
  74.7 0.6 collective-permute-start.8
  75.3 0.8 project_piece.4.refs_6_.refs_2_
  76.2 2.6 %collective-permute-start.6 = (bf16[128,512]{1,0:T(8,128)(2,1)S(1)}, bf16[128,512]{1,0:T(8,128)(2,1)S(1)}, u32[]{:S(2)}, u32[]{:S(2)}) collective-permute-start(bf16[128,512]{1,0:T(8,128)(2,1)S(1)} %project_piece.4.refs_6_.refs_2_), channel_id=1, source_target_pairs={{0,8},{8,16},{16,24},{24,0},{1,9},{9,17},{17,25},{25,1},{2,10},{10... | collective-permute-start | bytes 393224 | tf_op jit(solution)/shard_map/ppermute | solution.py:627
  78.8 2.8 %project_local.4 = (bf16[128,512]{1,0:T(8,128)(2,1)S(1)}, bf16[256,256]{1,0:T(8,128)(2,1)S(1)}, bf16[256,256]{1,0:T(8,128)(2,1)S(1)}, bf16[128,256]{1,0:T(8,128)(2,1)S(1)}) custom-call(bf16[64,2048]{1,0:T(8,128)(2,1)S(1)} %get-tuple-element.84.refs_0_, bf16[64,2048]{1,0:T(8,128)(2,1)S(1)} %get-tuple-element.81.mine_ref.refs_1_, ...), custom_call_target="tpu_custom_call" | custom-call | tf_op jit(solution)/shard_map/project_local/pallas_call | solution.py:395
  81.7 0.3 collective-permute-done.8.refs_0_.refs_1_
  82.0 1.2 attend.8.refs_9_
  83.2 0.8 collective-permute-done.6.refs_0_
  84.0 1.2 attend.9
  85.2 0.1 collective-permute-start.10
  85.3 1.3 collective-permute-done.10.got_ref
  86.6 16.8 %all-gather.3 = bf16[768,512]{1,0:T(8,128)(2,1)S(1)} all-gather(bf16[192,512]{1,0:T(8,128)(2,1)S(1)} %join.4), channel_id=5, replica_groups={{0,2,6,4},{1,3,7,5},{8,10,14,12},{9,11,15,13},{16,18,22,20},{17,19,23,2..., dimensions={0}, use_global_device_ids=true | all-gather | bytes 983040 | tf_op jit(solution)/shard_map/all_gather | solution.py:601
  103.4 0.9 out_project.4
  104.3 16.2 %all-gather.4 = bf16[768,512]{1,0:T(8,128)(2,1)S(1)} all-gather(bf16[192,512]{1,0:T(8,128)(2,1)S(1)} %out_project.4), channel_id=6, replica_groups={{0,2,6,4},{1,3,7,5},{8,10,14,12},{9,11,15,13},{16,18,22,20},{17,19,23,2..., dimensions={0}, use_global_device_ids=true | all-gather | bytes 983040 | tf_op jit(solution)/shard_map/all_gather | solution.py:601
  120.5 0.4 update.7
  120.8 0.1 collective-permute-start.13
  120.9 0.5 update.6
  121.4 0.6 collective-permute-start.11
  122.0 0.1 collective-permute-start.15
  122.1 0.4 collective-permute-done.13.other_ref.refs_5_
  122.4 0.8 project_piece.7.refs_7_
  123.3 0.1 collective-permute-start.14
  123.4 0.8 project_piece.6.refs_6_.refs_2_
  124.2 2.9 %collective-permute-start.12 = (bf16[128,512]{1,0:T(8,128)(2,1)S(1)}, bf16[128,512]{1,0:T(8,128)(2,1)S(1)}, u32[]{:S(2)}, u32[]{:S(2)}) collective-permute-start(bf16[128,512]{1,0:T(8,128)(2,1)S(1)} %project_piece.6.refs_6_.refs_2_), channel_id=1, source_target_pairs={{0,8},{8,16},{16,24},{24,0},{1,9},{9,17},{17,25},{25,1},{2,10},{10... | collective-permute-start | bytes 393224 | tf_op jit(solution)/shard_map/ppermute | solution.py:627
  127.2 2.8 %project_local.5 = (bf16[128,512]{1,0:T(8,128)(2,1)S(1)}, bf16[256,256]{1,0:T(8,128)(2,1)S(1)}, bf16[256,256]{1,0:T(8,128)(2,1)S(1)}, bf16[128,256]{1,0:T(8,128)(2,1)S(1)}) custom-call(bf16[64,2048]{1,0:T(8,128)(2,1)S(1)} %get-tuple-element.101.refs_0_, bf16[64,2048]{1,0:T(8,128)(2,1)S(1)} %get-tuple-element.99.mine_ref.refs_1_, ...), custom_call_target="tpu_custom_call" | custom-call | tf_op jit(solution)/shard_map/project_local/pallas_call | solution.py:395
  130.0 0.6 collective-permute-done.14.refs_0_.refs_1_
  130.6 1.2 attend.10.refs_9_
  131.8 0.8 collective-permute-done.12.refs_0_
  132.6 1.2 attend.11
  133.9 1.3 collective-permute-done.16.got_ref
  135.2 17.3 %all-gather.5 = bf16[768,512]{1,0:T(8,128)(2,1)S(1)} all-gather(bf16[192,512]{1,0:T(8,128)(2,1)S(1)} %join.5), channel_id=7, replica_groups={{0,2,6,4},{1,3,7,5},{8,10,14,12},{9,11,15,13},{16,18,22,20},{17,19,23,2..., dimensions={0}, use_global_device_ids=true | all-gather | bytes 983040 | tf_op jit(solution)/shard_map/all_gather | solution.py:601
  152.5 1.0 out_project.5
  153.5 1.0 collective-permute-start.17
  154.5 1.4 collective-permute-start.18
  155.9 1.8 %collective-permute-start.19 = (f32[1,192]{1,0:T(1,128)S(1)}, f32[1,192]{1,0:T(1,128)S(1)}, u32[]{:S(2)}, u32[]{:S(2)}) collective-permute-start(f32[1,192]{1,0:T(1,128)S(1)} %get-tuple-element.110.refs_5_), channel_id=1, source_target_pairs={{0,6},{1,7},{2,0},{3,1},{4,2},{5,3},{6,4},{7,5},{8,14},{9,15},{10,... | collective-permute-start | bytes 2312 | tf_op jit(solution)/shard_map/ppermute | solution.py:620
  157.7 1.2 collective-permute-done.17.refs_6_
  158.9 0.5 collective-permute-done.19.refs_8_
  159.5 0.4 finish.1
  159.9 0.1 collective-permute-start.20
  160.0 1.3 collective-permute-done.20.got_ref
  161.3 0.7 merge.1
  (22 shorter events, 0.2 us)
Async XLA Ops:
  0.0 53.9 %collective-permute-start.4 = (bf16[3,256,2048]{2,1,0:T(8,128)(2,1)}, bf16[3,256,2048]{2,1,0:T(8,128)(2,1)S(1)}, u32[]{:S(2)}, u32[]{:S(2)}) collective-permute-start(bf16[3,256,2048]{2,1,0:T(8,128)(2,1)} %mine_ref.5), channel_id=1, source_target_pairs={{0,1},{1,0},{2,3},{3,2},{4,5},{5,4},{6,7},{7,6},{8,9},{9,8},{10,11... | collective-permute-start | bytes 9437192 | tf_op jit(solution)/shard_map/ppermute | solution.py:595
  20.2 2.3 %collective-permute-start = (bf16[4,384,256]{2,1,0:T(8,128)(2,1)S(1)}, bf16[4,384,256]{2,1,0:T(8,128)(2,1)S(1)}, u32[]{:S(2)}, u32[]{:S(2)}) collective-permute-start(bf16[4,384,256]{2,1,0:T(8,128)(2,1)S(1)} %bitcast.6), channel_id=1, source_target_pairs={{0,1},{1,0},{2,3},{3,2},{4,5},{5,4},{6,7},{7,6},{8,9},{9,8},{10,11... | collective-permute-start | bytes 2359304 | tf_op jit(solution)/shard_map/ppermute | solution.py:595
  23.5 7.7 %collective-permute-start.2 = (bf16[144,512]{1,0:T(8,128)(2,1)S(1)}, bf16[144,512]{1,0:T(8,128)(2,1)S(1)}, u32[]{:S(2)}, u32[]{:S(2)}) collective-permute-start(bf16[144,512]{1,0:T(8,128)(2,1)S(1)} %get-tuple-element.65.refs_6_), channel_id=1, source_target_pairs={{0,8},{8,16},{16,24},{24,0},{1,9},{9,17},{17,25},{25,1},{2,10},{10... | collective-permute-start | bytes 442376 | tf_op jit(solution)/shard_map/ppermute | solution.py:627
  26.1 7.8 %collective-permute-start.1 = (bf16[144,512]{1,0:T(8,128)(2,1)S(1)}, bf16[144,512]{1,0:T(8,128)(2,1)S(1)}, u32[]{:S(2)}, u32[]{:S(2)}) collective-permute-start(bf16[144,512]{1,0:T(8,128)(2,1)S(1)} %get-tuple-element.64.refs_5_.refs_2_), channel_id=1, source_target_pairs={{0,8},{8,16},{16,24},{24,0},{1,9},{9,17},{17,25},{25,1},{2,10},{10... | collective-permute-start | bytes 442376 | tf_op jit(solution)/shard_map/ppermute | solution.py:627
  30.7 23.1 %copy-start.2 = (bf16[3,256,2048]{2,1,0:T(8,128)(2,1)S(1)}, bf16[3,256,2048]{2,1,0:T(8,128)(2,1)}, u32[]{:S(2)}) copy-start(bf16[3,256,2048]{2,1,0:T(8,128)(2,1)} %mine_ref.5) | copy-start | bytes 9437188
  35.1 1.4 collective-permute-start.3
  53.9 20.0 %copy-start.1 = (bf16[3,256,2048]{2,1,0:T(8,128)(2,1)S(1)}, bf16[3,256,2048]{2,1,0:T(8,128)(2,1)}, u32[]{:S(2)}) copy-start(bf16[3,256,2048]{2,1,0:T(8,128)(2,1)} %refs_11_.3) | copy-start | bytes 9437188
  54.7 19.1 %copy-start = (bf16[3,256,2048]{2,1,0:T(8,128)(2,1)S(1)}, bf16[3,256,2048]{2,1,0:T(8,128)(2,1)}, u32[]{:S(2)}) copy-start(bf16[3,256,2048]{2,1,0:T(8,128)(2,1)} %refs_10_.3) | copy-start | bytes 9437188
  72.2 1.6 collective-permute-start.7
  72.8 2.5 %collective-permute-start.5 = (bf16[64,2048]{1,0:T(8,128)(2,1)S(1)}, bf16[64,2048]{1,0:T(8,128)(2,1)S(1)}, u32[]{:S(2)}, u32[]{:S(2)}) collective-permute-start(bf16[64,2048]{1,0:T(8,128)(2,1)S(1)} %get-tuple-element.81.mine_ref.refs_1_), channel_id=1, source_target_pairs={{0,1},{1,0},{2,3},{3,2},{4,5},{5,4},{6,7},{7,6},{8,9},{9,8},{10,11... | collective-permute-start | bytes 786440 | tf_op jit(solution)/shard_map/ppermute | solution.py:595
  73.3 5.5 %collective-permute-start.9 = (bf16[64,2048]{1,0:T(8,128)(2,1)S(1)}, bf16[64,2048]{1,0:T(8,128)(2,1)S(1)}, u32[]{:S(2)}, u32[]{:S(2)}) collective-permute-start(bf16[64,2048]{1,0:T(8,128)(2,1)S(1)} %get-tuple-element.84.refs_0_), channel_id=1, source_target_pairs={{0,1},{1,0},{2,3},{3,2},{4,5},{5,4},{6,7},{7,6},{8,9},{9,8},{10,11... | collective-permute-start | bytes 786440 | tf_op jit(solution)/shard_map/ppermute | solution.py:595
  74.7 4.1 %copy-start.3 = (bf16[3,256,2048]{2,1,0:T(8,128)(2,1)S(1)}, bf16[3,256,2048]{2,1,0:T(8,128)(2,1)}, u32[]{:S(2)}) copy-start(bf16[3,256,2048]{2,1,0:T(8,128)(2,1)} %refs_12_.3) | copy-start | bytes 9437188
  74.7 4.1 %copy-start.4 = (bf16[3,256,2048]{2,1,0:T(8,128)(2,1)S(1)}, bf16[3,256,2048]{2,1,0:T(8,128)(2,1)}, u32[]{:S(2)}) copy-start(bf16[3,256,2048]{2,1,0:T(8,128)(2,1)} %refs_13_.3) | copy-start | bytes 9437188
  74.7 7.3 %collective-permute-start.8 = (bf16[128,512]{1,0:T(8,128)(2,1)S(1)}, bf16[128,512]{1,0:T(8,128)(2,1)S(1)}, u32[]{:S(2)}, u32[]{:S(2)}) collective-permute-start(bf16[128,512]{1,0:T(8,128)(2,1)S(1)} %project_piece.5.refs_7_), channel_id=1, source_target_pairs={{0,8},{8,16},{16,24},{24,0},{1,9},{9,17},{17,25},{25,1},{2,10},{10... | collective-permute-start | bytes 393224 | tf_op jit(solution)/shard_map/ppermute | solution.py:627
  76.2 7.8 %collective-permute-start.6 = (bf16[128,512]{1,0:T(8,128)(2,1)S(1)}, bf16[128,512]{1,0:T(8,128)(2,1)S(1)}, u32[]{:S(2)}, u32[]{:S(2)}) collective-permute-start(bf16[128,512]{1,0:T(8,128)(2,1)S(1)} %project_piece.4.refs_6_.refs_2_), channel_id=1, source_target_pairs={{0,8},{8,16},{16,24},{24,0},{1,9},{9,17},{17,25},{25,1},{2,10},{10... | collective-permute-start | bytes 393224 | tf_op jit(solution)/shard_map/ppermute | solution.py:627
  85.2 1.4 collective-permute-start.10
  120.8 1.6 collective-permute-start.13
  121.4 2.0 %collective-permute-start.11 = (bf16[64,2048]{1,0:T(8,128)(2,1)S(1)}, bf16[64,2048]{1,0:T(8,128)(2,1)S(1)}, u32[]{:S(2)}, u32[]{:S(2)}) collective-permute-start(bf16[64,2048]{1,0:T(8,128)(2,1)S(1)} %get-tuple-element.99.mine_ref.refs_1_), channel_id=1, source_target_pairs={{0,1},{1,0},{2,3},{3,2},{4,5},{5,4},{6,7},{7,6},{8,9},{9,8},{10,11... | collective-permute-start | bytes 786440 | tf_op jit(solution)/shard_map/ppermute | solution.py:595
  122.0 5.2 %collective-permute-start.15 = (bf16[64,2048]{1,0:T(8,128)(2,1)S(1)}, bf16[64,2048]{1,0:T(8,128)(2,1)S(1)}, u32[]{:S(2)}, u32[]{:S(2)}) collective-permute-start(bf16[64,2048]{1,0:T(8,128)(2,1)S(1)} %get-tuple-element.101.refs_0_), channel_id=1, source_target_pairs={{0,1},{1,0},{2,3},{3,2},{4,5},{5,4},{6,7},{7,6},{8,9},{9,8},{10,11... | collective-permute-start | bytes 786440 | tf_op jit(solution)/shard_map/ppermute | solution.py:595
  123.3 7.3 %collective-permute-start.14 = (bf16[128,512]{1,0:T(8,128)(2,1)S(1)}, bf16[128,512]{1,0:T(8,128)(2,1)S(1)}, u32[]{:S(2)}, u32[]{:S(2)}) collective-permute-start(bf16[128,512]{1,0:T(8,128)(2,1)S(1)} %project_piece.7.refs_7_), channel_id=1, source_target_pairs={{0,8},{8,16},{16,24},{24,0},{1,9},{9,17},{17,25},{25,1},{2,10},{10... | collective-permute-start | bytes 393224 | tf_op jit(solution)/shard_map/ppermute | solution.py:627
  124.2 8.3 %collective-permute-start.12 = (bf16[128,512]{1,0:T(8,128)(2,1)S(1)}, bf16[128,512]{1,0:T(8,128)(2,1)S(1)}, u32[]{:S(2)}, u32[]{:S(2)}) collective-permute-start(bf16[128,512]{1,0:T(8,128)(2,1)S(1)} %project_piece.6.refs_6_.refs_2_), channel_id=1, source_target_pairs={{0,8},{8,16},{16,24},{24,0},{1,9},{9,17},{17,25},{25,1},{2,10},{10... | collective-permute-start | bytes 393224 | tf_op jit(solution)/shard_map/ppermute | solution.py:627
  133.8 1.4 collective-permute-start.16
  153.5 5.4 %collective-permute-start.17 = (f32[1,192]{1,0:T(1,128)S(1)}, f32[1,192]{1,0:T(1,128)S(1)}, u32[]{:S(2)}, u32[]{:S(2)}) collective-permute-start(f32[1,192]{1,0:T(1,128)S(1)} %get-tuple-element.110.refs_5_), channel_id=1, source_target_pairs={{0,2},{1,3},{2,4},{3,5},{4,6},{5,7},{6,0},{7,1},{8,10},{9,11},{10,... | collective-permute-start | bytes 2312 | tf_op jit(solution)/shard_map/ppermute | solution.py:620
  154.5 4.5 %collective-permute-start.18 = (f32[1,192]{1,0:T(1,128)S(1)}, f32[1,192]{1,0:T(1,128)S(1)}, u32[]{:S(2)}, u32[]{:S(2)}) collective-permute-start(f32[1,192]{1,0:T(1,128)S(1)} %get-tuple-element.110.refs_5_), channel_id=1, source_target_pairs={{0,4},{1,5},{2,6},{3,7},{4,0},{5,1},{6,2},{7,3},{8,12},{9,13},{10,... | collective-permute-start | bytes 2312 | tf_op jit(solution)/shard_map/ppermute | solution.py:620
  155.9 3.6 %collective-permute-start.19 = (f32[1,192]{1,0:T(1,128)S(1)}, f32[1,192]{1,0:T(1,128)S(1)}, u32[]{:S(2)}, u32[]{:S(2)}) collective-permute-start(f32[1,192]{1,0:T(1,128)S(1)} %get-tuple-element.110.refs_5_), channel_id=1, source_target_pairs={{0,6},{1,7},{2,0},{3,1},{4,2},{5,3},{6,4},{7,5},{8,14},{9,15},{10,... | collective-permute-start | bytes 2312 | tf_op jit(solution)/shard_map/ppermute | solution.py:620
  159.9 1.4 collective-permute-start.20

commit v6 on v5

--- a/solution.py
+++ b/solution.py
@@ -294,25 +294,42 @@
 
 def attend_group(query, gate, ext_ref, seen, band_ref, mask, own):
     span = min(own, 128)
+    subs = span // HD
     lane = lax.broadcasted_iota(jnp.int32, (GROUP, span), 1) // HD
+    zero = jnp.zeros((), query.dtype)
+    heads = [
+        (start // HD + sub, slice(start, start + span), sub)
+        for start in range(0, own, span)
+        for sub in range(subs)
+    ]
+    scores = [
+        lax.dot_general(
+            jnp.where(lane == sub, query[:, cols], zero),
+            ext_ref[seen, cols],
+            rows_by_rows,
+            preferred_element_type=jnp.float32,
+        )
+        for _, cols, sub in heads
+    ]
+    scores = [part + band_ref[head] + mask for (head, _, _), part in zip(heads, scores)]
+    tops = [jnp.max(part, axis=1, keepdims=True) for part in scores]
+    lifted = [jnp.exp(part - top) for part, top in zip(scores, tops)]
+    totals = [jnp.sum(part, axis=1, keepdims=True) for part in lifted]
+    parts = [
+        jnp.dot(
+            part.astype(jnp.bfloat16),
+            ext_ref[seen, own + cols.start : own + cols.stop],
+            preferred_element_type=jnp.float32,
+        )
+        for (_, cols, _), part in zip(heads, lifted)
+    ]
+    parts = [part / total for part, total in zip(parts, totals)]
     results = []
-    for start in range(0, own, span):
-        cols = slice(start, start + span)
-        keys = ext_ref[seen, cols]
-        values = ext_ref[seen, own + start : own + start + span]
-        result = None
-        for sub in range(span // HD):
-            picked = jnp.where(lane == sub, query[:, cols], jnp.zeros((), query.dtype))
-            scores = lax.dot_general(
-                picked, keys, rows_by_rows, preferred_element_type=jnp.float32
-            )
-            scores = scores + band_ref[start // HD + sub] + mask
-            lifted = jnp.exp(scores - jnp.max(scores, axis=1, keepdims=True))
-            total = jnp.sum(lifted, axis=1, keepdims=True)
-            part = jnp.dot(lifted.astype(jnp.bfloat16), values, preferred_element_type=jnp.float32)
-            part = part / total
-            result = part if result is None else jnp.where(lane == sub, part, result)
-        wide = gate[:, cols].astype(jnp.float32)
+    for at in range(0, len(parts), subs):
+        result = parts[at]
+        for sub in range(1, subs):
+            result = jnp.where(lane == sub, parts[at + sub], result)
+        wide = gate[:, heads[at][1]].astype(jnp.float32)
         results.append((result * (wide / (1.0 + jnp.exp(-wide)))).astype(jnp.bfloat16))
     return results
 

time: 162 us -> 160 us (0.988)
  Pallas kernels: 29.2 us -> 23.5 us
  waiting for transfers between devices: 12.2 us -> 15.9 us
    pallas_call x6, Pallas kernels: 7.18 us -> 3.4 us  [attend(): pl.pallas_call(functools.partial(attend_body, layer, group, len(done)), o...]
    ppermute x6, waiting for transfers between devices: 4.49 us -> 8.23 us  [from_behind(): return lax.ppermute(block, 'sp', [(i, (i + 1) % size) for i in range(size)])]
    pallas_call x3, Pallas kernels: 8.72 us -> 6.83 us  [project_local(): pl.pallas_call(functools.partial(local_body, layer, count), out_shape=tup...]
  transfers between devices with their start and end apart: 21 -> 21, of which waited for: 14 -> 14; matrix products, arithmetic and copies ran while one was open for 0% -> 0% of each run, Pallas kernels for 14% -> 11%
where the time goes in v6:
time: 160 us
  blocking collectives  105 us (66%)
  Pallas kernels  23.5 us (15%)
  starting transfers between devices  15.9 us (10%)
  waiting for transfers between devices  15.9 us (10%)
    all_gather x6, blocking collectives, gather_chips(): return lax.all_gather(x, 'tp', axis=0, axis_index_groups=lines)  105 us
    ppermute x6, starting transfers between devices, from_behind(): return lax.ppermute(block, 'sp', [(i, (i + 1) % size) for i in range(size)])  9.43 us
    ppermute x6, waiting for transfers between devices, from_behind(): return lax.ppermute(block, 'sp', [(i, (i + 1) % size) for i in range(size)])  8.23 us
    pallas_call x3, Pallas kernels, project_local(): pl.pallas_call(functools.partial(local_body, layer, count), out_shape=tup...  6.83 us
    ppermute x12, waiting for transfers between devices, partner(): return lax.ppermute(x, 'tp', [(i, i ^ 1) for i in range(size)])  5.93 us
    ppermute x3, starting transfers between devices, total_over_chips(): lax.ppermute(square, 'tp', [(i, (i + hop) % size) for i in range(size)])  4.27 us
    pallas_call x6, Pallas kernels, attend(): pl.pallas_call(functools.partial(attend_body, layer, group, len(done)), o...  3.4 us
    pallas_call x4, Pallas kernels, project_piece(): pl.pallas_call(functools.partial(piece_body, layer), out_shape=jax.ShapeD...  3.35 us
  transfers between devices with their start and end apart: 21, of which 14 were waited for; matrix products, arithmetic and copies ran while one was open for 0% of the time, Pallas kernels for 11%

profile of v6, /device:TPU:0, one launch (start us, length us, event | category | flops | bytes accessed | tf_op | source)
XLA Modules:
  0.0 160.1 jit_solution(10658537334573455541)
XLA Ops:
  0.0 0.5 collective-permute-start.4
  0.5 19.7 %all-gather = bf16[1536,256]{1,0:T(8,128)(2,1)S(1)} all-gather(bf16[384,256]{1,0:T(8,128)(2,1)} %param.10), channel_id=2, replica_groups={{0,2,6,4},{1,3,7,5},{8,10,14,12},{9,11,15,13},{16,18,22,20},{17,19,23,2..., dimensions={0}, use_global_device_ids=true | all-gather | bytes 983040 | tf_op jit(solution)/shard_map/all_gather | solution.py:618
  20.2 2.3 %setup.1 = (bf16[4,256,2048]{2,1,0:T(8,128)(2,1)S(1)}, f32[3,2048]{1,0:T(4,128)S(1)}, f32[3,2048]{1,0:T(4,128)S(1)}, s32[1,384]{1,0:T(1,128)S(1)}, f32[1,128,384...) custom-call(f32[3,4,257]{2,1,0:T(4,128)} %bias_hbm.1, ...), custom_call_target="tpu_custom_call" | custom-call | tf_op jit(solution)/shard_map/setup/pallas_call | solution.py:109
  22.5 1.0 first_piece.3
  23.5 1.5 collective-permute-start.2
  25.1 1.0 first_piece.2
  26.1 1.5 collective-permute-start.1
  27.7 2.4 %project_local.3 = (bf16[64,2048]{1,0:T(8,128)(2,1)S(1)}, bf16[128,512]{1,0:T(8,128)(2,1)S(1)}, bf16[256,256]{1,0:T(8,128)(2,1)S(1)}, bf16[256,256]{1,0:T(8,128)(2,1)S(1)}, bf16[128,256]{1,0:T(8,128)(2,1)S(1)}) custom-call(bf16[4,384,256]{2,1,0:T(8,128)(2,1)S(1)} %bitcast.9, bf16[4,384,256]{2,1,0:T(8,128)(2,1)S(1)} %collective-permute-done.refs_1_, ...), custom_call_target="tpu_custom_call" | custom-call | tf_op jit(solution)/shard_map/project_local/pallas_call | solution.py:412
  30.1 1.1 collective-permute-done.2.refs_0_.refs_1_
  31.2 0.6 attend.6
  31.8 2.1 %collective-permute-done.1.refs_0_ = bf16[144,512]{1,0:T(8,128)(2,1)S(1)} collective-permute-done((bf16[144,512]{1,0:T(8,128)(2,1)S(1)}, bf16[144,512]{1,0:T(8,128)(2,1)S(1)}, u32[]{:S(2)}, u32[]{:S(2)}) %collective-permute-start.1) | collective-permute-done | bytes 147488 | tf_op jit(solution)/shard_map/ppermute | solution.py:644
  33.9 0.6 attend.7
  34.5 0.1 collective-permute-start.3
  34.6 1.3 collective-permute-done.3.got_ref
  35.9 17.4 %all-gather.1 = bf16[768,512]{1,0:T(8,128)(2,1)S(1)} all-gather(bf16[192,512]{1,0:T(8,128)(2,1)S(1)} %join.3), channel_id=3, replica_groups={{0,2,6,4},{1,3,7,5},{8,10,14,12},{9,11,15,13},{16,18,22,20},{17,19,23,2..., dimensions={0}, use_global_device_ids=true | all-gather | bytes 983040 | tf_op jit(solution)/shard_map/all_gather | solution.py:618
  53.3 0.9 out_project.3
  54.2 17.0 %all-gather.2 = bf16[768,512]{1,0:T(8,128)(2,1)S(1)} all-gather(bf16[192,512]{1,0:T(8,128)(2,1)S(1)} %out_project.3), channel_id=4, replica_groups={{0,2,6,4},{1,3,7,5},{8,10,14,12},{9,11,15,13},{16,18,22,20},{17,19,23,2..., dimensions={0}, use_global_device_ids=true | all-gather | bytes 983040 | tf_op jit(solution)/shard_map/all_gather | solution.py:618
  71.2 0.4 update.5
  71.5 0.1 collective-permute-start.7
  71.6 0.5 update.4
  72.1 0.6 collective-permute-start.5
  72.7 0.1 collective-permute-start.9
  72.7 0.4 collective-permute-done.7.other_ref.refs_5_
  73.1 0.8 project_piece.5.refs_7_
  74.0 0.7 collective-permute-start.8
  74.7 0.8 project_piece.4.refs_6_.refs_2_
  75.5 2.6 %collective-permute-start.6 = (bf16[128,512]{1,0:T(8,128)(2,1)S(1)}, bf16[128,512]{1,0:T(8,128)(2,1)S(1)}, u32[]{:S(2)}, u32[]{:S(2)}) collective-permute-start(bf16[128,512]{1,0:T(8,128)(2,1)S(1)} %project_piece.4.refs_6_.refs_2_), channel_id=1, source_target_pairs={{0,8},{8,16},{16,24},{24,0},{1,9},{9,17},{17,25},{25,1},{2,10},{10... | collective-permute-start | bytes 393224 | tf_op jit(solution)/shard_map/ppermute | solution.py:644
  78.1 2.2 %project_local.4 = (bf16[128,512]{1,0:T(8,128)(2,1)S(1)}, bf16[256,256]{1,0:T(8,128)(2,1)S(1)}, bf16[256,256]{1,0:T(8,128)(2,1)S(1)}, bf16[128,256]{1,0:T(8,128)(2,1)S(1)}) custom-call(bf16[64,2048]{1,0:T(8,128)(2,1)S(1)} %get-tuple-element.84.refs_0_, bf16[64,2048]{1,0:T(8,128)(2,1)S(1)} %get-tuple-element.81.mine_ref.refs_1_, ...), custom_call_target="tpu_custom_call" | custom-call | tf_op jit(solution)/shard_map/project_local/pallas_call | solution.py:412
  80.3 1.0 collective-permute-done.8.refs_0_.refs_1_
  81.3 0.6 attend.8.refs_9_
  81.9 1.4 collective-permute-done.6.refs_0_
  83.3 0.6 attend.9
  83.9 0.1 collective-permute-start.10
  84.0 1.3 collective-permute-done.10.got_ref
  85.3 16.9 %all-gather.3 = bf16[768,512]{1,0:T(8,128)(2,1)S(1)} all-gather(bf16[192,512]{1,0:T(8,128)(2,1)S(1)} %join.4), channel_id=5, replica_groups={{0,2,6,4},{1,3,7,5},{8,10,14,12},{9,11,15,13},{16,18,22,20},{17,19,23,2..., dimensions={0}, use_global_device_ids=true | all-gather | bytes 983040 | tf_op jit(solution)/shard_map/all_gather | solution.py:618
  102.1 0.9 out_project.4
  103.0 16.3 %all-gather.4 = bf16[768,512]{1,0:T(8,128)(2,1)S(1)} all-gather(bf16[192,512]{1,0:T(8,128)(2,1)S(1)} %out_project.4), channel_id=6, replica_groups={{0,2,6,4},{1,3,7,5},{8,10,14,12},{9,11,15,13},{16,18,22,20},{17,19,23,2..., dimensions={0}, use_global_device_ids=true | all-gather | bytes 983040 | tf_op jit(solution)/shard_map/all_gather | solution.py:618
  119.3 0.4 update.7
  119.6 0.1 collective-permute-start.13
  119.7 0.5 update.6
  120.2 0.6 collective-permute-start.11
  120.8 0.1 collective-permute-start.15
  120.8 0.4 collective-permute-done.13.other_ref.refs_5_
  121.2 0.8 project_piece.7.refs_7_
  122.2 0.8 project_piece.6.refs_6_.refs_2_
  123.0 3.0 %collective-permute-start.12 = (bf16[128,512]{1,0:T(8,128)(2,1)S(1)}, bf16[128,512]{1,0:T(8,128)(2,1)S(1)}, u32[]{:S(2)}, u32[]{:S(2)}) collective-permute-start(bf16[128,512]{1,0:T(8,128)(2,1)S(1)} %project_piece.6.refs_6_.refs_2_), channel_id=1, source_target_pairs={{0,8},{8,16},{16,24},{24,0},{1,9},{9,17},{17,25},{25,1},{2,10},{10... | collective-permute-start | bytes 393224 | tf_op jit(solution)/shard_map/ppermute | solution.py:644
  126.0 2.2 %project_local.5 = (bf16[128,512]{1,0:T(8,128)(2,1)S(1)}, bf16[256,256]{1,0:T(8,128)(2,1)S(1)}, bf16[256,256]{1,0:T(8,128)(2,1)S(1)}, bf16[128,256]{1,0:T(8,128)(2,1)S(1)}) custom-call(bf16[64,2048]{1,0:T(8,128)(2,1)S(1)} %get-tuple-element.101.refs_0_, bf16[64,2048]{1,0:T(8,128)(2,1)S(1)} %get-tuple-element.99.mine_ref.refs_1_, ...), custom_call_target="tpu_custom_call" | custom-call | tf_op jit(solution)/shard_map/project_local/pallas_call | solution.py:412
  128.2 1.2 collective-permute-done.14.refs_0_.refs_1_
  129.4 0.6 attend.10.refs_9_
  130.0 1.4 collective-permute-done.12.refs_0_
  131.4 0.6 attend.11
  132.0 0.1 collective-permute-start.16
  132.0 1.3 collective-permute-done.16.got_ref
  133.3 17.3 %all-gather.5 = bf16[768,512]{1,0:T(8,128)(2,1)S(1)} all-gather(bf16[192,512]{1,0:T(8,128)(2,1)S(1)} %join.5), channel_id=7, replica_groups={{0,2,6,4},{1,3,7,5},{8,10,14,12},{9,11,15,13},{16,18,22,20},{17,19,23,2..., dimensions={0}, use_global_device_ids=true | all-gather | bytes 983040 | tf_op jit(solution)/shard_map/all_gather | solution.py:618
  150.6 1.0 out_project.5
  151.7 0.9 collective-permute-start.17
  152.6 1.4 collective-permute-start.18
  154.0 2.0 %collective-permute-start.19 = (f32[1,192]{1,0:T(1,128)S(1)}, f32[1,192]{1,0:T(1,128)S(1)}, u32[]{:S(2)}, u32[]{:S(2)}) collective-permute-start(f32[1,192]{1,0:T(1,128)S(1)} %get-tuple-element.110.refs_5_), channel_id=1, source_target_pairs={{0,6},{1,7},{2,0},{3,1},{4,2},{5,3},{6,4},{7,5},{8,14},{9,15},{10,... | collective-permute-start | bytes 2312 | tf_op jit(solution)/shard_map/ppermute | solution.py:637
  155.9 1.1 collective-permute-done.17.refs_6_
  157.1 0.6 collective-permute-done.19.refs_8_
  157.6 0.4 finish.1
  158.0 0.1 collective-permute-start.20
  158.1 1.3 collective-permute-done.20.got_ref
  159.4 0.7 merge.1
  (22 shorter events, 0.2 us)
Async XLA Ops:
  0.0 53.3 %collective-permute-start.4 = (bf16[3,256,2048]{2,1,0:T(8,128)(2,1)}, bf16[3,256,2048]{2,1,0:T(8,128)(2,1)S(1)}, u32[]{:S(2)}, u32[]{:S(2)}) collective-permute-start(bf16[3,256,2048]{2,1,0:T(8,128)(2,1)} %mine_ref.5), channel_id=1, source_target_pairs={{0,1},{1,0},{2,3},{3,2},{4,5},{5,4},{6,7},{7,6},{8,9},{9,8},{10,11... | collective-permute-start | bytes 9437192 | tf_op jit(solution)/shard_map/ppermute | solution.py:612
  20.2 2.3 %collective-permute-start = (bf16[4,384,256]{2,1,0:T(8,128)(2,1)S(1)}, bf16[4,384,256]{2,1,0:T(8,128)(2,1)S(1)}, u32[]{:S(2)}, u32[]{:S(2)}) collective-permute-start(bf16[4,384,256]{2,1,0:T(8,128)(2,1)S(1)} %bitcast.6), channel_id=1, source_target_pairs={{0,1},{1,0},{2,3},{3,2},{4,5},{5,4},{6,7},{7,6},{8,9},{9,8},{10,11... | collective-permute-start | bytes 2359304 | tf_op jit(solution)/shard_map/ppermute | solution.py:612
  23.5 7.7 %collective-permute-start.2 = (bf16[144,512]{1,0:T(8,128)(2,1)S(1)}, bf16[144,512]{1,0:T(8,128)(2,1)S(1)}, u32[]{:S(2)}, u32[]{:S(2)}) collective-permute-start(bf16[144,512]{1,0:T(8,128)(2,1)S(1)} %get-tuple-element.65.refs_6_), channel_id=1, source_target_pairs={{0,8},{8,16},{16,24},{24,0},{1,9},{9,17},{17,25},{25,1},{2,10},{10... | collective-permute-start | bytes 442376 | tf_op jit(solution)/shard_map/ppermute | solution.py:644
  26.1 7.8 %collective-permute-start.1 = (bf16[144,512]{1,0:T(8,128)(2,1)S(1)}, bf16[144,512]{1,0:T(8,128)(2,1)S(1)}, u32[]{:S(2)}, u32[]{:S(2)}) collective-permute-start(bf16[144,512]{1,0:T(8,128)(2,1)S(1)} %get-tuple-element.64.refs_5_.refs_2_), channel_id=1, source_target_pairs={{0,8},{8,16},{16,24},{24,0},{1,9},{9,17},{17,25},{25,1},{2,10},{10... | collective-permute-start | bytes 442376 | tf_op jit(solution)/shard_map/ppermute | solution.py:644
  30.1 23.2 %copy-start.2 = (bf16[3,256,2048]{2,1,0:T(8,128)(2,1)S(1)}, bf16[3,256,2048]{2,1,0:T(8,128)(2,1)}, u32[]{:S(2)}) copy-start(bf16[3,256,2048]{2,1,0:T(8,128)(2,1)} %mine_ref.5) | copy-start | bytes 9437188
  34.5 1.4 collective-permute-start.3
  53.3 19.8 %copy-start.1 = (bf16[3,256,2048]{2,1,0:T(8,128)(2,1)S(1)}, bf16[3,256,2048]{2,1,0:T(8,128)(2,1)}, u32[]{:S(2)}) copy-start(bf16[3,256,2048]{2,1,0:T(8,128)(2,1)} %refs_11_.3) | copy-start | bytes 9437188
  54.2 19.0 %copy-start = (bf16[3,256,2048]{2,1,0:T(8,128)(2,1)S(1)}, bf16[3,256,2048]{2,1,0:T(8,128)(2,1)}, u32[]{:S(2)}) copy-start(bf16[3,256,2048]{2,1,0:T(8,128)(2,1)} %refs_10_.3) | copy-start | bytes 9437188
  71.5 1.6 collective-permute-start.7
  72.1 2.6 %collective-permute-start.5 = (bf16[64,2048]{1,0:T(8,128)(2,1)S(1)}, bf16[64,2048]{1,0:T(8,128)(2,1)S(1)}, u32[]{:S(2)}, u32[]{:S(2)}) collective-permute-start(bf16[64,2048]{1,0:T(8,128)(2,1)S(1)} %get-tuple-element.81.mine_ref.refs_1_), channel_id=1, source_target_pairs={{0,1},{1,0},{2,3},{3,2},{4,5},{5,4},{6,7},{7,6},{8,9},{9,8},{10,11... | collective-permute-start | bytes 786440 | tf_op jit(solution)/shard_map/ppermute | solution.py:612
  72.7 5.5 %collective-permute-start.9 = (bf16[64,2048]{1,0:T(8,128)(2,1)S(1)}, bf16[64,2048]{1,0:T(8,128)(2,1)S(1)}, u32[]{:S(2)}, u32[]{:S(2)}) collective-permute-start(bf16[64,2048]{1,0:T(8,128)(2,1)S(1)} %get-tuple-element.84.refs_0_), channel_id=1, source_target_pairs={{0,1},{1,0},{2,3},{3,2},{4,5},{5,4},{6,7},{7,6},{8,9},{9,8},{10,11... | collective-permute-start | bytes 786440 | tf_op jit(solution)/shard_map/ppermute | solution.py:612
  74.0 4.1 %copy-start.3 = (bf16[3,256,2048]{2,1,0:T(8,128)(2,1)S(1)}, bf16[3,256,2048]{2,1,0:T(8,128)(2,1)}, u32[]{:S(2)}) copy-start(bf16[3,256,2048]{2,1,0:T(8,128)(2,1)} %refs_12_.3) | copy-start | bytes 9437188
  74.0 4.1 %copy-start.4 = (bf16[3,256,2048]{2,1,0:T(8,128)(2,1)S(1)}, bf16[3,256,2048]{2,1,0:T(8,128)(2,1)}, u32[]{:S(2)}) copy-start(bf16[3,256,2048]{2,1,0:T(8,128)(2,1)} %refs_13_.3) | copy-start | bytes 9437188
  74.0 7.3 %collective-permute-start.8 = (bf16[128,512]{1,0:T(8,128)(2,1)S(1)}, bf16[128,512]{1,0:T(8,128)(2,1)S(1)}, u32[]{:S(2)}, u32[]{:S(2)}) collective-permute-start(bf16[128,512]{1,0:T(8,128)(2,1)S(1)} %project_piece.5.refs_7_), channel_id=1, source_target_pairs={{0,8},{8,16},{16,24},{24,0},{1,9},{9,17},{17,25},{25,1},{2,10},{10... | collective-permute-start | bytes 393224 | tf_op jit(solution)/shard_map/ppermute | solution.py:644
  75.5 7.8 %collective-permute-start.6 = (bf16[128,512]{1,0:T(8,128)(2,1)S(1)}, bf16[128,512]{1,0:T(8,128)(2,1)S(1)}, u32[]{:S(2)}, u32[]{:S(2)}) collective-permute-start(bf16[128,512]{1,0:T(8,128)(2,1)S(1)} %project_piece.4.refs_6_.refs_2_), channel_id=1, source_target_pairs={{0,8},{8,16},{16,24},{24,0},{1,9},{9,17},{17,25},{25,1},{2,10},{10... | collective-permute-start | bytes 393224 | tf_op jit(solution)/shard_map/ppermute | solution.py:644
  83.9 1.4 collective-permute-start.10
  119.6 1.6 collective-permute-start.13
  120.2 1.9 %collective-permute-start.11 = (bf16[64,2048]{1,0:T(8,128)(2,1)S(1)}, bf16[64,2048]{1,0:T(8,128)(2,1)S(1)}, u32[]{:S(2)}, u32[]{:S(2)}) collective-permute-start(bf16[64,2048]{1,0:T(8,128)(2,1)S(1)} %get-tuple-element.99.mine_ref.refs_1_), channel_id=1, source_target_pairs={{0,1},{1,0},{2,3},{3,2},{4,5},{5,4},{6,7},{7,6},{8,9},{9,8},{10,11... | collective-permute-start | bytes 786440 | tf_op jit(solution)/shard_map/ppermute | solution.py:612
  120.8 5.2 %collective-permute-start.15 = (bf16[64,2048]{1,0:T(8,128)(2,1)S(1)}, bf16[64,2048]{1,0:T(8,128)(2,1)S(1)}, u32[]{:S(2)}, u32[]{:S(2)}) collective-permute-start(bf16[64,2048]{1,0:T(8,128)(2,1)S(1)} %get-tuple-element.101.refs_0_), channel_id=1, source_target_pairs={{0,1},{1,0},{2,3},{3,2},{4,5},{5,4},{6,7},{7,6},{8,9},{9,8},{10,11... | collective-permute-start | bytes 786440 | tf_op jit(solution)/shard_map/ppermute | solution.py:612
  122.1 7.3 %collective-permute-start.14 = (bf16[128,512]{1,0:T(8,128)(2,1)S(1)}, bf16[128,512]{1,0:T(8,128)(2,1)S(1)}, u32[]{:S(2)}, u32[]{:S(2)}) collective-permute-start(bf16[128,512]{1,0:T(8,128)(2,1)S(1)} %project_piece.7.refs_7_), channel_id=1, source_target_pairs={{0,8},{8,16},{16,24},{24,0},{1,9},{9,17},{17,25},{25,1},{2,10},{10... | collective-permute-start | bytes 393224 | tf_op jit(solution)/shard_map/ppermute | solution.py:644
  123.0 8.4 %collective-permute-start.12 = (bf16[128,512]{1,0:T(8,128)(2,1)S(1)}, bf16[128,512]{1,0:T(8,128)(2,1)S(1)}, u32[]{:S(2)}, u32[]{:S(2)}) collective-permute-start(bf16[128,512]{1,0:T(8,128)(2,1)S(1)} %project_piece.6.refs_6_.refs_2_), channel_id=1, source_target_pairs={{0,8},{8,16},{16,24},{24,0},{1,9},{9,17},{17,25},{25,1},{2,10},{10... | collective-permute-start | bytes 393224 | tf_op jit(solution)/shard_map/ppermute | solution.py:644
  132.0 1.4 collective-permute-start.16
  151.7 5.4 %collective-permute-start.17 = (f32[1,192]{1,0:T(1,128)S(1)}, f32[1,192]{1,0:T(1,128)S(1)}, u32[]{:S(2)}, u32[]{:S(2)}) collective-permute-start(f32[1,192]{1,0:T(1,128)S(1)} %get-tuple-element.110.refs_5_), channel_id=1, source_target_pairs={{0,2},{1,3},{2,4},{3,5},{4,6},{5,7},{6,0},{7,1},{8,10},{9,11},{10,... | collective-permute-start | bytes 2312 | tf_op jit(solution)/shard_map/ppermute | solution.py:637
  152.6 4.5 %collective-permute-start.18 = (f32[1,192]{1,0:T(1,128)S(1)}, f32[1,192]{1,0:T(1,128)S(1)}, u32[]{:S(2)}, u32[]{:S(2)}) collective-permute-start(f32[1,192]{1,0:T(1,128)S(1)} %get-tuple-element.110.refs_5_), channel_id=1, source_target_pairs={{0,4},{1,5},{2,6},{3,7},{4,0},{5,1},{6,2},{7,3},{8,12},{9,13},{10,... | collective-permute-start | bytes 2312 | tf_op jit(solution)/shard_map/ppermute | solution.py:637
  154.0 3.7 %collective-permute-start.19 = (f32[1,192]{1,0:T(1,128)S(1)}, f32[1,192]{1,0:T(1,128)S(1)}, u32[]{:S(2)}, u32[]{:S(2)}) collective-permute-start(f32[1,192]{1,0:T(1,128)S(1)} %get-tuple-element.110.refs_5_), channel_id=1, source_target_pairs={{0,6},{1,7},{2,0},{3,1},{4,2},{5,3},{6,4},{7,5},{8,14},{9,15},{10,... | collective-permute-start | bytes 2312 | tf_op jit(solution)/shard_map/ppermute | solution.py:637
  158.0 1.4 collective-permute-start.20

commit v7 on v6

--- a/solution.py
+++ b/solution.py
@@ -237,6 +237,31 @@
     ).astype(jnp.bfloat16)
 
 
+def turned_body(layer, count, *refs):
+    out_ref = refs[-1]
+    own = refs[0].shape[1]
+    for at in range(count):
+        out_ref[:, at * own : (at + 1) * own] = jnp.transpose(refs[at][layer])
+
+
+def turned(layer, weights, after):
+    own = weights[0].shape[1]
+    return pl.pallas_call(
+        functools.partial(turned_body, layer, len(weights)),
+        out_shape=jax.ShapeDtypeStruct((D, len(weights) * own), weights[0].dtype),
+        in_specs=[vmem] * (len(weights) + 1),
+        out_specs=vmem,
+        compiler_params=params,
+        name="turned",
+    )(*weights, after)
+
+
+def columns_product(rows_ref, weight_ref):
+    return jnp.dot(
+        rows_ref[...], weight_ref[...], preferred_element_type=jnp.float32
+    ).astype(jnp.bfloat16)
+
+
 def weight_of(layer, weights, at):
     return weights[0][at] if layer == 0 else weights[at][layer]
 
@@ -271,25 +296,22 @@
     )(*operands)
 
 
-def piece_body(layer, mine_ref, other_ref, key_ref, value_ref, kv_ref, rows_ref):
+def piece_body(mine_ref, other_ref, weight_ref, kv_ref, rows_ref):
     rows_ref[half_rows(True), :] = mine_ref[...]
     rows_ref[half_rows(False), :] = other_ref[...]
-    own = kv_ref.shape[1] // 2
-    kv_ref[:, :own] = product(rows_ref, key_ref[layer])
-    kv_ref[:, own:] = product(rows_ref, value_ref[layer])
-
-
-def project_piece(layer, mine, other, key_weight, value_weight):
-    own = key_weight.shape[1]
-    return pl.pallas_call(
-        functools.partial(piece_body, layer),
-        out_shape=jax.ShapeDtypeStruct((GROUP, 2 * own), jnp.bfloat16),
-        in_specs=[vmem] * 4,
+    kv_ref[...] = columns_product(rows_ref, weight_ref)
+
+
+def project_piece(mine, other, weight):
+    return pl.pallas_call(
+        piece_body,
+        out_shape=jax.ShapeDtypeStruct((GROUP, weight.shape[1]), jnp.bfloat16),
+        in_specs=[vmem] * 3,
         out_specs=vmem,
         scratch_shapes=[pltpu.VMEM((GROUP, D), jnp.bfloat16)],
         compiler_params=params,
         name="project_piece",
-    )(mine, other, key_weight, value_weight)
+    )(mine, other, weight)
 
 
 def attend_group(query, gate, ext_ref, seen, band_ref, mask, own):
@@ -420,13 +442,13 @@
     )(*operands)
 
 
-def attend_body(layer, group, done, *refs):
+def attend_body(layer, group, done, waited, *refs):
     halo_count = PAST // GROUP - group
     chunks, refs = refs[: WINDOW // GROUP], refs[WINDOW // GROUP :]
     query_ref, gate_ref, band_ref, docs_ref, refs = *refs[:4], refs[4:]
     known = halo_count if layer else halo_count - 1
     told_refs, refs = refs[:known], refs[known:]
-    done_refs, refs = refs[:done], refs[done:]
+    done_refs, refs = refs[:done], refs[done + waited :]
     keep_ref = give_ref = None
     if group == 0:
         (keep_ref, give_ref), refs = refs[:2], refs[2:]
@@ -459,10 +481,10 @@
             give_ref[at] = ref[half_rows(False), :]
 
 
-def attend(layer, group, chunks, query, gate, band, docs, told, done):
+def attend(layer, group, chunks, query, gate, band, docs, told, done, waited):
     own = query.shape[1]
     bf = jnp.bfloat16
-    operands = (*chunks, query, gate, band, docs, *told, *done)
+    operands = (*chunks, query, gate, band, docs, *told, *done, *waited)
     shapes = [jax.ShapeDtypeStruct((GROUP, own), bf)]
     scratch = [pltpu.VMEM((WINDOW, 2 * own), bf)]
     if group == 0:
@@ -471,7 +493,7 @@
     if layer == 0:
         shapes.append(jax.ShapeDtypeStruct((1, GROUP), jnp.int32))
     return pl.pallas_call(
-        functools.partial(attend_body, layer, group, len(done)),
+        functools.partial(attend_body, layer, group, len(done), len(waited)),
         out_shape=tuple(shapes),
         in_specs=[vmem] * len(operands),
         out_specs=(vmem,) * len(shapes),
@@ -508,103 +530,120 @@
     )(keep, got)
 
 
-def out_body(layer, last, blocks_ref, mine_ref, other_ref, branch_ref, *rest):
-    mixed_ref = rest[-1]
+def out_body(last, blocks_ref, weight_ref, *refs):
+    mixed_ref = refs[-1]
     width = blocks_ref.shape[2]
     own = width // CORES
     for ref, slot, col in chip_columns(blocks_ref):
         mixed_ref[:, col : col + width] = ref[slot]
-    mine = product(mixed_ref, mine_ref[layer])
-    other = product(mixed_ref, other_ref[layer])
-
-    def place(core):
-        branch_ref[:, core * own : (core + 1) * own] = mine
-        branch_ref[:, (1 - core) * own : (2 - core) * own] = other
-
-    by_core(place)
+    branch = columns_product(mixed_ref, weight_ref)
+    mine, other = branch[:, :own], branch[:, own:]
+    if not last:
+        branch_ref = refs[0]
+
+        def place(core):
+            branch_ref[:, core * own : (core + 1) * own] = mine
+            branch_ref[:, (1 - core) * own : (2 - core) * own] = other
+
+        by_core(place)
+        return
+    keep_ref, give_ref, square_ref = refs[:3]
+    keep_ref[...] = mine
+    give_ref[...] = other
+    total = 0.0
+    for part in (mine, other):
+        wide = part.astype(jnp.float32)
+        total = total + jnp.sum(wide * wide, axis=1, keepdims=True)
+    empty = jnp.zeros((1, HALF), jnp.float32)
+    for group in range(total.shape[0] // HALF):
+        row = turn(total[group * HALF : (group + 1) * HALF], 0)
+
+        def place(core):
+            pair = (row, empty) if core == 0 else (empty, row)
+            square_ref[:, group * GROUP : (group + 1) * GROUP] = jnp.concatenate(pair, axis=1)
+
+        by_core(place)
+
+
+def out_project(blocks, weight, last):
+    rows, width = blocks.shape[1:]
+    bf = jnp.bfloat16
+    shapes = [jax.ShapeDtypeStruct((rows, width), bf)]
     if last:
-        square_ref = rest[0]
-        wide = mine.astype(jnp.float32)
-        total = jnp.sum(wide * wide, axis=1, keepdims=True)
-        wide = other.astype(jnp.float32)
-        total = total + jnp.sum(wide * wide, axis=1, keepdims=True)
-        for start in range(0, total.shape[0], HALF):
-            at = slice(start, start + HALF)
-            square_ref[:, at] = turn(total[at], 0)
-
-
-def out_project(layer, blocks, mine, other, last):
-    rows, width = blocks.shape[1:]
-    shapes = [jax.ShapeDtypeStruct((rows, width), jnp.bfloat16)]
-    if last:
-        shapes.append(jax.ShapeDtypeStruct((1, rows), jnp.float32))
-    return pl.pallas_call(
-        functools.partial(out_body, layer, last),
+        shapes = [jax.ShapeDtypeStruct((rows, width // CORES), bf)] * CORES
+        shapes.append(jax.ShapeDtypeStruct((1, CORES * rows), jnp.float32))
+    return pl.pallas_call(
+        functools.partial(out_body, last),
         out_shape=tuple(shapes),
-        in_specs=[vmem] * 3,
+        in_specs=[vmem] * 2,
         out_specs=(vmem,) * len(shapes),
-        scratch_shapes=[pltpu.VMEM((rows, D), jnp.bfloat16)],
+        scratch_shapes=[pltpu.VMEM((rows, D), bf)],
         compiler_params=params,
         name="out_project",
-    )(blocks, mine, other)
-
-
-def finish_body(groups, *refs):
-    resid_refs, (branch_ref, gain_ref), refs = refs[:groups], refs[groups : groups + 2], refs[groups + 2 :]
+    )(blocks, weight)
+
+
+def chip_slice(width):
+    chip = lax.div(lax.axis_index("tp"), CORES)
+    return pl.ds(pl.multiple_of(chip * width, 128), width)
+
+
+def split_body(groups, *refs):
     keep_ref, give_ref = refs[-2:]
+    own = keep_ref.shape[1]
+    for group in range(groups):
+        at = slice(group * HALF, (group + 1) * HALF)
+        rows = refs[group][:, chip_slice(CORES * own)]
+
+        def place(core):
+            keep_ref[at] = rows[:, core * own : (core + 1) * own]
+            give_ref[at] = rows[:, (1 - core) * own : (2 - core) * own]
+
+        by_core(place)
+
+
+def split(halves, own, after):
+    shape = jax.ShapeDtypeStruct((len(halves) * HALF, own), jnp.bfloat16)
+    return pl.pallas_call(
+        functools.partial(split_body, len(halves)),
+        out_shape=(shape,) * 2,
+        in_specs=[vmem] * (len(halves) + 1),
+        out_specs=(vmem,) * 2,
+        compiler_params=params,
+        name="split",
+    )(*halves, after)
+
+
+def finish_body(old_keep, old_got, keep_ref, got_ref, gain_ref, *refs):
+    out_ref, old_ref, branch_ref = refs[-3:]
     total = refs[0][...]
-    for ref in refs[1:-2]:
+    for ref in refs[1:-3]:
         total = total + ref[...]
-    width = branch_ref.shape[1]
-    own = width // CORES
-    chip = lax.div(lax.axis_index("tp"), CORES)
-    cols = pl.ds(pl.multiple_of(chip * width, 128), width)
-    gain = gain_ref[gain_ref.shape[0] - 1 :, cols]
-    for group, ref in enumerate(resid_refs):
-        at = slice(group * HALF, (group + 1) * HALF)
+    own = out_ref.shape[1]
+    gain = gain_ref[gain_ref.shape[0] - 1 :, chip_slice(CORES * own)]
+    gain = jnp.where(core_at() == 0, gain[:, :own], gain[:, own:])
+    for group in range(out_ref.shape[0] // GROUP):
+        at = slice(group * GROUP, (group + 1) * GROUP)
+        half = slice(group * HALF, (group + 1) * HALF)
+        for target, mine, other in ((old_ref, old_keep, old_got), (branch_ref, keep_ref, got_ref)):
+            target[half_rows(True), :] = mine[half].astype(jnp.float32)
+            target[half_rows(False), :] = other[half].astype(jnp.float32)
         inv_out = lax.rsqrt(turn(total[:, at], 1) / D + norm_eps)
-        old = ref[:, cols].astype(jnp.float32)
-        branch = branch_ref[at].astype(jnp.float32)
-        new = (old + branch * inv_out * gain).astype(jnp.bfloat16)
-
-        def place(core):
-            keep_ref[at] = new[:, core * own : (core + 1) * own]
-            give_ref[at] = new[:, (1 - core) * own : (2 - core) * own]
-
-        by_core(place)
-
-
-def finish(resids, branch, gain, totals):
-    rows, width = branch.shape
-    operands = (*resids, branch, gain, *totals)
-    return pl.pallas_call(
-        functools.partial(finish_body, len(resids)),
-        out_shape=(jax.ShapeDtypeStruct((rows, width // CORES), jnp.bfloat16),) * 2,
+        out_ref[at] = (old_ref[...] + branch_ref[...] * inv_out * gain).astype(jnp.bfloat16)
+
+
+def finish(old_keep, old_got, keep, got, gain, totals):
+    rows, own = keep.shape
+    operands = (old_keep, old_got, keep, got, gain, *totals)
+    return pl.pallas_call(
+        finish_body,
+        out_shape=jax.ShapeDtypeStruct((CORES * rows, own), jnp.bfloat16),
         in_specs=[vmem] * len(operands),
-        out_specs=(vmem,) * 2,
+        out_specs=vmem,
+        scratch_shapes=[pltpu.VMEM((GROUP, own), jnp.float32)] * 2,
         compiler_params=params,
         name="finish",
     )(*operands)
-
-
-def merge_body(keep_ref, got_ref, out_ref):
-    for group in range(out_ref.shape[0] // GROUP):
-        at = slice(group * HALF, (group + 1) * HALF)
-        rows_ref = out_ref.at[pl.ds(group * GROUP, GROUP)]
-        rows_ref[half_rows(True), :] = keep_ref[at]
-        rows_ref[half_rows(False), :] = got_ref[at]
-
-
-def merge(keep, got):
-    rows, own = keep.shape
-    return pl.pallas_call(
-        merge_body,
-        out_shape=jax.ShapeDtypeStruct((CORES * rows, own), keep.dtype),
-        in_specs=[vmem] * 2,
-        out_specs=vmem,
-        compiler_params=params,
-        name="merge",
-    )(keep, got)
 
 
 def partner(x):
@@ -628,13 +667,13 @@
     return (own, partner(own)) if own.shape[2] < D else (own,)
 
 
-def total_over_chips(square):
+def total_over_tp(square):
     size = lax.axis_size("tp")
     if size > 8:
-        lines = [list(range(core, size, CORES)) for core in range(CORES)]
-        return (lax.psum(square, "tp", axis_index_groups=lines),)
-    return (square,) + tuple(
-        lax.ppermute(square, "tp", [(i, (i + hop) % size) for i in range(size)])
+        return (lax.psum(square, "tp"),)
+    both = square + partner(square)
+    return (both,) + tuple(
+        lax.ppermute(both, "tp", [(i, (i + hop) % size) for i in range(size)])
         for hop in range(CORES, size, CORES)
     )
 
@@ -660,7 +699,7 @@
     groups = rows // GROUP
     first = (rows - PAST) // GROUP
     weights = (key_weight, value_weight, query_weight, gate_weight)
-    other_out = partner(out_weight)
+    out_pair = (out_weight, partner(out_weight))
     gathered, documents = lax.optimization_barrier((gather_tokens(tokens), documents))
     blocks = swapped(gathered)
     stage, pre, post, docs, mask, *bands = setup(
@@ -677,7 +716,7 @@
                     halves[at], normed[at], other[at] = half, row, partner(row)
         for group in reversed(range(first, groups)):
             if layer:
-                pieces[group] = project_piece(layer, normed[group], other[group], *weights[:2])
+                pieces[group] = project_piece(normed[group], other[group], key_value)
             else:
                 halves[group], normed[group], pieces[group] = first_piece(
                     blocks, group * GROUP, docs, pre, stage
@@ -689,27 +728,44 @@
         )
         if half:
             halves[0] = half[0]
+        last = layer + 1 == LAYERS
+        ready = [turned(layer, out_pair, local_mixed)]
+        if last:
+            old_keep, old_give = split(halves, tokens.shape[1], local_mixed)
+            old_got = partner(old_give)
+            ready.append(old_keep)
+        else:
+            ready.append(turned(layer + 1, weights[:2], local_mixed))
+            key_value = ready[1]
         done = [local_mixed]
         known = [*halos[first:], head, *pieces[first:]]
         for group in reversed(range(PAST // GROUP)):
             chunks = known[group : group + WINDOW // GROUP]
             told = behind[group if layer else group + 1 :]
             made = attend(
-                layer, group, chunks, query, gate, bands[layer], docs, told, done if group == 0 else []
+                layer,
+                group,
+                chunks,
+                query,
+                gate,
+                bands[layer],
+                docs,
+                told,
+                () if group else done,
+                () if group else ready,
             )
             if layer == 0:
                 *made, behind[group] = made
             if group:
                 done = [made[0], *done]
         keep, give = made
-        last = layer + 1 == LAYERS
         mixed = gather_chips(join(keep, partner(give)))
-        result = out_project(layer, mixed, out_weight, other_out, last)
+        result = out_project(mixed, ready[0], last)
         if not last:
             blocks = gather_chips(result[0])
-    branch, square = result
-    keep, give = finish(halves, branch, post, total_over_chips(square))
-    return merge(keep, partner(give))
+    keep, give, square = result
+    totals = total_over_tp(square)
+    return finish(old_keep, old_got, keep, partner(give), post, totals)
 
 
 def solution(mesh):

time: 160 us -> 158 us (0.988)
  waiting for transfers between devices: 15.9 us -> 11.9 us
    ppermute x6, waiting for transfers between devices: 8.23 us -> 4.95 us  [from_behind(): return lax.ppermute(block, 'sp', [(i, (i + 1) % size) for i in range(size)])]
    ppermute x12 -> x14, waiting for transfers between devices: 5.93 us -> 5.16 us  [partner(): return lax.ppermute(x, 'tp', [(i, i ^ 1) for i in range(size)])]
    pallas_call x15 -> x20, Pallas kernels: 10.6 us -> 10.9 us  [the longest x6 3.39 us: attend(): pl.pallas_call(functools.partial(attend_body, layer, group, len(done), le...]
  transfers between devices with their start and end apart: 21 -> 23, of which waited for: 14 -> 16; matrix products, arithmetic and copies ran while one was open for 0% -> 0% of each run, Pallas kernels for 11% -> 12%
where the time goes in v7:
time: 158 us
  blocking collectives  104 us (66%)
  Pallas kernels  23.8 us (15%)
  starting transfers between devices  16.6 us (11%)
  waiting for transfers between devices  11.9 us (8%)
    all_gather x6, blocking collectives, gather_chips(): return lax.all_gather(x, 'tp', axis=0, axis_index_groups=lines)  104 us
    ppermute x6, starting transfers between devices, from_behind(): return lax.ppermute(block, 'sp', [(i, (i + 1) % size) for i in range(size)])  9.25 us
    pallas_call x3, Pallas kernels, project_local(): pl.pallas_call(functools.partial(local_body, layer, count), out_shape=tup...  6.85 us
    ppermute x14, waiting for transfers between devices, partner(): return lax.ppermute(x, 'tp', [(i, i ^ 1) for i in range(size)])  5.16 us
    ppermute x6, waiting for transfers between devices, from_behind(): return lax.ppermute(block, 'sp', [(i, (i + 1) % size) for i in range(size)])  4.95 us
    ppermute x3, starting transfers between devices, total_over_tp(): lax.ppermute(both, 'tp', [(i, (i + hop) % size) for i in range(size)])  4.17 us
    pallas_call x6, Pallas kernels, attend(): pl.pallas_call(functools.partial(attend_body, layer, group, len(done), le...  3.39 us
    ppermute x14, starting transfers between devices, partner(): return lax.ppermute(x, 'tp', [(i, i ^ 1) for i in range(size)])  3.17 us
  transfers between devices with their start and end apart: 23, of which 16 were waited for; matrix products, arithmetic and copies ran while one was open for 0% of the time, Pallas kernels for 12%

profile of v7, /device:TPU:0, one launch (start us, length us, event | category | flops | bytes accessed | tf_op | source)
XLA Modules:
  0.0 158.0 jit_solution(15054990770625761355)
XLA Ops:
  0.0 0.5 collective-permute-start.3
  0.5 19.7 %all-gather = bf16[1536,256]{1,0:T(8,128)(2,1)S(1)} all-gather(bf16[384,256]{1,0:T(8,128)(2,1)} %param.10), channel_id=2, replica_groups={{0,2,6,4},{1,3,7,5},{8,10,14,12},{9,11,15,13},{16,18,22,20},{17,19,23,2..., dimensions={0}, use_global_device_ids=true | all-gather | bytes 983040 | tf_op jit(solution)/shard_map/all_gather | solution.py:657
  20.2 2.3 %setup.1 = (bf16[4,256,2048]{2,1,0:T(8,128)(2,1)S(1)}, f32[3,2048]{1,0:T(4,128)S(1)}, f32[3,2048]{1,0:T(4,128)S(1)}, s32[1,384]{1,0:T(1,128)S(1)}, f32[1,128,384...) custom-call(f32[3,4,257]{2,1,0:T(4,128)} %bias_hbm.1, ...), custom_call_target="tpu_custom_call" | custom-call | tf_op jit(solution)/shard_map/setup/pallas_call | solution.py:109
  22.5 1.0 first_piece.3
  23.5 1.5 collective-permute-start.2
  25.1 1.0 first_piece.2
  26.1 1.5 collective-permute-start.1
  27.6 2.4 %project_local.3 = (bf16[64,2048]{1,0:T(8,128)(2,1)S(1)}, bf16[128,512]{1,0:T(8,128)(2,1)S(1)}, bf16[256,256]{1,0:T(8,128)(2,1)S(1)}, bf16[256,256]{1,0:T(8,128)(2,1)S(1)}, bf16[128,256]{1,0:T(8,128)(2,1)S(1)}) custom-call(bf16[4,384,256]{2,1,0:T(8,128)(2,1)S(1)} %bitcast.9, bf16[4,384,256]{2,1,0:T(8,128)(2,1)S(1)} %collective-permute-done.refs_1_, ...), custom_call_target="tpu_custom_call" | custom-call | tf_op jit(solution)/shard_map/project_local/pallas_call | solution.py:434
  30.1 0.4 copy-done.1
  30.5 0.6 turned.6.refs_11_.weight_ref
  31.2 0.6 attend.6
  31.8 0.6 copy-done.2
  32.4 0.6 turned.5.refs_10_.weight_ref
  33.0 0.9 collective-permute-done.1.refs_0_
  33.9 0.6 attend.7
  34.6 1.3 collective-permute-done.4.got_ref
  35.9 17.3 %all-gather.1 = bf16[768,512]{1,0:T(8,128)(2,1)S(1)} all-gather(bf16[192,512]{1,0:T(8,128)(2,1)S(1)} %join.3), channel_id=3, replica_groups={{0,2,6,4},{1,3,7,5},{8,10,14,12},{9,11,15,13},{16,18,22,20},{17,19,23,2..., dimensions={0}, use_global_device_ids=true | all-gather | bytes 983040 | tf_op jit(solution)/shard_map/all_gather | solution.py:657
  53.2 0.6 out_project.3
  53.8 17.0 %all-gather.2 = bf16[768,512]{1,0:T(8,128)(2,1)S(1)} all-gather(bf16[192,512]{1,0:T(8,128)(2,1)S(1)} %out_project.3), channel_id=4, replica_groups={{0,2,6,4},{1,3,7,5},{8,10,14,12},{9,11,15,13},{16,18,22,20},{17,19,23,2..., dimensions={0}, use_global_device_ids=true | all-gather | bytes 983040 | tf_op jit(solution)/shard_map/all_gather | solution.py:657
  70.8 0.4 update.5
  71.3 0.5 update.4
  71.8 0.5 collective-permute-start.5
  72.4 0.4 collective-permute-done.7.other_ref.refs_5_
  72.7 0.5 project_piece.5.refs_7_
  73.2 0.6 collective-permute-start.8
  73.8 0.4 project_piece.4.refs_6_.refs_2_
  74.3 2.7 %collective-permute-start.6 = (bf16[128,512]{1,0:T(8,128)(2,1)S(1)}, bf16[128,512]{1,0:T(8,128)(2,1)S(1)}, u32[]{:S(2)}, u32[]{:S(2)}) collective-permute-start(bf16[128,512]{1,0:T(8,128)(2,1)S(1)} %project_piece.4.refs_6_.refs_2_), channel_id=1, source_target_pairs={{0,8},{8,16},{16,24},{24,0},{1,9},{9,17},{17,25},{25,1},{2,10},{10... | collective-permute-start | bytes 393224 | tf_op jit(solution)/shard_map/ppermute | solution.py:683
  76.9 2.2 %project_local.4 = (bf16[128,512]{1,0:T(8,128)(2,1)S(1)}, bf16[256,256]{1,0:T(8,128)(2,1)S(1)}, bf16[256,256]{1,0:T(8,128)(2,1)S(1)}, bf16[128,256]{1,0:T(8,128)(2,1)S(1)}) custom-call(bf16[64,2048]{1,0:T(8,128)(2,1)S(1)} %get-tuple-element.85.refs_0_, bf16[64,2048]{1,0:T(8,128)(2,1)S(1)} %get-tuple-element.82.mine_ref.refs_1_, ...), custom_call_target="tpu_custom_call" | custom-call | tf_op jit(solution)/shard_map/project_local/pallas_call | solution.py:434
  79.2 0.6 turned.8.refs_12_.weight_ref
  79.8 0.6 turned.7.refs_11_.weight_ref
  80.4 0.2 collective-permute-done.8.refs_0_.refs_1_
  80.5 0.6 attend.8.refs_9_
  81.1 1.4 collective-permute-done.6.refs_0_
  82.5 0.6 attend.9
  83.1 1.3 collective-permute-done.10.got_ref
  84.4 16.8 %all-gather.3 = bf16[768,512]{1,0:T(8,128)(2,1)S(1)} all-gather(bf16[192,512]{1,0:T(8,128)(2,1)S(1)} %join.4), channel_id=5, replica_groups={{0,2,6,4},{1,3,7,5},{8,10,14,12},{9,11,15,13},{16,18,22,20},{17,19,23,2..., dimensions={0}, use_global_device_ids=true | all-gather | bytes 983040 | tf_op jit(solution)/shard_map/all_gather | solution.py:657
  101.3 0.6 out_project.4
  101.9 16.2 %all-gather.4 = bf16[768,512]{1,0:T(8,128)(2,1)S(1)} all-gather(bf16[192,512]{1,0:T(8,128)(2,1)S(1)} %out_project.4), channel_id=6, replica_groups={{0,2,6,4},{1,3,7,5},{8,10,14,12},{9,11,15,13},{16,18,22,20},{17,19,23,2..., dimensions={0}, use_global_device_ids=true | all-gather | bytes 983040 | tf_op jit(solution)/shard_map/all_gather | solution.py:657
  118.1 0.4 update.7
  118.5 0.5 update.6
  119.0 0.6 collective-permute-start.12
  119.7 0.4 collective-permute-done.13.other_ref.refs_5_
  120.1 0.4 project_piece.7.refs_7_
  120.6 0.2 collective-permute-done.12.other_ref.refs_4_
  120.8 0.4 project_piece.6.refs_6_.refs_2_
  121.2 2.8 %collective-permute-start.15 = (bf16[128,512]{1,0:T(8,128)(2,1)S(1)}, bf16[128,512]{1,0:T(8,128)(2,1)S(1)}, u32[]{:S(2)}, u32[]{:S(2)}) collective-permute-start(bf16[128,512]{1,0:T(8,128)(2,1)S(1)} %project_piece.6.refs_6_.refs_2_), channel_id=1, source_target_pairs={{0,8},{8,16},{16,24},{24,0},{1,9},{9,17},{17,25},{25,1},{2,10},{10... | collective-permute-start | bytes 393224 | tf_op jit(solution)/shard_map/ppermute | solution.py:683
  124.0 2.2 %project_local.5 = (bf16[128,512]{1,0:T(8,128)(2,1)S(1)}, bf16[256,256]{1,0:T(8,128)(2,1)S(1)}, bf16[256,256]{1,0:T(8,128)(2,1)S(1)}, bf16[128,256]{1,0:T(8,128)(2,1)S(1)}) custom-call(bf16[64,2048]{1,0:T(8,128)(2,1)S(1)} %get-tuple-element.100.refs_0_, bf16[64,2048]{1,0:T(8,128)(2,1)S(1)} %get-tuple-element.101.mine_ref.refs_1_, ...), custom_call_target="tpu_custom_call" | custom-call | tf_op jit(solution)/shard_map/project_local/pallas_call | solution.py:434
  126.3 0.6 turned.9.refs_11_.weight_ref
  126.9 0.9 collective-permute-done.16.refs_0_.refs_1_
  127.8 0.6 attend.10.refs_9_
  128.4 1.4 collective-permute-done.15.refs_0_
  129.8 0.6 attend.11
  130.5 0.5 collective-permute-start.14
  131.0 0.8 collective-permute-done.17.got_ref
  131.8 17.3 %all-gather.5 = bf16[768,512]{1,0:T(8,128)(2,1)S(1)} all-gather(bf16[192,512]{1,0:T(8,128)(2,1)S(1)} %join.5), channel_id=7, replica_groups={{0,2,6,4},{1,3,7,5},{8,10,14,12},{9,11,15,13},{16,18,22,20},{17,19,23,2..., dimensions={0}, use_global_device_ids=true | all-gather | bytes 983040 | tf_op jit(solution)/shard_map/all_gather | solution.py:657
  149.0 0.7 out_project.5
  149.8 0.5 collective-permute-start.19
  150.3 0.8 collective-permute-done.19
  151.1 1.0 collective-permute-start.20
  152.1 1.4 collective-permute-start.21
  153.6 1.8 %collective-permute-start.22 = (f32[1,384]{1,0:T(1,128)S(1)}, f32[1,384]{1,0:T(1,128)S(1)}, u32[]{:S(2)}, u32[]{:S(2)}) collective-permute-start(f32[1,384]{1,0:T(1,128)S(1)} %add.3.refs_0_), channel_id=1, source_target_pairs={{0,6},{1,7},{2,0},{3,1},{4,2},{5,3},{6,4},{7,5},{8,14},{9,15},{10,... | collective-permute-start | bytes 4616 | tf_op jit(solution)/shard_map/ppermute | solution.py:676
  155.3 1.2 collective-permute-done.20.refs_1_
  156.6 0.5 collective-permute-done.22.refs_3_
  157.1 0.9 finish.1
  (32 shorter events, 1.0 us)
Async XLA Ops:
  0.0 31.8 %collective-permute-start.3 = (bf16[3,256,2048]{2,1,0:T(8,128)(2,1)}, bf16[3,256,2048]{2,1,0:T(8,128)(2,1)S(1)}, u32[]{:S(2)}, u32[]{:S(2)}) collective-permute-start(bf16[3,256,2048]{2,1,0:T(8,128)(2,1)} %refs_0_.11), channel_id=1, source_target_pairs={{0,1},{1,0},{2,3},{3,2},{4,5},{5,4},{6,7},{7,6},{8,9},{9,8},{10,11... | collective-permute-start | bytes 9437192 | tf_op jit(solution)/shard_map/ppermute | solution.py:651
  20.2 2.3 %collective-permute-start = (bf16[4,384,256]{2,1,0:T(8,128)(2,1)S(1)}, bf16[4,384,256]{2,1,0:T(8,128)(2,1)S(1)}, u32[]{:S(2)}, u32[]{:S(2)}) collective-permute-start(bf16[4,384,256]{2,1,0:T(8,128)(2,1)S(1)} %bitcast.6), channel_id=1, source_target_pairs={{0,1},{1,0},{2,3},{3,2},{4,5},{5,4},{6,7},{7,6},{8,9},{9,8},{10,11... | collective-permute-start | bytes 2359304 | tf_op jit(solution)/shard_map/ppermute | solution.py:651
  23.5 7.7 %collective-permute-start.2 = (bf16[144,512]{1,0:T(8,128)(2,1)S(1)}, bf16[144,512]{1,0:T(8,128)(2,1)S(1)}, u32[]{:S(2)}, u32[]{:S(2)}) collective-permute-start(bf16[144,512]{1,0:T(8,128)(2,1)S(1)} %get-tuple-element.66.refs_6_), channel_id=1, source_target_pairs={{0,8},{8,16},{16,24},{24,0},{1,9},{9,17},{17,25},{25,1},{2,10},{10... | collective-permute-start | bytes 442376 | tf_op jit(solution)/shard_map/ppermute | solution.py:683
  26.1 7.8 %collective-permute-start.1 = (bf16[144,512]{1,0:T(8,128)(2,1)S(1)}, bf16[144,512]{1,0:T(8,128)(2,1)S(1)}, u32[]{:S(2)}, u32[]{:S(2)}) collective-permute-start(bf16[144,512]{1,0:T(8,128)(2,1)S(1)} %get-tuple-element.65.refs_5_.refs_2_), channel_id=1, source_target_pairs={{0,8},{8,16},{16,24},{24,0},{1,9},{9,17},{17,25},{25,1},{2,10},{10... | collective-permute-start | bytes 442376 | tf_op jit(solution)/shard_map/ppermute | solution.py:683
  27.6 2.4 %copy-start = (bf16[3,256,2048]{2,1,0:T(8,128)(2,1)S(1)}, bf16[3,256,2048]{2,1,0:T(8,128)(2,1)}, u32[]{:S(2)}) copy-start(bf16[3,256,2048]{2,1,0:T(8,128)(2,1)} %refs_10_.3) | copy-start | bytes 9437188
  27.6 2.8 %copy-start.1 = (bf16[3,256,2048]{2,1,0:T(8,128)(2,1)S(1)}, bf16[3,256,2048]{2,1,0:T(8,128)(2,1)}, u32[]{:S(2)}) copy-start(bf16[3,256,2048]{2,1,0:T(8,128)(2,1)} %refs_11_.3) | copy-start | bytes 9437188
  30.5 1.9 %copy-start.2 = (bf16[3,256,2048]{2,1,0:T(8,128)(2,1)S(1)}, bf16[3,256,2048]{2,1,0:T(8,128)(2,1)}, u32[]{:S(2)}) copy-start(bf16[3,256,2048]{2,1,0:T(8,128)(2,1)} %refs_0_.11) | copy-start | bytes 9437188
  34.5 1.4 collective-permute-start.4
  71.1 1.6 %collective-permute-start.7 = (bf16[64,2048]{1,0:T(8,128)(2,1)S(1)}, bf16[64,2048]{1,0:T(8,128)(2,1)S(1)}, u32[]{:S(2)}, u32[]{:S(2)}) collective-permute-start(bf16[64,2048]{1,0:T(8,128)(2,1)S(1)} %get-tuple-element.84.mine_ref.refs_2_), channel_id=1, source_target_pairs={{0,1},{1,0},{2,3},{3,2},{4,5},{5,4},{6,7},{7,6},{8,9},{9,8},{10,11... | collective-permute-start | bytes 786440 | tf_op jit(solution)/shard_map/ppermute | solution.py:651
  71.2 5.7 %copy-start.3 = (bf16[3,256,2048]{2,1,0:T(8,128)(2,1)S(1)}, bf16[3,256,2048]{2,1,0:T(8,128)(2,1)}, u32[]{:S(2)}) copy-start(bf16[3,256,2048]{2,1,0:T(8,128)(2,1)} %refs_12_.3) | copy-start | bytes 9437188
  71.2 5.7 %copy-start.4 = (bf16[3,256,2048]{2,1,0:T(8,128)(2,1)S(1)}, bf16[3,256,2048]{2,1,0:T(8,128)(2,1)}, u32[]{:S(2)}) copy-start(bf16[3,256,2048]{2,1,0:T(8,128)(2,1)} %refs_13_.3) | copy-start | bytes 9437188
  71.8 2.1 %collective-permute-start.5 = (bf16[64,2048]{1,0:T(8,128)(2,1)S(1)}, bf16[64,2048]{1,0:T(8,128)(2,1)S(1)}, u32[]{:S(2)}, u32[]{:S(2)}) collective-permute-start(bf16[64,2048]{1,0:T(8,128)(2,1)S(1)} %get-tuple-element.82.mine_ref.refs_1_), channel_id=1, source_target_pairs={{0,1},{1,0},{2,3},{3,2},{4,5},{5,4},{6,7},{7,6},{8,9},{9,8},{10,11... | collective-permute-start | bytes 786440 | tf_op jit(solution)/shard_map/ppermute | solution.py:651
  72.3 4.6 %collective-permute-start.9 = (bf16[64,2048]{1,0:T(8,128)(2,1)S(1)}, bf16[64,2048]{1,0:T(8,128)(2,1)S(1)}, u32[]{:S(2)}, u32[]{:S(2)}) collective-permute-start(bf16[64,2048]{1,0:T(8,128)(2,1)S(1)} %get-tuple-element.85.refs_0_), channel_id=1, source_target_pairs={{0,1},{1,0},{2,3},{3,2},{4,5},{5,4},{6,7},{7,6},{8,9},{9,8},{10,11... | collective-permute-start | bytes 786440 | tf_op jit(solution)/shard_map/ppermute | solution.py:651
  73.2 7.3 %collective-permute-start.8 = (bf16[128,512]{1,0:T(8,128)(2,1)S(1)}, bf16[128,512]{1,0:T(8,128)(2,1)S(1)}, u32[]{:S(2)}, u32[]{:S(2)}) collective-permute-start(bf16[128,512]{1,0:T(8,128)(2,1)S(1)} %project_piece.5.refs_7_), channel_id=1, source_target_pairs={{0,8},{8,16},{16,24},{24,0},{1,9},{9,17},{17,25},{25,1},{2,10},{10... | collective-permute-start | bytes 393224 | tf_op jit(solution)/shard_map/ppermute | solution.py:683
  74.3 8.2 %collective-permute-start.6 = (bf16[128,512]{1,0:T(8,128)(2,1)S(1)}, bf16[128,512]{1,0:T(8,128)(2,1)S(1)}, u32[]{:S(2)}, u32[]{:S(2)}) collective-permute-start(bf16[128,512]{1,0:T(8,128)(2,1)S(1)} %project_piece.4.refs_6_.refs_2_), channel_id=1, source_target_pairs={{0,8},{8,16},{16,24},{24,0},{1,9},{9,17},{17,25},{25,1},{2,10},{10... | collective-permute-start | bytes 393224 | tf_op jit(solution)/shard_map/ppermute | solution.py:683
  83.1 1.4 collective-permute-start.10
  118.5 1.6 %collective-permute-start.13 = (bf16[64,2048]{1,0:T(8,128)(2,1)S(1)}, bf16[64,2048]{1,0:T(8,128)(2,1)S(1)}, u32[]{:S(2)}, u32[]{:S(2)}) collective-permute-start(bf16[64,2048]{1,0:T(8,128)(2,1)S(1)} %get-tuple-element.102.mine_ref.refs_2_), channel_id=1, source_target_pairs={{0,1},{1,0},{2,3},{3,2},{4,5},{5,4},{6,7},{7,6},{8,9},{9,8},{10,11... | collective-permute-start | bytes 786440 | tf_op jit(solution)/shard_map/ppermute | solution.py:651
  119.0 1.7 %collective-permute-start.12 = (bf16[64,2048]{1,0:T(8,128)(2,1)S(1)}, bf16[64,2048]{1,0:T(8,128)(2,1)S(1)}, u32[]{:S(2)}, u32[]{:S(2)}) collective-permute-start(bf16[64,2048]{1,0:T(8,128)(2,1)S(1)} %get-tuple-element.101.mine_ref.refs_1_), channel_id=1, source_target_pairs={{0,1},{1,0},{2,3},{3,2},{4,5},{5,4},{6,7},{7,6},{8,9},{9,8},{10,11... | collective-permute-start | bytes 786440 | tf_op jit(solution)/shard_map/ppermute | solution.py:651
  119.6 4.4 %collective-permute-start.11 = (bf16[64,2048]{1,0:T(8,128)(2,1)S(1)}, bf16[64,2048]{1,0:T(8,128)(2,1)S(1)}, u32[]{:S(2)}, u32[]{:S(2)}) collective-permute-start(bf16[64,2048]{1,0:T(8,128)(2,1)S(1)} %get-tuple-element.100.refs_0_), channel_id=1, source_target_pairs={{0,1},{1,0},{2,3},{3,2},{4,5},{5,4},{6,7},{7,6},{8,9},{9,8},{10,11... | collective-permute-start | bytes 786440 | tf_op jit(solution)/shard_map/ppermute | solution.py:651
  120.5 7.3 %collective-permute-start.16 = (bf16[128,512]{1,0:T(8,128)(2,1)S(1)}, bf16[128,512]{1,0:T(8,128)(2,1)S(1)}, u32[]{:S(2)}, u32[]{:S(2)}) collective-permute-start(bf16[128,512]{1,0:T(8,128)(2,1)S(1)} %project_piece.7.refs_7_), channel_id=1, source_target_pairs={{0,8},{8,16},{16,24},{24,0},{1,9},{9,17},{17,25},{25,1},{2,10},{10... | collective-permute-start | bytes 393224 | tf_op jit(solution)/shard_map/ppermute | solution.py:683
  121.2 8.6 %collective-permute-start.15 = (bf16[128,512]{1,0:T(8,128)(2,1)S(1)}, bf16[128,512]{1,0:T(8,128)(2,1)S(1)}, u32[]{:S(2)}, u32[]{:S(2)}) collective-permute-start(bf16[128,512]{1,0:T(8,128)(2,1)S(1)} %project_piece.6.refs_6_.refs_2_), channel_id=1, source_target_pairs={{0,8},{8,16},{16,24},{24,0},{1,9},{9,17},{17,25},{25,1},{2,10},{10... | collective-permute-start | bytes 393224 | tf_op jit(solution)/shard_map/ppermute | solution.py:683
  130.4 1.4 collective-permute-start.17
  130.5 24.9 %collective-permute-start.14 = (bf16[192,256]{1,0:T(8,128)(2,1)S(1)}, bf16[192,256]{1,0:T(8,128)(2,1)S(1)}, u32[]{:S(2)}, u32[]{:S(2)}) collective-permute-start(bf16[192,256]{1,0:T(8,128)(2,1)S(1)} %get-tuple-element.106), channel_id=1, source_target_pairs={{0,1},{1,0},{2,3},{3,2},{4,5},{5,4},{6,7},{7,6},{8,9},{9,8},{10,11... | collective-permute-start | bytes 294920 | tf_op jit(solution)/shard_map/ppermute | solution.py:651
  149.7 7.4 %collective-permute-start.18 = (bf16[192,256]{1,0:T(8,128)(2,1)S(1)}, bf16[192,256]{1,0:T(8,128)(2,1)S(1)}, u32[]{:S(2)}, u32[]{:S(2)}) collective-permute-start(bf16[192,256]{1,0:T(8,128)(2,1)S(1)} %get-tuple-element.113), channel_id=1, source_target_pairs={{0,1},{1,0},{2,3},{3,2},{4,5},{5,4},{6,7},{7,6},{8,9},{9,8},{10,11... | collective-permute-start | bytes 294920 | tf_op jit(solution)/shard_map/ppermute | solution.py:651
  149.8 1.3 collective-permute-start.19
  151.1 5.4 %collective-permute-start.20 = (f32[1,384]{1,0:T(1,128)S(1)}, f32[1,384]{1,0:T(1,128)S(1)}, u32[]{:S(2)}, u32[]{:S(2)}) collective-permute-start(f32[1,384]{1,0:T(1,128)S(1)} %add.3.refs_0_), channel_id=1, source_target_pairs={{0,2},{1,3},{2,4},{3,5},{4,6},{5,7},{6,0},{7,1},{8,10},{9,11},{10,... | collective-permute-start | bytes 4616 | tf_op jit(solution)/shard_map/ppermute | solution.py:676
  152.1 4.5 %collective-permute-start.21 = (f32[1,384]{1,0:T(1,128)S(1)}, f32[1,384]{1,0:T(1,128)S(1)}, u32[]{:S(2)}, u32[]{:S(2)}) collective-permute-start(f32[1,384]{1,0:T(1,128)S(1)} %add.3.refs_0_), channel_id=1, source_target_pairs={{0,4},{1,5},{2,6},{3,7},{4,0},{5,1},{6,2},{7,3},{8,12},{9,13},{10,... | collective-permute-start | bytes 4616 | tf_op jit(solution)/shard_map/ppermute | solution.py:676
  153.6 3.6 %collective-permute-start.22 = (f32[1,384]{1,0:T(1,128)S(1)}, f32[1,384]{1,0:T(1,128)S(1)}, u32[]{:S(2)}, u32[]{:S(2)}) collective-permute-start(f32[1,384]{1,0:T(1,128)S(1)} %add.3.refs_0_), channel_id=1, source_target_pairs={{0,6},{1,7},{2,0},{3,1},{4,2},{5,3},{6,4},{7,5},{8,14},{9,15},{10,... | collective-permute-start | bytes 4616 | tf_op jit(solution)/shard_map/ppermute | solution.py:676

commit v8 on v7

--- a/solution.py
+++ b/solution.py
@@ -200,8 +200,9 @@
     return [(ref, slot, z * width) for slot, z in enumerate(ring_order(ref.shape[0]))]
 
 
-def update_body(layer, groups, blocks_ref, post_ref, pre_ref, *refs):
+def update_body(layer, groups, waited, blocks_ref, post_ref, pre_ref, *refs):
     count = len(groups)
+    refs = refs[waited:]
     olds, news, normed = [refs[at * count : (at + 1) * count] for at in range(3)]
     placed = chip_columns(blocks_ref)
     for index, group in enumerate(groups):
@@ -217,11 +218,11 @@
         )
 
 
-def update(layer, groups, blocks, post, pre, olds):
+def update(layer, groups, blocks, post, pre, olds, waited):
     shape = jax.ShapeDtypeStruct((HALF, D), jnp.bfloat16)
-    operands = (blocks, post, pre, *olds)
+    operands = (blocks, post, pre, *waited, *olds)
     made = pl.pallas_call(
-        functools.partial(update_body, layer, groups),
+        functools.partial(update_body, layer, groups, len(waited)),
         out_shape=(shape,) * (2 * len(groups)),
         in_specs=[vmem] * len(operands),
         out_specs=(vmem,) * (2 * len(groups)),
@@ -531,6 +532,7 @@
 
 
 def out_body(last, blocks_ref, weight_ref, *refs):
+    refs = refs[1:] if last else refs
     mixed_ref = refs[-1]
     width = blocks_ref.shape[2]
     own = width // CORES
@@ -565,7 +567,7 @@
         by_core(place)
 
 
-def out_project(blocks, weight, last):
+def out_project(blocks, weight, last, waited):
     rows, width = blocks.shape[1:]
     bf = jnp.bfloat16
     shapes = [jax.ShapeDtypeStruct((rows, width), bf)]
@@ -575,12 +577,12 @@
     return pl.pallas_call(
         functools.partial(out_body, last),
         out_shape=tuple(shapes),
-        in_specs=[vmem] * 2,
+        in_specs=[vmem] * (2 + len(waited)),
         out_specs=(vmem,) * len(shapes),
         scratch_shapes=[pltpu.VMEM((rows, D), bf)],
         compiler_params=params,
         name="out_project",
-    )(blocks, weight)
+    )(blocks, weight, *waited)
 
 
 def chip_slice(width):
@@ -667,15 +669,15 @@
     return (own, partner(own)) if own.shape[2] < D else (own,)
 
 
-def total_over_tp(square):
+def total_over_tp(square, give):
     size = lax.axis_size("tp")
     if size > 8:
-        return (lax.psum(square, "tp"),)
-    both = square + partner(square)
+        return (lax.psum(square, "tp"),), give
+    both, give = lax.optimization_barrier((square + partner(square), give))
     return (both,) + tuple(
         lax.ppermute(both, "tp", [(i, (i + hop) % size) for i in range(size)])
         for hop in range(CORES, size, CORES)
-    )
+    ), give
 
 
 def from_behind(block):
@@ -711,7 +713,9 @@
         if layer:
             late = tuple(range(groups - 1))
             for batch in ((groups - 1,), late[::-1]):
-                made = update(layer, batch, blocks, post, pre, [halves[at] for at in batch])
+                olds = [halves[at] for at in batch]
+                waited = normed[groups - 1 :] if batch == late[::-1] else ()
+                made = update(layer, batch, blocks, post, pre, olds, waited)
                 for at, half, row in zip(batch, *made):
                     halves[at], normed[at], other[at] = half, row, partner(row)
         for group in reversed(range(first, groups)):
@@ -760,11 +764,11 @@
                 done = [made[0], *done]
         keep, give = made
         mixed = gather_chips(join(keep, partner(give)))
-        result = out_project(mixed, ready[0], last)
+        result = out_project(mixed, ready[0], last, (old_got,) if last else ())
         if not last:
             blocks = gather_chips(result[0])
     keep, give, square = result
-    totals = total_over_tp(square)
+    totals, give = total_over_tp(square, give)
     return finish(old_keep, old_got, keep, partner(give), post, totals)
 
 

time: 158 us -> 158 us (level)
  transfers between devices with their start and end apart: 23 -> 23, of which waited for: 16 -> 15; matrix products, arithmetic and copies ran while one was open for 0% -> 0% of each run, Pallas kernels for 12% -> 12%
where the time goes in v8:
time: 158 us
  blocking collectives  104 us (66%)
  Pallas kernels  23.8 us (15%)
  starting transfers between devices  16.4 us (10%)
  waiting for transfers between devices  12.1 us (8%)
    all_gather x6, blocking collectives, gather_chips(): return lax.all_gather(x, 'tp', axis=0, axis_index_groups=lines)  104 us
    ppermute x6, starting transfers between devices, from_behind(): return lax.ppermute(block, 'sp', [(i, (i + 1) % size) for i in range(size)])  9.27 us
    pallas_call x3, Pallas kernels, project_local(): pl.pallas_call(functools.partial(local_body, layer, count), out_shape=tup...  6.86 us
    ppermute x14, waiting for transfers between devices, partner(): return lax.ppermute(x, 'tp', [(i, i ^ 1) for i in range(size)])  5.46 us
    ppermute x6, waiting for transfers between devices, from_behind(): return lax.ppermute(block, 'sp', [(i, (i + 1) % size) for i in range(size)])  4.91 us
    ppermute x3, starting transfers between devices, total_over_tp(): lax.ppermute(both, 'tp', [(i, (i + hop) % size) for i in range(size)])  4.25 us
    pallas_call x6, Pallas kernels, attend(): pl.pallas_call(functools.partial(attend_body, layer, group, len(done), le...  3.4 us
  transfers between devices with their start and end apart: 23, of which 15 were waited for; matrix products, arithmetic and copies ran while one was open for 0% of the time, Pallas kernels for 12%

profile of v8, /device:TPU:0, one launch (start us, length us, event | category | flops | bytes accessed | tf_op | source)
XLA Modules:
  0.0 158.0 jit_solution(10484477088511791313)
XLA Ops:
  0.0 0.5 collective-permute-start.3
  0.5 19.7 %all-gather = bf16[1536,256]{1,0:T(8,128)(2,1)S(1)} all-gather(bf16[384,256]{1,0:T(8,128)(2,1)} %param.10), channel_id=2, replica_groups={{0,2,6,4},{1,3,7,5},{8,10,14,12},{9,11,15,13},{16,18,22,20},{17,19,23,2..., dimensions={0}, use_global_device_ids=true | all-gather | bytes 983040 | tf_op jit(solution)/shard_map/all_gather | solution.py:659
  20.2 2.3 %setup.1 = (bf16[4,256,2048]{2,1,0:T(8,128)(2,1)S(1)}, f32[3,2048]{1,0:T(4,128)S(1)}, f32[3,2048]{1,0:T(4,128)S(1)}, s32[1,384]{1,0:T(1,128)S(1)}, f32[1,128,384...) custom-call(f32[3,4,257]{2,1,0:T(4,128)} %bias_hbm.1, ...), custom_call_target="tpu_custom_call" | custom-call | tf_op jit(solution)/shard_map/setup/pallas_call | solution.py:109
  22.5 1.0 first_piece.3
  23.5 1.5 collective-permute-start.2
  25.1 1.0 first_piece.2
  26.1 1.6 collective-permute-start.1
  27.7 2.4 %project_local.3 = (bf16[64,2048]{1,0:T(8,128)(2,1)S(1)}, bf16[128,512]{1,0:T(8,128)(2,1)S(1)}, bf16[256,256]{1,0:T(8,128)(2,1)S(1)}, bf16[256,256]{1,0:T(8,128)(2,1)S(1)}, bf16[128,256]{1,0:T(8,128)(2,1)S(1)}) custom-call(bf16[4,384,256]{2,1,0:T(8,128)(2,1)S(1)} %bitcast.9, bf16[4,384,256]{2,1,0:T(8,128)(2,1)S(1)} %collective-permute-done.refs_1_, ...), custom_call_target="tpu_custom_call" | custom-call | tf_op jit(solution)/shard_map/project_local/pallas_call | solution.py:435
  30.1 0.4 copy-done.1
  30.5 0.6 turned.6.refs_11_.weight_ref
  31.2 0.6 attend.6
  31.8 0.6 copy-done.2
  32.4 0.6 turned.5.refs_10_.weight_ref
  33.0 0.9 collective-permute-done.1.refs_0_
  33.9 0.6 attend.7
  34.6 1.3 collective-permute-done.4.got_ref
  35.9 17.4 %all-gather.1 = bf16[768,512]{1,0:T(8,128)(2,1)S(1)} all-gather(bf16[192,512]{1,0:T(8,128)(2,1)S(1)} %join.3), channel_id=3, replica_groups={{0,2,6,4},{1,3,7,5},{8,10,14,12},{9,11,15,13},{16,18,22,20},{17,19,23,2..., dimensions={0}, use_global_device_ids=true | all-gather | bytes 983040 | tf_op jit(solution)/shard_map/all_gather | solution.py:659
  53.3 0.6 out_project.3
  53.9 16.9 %all-gather.2 = bf16[768,512]{1,0:T(8,128)(2,1)S(1)} all-gather(bf16[192,512]{1,0:T(8,128)(2,1)S(1)} %out_project.3), channel_id=4, replica_groups={{0,2,6,4},{1,3,7,5},{8,10,14,12},{9,11,15,13},{16,18,22,20},{17,19,23,2..., dimensions={0}, use_global_device_ids=true | all-gather | bytes 983040 | tf_op jit(solution)/shard_map/all_gather | solution.py:659
  70.7 0.4 update.4
  71.2 0.5 update.5
  71.7 0.5 collective-permute-start.5
  72.3 0.4 collective-permute-done.7.other_ref.refs_5_
  72.7 0.4 project_piece.5.refs_7_
  73.1 0.7 collective-permute-start.8
  73.8 0.4 project_piece.4.refs_6_.refs_2_
  74.3 2.6 %collective-permute-start.6 = (bf16[128,512]{1,0:T(8,128)(2,1)S(1)}, bf16[128,512]{1,0:T(8,128)(2,1)S(1)}, u32[]{:S(2)}, u32[]{:S(2)}) collective-permute-start(bf16[128,512]{1,0:T(8,128)(2,1)S(1)} %project_piece.4.refs_6_.refs_2_), channel_id=1, source_target_pairs={{0,8},{8,16},{16,24},{24,0},{1,9},{9,17},{17,25},{25,1},{2,10},{10... | collective-permute-start | bytes 393224 | tf_op jit(solution)/shard_map/ppermute | solution.py:685
  76.9 2.2 %project_local.4 = (bf16[128,512]{1,0:T(8,128)(2,1)S(1)}, bf16[256,256]{1,0:T(8,128)(2,1)S(1)}, bf16[256,256]{1,0:T(8,128)(2,1)S(1)}, bf16[128,256]{1,0:T(8,128)(2,1)S(1)}) custom-call(bf16[64,2048]{1,0:T(8,128)(2,1)S(1)} %get-tuple-element.87.refs_0_, bf16[64,2048]{1,0:T(8,128)(2,1)S(1)} %get-tuple-element.86.mine_ref.refs_1_, ...), custom_call_target="tpu_custom_call" | custom-call | tf_op jit(solution)/shard_map/project_local/pallas_call | solution.py:435
  79.1 0.6 turned.8.refs_12_.weight_ref
  79.7 0.6 turned.7.refs_11_.weight_ref
  80.3 0.2 collective-permute-done.8.refs_0_.refs_1_
  80.5 0.6 attend.8.refs_9_
  81.0 1.4 collective-permute-done.6.refs_0_
  82.4 0.6 attend.9
  83.1 1.3 collective-permute-done.10.got_ref
  84.4 16.9 %all-gather.3 = bf16[768,512]{1,0:T(8,128)(2,1)S(1)} all-gather(bf16[192,512]{1,0:T(8,128)(2,1)S(1)} %join.4), channel_id=5, replica_groups={{0,2,6,4},{1,3,7,5},{8,10,14,12},{9,11,15,13},{16,18,22,20},{17,19,23,2..., dimensions={0}, use_global_device_ids=true | all-gather | bytes 983040 | tf_op jit(solution)/shard_map/all_gather | solution.py:659
  101.3 0.6 out_project.4
  101.9 16.3 %all-gather.4 = bf16[768,512]{1,0:T(8,128)(2,1)S(1)} all-gather(bf16[192,512]{1,0:T(8,128)(2,1)S(1)} %out_project.4), channel_id=6, replica_groups={{0,2,6,4},{1,3,7,5},{8,10,14,12},{9,11,15,13},{16,18,22,20},{17,19,23,2..., dimensions={0}, use_global_device_ids=true | all-gather | bytes 983040 | tf_op jit(solution)/shard_map/all_gather | solution.py:659
  118.1 0.4 update.6
  118.6 0.5 update.7
  119.1 0.6 collective-permute-start.12
  119.7 0.4 collective-permute-done.13.other_ref.refs_5_
  120.1 0.4 project_piece.7.refs_7_
  120.6 0.2 collective-permute-done.12.other_ref.refs_4_
  120.8 0.4 project_piece.6.refs_6_.refs_2_
  121.2 2.8 %collective-permute-start.15 = (bf16[128,512]{1,0:T(8,128)(2,1)S(1)}, bf16[128,512]{1,0:T(8,128)(2,1)S(1)}, u32[]{:S(2)}, u32[]{:S(2)}) collective-permute-start(bf16[128,512]{1,0:T(8,128)(2,1)S(1)} %project_piece.6.refs_6_.refs_2_), channel_id=1, source_target_pairs={{0,8},{8,16},{16,24},{24,0},{1,9},{9,17},{17,25},{25,1},{2,10},{10... | collective-permute-start | bytes 393224 | tf_op jit(solution)/shard_map/ppermute | solution.py:685
  124.1 2.2 %project_local.5 = (bf16[128,512]{1,0:T(8,128)(2,1)S(1)}, bf16[256,256]{1,0:T(8,128)(2,1)S(1)}, bf16[256,256]{1,0:T(8,128)(2,1)S(1)}, bf16[128,256]{1,0:T(8,128)(2,1)S(1)}) custom-call(bf16[64,2048]{1,0:T(8,128)(2,1)S(1)} %get-tuple-element.103.refs_0_, bf16[64,2048]{1,0:T(8,128)(2,1)S(1)} %get-tuple-element.104.mine_ref.refs_1_, ...), custom_call_target="tpu_custom_call" | custom-call | tf_op jit(solution)/shard_map/project_local/pallas_call | solution.py:435
  126.4 0.6 turned.9.refs_11_.weight_ref
  127.0 0.9 collective-permute-done.16.refs_0_.refs_1_
  127.9 0.6 attend.10.refs_9_
  128.4 1.4 collective-permute-done.15.refs_0_
  129.9 0.6 attend.11
  130.5 0.5 collective-permute-start.14
  131.0 0.8 collective-permute-done.17.got_ref
  131.8 17.3 %all-gather.5 = bf16[768,512]{1,0:T(8,128)(2,1)S(1)} all-gather(bf16[192,512]{1,0:T(8,128)(2,1)S(1)} %join.5), channel_id=7, replica_groups={{0,2,6,4},{1,3,7,5},{8,10,14,12},{9,11,15,13},{16,18,22,20},{17,19,23,2..., dimensions={0}, use_global_device_ids=true | all-gather | bytes 983040 | tf_op jit(solution)/shard_map/all_gather | solution.py:659
  149.1 0.7 out_project.5
  149.9 1.1 collective-permute-done.18
  151.0 0.2 collective-permute-start.19
  151.2 0.9 collective-permute-start.20
  152.1 1.4 collective-permute-start.21
  153.5 2.0 %collective-permute-start.22 = (f32[1,384]{1,0:T(1,128)S(1)}, f32[1,384]{1,0:T(1,128)S(1)}, u32[]{:S(2)}, u32[]{:S(2)}) collective-permute-start(f32[1,384]{1,0:T(1,128)S(1)} %add.3.refs_0_), channel_id=1, source_target_pairs={{0,6},{1,7},{2,0},{3,1},{4,2},{5,3},{6,4},{7,5},{8,14},{9,15},{10,... | collective-permute-start | bytes 4616 | tf_op jit(solution)/shard_map/ppermute | solution.py:678
  155.5 1.1 collective-permute-done.20.refs_1_
  156.6 0.6 collective-permute-done.22.refs_3_
  157.2 0.9 finish.1
  (32 shorter events, 0.9 us)
Async XLA Ops:
  0.0 31.8 %collective-permute-start.3 = (bf16[3,256,2048]{2,1,0:T(8,128)(2,1)}, bf16[3,256,2048]{2,1,0:T(8,128)(2,1)S(1)}, u32[]{:S(2)}, u32[]{:S(2)}) collective-permute-start(bf16[3,256,2048]{2,1,0:T(8,128)(2,1)} %refs_0_.11), channel_id=1, source_target_pairs={{0,1},{1,0},{2,3},{3,2},{4,5},{5,4},{6,7},{7,6},{8,9},{9,8},{10,11... | collective-permute-start | bytes 9437192 | tf_op jit(solution)/shard_map/ppermute | solution.py:653
  20.2 2.3 %collective-permute-start = (bf16[4,384,256]{2,1,0:T(8,128)(2,1)S(1)}, bf16[4,384,256]{2,1,0:T(8,128)(2,1)S(1)}, u32[]{:S(2)}, u32[]{:S(2)}) collective-permute-start(bf16[4,384,256]{2,1,0:T(8,128)(2,1)S(1)} %bitcast.6), channel_id=1, source_target_pairs={{0,1},{1,0},{2,3},{3,2},{4,5},{5,4},{6,7},{7,6},{8,9},{9,8},{10,11... | collective-permute-start | bytes 2359304 | tf_op jit(solution)/shard_map/ppermute | solution.py:653
  23.5 7.7 %collective-permute-start.2 = (bf16[144,512]{1,0:T(8,128)(2,1)S(1)}, bf16[144,512]{1,0:T(8,128)(2,1)S(1)}, u32[]{:S(2)}, u32[]{:S(2)}) collective-permute-start(bf16[144,512]{1,0:T(8,128)(2,1)S(1)} %get-tuple-element.68.refs_6_), channel_id=1, source_target_pairs={{0,8},{8,16},{16,24},{24,0},{1,9},{9,17},{17,25},{25,1},{2,10},{10... | collective-permute-start | bytes 442376 | tf_op jit(solution)/shard_map/ppermute | solution.py:685
  26.1 7.8 %collective-permute-start.1 = (bf16[144,512]{1,0:T(8,128)(2,1)S(1)}, bf16[144,512]{1,0:T(8,128)(2,1)S(1)}, u32[]{:S(2)}, u32[]{:S(2)}) collective-permute-start(bf16[144,512]{1,0:T(8,128)(2,1)S(1)} %get-tuple-element.67.refs_5_.refs_2_), channel_id=1, source_target_pairs={{0,8},{8,16},{16,24},{24,0},{1,9},{9,17},{17,25},{25,1},{2,10},{10... | collective-permute-start | bytes 442376 | tf_op jit(solution)/shard_map/ppermute | solution.py:685
  27.7 2.4 %copy-start = (bf16[3,256,2048]{2,1,0:T(8,128)(2,1)S(1)}, bf16[3,256,2048]{2,1,0:T(8,128)(2,1)}, u32[]{:S(2)}) copy-start(bf16[3,256,2048]{2,1,0:T(8,128)(2,1)} %refs_10_.3) | copy-start | bytes 9437188
  27.7 2.8 %copy-start.1 = (bf16[3,256,2048]{2,1,0:T(8,128)(2,1)S(1)}, bf16[3,256,2048]{2,1,0:T(8,128)(2,1)}, u32[]{:S(2)}) copy-start(bf16[3,256,2048]{2,1,0:T(8,128)(2,1)} %refs_11_.3) | copy-start | bytes 9437188
  30.5 1.9 %copy-start.2 = (bf16[3,256,2048]{2,1,0:T(8,128)(2,1)S(1)}, bf16[3,256,2048]{2,1,0:T(8,128)(2,1)}, u32[]{:S(2)}) copy-start(bf16[3,256,2048]{2,1,0:T(8,128)(2,1)} %refs_0_.11) | copy-start | bytes 9437188
  34.5 1.4 collective-permute-start.4
  71.1 1.6 %collective-permute-start.7 = (bf16[64,2048]{1,0:T(8,128)(2,1)S(1)}, bf16[64,2048]{1,0:T(8,128)(2,1)S(1)}, u32[]{:S(2)}, u32[]{:S(2)}) collective-permute-start(bf16[64,2048]{1,0:T(8,128)(2,1)S(1)} %get-tuple-element.83.refs_0_.mine_ref.refs_2_), channel_id=1, source_target_pairs={{0,1},{1,0},{2,3},{3,2},{4,5},{5,4},{6,7},{7,6},{8,9},{9,8},{10,11... | collective-permute-start | bytes 786440 | tf_op jit(solution)/shard_map/ppermute | solution.py:653
  71.2 5.7 %copy-start.4 = (bf16[3,256,2048]{2,1,0:T(8,128)(2,1)S(1)}, bf16[3,256,2048]{2,1,0:T(8,128)(2,1)}, u32[]{:S(2)}) copy-start(bf16[3,256,2048]{2,1,0:T(8,128)(2,1)} %refs_13_.3) | copy-start | bytes 9437188
  71.7 5.2 %copy-start.3 = (bf16[3,256,2048]{2,1,0:T(8,128)(2,1)S(1)}, bf16[3,256,2048]{2,1,0:T(8,128)(2,1)}, u32[]{:S(2)}) copy-start(bf16[3,256,2048]{2,1,0:T(8,128)(2,1)} %refs_12_.3) | copy-start | bytes 9437188
  71.7 2.1 %collective-permute-start.5 = (bf16[64,2048]{1,0:T(8,128)(2,1)S(1)}, bf16[64,2048]{1,0:T(8,128)(2,1)S(1)}, u32[]{:S(2)}, u32[]{:S(2)}) collective-permute-start(bf16[64,2048]{1,0:T(8,128)(2,1)S(1)} %get-tuple-element.86.mine_ref.refs_1_), channel_id=1, source_target_pairs={{0,1},{1,0},{2,3},{3,2},{4,5},{5,4},{6,7},{7,6},{8,9},{9,8},{10,11... | collective-permute-start | bytes 786440 | tf_op jit(solution)/shard_map/ppermute | solution.py:653
  72.2 4.6 %collective-permute-start.9 = (bf16[64,2048]{1,0:T(8,128)(2,1)S(1)}, bf16[64,2048]{1,0:T(8,128)(2,1)S(1)}, u32[]{:S(2)}, u32[]{:S(2)}) collective-permute-start(bf16[64,2048]{1,0:T(8,128)(2,1)S(1)} %get-tuple-element.87.refs_0_), channel_id=1, source_target_pairs={{0,1},{1,0},{2,3},{3,2},{4,5},{5,4},{6,7},{7,6},{8,9},{9,8},{10,11... | collective-permute-start | bytes 786440 | tf_op jit(solution)/shard_map/ppermute | solution.py:653
  73.1 7.3 %collective-permute-start.8 = (bf16[128,512]{1,0:T(8,128)(2,1)S(1)}, bf16[128,512]{1,0:T(8,128)(2,1)S(1)}, u32[]{:S(2)}, u32[]{:S(2)}) collective-permute-start(bf16[128,512]{1,0:T(8,128)(2,1)S(1)} %project_piece.5.refs_7_), channel_id=1, source_target_pairs={{0,8},{8,16},{16,24},{24,0},{1,9},{9,17},{17,25},{25,1},{2,10},{10... | collective-permute-start | bytes 393224 | tf_op jit(solution)/shard_map/ppermute | solution.py:685
  74.3 8.2 %collective-permute-start.6 = (bf16[128,512]{1,0:T(8,128)(2,1)S(1)}, bf16[128,512]{1,0:T(8,128)(2,1)S(1)}, u32[]{:S(2)}, u32[]{:S(2)}) collective-permute-start(bf16[128,512]{1,0:T(8,128)(2,1)S(1)} %project_piece.4.refs_6_.refs_2_), channel_id=1, source_target_pairs={{0,8},{8,16},{16,24},{24,0},{1,9},{9,17},{17,25},{25,1},{2,10},{10... | collective-permute-start | bytes 393224 | tf_op jit(solution)/shard_map/ppermute | solution.py:685
  83.0 1.4 collective-permute-start.10
  118.5 1.6 %collective-permute-start.13 = (bf16[64,2048]{1,0:T(8,128)(2,1)S(1)}, bf16[64,2048]{1,0:T(8,128)(2,1)S(1)}, u32[]{:S(2)}, u32[]{:S(2)}) collective-permute-start(bf16[64,2048]{1,0:T(8,128)(2,1)S(1)} %get-tuple-element.97.refs_0_.mine_ref.refs_2_), channel_id=1, source_target_pairs={{0,1},{1,0},{2,3},{3,2},{4,5},{5,4},{6,7},{7,6},{8,9},{9,8},{10,11... | collective-permute-start | bytes 786440 | tf_op jit(solution)/shard_map/ppermute | solution.py:653
  119.1 1.7 %collective-permute-start.12 = (bf16[64,2048]{1,0:T(8,128)(2,1)S(1)}, bf16[64,2048]{1,0:T(8,128)(2,1)S(1)}, u32[]{:S(2)}, u32[]{:S(2)}) collective-permute-start(bf16[64,2048]{1,0:T(8,128)(2,1)S(1)} %get-tuple-element.104.mine_ref.refs_1_), channel_id=1, source_target_pairs={{0,1},{1,0},{2,3},{3,2},{4,5},{5,4},{6,7},{7,6},{8,9},{9,8},{10,11... | collective-permute-start | bytes 786440 | tf_op jit(solution)/shard_map/ppermute | solution.py:653
  119.6 4.5 %collective-permute-start.11 = (bf16[64,2048]{1,0:T(8,128)(2,1)S(1)}, bf16[64,2048]{1,0:T(8,128)(2,1)S(1)}, u32[]{:S(2)}, u32[]{:S(2)}) collective-permute-start(bf16[64,2048]{1,0:T(8,128)(2,1)S(1)} %get-tuple-element.103.refs_0_), channel_id=1, source_target_pairs={{0,1},{1,0},{2,3},{3,2},{4,5},{5,4},{6,7},{7,6},{8,9},{9,8},{10,11... | collective-permute-start | bytes 786440 | tf_op jit(solution)/shard_map/ppermute | solution.py:653
  120.6 7.3 %collective-permute-start.16 = (bf16[128,512]{1,0:T(8,128)(2,1)S(1)}, bf16[128,512]{1,0:T(8,128)(2,1)S(1)}, u32[]{:S(2)}, u32[]{:S(2)}) collective-permute-start(bf16[128,512]{1,0:T(8,128)(2,1)S(1)} %project_piece.7.refs_7_), channel_id=1, source_target_pairs={{0,8},{8,16},{16,24},{24,0},{1,9},{9,17},{17,25},{25,1},{2,10},{10... | collective-permute-start | bytes 393224 | tf_op jit(solution)/shard_map/ppermute | solution.py:685
  121.2 8.6 %collective-permute-start.15 = (bf16[128,512]{1,0:T(8,128)(2,1)S(1)}, bf16[128,512]{1,0:T(8,128)(2,1)S(1)}, u32[]{:S(2)}, u32[]{:S(2)}) collective-permute-start(bf16[128,512]{1,0:T(8,128)(2,1)S(1)} %project_piece.6.refs_6_.refs_2_), channel_id=1, source_target_pairs={{0,8},{8,16},{16,24},{24,0},{1,9},{9,17},{17,25},{25,1},{2,10},{10... | collective-permute-start | bytes 393224 | tf_op jit(solution)/shard_map/ppermute | solution.py:685
  130.4 1.4 collective-permute-start.17
  130.5 18.6 %collective-permute-start.14 = (bf16[192,256]{1,0:T(8,128)(2,1)S(1)}, bf16[192,256]{1,0:T(8,128)(2,1)S(1)}, u32[]{:S(2)}, u32[]{:S(2)}) collective-permute-start(bf16[192,256]{1,0:T(8,128)(2,1)S(1)} %get-tuple-element.108), channel_id=1, source_target_pairs={{0,1},{1,0},{2,3},{3,2},{4,5},{5,4},{6,7},{7,6},{8,9},{9,8},{10,11... | collective-permute-start | bytes 294920 | tf_op jit(solution)/shard_map/ppermute | solution.py:653
  149.8 1.2 collective-permute-start.18
  151.0 6.1 %collective-permute-start.19 = (bf16[192,256]{1,0:T(8,128)(2,1)S(1)}, bf16[192,256]{1,0:T(8,128)(2,1)S(1)}, u32[]{:S(2)}, u32[]{:S(2)}) collective-permute-start(bf16[192,256]{1,0:T(8,128)(2,1)S(1)} %get-tuple-element.117), channel_id=1, source_target_pairs={{0,1},{1,0},{2,3},{3,2},{4,5},{5,4},{6,7},{7,6},{8,9},{9,8},{10,11... | collective-permute-start | bytes 294920 | tf_op jit(solution)/shard_map/ppermute | solution.py:653
  151.2 5.4 %collective-permute-start.20 = (f32[1,384]{1,0:T(1,128)S(1)}, f32[1,384]{1,0:T(1,128)S(1)}, u32[]{:S(2)}, u32[]{:S(2)}) collective-permute-start(f32[1,384]{1,0:T(1,128)S(1)} %add.3.refs_0_), channel_id=1, source_target_pairs={{0,2},{1,3},{2,4},{3,5},{4,6},{5,7},{6,0},{7,1},{8,10},{9,11},{10,... | collective-permute-start | bytes 4616 | tf_op jit(solution)/shard_map/ppermute | solution.py:678
  152.1 4.5 %collective-permute-start.21 = (f32[1,384]{1,0:T(1,128)S(1)}, f32[1,384]{1,0:T(1,128)S(1)}, u32[]{:S(2)}, u32[]{:S(2)}) collective-permute-start(f32[1,384]{1,0:T(1,128)S(1)} %add.3.refs_0_), channel_id=1, source_target_pairs={{0,4},{1,5},{2,6},{3,7},{4,0},{5,1},{6,2},{7,3},{8,12},{9,13},{10,... | collective-permute-start | bytes 4616 | tf_op jit(solution)/shard_map/ppermute | solution.py:678
  153.5 3.7 %collective-permute-start.22 = (f32[1,384]{1,0:T(1,128)S(1)}, f32[1,384]{1,0:T(1,128)S(1)}, u32[]{:S(2)}, u32[]{:S(2)}) collective-permute-start(f32[1,384]{1,0:T(1,128)S(1)} %add.3.refs_0_), channel_id=1, source_target_pairs={{0,6},{1,7},{2,0},{3,1},{4,2},{5,3},{6,4},{7,5},{8,14},{9,15},{10,... | collective-permute-start | bytes 4616 | tf_op jit(solution)/shard_map/ppermute | solution.py:678

commit v9 on v7

--- a/solution.py
+++ b/solution.py
@@ -615,9 +615,9 @@
 
 
 def finish_body(old_keep, old_got, keep_ref, got_ref, gain_ref, *refs):
-    out_ref, old_ref, branch_ref = refs[-3:]
+    out_ref = refs[-1]
     total = refs[0][...]
-    for ref in refs[1:-3]:
+    for ref in refs[1:-1]:
         total = total + ref[...]
     own = out_ref.shape[1]
     gain = gain_ref[gain_ref.shape[0] - 1 :, chip_slice(CORES * own)]
@@ -625,11 +625,16 @@
     for group in range(out_ref.shape[0] // GROUP):
         at = slice(group * GROUP, (group + 1) * GROUP)
         half = slice(group * HALF, (group + 1) * HALF)
-        for target, mine, other in ((old_ref, old_keep, old_got), (branch_ref, keep_ref, got_ref)):
-            target[half_rows(True), :] = mine[half].astype(jnp.float32)
-            target[half_rows(False), :] = other[half].astype(jnp.float32)
+        old, branch = [
+            jnp.where(
+                core_at() == 0,
+                jnp.concatenate([mine[half], other[half]]),
+                jnp.concatenate([other[half], mine[half]]),
+            ).astype(jnp.float32)
+            for mine, other in ((old_keep, old_got), (keep_ref, got_ref))
+        ]
         inv_out = lax.rsqrt(turn(total[:, at], 1) / D + norm_eps)
-        out_ref[at] = (old_ref[...] + branch_ref[...] * inv_out * gain).astype(jnp.bfloat16)
+        out_ref[at] = (old + branch * inv_out * gain).astype(jnp.bfloat16)
 
 
 def finish(old_keep, old_got, keep, got, gain, totals):
@@ -640,7 +645,6 @@
         out_shape=jax.ShapeDtypeStruct((CORES * rows, own), jnp.bfloat16),
         in_specs=[vmem] * len(operands),
         out_specs=vmem,
-        scratch_shapes=[pltpu.VMEM((GROUP, own), jnp.float32)] * 2,
         compiler_params=params,
         name="finish",
     )(*operands)

time: 158 us -> 158 us (level)
  no operation moved by 1% of the time
where the time goes in v9:
time: 158 us
  blocking collectives  104 us (66%)
  Pallas kernels  23.8 us (15%)
  starting transfers between devices  16.6 us (11%)
  waiting for transfers between devices  11.9 us (8%)
    all_gather x6, blocking collectives, gather_chips(): return lax.all_gather(x, 'tp', axis=0, axis_index_groups=lines)  104 us
    ppermute x6, starting transfers between devices, from_behind(): return lax.ppermute(block, 'sp', [(i, (i + 1) % size) for i in range(size)])  9.25 us
    pallas_call x3, Pallas kernels, project_local(): pl.pallas_call(functools.partial(local_body, layer, count), out_shape=tup...  6.85 us
    ppermute x14, waiting for transfers between devices, partner(): return lax.ppermute(x, 'tp', [(i, i ^ 1) for i in range(size)])  5.16 us
    ppermute x6, waiting for transfers between devices, from_behind(): return lax.ppermute(block, 'sp', [(i, (i + 1) % size) for i in range(size)])  4.95 us
    ppermute x3, starting transfers between devices, total_over_tp(): lax.ppermute(both, 'tp', [(i, (i + hop) % size) for i in range(size)])  4.17 us
    pallas_call x6, Pallas kernels, attend(): pl.pallas_call(functools.partial(attend_body, layer, group, len(done), le...  3.39 us
    ppermute x14, starting transfers between devices, partner(): return lax.ppermute(x, 'tp', [(i, i ^ 1) for i in range(size)])  3.17 us
  transfers between devices with their start and end apart: 23, of which 16 were waited for; matrix products, arithmetic and copies ran while one was open for 0% of the time, Pallas kernels for 12%

profile of v9, /device:TPU:0, one launch (start us, length us, event | category | flops | bytes accessed | tf_op | source)
XLA Modules:
  0.0 158.0 jit_solution(15479836287803997105)
XLA Ops:
  0.0 0.5 collective-permute-start.3
  0.5 19.7 %all-gather = bf16[1536,256]{1,0:T(8,128)(2,1)S(1)} all-gather(bf16[384,256]{1,0:T(8,128)(2,1)} %param.10), channel_id=2, replica_groups={{0,2,6,4},{1,3,7,5},{8,10,14,12},{9,11,15,13},{16,18,22,20},{17,19,23,2..., dimensions={0}, use_global_device_ids=true | all-gather | bytes 983040 | tf_op jit(solution)/shard_map/all_gather | solution.py:661
  20.2 2.3 %setup.1 = (bf16[4,256,2048]{2,1,0:T(8,128)(2,1)S(1)}, f32[3,2048]{1,0:T(4,128)S(1)}, f32[3,2048]{1,0:T(4,128)S(1)}, s32[1,384]{1,0:T(1,128)S(1)}, f32[1,128,384...) custom-call(f32[3,4,257]{2,1,0:T(4,128)} %bias_hbm.1, ...), custom_call_target="tpu_custom_call" | custom-call | tf_op jit(solution)/shard_map/setup/pallas_call | solution.py:109
  22.5 1.0 first_piece.3
  23.5 1.5 collective-permute-start.2
  25.1 1.0 first_piece.2
  26.1 1.5 collective-permute-start.1
  27.6 2.4 %project_local.3 = (bf16[64,2048]{1,0:T(8,128)(2,1)S(1)}, bf16[128,512]{1,0:T(8,128)(2,1)S(1)}, bf16[256,256]{1,0:T(8,128)(2,1)S(1)}, bf16[256,256]{1,0:T(8,128)(2,1)S(1)}, bf16[128,256]{1,0:T(8,128)(2,1)S(1)}) custom-call(bf16[4,384,256]{2,1,0:T(8,128)(2,1)S(1)} %bitcast.9, bf16[4,384,256]{2,1,0:T(8,128)(2,1)S(1)} %collective-permute-done.refs_1_, ...), custom_call_target="tpu_custom_call" | custom-call | tf_op jit(solution)/shard_map/project_local/pallas_call | solution.py:434
  30.1 0.4 copy-done.1
  30.5 0.6 turned.6.refs_11_.weight_ref
  31.2 0.6 attend.6
  31.8 0.6 copy-done.2
  32.4 0.6 turned.5.refs_10_.weight_ref
  33.0 0.9 collective-permute-done.1.refs_0_
  33.9 0.6 attend.7
  34.6 1.3 collective-permute-done.4.got_ref
  35.9 17.3 %all-gather.1 = bf16[768,512]{1,0:T(8,128)(2,1)S(1)} all-gather(bf16[192,512]{1,0:T(8,128)(2,1)S(1)} %join.3), channel_id=3, replica_groups={{0,2,6,4},{1,3,7,5},{8,10,14,12},{9,11,15,13},{16,18,22,20},{17,19,23,2..., dimensions={0}, use_global_device_ids=true | all-gather | bytes 983040 | tf_op jit(solution)/shard_map/all_gather | solution.py:661
  53.2 0.6 out_project.3
  53.8 17.0 %all-gather.2 = bf16[768,512]{1,0:T(8,128)(2,1)S(1)} all-gather(bf16[192,512]{1,0:T(8,128)(2,1)S(1)} %out_project.3), channel_id=4, replica_groups={{0,2,6,4},{1,3,7,5},{8,10,14,12},{9,11,15,13},{16,18,22,20},{17,19,23,2..., dimensions={0}, use_global_device_ids=true | all-gather | bytes 983040 | tf_op jit(solution)/shard_map/all_gather | solution.py:661
  70.8 0.4 update.5
  71.3 0.5 update.4
  71.8 0.5 collective-permute-start.5
  72.4 0.4 collective-permute-done.7.other_ref.refs_5_
  72.7 0.5 project_piece.5.refs_7_
  73.2 0.6 collective-permute-start.8
  73.8 0.4 project_piece.4.refs_6_.refs_2_
  74.3 2.7 %collective-permute-start.6 = (bf16[128,512]{1,0:T(8,128)(2,1)S(1)}, bf16[128,512]{1,0:T(8,128)(2,1)S(1)}, u32[]{:S(2)}, u32[]{:S(2)}) collective-permute-start(bf16[128,512]{1,0:T(8,128)(2,1)S(1)} %project_piece.4.refs_6_.refs_2_), channel_id=1, source_target_pairs={{0,8},{8,16},{16,24},{24,0},{1,9},{9,17},{17,25},{25,1},{2,10},{10... | collective-permute-start | bytes 393224 | tf_op jit(solution)/shard_map/ppermute | solution.py:687
  76.9 2.2 %project_local.4 = (bf16[128,512]{1,0:T(8,128)(2,1)S(1)}, bf16[256,256]{1,0:T(8,128)(2,1)S(1)}, bf16[256,256]{1,0:T(8,128)(2,1)S(1)}, bf16[128,256]{1,0:T(8,128)(2,1)S(1)}) custom-call(bf16[64,2048]{1,0:T(8,128)(2,1)S(1)} %get-tuple-element.85.refs_0_, bf16[64,2048]{1,0:T(8,128)(2,1)S(1)} %get-tuple-element.82.mine_ref.refs_1_, ...), custom_call_target="tpu_custom_call" | custom-call | tf_op jit(solution)/shard_map/project_local/pallas_call | solution.py:434
  79.2 0.6 turned.8.refs_12_.weight_ref
  79.8 0.6 turned.7.refs_11_.weight_ref
  80.4 0.2 collective-permute-done.8.refs_0_.refs_1_
  80.5 0.6 attend.8.refs_9_
  81.1 1.4 collective-permute-done.6.refs_0_
  82.5 0.6 attend.9
  83.1 1.3 collective-permute-done.10.got_ref
  84.4 16.8 %all-gather.3 = bf16[768,512]{1,0:T(8,128)(2,1)S(1)} all-gather(bf16[192,512]{1,0:T(8,128)(2,1)S(1)} %join.4), channel_id=5, replica_groups={{0,2,6,4},{1,3,7,5},{8,10,14,12},{9,11,15,13},{16,18,22,20},{17,19,23,2..., dimensions={0}, use_global_device_ids=true | all-gather | bytes 983040 | tf_op jit(solution)/shard_map/all_gather | solution.py:661
  101.3 0.6 out_project.4
  101.9 16.2 %all-gather.4 = bf16[768,512]{1,0:T(8,128)(2,1)S(1)} all-gather(bf16[192,512]{1,0:T(8,128)(2,1)S(1)} %out_project.4), channel_id=6, replica_groups={{0,2,6,4},{1,3,7,5},{8,10,14,12},{9,11,15,13},{16,18,22,20},{17,19,23,2..., dimensions={0}, use_global_device_ids=true | all-gather | bytes 983040 | tf_op jit(solution)/shard_map/all_gather | solution.py:661
  118.1 0.4 update.7
  118.5 0.5 update.6
  119.0 0.6 collective-permute-start.12
  119.7 0.4 collective-permute-done.13.other_ref.refs_5_
  120.1 0.4 project_piece.7.refs_7_
  120.6 0.2 collective-permute-done.12.other_ref.refs_4_
  120.8 0.4 project_piece.6.refs_6_.refs_2_
  121.2 2.8 %collective-permute-start.15 = (bf16[128,512]{1,0:T(8,128)(2,1)S(1)}, bf16[128,512]{1,0:T(8,128)(2,1)S(1)}, u32[]{:S(2)}, u32[]{:S(2)}) collective-permute-start(bf16[128,512]{1,0:T(8,128)(2,1)S(1)} %project_piece.6.refs_6_.refs_2_), channel_id=1, source_target_pairs={{0,8},{8,16},{16,24},{24,0},{1,9},{9,17},{17,25},{25,1},{2,10},{10... | collective-permute-start | bytes 393224 | tf_op jit(solution)/shard_map/ppermute | solution.py:687
  124.0 2.2 %project_local.5 = (bf16[128,512]{1,0:T(8,128)(2,1)S(1)}, bf16[256,256]{1,0:T(8,128)(2,1)S(1)}, bf16[256,256]{1,0:T(8,128)(2,1)S(1)}, bf16[128,256]{1,0:T(8,128)(2,1)S(1)}) custom-call(bf16[64,2048]{1,0:T(8,128)(2,1)S(1)} %get-tuple-element.100.refs_0_, bf16[64,2048]{1,0:T(8,128)(2,1)S(1)} %get-tuple-element.101.mine_ref.refs_1_, ...), custom_call_target="tpu_custom_call" | custom-call | tf_op jit(solution)/shard_map/project_local/pallas_call | solution.py:434
  126.3 0.6 turned.9.refs_11_.weight_ref
  126.9 0.9 collective-permute-done.16.refs_0_.refs_1_
  127.8 0.6 attend.10.refs_9_
  128.4 1.4 collective-permute-done.15.refs_0_
  129.8 0.6 attend.11
  130.5 0.5 collective-permute-start.14
  131.0 0.8 collective-permute-done.17.got_ref
  131.8 17.3 %all-gather.5 = bf16[768,512]{1,0:T(8,128)(2,1)S(1)} all-gather(bf16[192,512]{1,0:T(8,128)(2,1)S(1)} %join.5), channel_id=7, replica_groups={{0,2,6,4},{1,3,7,5},{8,10,14,12},{9,11,15,13},{16,18,22,20},{17,19,23,2..., dimensions={0}, use_global_device_ids=true | all-gather | bytes 983040 | tf_op jit(solution)/shard_map/all_gather | solution.py:661
  149.0 0.7 out_project.5
  149.8 0.5 collective-permute-start.19
  150.3 0.8 collective-permute-done.19
  151.1 1.0 collective-permute-start.20
  152.1 1.4 collective-permute-start.21
  153.6 1.8 %collective-permute-start.22 = (f32[1,384]{1,0:T(1,128)S(1)}, f32[1,384]{1,0:T(1,128)S(1)}, u32[]{:S(2)}, u32[]{:S(2)}) collective-permute-start(f32[1,384]{1,0:T(1,128)S(1)} %add.3.refs_0_), channel_id=1, source_target_pairs={{0,6},{1,7},{2,0},{3,1},{4,2},{5,3},{6,4},{7,5},{8,14},{9,15},{10,... | collective-permute-start | bytes 4616 | tf_op jit(solution)/shard_map/ppermute | solution.py:680
  155.3 1.2 collective-permute-done.20.refs_1_
  156.6 0.5 collective-permute-done.22.refs_3_
  157.1 0.9 finish.1
  (32 shorter events, 1.0 us)
Async XLA Ops:
  0.0 31.8 %collective-permute-start.3 = (bf16[3,256,2048]{2,1,0:T(8,128)(2,1)}, bf16[3,256,2048]{2,1,0:T(8,128)(2,1)S(1)}, u32[]{:S(2)}, u32[]{:S(2)}) collective-permute-start(bf16[3,256,2048]{2,1,0:T(8,128)(2,1)} %refs_0_.11), channel_id=1, source_target_pairs={{0,1},{1,0},{2,3},{3,2},{4,5},{5,4},{6,7},{7,6},{8,9},{9,8},{10,11... | collective-permute-start | bytes 9437192 | tf_op jit(solution)/shard_map/ppermute | solution.py:655
  20.2 2.3 %collective-permute-start = (bf16[4,384,256]{2,1,0:T(8,128)(2,1)S(1)}, bf16[4,384,256]{2,1,0:T(8,128)(2,1)S(1)}, u32[]{:S(2)}, u32[]{:S(2)}) collective-permute-start(bf16[4,384,256]{2,1,0:T(8,128)(2,1)S(1)} %bitcast.6), channel_id=1, source_target_pairs={{0,1},{1,0},{2,3},{3,2},{4,5},{5,4},{6,7},{7,6},{8,9},{9,8},{10,11... | collective-permute-start | bytes 2359304 | tf_op jit(solution)/shard_map/ppermute | solution.py:655
  23.5 7.7 %collective-permute-start.2 = (bf16[144,512]{1,0:T(8,128)(2,1)S(1)}, bf16[144,512]{1,0:T(8,128)(2,1)S(1)}, u32[]{:S(2)}, u32[]{:S(2)}) collective-permute-start(bf16[144,512]{1,0:T(8,128)(2,1)S(1)} %get-tuple-element.66.refs_6_), channel_id=1, source_target_pairs={{0,8},{8,16},{16,24},{24,0},{1,9},{9,17},{17,25},{25,1},{2,10},{10... | collective-permute-start | bytes 442376 | tf_op jit(solution)/shard_map/ppermute | solution.py:687
  26.1 7.8 %collective-permute-start.1 = (bf16[144,512]{1,0:T(8,128)(2,1)S(1)}, bf16[144,512]{1,0:T(8,128)(2,1)S(1)}, u32[]{:S(2)}, u32[]{:S(2)}) collective-permute-start(bf16[144,512]{1,0:T(8,128)(2,1)S(1)} %get-tuple-element.65.refs_5_.refs_2_), channel_id=1, source_target_pairs={{0,8},{8,16},{16,24},{24,0},{1,9},{9,17},{17,25},{25,1},{2,10},{10... | collective-permute-start | bytes 442376 | tf_op jit(solution)/shard_map/ppermute | solution.py:687
  27.6 2.4 %copy-start = (bf16[3,256,2048]{2,1,0:T(8,128)(2,1)S(1)}, bf16[3,256,2048]{2,1,0:T(8,128)(2,1)}, u32[]{:S(2)}) copy-start(bf16[3,256,2048]{2,1,0:T(8,128)(2,1)} %refs_10_.3) | copy-start | bytes 9437188
  27.6 2.8 %copy-start.1 = (bf16[3,256,2048]{2,1,0:T(8,128)(2,1)S(1)}, bf16[3,256,2048]{2,1,0:T(8,128)(2,1)}, u32[]{:S(2)}) copy-start(bf16[3,256,2048]{2,1,0:T(8,128)(2,1)} %refs_11_.3) | copy-start | bytes 9437188
  30.5 1.9 %copy-start.2 = (bf16[3,256,2048]{2,1,0:T(8,128)(2,1)S(1)}, bf16[3,256,2048]{2,1,0:T(8,128)(2,1)}, u32[]{:S(2)}) copy-start(bf16[3,256,2048]{2,1,0:T(8,128)(2,1)} %refs_0_.11) | copy-start | bytes 9437188
  34.5 1.4 collective-permute-start.4
  71.1 1.6 %collective-permute-start.7 = (bf16[64,2048]{1,0:T(8,128)(2,1)S(1)}, bf16[64,2048]{1,0:T(8,128)(2,1)S(1)}, u32[]{:S(2)}, u32[]{:S(2)}) collective-permute-start(bf16[64,2048]{1,0:T(8,128)(2,1)S(1)} %get-tuple-element.84.mine_ref.refs_2_), channel_id=1, source_target_pairs={{0,1},{1,0},{2,3},{3,2},{4,5},{5,4},{6,7},{7,6},{8,9},{9,8},{10,11... | collective-permute-start | bytes 786440 | tf_op jit(solution)/shard_map/ppermute | solution.py:655
  71.2 5.7 %copy-start.3 = (bf16[3,256,2048]{2,1,0:T(8,128)(2,1)S(1)}, bf16[3,256,2048]{2,1,0:T(8,128)(2,1)}, u32[]{:S(2)}) copy-start(bf16[3,256,2048]{2,1,0:T(8,128)(2,1)} %refs_12_.3) | copy-start | bytes 9437188
  71.2 5.7 %copy-start.4 = (bf16[3,256,2048]{2,1,0:T(8,128)(2,1)S(1)}, bf16[3,256,2048]{2,1,0:T(8,128)(2,1)}, u32[]{:S(2)}) copy-start(bf16[3,256,2048]{2,1,0:T(8,128)(2,1)} %refs_13_.3) | copy-start | bytes 9437188
  71.8 2.1 %collective-permute-start.5 = (bf16[64,2048]{1,0:T(8,128)(2,1)S(1)}, bf16[64,2048]{1,0:T(8,128)(2,1)S(1)}, u32[]{:S(2)}, u32[]{:S(2)}) collective-permute-start(bf16[64,2048]{1,0:T(8,128)(2,1)S(1)} %get-tuple-element.82.mine_ref.refs_1_), channel_id=1, source_target_pairs={{0,1},{1,0},{2,3},{3,2},{4,5},{5,4},{6,7},{7,6},{8,9},{9,8},{10,11... | collective-permute-start | bytes 786440 | tf_op jit(solution)/shard_map/ppermute | solution.py:655
  72.3 4.6 %collective-permute-start.9 = (bf16[64,2048]{1,0:T(8,128)(2,1)S(1)}, bf16[64,2048]{1,0:T(8,128)(2,1)S(1)}, u32[]{:S(2)}, u32[]{:S(2)}) collective-permute-start(bf16[64,2048]{1,0:T(8,128)(2,1)S(1)} %get-tuple-element.85.refs_0_), channel_id=1, source_target_pairs={{0,1},{1,0},{2,3},{3,2},{4,5},{5,4},{6,7},{7,6},{8,9},{9,8},{10,11... | collective-permute-start | bytes 786440 | tf_op jit(solution)/shard_map/ppermute | solution.py:655
  73.2 7.3 %collective-permute-start.8 = (bf16[128,512]{1,0:T(8,128)(2,1)S(1)}, bf16[128,512]{1,0:T(8,128)(2,1)S(1)}, u32[]{:S(2)}, u32[]{:S(2)}) collective-permute-start(bf16[128,512]{1,0:T(8,128)(2,1)S(1)} %project_piece.5.refs_7_), channel_id=1, source_target_pairs={{0,8},{8,16},{16,24},{24,0},{1,9},{9,17},{17,25},{25,1},{2,10},{10... | collective-permute-start | bytes 393224 | tf_op jit(solution)/shard_map/ppermute | solution.py:687
  74.3 8.2 %collective-permute-start.6 = (bf16[128,512]{1,0:T(8,128)(2,1)S(1)}, bf16[128,512]{1,0:T(8,128)(2,1)S(1)}, u32[]{:S(2)}, u32[]{:S(2)}) collective-permute-start(bf16[128,512]{1,0:T(8,128)(2,1)S(1)} %project_piece.4.refs_6_.refs_2_), channel_id=1, source_target_pairs={{0,8},{8,16},{16,24},{24,0},{1,9},{9,17},{17,25},{25,1},{2,10},{10... | collective-permute-start | bytes 393224 | tf_op jit(solution)/shard_map/ppermute | solution.py:687
  83.1 1.4 collective-permute-start.10
  118.5 1.6 %collective-permute-start.13 = (bf16[64,2048]{1,0:T(8,128)(2,1)S(1)}, bf16[64,2048]{1,0:T(8,128)(2,1)S(1)}, u32[]{:S(2)}, u32[]{:S(2)}) collective-permute-start(bf16[64,2048]{1,0:T(8,128)(2,1)S(1)} %get-tuple-element.102.mine_ref.refs_2_), channel_id=1, source_target_pairs={{0,1},{1,0},{2,3},{3,2},{4,5},{5,4},{6,7},{7,6},{8,9},{9,8},{10,11... | collective-permute-start | bytes 786440 | tf_op jit(solution)/shard_map/ppermute | solution.py:655
  119.0 1.7 %collective-permute-start.12 = (bf16[64,2048]{1,0:T(8,128)(2,1)S(1)}, bf16[64,2048]{1,0:T(8,128)(2,1)S(1)}, u32[]{:S(2)}, u32[]{:S(2)}) collective-permute-start(bf16[64,2048]{1,0:T(8,128)(2,1)S(1)} %get-tuple-element.101.mine_ref.refs_1_), channel_id=1, source_target_pairs={{0,1},{1,0},{2,3},{3,2},{4,5},{5,4},{6,7},{7,6},{8,9},{9,8},{10,11... | collective-permute-start | bytes 786440 | tf_op jit(solution)/shard_map/ppermute | solution.py:655
  119.6 4.4 %collective-permute-start.11 = (bf16[64,2048]{1,0:T(8,128)(2,1)S(1)}, bf16[64,2048]{1,0:T(8,128)(2,1)S(1)}, u32[]{:S(2)}, u32[]{:S(2)}) collective-permute-start(bf16[64,2048]{1,0:T(8,128)(2,1)S(1)} %get-tuple-element.100.refs_0_), channel_id=1, source_target_pairs={{0,1},{1,0},{2,3},{3,2},{4,5},{5,4},{6,7},{7,6},{8,9},{9,8},{10,11... | collective-permute-start | bytes 786440 | tf_op jit(solution)/shard_map/ppermute | solution.py:655
  120.5 7.3 %collective-permute-start.16 = (bf16[128,512]{1,0:T(8,128)(2,1)S(1)}, bf16[128,512]{1,0:T(8,128)(2,1)S(1)}, u32[]{:S(2)}, u32[]{:S(2)}) collective-permute-start(bf16[128,512]{1,0:T(8,128)(2,1)S(1)} %project_piece.7.refs_7_), channel_id=1, source_target_pairs={{0,8},{8,16},{16,24},{24,0},{1,9},{9,17},{17,25},{25,1},{2,10},{10... | collective-permute-start | bytes 393224 | tf_op jit(solution)/shard_map/ppermute | solution.py:687
  121.2 8.6 %collective-permute-start.15 = (bf16[128,512]{1,0:T(8,128)(2,1)S(1)}, bf16[128,512]{1,0:T(8,128)(2,1)S(1)}, u32[]{:S(2)}, u32[]{:S(2)}) collective-permute-start(bf16[128,512]{1,0:T(8,128)(2,1)S(1)} %project_piece.6.refs_6_.refs_2_), channel_id=1, source_target_pairs={{0,8},{8,16},{16,24},{24,0},{1,9},{9,17},{17,25},{25,1},{2,10},{10... | collective-permute-start | bytes 393224 | tf_op jit(solution)/shard_map/ppermute | solution.py:687
  130.4 1.4 collective-permute-start.17
  130.5 24.9 %collective-permute-start.14 = (bf16[192,256]{1,0:T(8,128)(2,1)S(1)}, bf16[192,256]{1,0:T(8,128)(2,1)S(1)}, u32[]{:S(2)}, u32[]{:S(2)}) collective-permute-start(bf16[192,256]{1,0:T(8,128)(2,1)S(1)} %get-tuple-element.106), channel_id=1, source_target_pairs={{0,1},{1,0},{2,3},{3,2},{4,5},{5,4},{6,7},{7,6},{8,9},{9,8},{10,11... | collective-permute-start | bytes 294920 | tf_op jit(solution)/shard_map/ppermute | solution.py:655
  149.7 7.4 %collective-permute-start.18 = (bf16[192,256]{1,0:T(8,128)(2,1)S(1)}, bf16[192,256]{1,0:T(8,128)(2,1)S(1)}, u32[]{:S(2)}, u32[]{:S(2)}) collective-permute-start(bf16[192,256]{1,0:T(8,128)(2,1)S(1)} %get-tuple-element.113), channel_id=1, source_target_pairs={{0,1},{1,0},{2,3},{3,2},{4,5},{5,4},{6,7},{7,6},{8,9},{9,8},{10,11... | collective-permute-start | bytes 294920 | tf_op jit(solution)/shard_map/ppermute | solution.py:655
  149.8 1.3 collective-permute-start.19
  151.1 5.4 %collective-permute-start.20 = (f32[1,384]{1,0:T(1,128)S(1)}, f32[1,384]{1,0:T(1,128)S(1)}, u32[]{:S(2)}, u32[]{:S(2)}) collective-permute-start(f32[1,384]{1,0:T(1,128)S(1)} %add.3.refs_0_), channel_id=1, source_target_pairs={{0,2},{1,3},{2,4},{3,5},{4,6},{5,7},{6,0},{7,1},{8,10},{9,11},{10,... | collective-permute-start | bytes 4616 | tf_op jit(solution)/shard_map/ppermute | solution.py:680
  152.1 4.5 %collective-permute-start.21 = (f32[1,384]{1,0:T(1,128)S(1)}, f32[1,384]{1,0:T(1,128)S(1)}, u32[]{:S(2)}, u32[]{:S(2)}) collective-permute-start(f32[1,384]{1,0:T(1,128)S(1)} %add.3.refs_0_), channel_id=1, source_target_pairs={{0,4},{1,5},{2,6},{3,7},{4,0},{5,1},{6,2},{7,3},{8,12},{9,13},{10,... | collective-permute-start | bytes 4616 | tf_op jit(solution)/shard_map/ppermute | solution.py:680
  153.6 3.6 %collective-permute-start.22 = (f32[1,384]{1,0:T(1,128)S(1)}, f32[1,384]{1,0:T(1,128)S(1)}, u32[]{:S(2)}, u32[]{:S(2)}) collective-permute-start(f32[1,384]{1,0:T(1,128)S(1)} %add.3.refs_0_), channel_id=1, source_target_pairs={{0,6},{1,7},{2,0},{3,1},{4,2},{5,3},{6,4},{7,5},{8,14},{9,15},{10,... | collective-permute-start | bytes 4616 | tf_op jit(solution)/shard_map/ppermute | solution.py:680
